TPU v7x, 256 devices: a whole 4x4x8 slice. The times are simulated.
256 devices in a mesh: ra: 32 (over z, y), cb: 4 (over x), dp: 2 (over core).
Axes of the slice: x: 4, y: 4, z: 8, core: 2. Of those that a mesh axis runs over, the one named last changes fastest.
Arguments:
- stream: bfloat16 [3072, 4096], P(('cb', 'dp'), 'ra'), may hold values from -20 to 20
- up_first: bfloat16 [4096, 16384], P('cb', 'ra'), may hold values from -0.09375 to 0.09375
- down_first: bfloat16 [16384, 4096], P('ra', 'cb'), may hold values from -0.046875 to 0.046875
- up_second: bfloat16 [4096, 16384], P('cb', 'ra'), may hold values from -0.09375 to 0.09375
- down_second: bfloat16 [16384, 4096], P('ra', 'cb'), may hold values from -0.046875 to 0.046875
- gain_first: float32 [4096], P('ra'), may hold values from 0.1 to 1.9
- bias_first: float32 [4096], P('ra'), may hold values from -3 to 3
- gain_second: float32 [4096], P('ra'), may hold values from 0.1 to 1.9
- bias_second: float32 [4096], P('ra'), may hold values from -3 to 3
Outputs:
- result: bfloat16 [3072, 4096], P(('cb', 'dp'), 'ra')
All inputs are finite; a program needn't handle non-finite values.
Results may differ from a plain program's by a relative error of at most 0.0093.
Values may be sent and summed in bfloat16 or wider, within the bound.
No kernel may reach another device: no remote copies, remote signals or barrier semaphores. Data moves between devices by JAX's collectives and lax.ppermute only.
A program may use at most 64 MiB of HBM per device.

v0:
```python
import jax
import jax.numpy as jnp
from jax import lax
from jax.experimental import pallas as pl
from jax.experimental.pallas import tpu as pltpu
from jax.sharding import Mesh
from jax.sharding import PartitionSpec as P


Z, Y, X, C = "ra_0", "ra_1", "cb", "dp"
RA = (Z, Y)
ALL = (Z, Y, X, C)
RESID = 1.4142135
EPS = 0.5
BF = jnp.bfloat16
F32 = jnp.float32
NZ, NY = 8, 4


def place(z, y, core, nz, ny):
    z, y = (z - core) % nz, (y - core) % ny
    return (y % 2) * 2 + z % 2, (y // 2) * (nz // 2) + z // 2


def groups_of(sizes):
    nz, ny, nx, nc = sizes
    near, far = {}, {}
    for z in range(nz):
        for y in range(ny):
            for x in range(nx):
                for c in range(nc):
                    at = ((z * ny + y) * nx + x) * nc + c
                    a, b = place(z, y, c, nz, ny)
                    near.setdefault((x, c, b), {})[a] = at
                    far.setdefault((x, c, a), {})[b] = at
    return [[[m[i] for i in sorted(m)] for m in g.values()] for g in (near, far)]


def swap(blocks, groups):
    return lax.all_to_all(blocks, ALL, 0, 0, axis_index_groups=groups, tiled=True)


def to_all(block, groups):
    return swap(jnp.broadcast_to(block[None], (len(groups[0]), *block.shape)), groups)


def gathered(block, near, far):
    return to_all(to_all(block, far), near)


def scattered_sum(parts, near, far):
    some = jnp.sum(swap(parts, near).astype(F32), axis=0).astype(BF)
    return jnp.sum(swap(some, far).astype(F32), axis=0)


def stats_to_all(row):
    n = lax.axis_size(RA)
    return lax.all_to_all(jnp.broadcast_to(row[None], (n, *row.shape)), RA, 0, 0, tiled=True)


def shift(a, axis, by):
    n = lax.axis_size(axis)
    return lax.ppermute(a, axis, [(i, (i + by) % n) for i in range(n)])


def half_of(w):
    rows = w.shape[0] // 2
    return lax.dynamic_slice_in_dim(w, lax.axis_index(C) * rows, rows, 0)


def split3(v):
    hi = lax.reduce_precision(v, 8, 7)
    mid = lax.reduce_precision(v - hi, 8, 7)
    return [hi, mid, v - hi - mid]


def at_core(z, y, core, nz, ny):
    a0, b0 = place(z, y, 0, nz, ny)
    a1, b1 = place(z, y, 1, nz, ny)
    return a0 + core * (a1 - a0), b0 + core * (b1 - b0)


def matmuls(core, xs, upv, dv, ov, out, out_sems, wait_up, wait_down, nx):
    ny, nz = NY, NZ
    wait_up()
    pre = jnp.dot(xs[...], upv[...], preferred_element_type=F32)
    hidden = jnp.square(jnp.maximum(pre, 0.0)).astype(BF)
    half = hidden.shape[1] // 2
    copies = []
    for j in range(nx):
        wait_down(j)
        part = jnp.dot(hidden[:, :half], dv[2 * j], preferred_element_type=F32)
        part = part + jnp.dot(hidden[:, half:], dv[2 * j + 1], preferred_element_type=F32)
        part = part.astype(BF)
        per = nz // nx
        for zz in range(per):
            for y in range(ny):
                at = (zz * ny + y) * 128
                z = j * per + zz
                b = z * ny + y
                ov[b] = part[:, at : at + 128]
                copy = pltpu.make_async_copy(ov.at[b], out.at[at_core(z, y, core, nz, ny)], out_sems.at[b])
                copy.start()
                copies.append(copy)
    for copy in copies:
        copy.wait()


def first_kernel(
    idx, x, up, own, m1, m2, m3, o1, o2, o3, out, gain, bias, xs, tv, upv, dv, ov, x_sem, t_sem, up_sem, d_sems, out_sems
):
    nx = dv.shape[0] // 2
    rows = dv.shape[1]
    me, core = idx[0], idx[1]
    up_copy = pltpu.make_async_copy(up, upv, up_sem)
    tokens = xs.shape[0]
    ny, nz = NY, NZ
    x_copies, t_copies = [], []
    for z in range(nz):
        for y in range(ny):
            b = z * ny + y
            p, q = at_core(z, y, core, nz, ny)
            copy = pltpu.make_async_copy(
                x.at[p, q, pl.ds(0, tokens)], xs.at[:, pl.ds(b * 128, 128)], x_sem.at[b]
            )
            copy.start()
            x_copies.append(copy)
            copy = pltpu.make_async_copy(x.at[p, q, pl.ds(tokens, 8)], tv.at[b], t_sem.at[b])
            copy.start()
            t_copies.append(copy)
    up_copy.start()
    d_copies = [
        pltpu.make_async_copy(own.at[pl.ds(0, rows)], dv.at[2 * me], d_sems.at[0]),
        pltpu.make_async_copy(own.at[pl.ds(rows, rows)], dv.at[2 * me + 1], d_sems.at[1]),
    ]
    for i, (by, mine, other) in enumerate(((1, m1, o1), (nx - 1, m2, o2), (2, m3, o3))):
        source = lax.rem(me + (nx - by), nx)
        d_copies.append(pltpu.make_async_copy(mine, dv.at[2 * source + core], d_sems.at[2 + 2 * i]))
        d_copies.append(pltpu.make_async_copy(other, dv.at[2 * source + 1 - core], d_sems.at[3 + 2 * i]))
    for copy in d_copies:
        copy.start()

    def wait_up():
        for copy in x_copies:
            copy.wait()
        up_copy.wait()

    def wait_down(j):
        if j == 0:
            for copy in d_copies:
                copy.wait()

    matmuls(core, xs, upv, dv, ov, out, out_sems, wait_up, wait_down, nx)
    for b in range(nz * ny):
        t_copies[b].wait()
        t = tv[b].astype(F32)
        gain[b : b + 1] = t[0:1] + t[1:2] + t[2:3]
        bias[b : b + 1] = t[3:4] + t[4:5] + t[5:6]


def second_kernel(
    idx, x, up, down, gain, bias, mixed, own_gain, own_bias, out, own, xs, xv, upv, dv, ov, x_sem, up_sem, d_sem, out_sems
):
    nx = dv.shape[0] // 2
    ny, nz = NY, NZ
    core = idx[1]
    tokens = xs.shape[0]
    x_copies = []
    for z in range(nz):
        for y in range(ny):
            b = z * ny + y
            copy = pltpu.make_async_copy(x.at[at_core(z, y, core, nz, ny)], xv.at[b], x_sem.at[b])
            copy.start()
            x_copies.append(copy)
    up_copy = pltpu.make_async_copy(up, upv, up_sem)
    d_copy = pltpu.make_async_copy(down, dv, d_sem)
    up_copy.start()
    d_copy.start()
    for copy in x_copies:
        copy.wait()
    step = 64
    width = ny * nz * 128

    def norm(i, carry):
        rows = pl.ds(pl.multiple_of(i * step, step), step)
        acc = jnp.zeros((step, 128), F32)
        for b in range(nz * ny):
            acc = acc + xv[b, rows, :].astype(F32)
        mean = jnp.sum(acc, axis=1, keepdims=True) / width
        acc = jnp.zeros((step, 128), F32)
        for b in range(nz * ny):
            d = xv[b, rows, :].astype(F32) - mean
            acc = acc + d * d
        scale = lax.rsqrt(jnp.sum(acc, axis=1, keepdims=True) / width + EPS)
        for b in range(nz * ny):
            d = (xv[b, rows, :].astype(F32) - mean) * scale
            xs[rows, b * 128 : (b + 1) * 128] = (d * gain[b : b + 1] + bias[b : b + 1]).astype(BF)
        own[rows, :] = ((mixed[rows, :] - mean) * scale * own_gain[...] + own_bias[...]).astype(BF)
        return carry

    lax.fori_loop(0, tokens // step, norm, 0)

    def wait_down(j):
        if j == 0:
            d_copy.wait()

    matmuls(core, xs, upv, dv, ov, out, out_sems, up_copy.wait, wait_down, nx)


ANY = pl.BlockSpec(memory_space=pltpu.MemorySpace.HBM)
VMEM = pl.BlockSpec(memory_space=pltpu.MemorySpace.VMEM)
SMEM = pl.BlockSpec(memory_space=pltpu.MemorySpace.SMEM)


def first_ffn(idx, x, tokens, up, own, mine, others):
    width, ff = up.shape
    nx, nb = lax.axis_size(X), NZ * NY
    vector = jax.ShapeDtypeStruct((nb, 128), F32)
    return pl.pallas_call(
        first_kernel,
        out_shape=(jax.ShapeDtypeStruct((4, nb // 4, tokens, 128), BF), vector, vector),
        in_specs=[SMEM] + [ANY] * 9,
        out_specs=(ANY, VMEM, VMEM),
        scratch_shapes=[
            pltpu.VMEM((tokens, width), BF),
            pltpu.VMEM((nb, 8, 128), BF),
            pltpu.VMEM((width, ff), BF),
            pltpu.VMEM((2 * nx, ff // 2, width // nx), BF),
            pltpu.VMEM((nb, tokens, 128), BF),
            pltpu.SemaphoreType.DMA((nb,)),
            pltpu.SemaphoreType.DMA((nb,)),
            pltpu.SemaphoreType.DMA,
            pltpu.SemaphoreType.DMA((8,)),
            pltpu.SemaphoreType.DMA((nb,)),
        ],
        cost_estimate=pl.CostEstimate(flops=4 * tokens * width * ff, bytes_accessed=14 << 20, transcendentals=0),
        name="first_ffn",
    )(idx, x, up, own, *mine, *others)


def second_ffn(idx, x, up, down, gain, bias, mixed, own_gain, own_bias):
    tokens = x.shape[2]
    width, ff = up.shape
    nx, nb = lax.axis_size(X), NZ * NY
    return pl.pallas_call(
        second_kernel,
        out_shape=(jax.ShapeDtypeStruct(x.shape, BF), jax.ShapeDtypeStruct((tokens, 128), BF)),
        in_specs=[SMEM] + [ANY] * 3 + [VMEM] * 5,
        out_specs=(ANY, VMEM),
        scratch_shapes=[
            pltpu.VMEM((tokens, width), BF),
            pltpu.VMEM((nb, tokens, 128), BF),
            pltpu.VMEM((width, ff), BF),
            pltpu.VMEM((2 * nx, ff // 2, width // nx), BF),
            pltpu.VMEM((nb, tokens, 128), BF),
            pltpu.SemaphoreType.DMA((nb,)),
            pltpu.SemaphoreType.DMA,
            pltpu.SemaphoreType.DMA,
            pltpu.SemaphoreType.DMA((nb,)),
        ],
        cost_estimate=pl.CostEstimate(flops=4 * tokens * width * ff, bytes_accessed=14 << 20, transcendentals=0),
        name="second_ffn",
    )(idx, x, up, down, gain, bias, mixed, own_gain, own_bias)


def body(
    stream,
    up_first,
    down_first,
    up_second,
    down_second,
    gain_first,
    bias_first,
    gain_second,
    bias_second,
):
    tokens = stream.shape[0]
    near, far = groups_of([lax.axis_size(axis) for axis in ALL])
    half = half_of(down_first)
    mine = [shift(half, X, by) for by in (1, -1, 2)]
    up_1 = lax.all_gather(half_of(up_first), (X, C), axis=0, tiled=True)
    tail = jnp.stack(split3(gain_first) + split3(bias_first) + [jnp.zeros_like(gain_first)] * 2)
    x_far = to_all(jnp.concatenate([stream, tail.astype(BF)], axis=0), far)
    x_all = to_all(x_far, near)
    others = [shift(m, C, 1) for m in mine]
    up_2 = lax.all_gather(half_of(up_second), (X, C), axis=0, tiled=True)
    down_2 = lax.all_gather(half_of(down_second), (X, C), axis=0, tiled=False)
    down_2 = down_2.reshape(-1, *half.shape)
    idx = jnp.stack([lax.axis_index(X), lax.axis_index(C)]).astype(jnp.int32)
    parts, gain, bias = first_ffn(idx, x_all, tokens, up_1, down_first, mine, others)
    mixed = RESID * stream.astype(F32) + scattered_sum(parts, near, far)
    mixed_all = gathered(mixed.astype(BF), near, far)
    parts, x = second_ffn(
        idx, mixed_all, up_2, down_2, gain, bias, mixed, gain_first[None], bias_first[None]
    )
    mixed = RESID * x.astype(F32) + scattered_sum(parts, near, far)
    width = mixed.shape[1] * lax.axis_size(RA)
    sums = jnp.concatenate([jnp.sum(mixed, axis=1), jnp.sum(mixed * mixed, axis=1)])
    sums = jnp.sum(stats_to_all(sums[None]), axis=0)[0]
    mean = sums[:tokens, None] / width
    var = sums[tokens:, None] / width - mean * mean
    return ((mixed - mean) * lax.rsqrt(var + EPS) * gain_second + bias_second).astype(BF)


def solution(mesh):
    torus = Mesh(mesh.devices.reshape(NZ, NY, mesh.shape["cb"], mesh.shape["dp"]), (Z, Y, X, C))
    in_specs = (
        P((X, C), RA),
        P(X, RA),
        P(RA, X),
        P(X, RA),
        P(RA, X),
        P(RA),
        P(RA),
        P(RA),
        P(RA),
    )
    out_specs = P((X, C), RA)

    return jax.shard_map(body, mesh=torus, in_specs=in_specs, out_specs=out_specs, check_vma=False)
```

profile of v0, /device:TPU:2, one launch (start us, length us, event | category | flops | bytes accessed | tf_op | source)
XLA Modules:
  0.0 309.8 jit_solution(17371740104639328938)
XLA Ops:
  6.5 1.2 copy-done
  7.8 0.8 constant_dynamic-slice_fusion.3
  8.6 0.0 all-gather.5.cloned.1.call-update
  8.6 0.7 fusion.6
  9.3 0.9 concatenate.7
  10.3 0.1 broadcast_in_dim.14
  10.4 33.5 %all_to_all.45 = bf16[8,392,128]{2,1,0:T(8,128)(2,1)S(1)} all-to-all(bf16[8,392,128]{2,1,0:T(8,128)(2,1)S(1)} %broadcast_in_dim.14), channel_id=1, replica_groups={{0,64,128,192,16,80,144,208},{81,145,209,17,65,129,193,1},{2,66,130,194..., dimensions={0} | all-to-all | bytes 1605632 | tf_op jit(solution)/shard_map/all_to_all | solution.py:40
  43.8 2.2 broadcast_in_dim.15
  46.0 5.8 %all-to-all-start.1 = ((bf16[4,8,392,128]{3,2,1,0:T(8,128)(2,1)}), bf16[4,8,392,128]{3,2,1,0:T(8,128)(2,1)}, u32[]{:S(2)}, u32[]{:S(2)}) async-start(bf16[4,8,392,128]{3,2,1,0:T(8,128)(2,1)} %broadcast_in_dim.15), calls=%async_computation.1 | async-start | bytes 6422528 | tf_op jit(solution)/shard_map/all_to_all | solution.py:40
  51.8 0.8 constant_dynamic-slice_fusion.1
  52.6 0.0 all-gather.7.cloned.1.call-update
  52.7 1.6 collective-permute-start
  54.3 0.5 collective-permute-start.1
  54.8 2.1 collective-permute-start.2
  57.0 10.7 %collective-permute-done.m1 = bf16[256,1024]{1,0:T(8,128)(2,1)S(1)} collective-permute-done((bf16[256,1024]{1,0:T(8,128)(2,1)S(1)}, bf16[256,1024]{1,0:T(8,128)(2,1)S(1)}, u32[]{:S(2)}, u32[]{:S(2)}) %collective-permute-start) | collective-permute-done | bytes 524320 | tf_op jit(solution)/shard_map/ppermute | solution.py:63
  67.7 0.0 collective-permute-start.3
  67.7 0.8 collective-permute-done.1.m2
  68.5 0.0 collective-permute-start.4
  68.5 22.8 %collective-permute-done.2.m3 = bf16[256,1024]{1,0:T(8,128)(2,1)S(1)} collective-permute-done((bf16[256,1024]{1,0:T(8,128)(2,1)S(1)}, bf16[256,1024]{1,0:T(8,128)(2,1)S(1)}, u32[]{:S(2)}, u32[]{:S(2)}) %collective-permute-start.2) | collective-permute-done | bytes 524320 | tf_op jit(solution)/shard_map/ppermute | solution.py:63
  91.3 0.0 collective-permute-start.5
  91.3 0.7 pad_add_fusion.idx
  92.1 0.0 collective-permute-done.4.o2
  92.1 1.5 collective-permute-done.5.o3
  93.6 11.6 %first_ffn.1 = (bf16[4,8,384,128]{3,2,1,0:T(8,128)(2,1)}, f32[32,128]{1,0:T(8,128)}, f32[32,128]{1,0:T(8,128)}) custom-call(s32[2]{0:T(128)} %pad_add_fusion.idx, bf16[4,8,392,128]{3,2,1,0:T(8,128)(2,1)} %all-to-all-done.1.x, bf16[4096,512]{1,0:T(8,128)(2,1)} %all-gather.5.cloned.1.call-done.up, bf16[512,1024]{1,0:T(8,128)(2,1)} %own.1, ...), custom_call_target="tpu_custom_call" | custom-call | flops 3221225472 | bytes 14680064 | tf_op jit(solution)/shard_map/first_ffn/pallas_call | solution.py:219
  105.2 26.5 %all_to_all.46 = bf16[4,8,384,128]{3,2,1,0:T(8,128)(2,1)} all-to-all(bf16[4,8,384,128]{3,2,1,0:T(8,128)(2,1)} %get-tuple-element.10), channel_id=1, replica_groups={{0,32,8,40},{249,25,225,1},{2,34,10,42},{251,27,227,3},{4,36,12,44},{25..., dimensions={0} | all-to-all | bytes 6291456 | tf_op jit(solution)/shard_map/all_to_all | solution.py:40
  131.7 3.6 %reduce_sum.71 = bf16[8,384,128]{2,1,0:T(8,128)(2,1)} reduce(bf16[4,8,384,128]{3,2,1,0:T(8,128)(2,1)} %all_to_all.46, bf16[]{:T(256)} %constant.10.clone.1), dimensions={0}, to_apply=%region_0.0 | reduce | flops 1179648 | bytes 3932162 | tf_op jit(solution)/shard_map/reduce_sum | solution.py:52
  135.4 4.6 %all-to-all-start.3 = ((bf16[8,384,128]{2,1,0:T(8,128)(2,1)}), bf16[8,384,128]{2,1,0:T(8,128)(2,1)S(1)}, u32[]{:S(2)}, u32[]{:S(2)}) async-start(bf16[8,384,128]{2,1,0:T(8,128)(2,1)} %reduce_sum.71), calls=%async_computation.3 | async-start | bytes 1572864 | tf_op jit(solution)/shard_map/all_to_all | solution.py:40
  140.0 0.0 all-gather.9.cloned.1.call-start
  140.0 0.9 constant_dynamic-slice_fusion
  140.9 0.0 all-gather.9.cloned.1.call-update
  140.9 22.2 %all-to-all-done.3 = bf16[8,384,128]{2,1,0:T(8,128)(2,1)S(1)} async-done(((bf16[8,384,128]{2,1,0:T(8,128)(2,1)}), bf16[8,384,128]{2,1,0:T(8,128)(2,1)S(1)}, u32[]{:S(2)}, u32[]{:S(2)}) %all-to-all-start.3) | async-done | bytes 786464 | tf_op jit(solution)/shard_map/all_to_all | solution.py:40
  163.1 0.1 convert_reduce_fusion.1
  163.2 0.7 fusion.11
  163.9 0.1 broadcast_in_dim.16
  164.0 26.8 %all_to_all.47 = bf16[8,384,128]{2,1,0:T(8,128)(2,1)S(1)} all-to-all(bf16[8,384,128]{2,1,0:T(8,128)(2,1)S(1)} %broadcast_in_dim.16), channel_id=1, replica_groups={{0,64,128,192,16,80,144,208},{81,145,209,17,65,129,193,1},{2,66,130,194..., dimensions={0} | all-to-all | bytes 1572864 | tf_op jit(solution)/shard_map/all_to_all | solution.py:40
  190.8 2.4 broadcast_in_dim.17
  193.3 5.1 %all-to-all-start.5 = ((bf16[4,8,384,128]{3,2,1,0:T(8,128)(2,1)}), bf16[4,8,384,128]{3,2,1,0:T(8,128)(2,1)}, u32[]{:S(2)}, u32[]{:S(2)}) async-start(bf16[4,8,384,128]{3,2,1,0:T(8,128)(2,1)} %broadcast_in_dim.17), calls=%async_computation.5 | async-start | bytes 6291456 | tf_op jit(solution)/shard_map/all_to_all | solution.py:40
  198.4 20.9 %all-to-all-done.5.x = bf16[4,8,384,128]{3,2,1,0:T(8,128)(2,1)} async-done(((bf16[4,8,384,128]{3,2,1,0:T(8,128)(2,1)}), bf16[4,8,384,128]{3,2,1,0:T(8,128)(2,1)}, u32[]{:S(2)}, u32[]{:S(2)}) %all-to-all-start.5) | async-done | bytes 3145760 | tf_op jit(solution)/shard_map/all_to_all | solution.py:40
  219.3 11.7 %second_ffn.1 = (bf16[4,8,384,128]{3,2,1,0:T(8,128)(2,1)}, bf16[384,128]{1,0:T(8,128)(2,1)}) custom-call(s32[2]{0:T(128)} %pad_add_fusion.idx, bf16[4,8,384,128]{3,2,1,0:T(8,128)(2,1)} %all-to-all-done.5.x, bf16[4096,512]{1,0:T(8,128)(2,1)} %all-gather.7.cloned.1.call-done.up, bf16[8,256,1024]{2,1,0:T(8,128)(2,1)} %bitcast.19, ...), custom_call_target="tpu_custom_call" | custom-call | flops 3221225472 | bytes 14680064 | tf_op jit(solution)/shard_map/second_ffn/pallas_call | solution.py:245
  231.0 26.5 %all_to_all.48 = bf16[4,8,384,128]{3,2,1,0:T(8,128)(2,1)} all-to-all(bf16[4,8,384,128]{3,2,1,0:T(8,128)(2,1)} %get-tuple-element.14), channel_id=1, replica_groups={{0,32,8,40},{249,25,225,1},{2,34,10,42},{251,27,227,3},{4,36,12,44},{25..., dimensions={0} | all-to-all | bytes 6291456 | tf_op jit(solution)/shard_map/all_to_all | solution.py:40
  257.5 2.5 reduce_sum.73
  260.0 27.1 %all_to_all.49 = bf16[8,384,128]{2,1,0:T(8,128)(2,1)S(1)} all-to-all(bf16[8,384,128]{2,1,0:T(8,128)(2,1)S(1)} %reduce_sum.73), channel_id=1, replica_groups={{0,64,128,192,16,80,144,208},{81,145,209,17,65,129,193,1},{2,66,130,194..., dimensions={0} | all-to-all | bytes 1572864 | tf_op jit(solution)/shard_map/all_to_all | solution.py:40
  287.2 0.1 convert_reduce_fusion
  287.3 0.2 fusion
  287.5 0.1 broadcast_in_dim.20
  287.5 14.7 %all_to_all.50 = f32[32,1,768]{2,1,0:T(1,128)S(1)} all-to-all(f32[32,1,768]{2,1,0:T(1,128)S(1)} %broadcast_in_dim.20), channel_id=1, replica_groups=mesh['ra_0'=8,'ra_1'=4,'cb'=4,'dp'=2] {'ra_0','ra_1'}, dimensions={0} | all-to-all | bytes 196608 | tf_op jit(solution)/shard_map/all_to_all | solution.py:58
  302.3 0.1 reduce_sum.77
  302.4 0.8 add_convert_fusion
  (36 shorter events, 0.1 us)
Async XLA Ops:
  6.5 1.2 copy-start
  6.5 87.0 %all-gather.5.cloned.1.call-start = ((), (), s32[]{:S(2)}) async-start(), calls=%async_computation.9 | async-start | bytes 4718592 | tf_op jit(solution)/shard_map/all_gather | solution.py:281
  46.0 5.8 %copy-start.3 = (bf16[1024,512]{1,0:T(8,128)(2,1)S(1)}, bf16[1024,512]{1,0:T(8,128)(2,1)}, u32[]{:S(2)}) copy-start(bf16[1024,512]{1,0:T(8,128)(2,1)} %param.12) | copy-start | bytes 3145732
  46.0 6.7 %copy-start.4 = (bf16[512,1024]{1,0:T(8,128)(2,1)S(1)}, bf16[512,1024]{1,0:T(8,128)(2,1)}, u32[]{:S(2)}) copy-start(bf16[512,1024]{1,0:T(8,128)(2,1)} %own.1) | copy-start | bytes 3145732
  46.0 47.5 %all-to-all-start.1 = ((bf16[4,8,392,128]{3,2,1,0:T(8,128)(2,1)}), bf16[4,8,392,128]{3,2,1,0:T(8,128)(2,1)}, u32[]{:S(2)}, u32[]{:S(2)}) async-start(bf16[4,8,392,128]{3,2,1,0:T(8,128)(2,1)} %broadcast_in_dim.15), calls=%async_computation.1 | async-start | bytes 6422528 | tf_op jit(solution)/shard_map/all_to_all | solution.py:40
  51.8 146.6 %all-gather.7.cloned.1.call-start = ((), (), s32[]{:S(2)}) async-start(), calls=%async_computation.10 | async-start | bytes 4718592 | tf_op jit(solution)/shard_map/all_gather | solution.py:286
  52.7 15.0 %collective-permute-start = (bf16[256,1024]{1,0:T(8,128)(2,1)S(1)}, bf16[256,1024]{1,0:T(8,128)(2,1)S(1)}, u32[]{:S(2)}, u32[]{:S(2)}) collective-permute-start(bf16[256,1024]{1,0:T(8,128)(2,1)S(1)} %constant_dynamic-slice_fusion.2), channel_id=1, source_target_pairs={{0,2},{2,4},{4,6},{6,0},{1,3},{3,5},{5,7},{7,1},{8,10},{10,12},{12... | collective-permute-start | bytes 1572872 | tf_op jit(solution)/shard_map/ppermute | solution.py:63
  54.3 14.2 %collective-permute-start.1 = (bf16[256,1024]{1,0:T(8,128)(2,1)S(1)}, bf16[256,1024]{1,0:T(8,128)(2,1)S(1)}, u32[]{:S(2)}, u32[]{:S(2)}) collective-permute-start(bf16[256,1024]{1,0:T(8,128)(2,1)S(1)} %constant_dynamic-slice_fusion.2), channel_id=1, source_target_pairs={{0,6},{2,0},{4,2},{6,4},{1,7},{3,1},{5,3},{7,5},{8,14},{10,8},{12,... | collective-permute-start | bytes 1572872 | tf_op jit(solution)/shard_map/ppermute | solution.py:63
  54.8 36.5 %collective-permute-start.2 = (bf16[256,1024]{1,0:T(8,128)(2,1)S(1)}, bf16[256,1024]{1,0:T(8,128)(2,1)S(1)}, u32[]{:S(2)}, u32[]{:S(2)}) collective-permute-start(bf16[256,1024]{1,0:T(8,128)(2,1)S(1)} %constant_dynamic-slice_fusion.2), channel_id=1, source_target_pairs={{0,4},{2,6},{4,0},{6,2},{1,5},{3,7},{5,1},{7,3},{8,12},{10,14},{12... | collective-permute-start | bytes 1572872 | tf_op jit(solution)/shard_map/ppermute | solution.py:63
  67.7 25.9 %copy-start.8 = (bf16[256,1024]{1,0:T(8,128)(2,1)}, bf16[256,1024]{1,0:T(8,128)(2,1)S(1)}, u32[]{:S(2)}) copy-start(bf16[256,1024]{1,0:T(8,128)(2,1)S(1)} %collective-permute-done.m1) | copy-start | bytes 1572868
  67.7 24.4 %collective-permute-start.3 = (bf16[256,1024]{1,0:T(8,128)(2,1)S(1)}, bf16[256,1024]{1,0:T(8,128)(2,1)S(1)}, u32[]{:S(2)}, u32[]{:S(2)}) collective-permute-start(bf16[256,1024]{1,0:T(8,128)(2,1)S(1)} %collective-permute-done.m1), channel_id=1, source_target_pairs={{0,1},{1,0},{2,3},{3,2},{4,5},{5,4},{6,7},{7,6},{8,9},{9,8},{10,11... | collective-permute-start | bytes 1572872 | tf_op jit(solution)/shard_map/ppermute | solution.py:63
  68.5 25.1 %copy-start.9 = (bf16[256,1024]{1,0:T(8,128)(2,1)}, bf16[256,1024]{1,0:T(8,128)(2,1)S(1)}, u32[]{:S(2)}) copy-start(bf16[256,1024]{1,0:T(8,128)(2,1)S(1)} %collective-permute-done.1.m2) | copy-start | bytes 1572868
  68.5 23.6 %collective-permute-start.4 = (bf16[256,1024]{1,0:T(8,128)(2,1)S(1)}, bf16[256,1024]{1,0:T(8,128)(2,1)}, u32[]{:S(2)}, u32[]{:S(2)}) collective-permute-start(bf16[256,1024]{1,0:T(8,128)(2,1)S(1)} %collective-permute-done.1.m2), channel_id=1, source_target_pairs={{0,1},{1,0},{2,3},{3,2},{4,5},{5,4},{6,7},{7,6},{8,9},{9,8},{10,11... | collective-permute-start | bytes 1572872 | tf_op jit(solution)/shard_map/ppermute | solution.py:63
  91.3 2.3 copy-start.10
  91.3 2.2 collective-permute-start.5
  92.0 1.5 copy-start.11
  131.7 8.3 %copy-start.5 = (bf16[512,1024]{1,0:T(8,128)(2,1)S(1)}, bf16[512,1024]{1,0:T(8,128)(2,1)}, u32[]{:S(2)}) copy-start(bf16[512,1024]{1,0:T(8,128)(2,1)} %param.13) | copy-start | bytes 3145732
  131.7 31.4 %copy-start.1 = (bf16[384,128]{1,0:T(8,128)(2,1)S(1)}, bf16[384,128]{1,0:T(8,128)(2,1)}, u32[]{:S(2)}) copy-start(bf16[384,128]{1,0:T(8,128)(2,1)} %param.9) | copy-start | bytes 294916
  135.4 27.7 %all-to-all-start.3 = ((bf16[8,384,128]{2,1,0:T(8,128)(2,1)}), bf16[8,384,128]{2,1,0:T(8,128)(2,1)S(1)}, u32[]{:S(2)}, u32[]{:S(2)}) async-start(bf16[8,384,128]{2,1,0:T(8,128)(2,1)} %reduce_sum.71), calls=%async_computation.3 | async-start | bytes 1572864 | tf_op jit(solution)/shard_map/all_to_all | solution.py:40
  140.0 58.4 %all-gather.9.cloned.1.call-start = ((), (), s32[]{:S(2)}) async-start(), calls=%async_computation.11 | async-start | bytes 4718592 | tf_op jit(solution)/shard_map/all_gather | solution.py:287
  193.3 26.0 %all-to-all-start.5 = ((bf16[4,8,384,128]{3,2,1,0:T(8,128)(2,1)}), bf16[4,8,384,128]{3,2,1,0:T(8,128)(2,1)}, u32[]{:S(2)}, u32[]{:S(2)}) async-start(bf16[4,8,384,128]{3,2,1,0:T(8,128)(2,1)} %broadcast_in_dim.17), calls=%async_computation.5 | async-start | bytes 6291456 | tf_op jit(solution)/shard_map/all_to_all | solution.py:40
  257.5 29.8 %copy-start.2 = (bf16[384,128]{1,0:T(8,128)(2,1)S(1)}, bf16[384,128]{1,0:T(8,128)(2,1)}, u32[]{:S(2)}) copy-start(bf16[384,128]{1,0:T(8,128)(2,1)} %get-tuple-element.13) | copy-start | bytes 294916
  257.5 44.9 %copy-start.6 = (f32[128]{0:T(128)S(1)}, f32[128]{0:T(128)}, u32[]{:S(2)}) copy-start(f32[128]{0:T(128)} %param.17) | copy-start | bytes 1540
  257.5 44.9 %copy-start.7 = (f32[128]{0:T(128)S(1)}, f32[128]{0:T(128)}, u32[]{:S(2)}) copy-start(f32[128]{0:T(128)} %param.16) | copy-start | bytes 1540
Sparse Core Ops, SparseCore 0:
  9.2 36.5 all-gather.4
  54.5 43.3 all-gather.6
  142.6 34.0 all-gather.8
where the time goes:
time: 311 us; the launch traced here: 310 us
  blocking collectives  155 us (50%)
  waiting for transfers between devices  79 us (25%)
  Pallas kernels  23.3 us (7%)
  starting transfers between devices  19.8 us (6%)
  between operations  13.3 us (4%)
  local copies, waits for them, and re-layouts  9.66 us (3%)
  other arithmetic  9.61 us (3%)
    all_to_all x5, blocking collectives, swap(): lax.all_to_all(blocks, ALL, 0, 0, axis_index_groups=groups, tiled=True)  140 us
    all_to_all x3, waiting for transfers between devices, swap(): lax.all_to_all(blocks, ALL, 0, 0, axis_index_groups=groups, tiled=True)  43.1 us
    ppermute x6, waiting for transfers between devices, shift(): return lax.ppermute(a, axis, [(i, (i + by) % n) for i in range(n)])  35.8 us
    all_to_all x3, starting transfers between devices, swap(): lax.all_to_all(blocks, ALL, 0, 0, axis_index_groups=groups, tiled=True)  15.5 us
    all_to_all x1, blocking collectives, stats_to_all(): lax.all_to_all(jnp.broadcast_to(row[None], (n, *row.shape)), RA, 0, 0, ti...  14.7 us
    pallas_call x1, Pallas kernels, second_ffn(): pl.pallas_call(second_kernel, out_shape=(jax.ShapeDtypeStruct(x.shape, BF...  11.7 us
    pallas_call x1, Pallas kernels, first_ffn(): pl.pallas_call(first_kernel, out_shape=(jax.ShapeDtypeStruct((4, nb // 4,...  11.6 us
  transfers between devices with their start and end apart: 12, of which 6 were waited for; matrix products, arithmetic and copies ran while one was open for 4% of the time, Pallas kernels for 4%

commit v1 on v0

v1 whole, which is shorter than its diff:
```python
import jax
import jax.numpy as jnp
from jax import lax
from jax.experimental import pallas as pl
from jax.experimental.pallas import tpu as pltpu
from jax.sharding import Mesh
from jax.sharding import PartitionSpec as P


Z, Y, X, C = "ra_0", "ra_1", "cb", "dp"
RA = (Z, Y)
ALL = (Z, Y, X, C)
RESID = 1.4142135
EPS = 0.5
BF = jnp.bfloat16
F32 = jnp.float32
NZ, NY = 8, 4


def place(z, y, core, nz, ny):
    z, y = (z - core) % nz, (y - core) % ny
    return (y % 2) * 2 + z % 2, (y // 2) * (nz // 2) + z // 2


def groups_of(sizes):
    nz, ny, nx, nc = sizes
    near, far = {}, {}
    for z in range(nz):
        for y in range(ny):
            for x in range(nx):
                for c in range(nc):
                    at = ((z * ny + y) * nx + x) * nc + c
                    a, b = place(z, y, c, nz, ny)
                    near.setdefault((x, c, b), {})[a] = at
                    far.setdefault((x, c, a), {})[b] = at
    pairs = [[(g[a], g[a ^ d]) for g in near.values() for a in range(4)] for d in range(4)]
    return pairs, [[m[i] for i in sorted(m)] for m in far.values()]


def far_swap(blocks, far):
    return lax.all_to_all(blocks, ALL, 0, 0, axis_index_groups=far, tiled=True)


def far_to_all(block, far):
    return far_swap(jnp.broadcast_to(block[None], (len(far[0]), *block.shape)), far)


def near_send(blocks, near):
    return [blocks[0]] + [lax.ppermute(blocks[d], ALL, near[d]) for d in (3, 1, 2)]


def near_swap(blocks, near):
    own, diagonal, one, two = near_send(blocks, near)
    return [own, one, two, diagonal]


def gathered(block, near, far):
    return near_swap([far_to_all(block, far)] * 4, near)


def scattered_sum(parts, near, far):
    some = sum(p.astype(F32) for p in near_swap(parts, near)).astype(BF)
    return jnp.sum(far_swap(some, far).astype(F32), axis=0)


def stats_to_all(row):
    n = lax.axis_size(RA)
    return lax.all_to_all(jnp.broadcast_to(row[None], (n, *row.shape)), RA, 0, 0, tiled=True)


def shift(a, axis, by):
    n = lax.axis_size(axis)
    return lax.ppermute(a, axis, [(i, (i + by) % n) for i in range(n)])


def half_of(w):
    rows = w.shape[0] // 2
    return lax.dynamic_slice_in_dim(w, lax.axis_index(C) * rows, rows, 0)


def split3(v):
    hi = lax.reduce_precision(v, 8, 7)
    mid = lax.reduce_precision(v - hi, 8, 7)
    return [hi, mid, v - hi - mid]


def from_peer(idx, d, q):
    core, p = idx[1], idx[2] ^ d
    z = ((q % (NZ // 2)) * 2 + (p & 1) + core) & (NZ - 1)
    y = ((q // (NZ // 2)) * 2 + (p >> 1) + core) & (NY - 1)
    return z * NY + y


def to_peer(idx, d, j, yh):
    core, p = idx[1], idx[2] ^ d
    zz = (p & 1) ^ core
    zh = (j - core * (1 - zz)) & (NZ // 2 - 1)
    y = (yh * 2 + (p >> 1) + core) & (NY - 1)
    return (2 * j + zz) * NY + y, yh * (NZ // 2) + zh


def matmuls(idx, xs, upv, dv, ov, outs, out_sems, wait_up, wait_down, nx):
    deep = xs.shape[1] // nx
    pre = None
    for k in range(nx):
        wait_up(k)
        rows = slice(k * deep, (k + 1) * deep)
        term = jnp.dot(xs[:, rows], upv[rows, :], preferred_element_type=F32)
        pre = term if pre is None else pre + term
    hidden = jnp.square(jnp.maximum(pre, 0.0)).astype(BF)
    half = hidden.shape[1] // 2
    copies = []
    wait_down()
    for j in range(nx):
        part = jnp.dot(hidden[:, :half], dv[2 * j], preferred_element_type=F32)
        part = part + jnp.dot(hidden[:, half:], dv[2 * j + 1], preferred_element_type=F32)
        part = part.astype(BF)
        for i in range(2 * NY):
            ov[2 * NY * j + i] = part[:, i * 128 : (i + 1) * 128]
        for d in range(4):
            for yh in range(NY // 2):
                slot, q = to_peer(idx, d, j, yh)
                sem = out_sems.at[(d * nx + j) * 2 + yh]
                copy = pltpu.make_async_copy(ov.at[slot], outs[d].at[q], sem)
                copy.start()
                copies.append(copy)
    for copy in copies:
        copy.wait()


def first_kernel(
    idx, x0, x1, x2, x3, up, own, m1, m2, m3, o1, o2, o3, u0, u1, u2, u3, xs, upv, dv, ov, x_sem, up_sem, d_sems, out_sems
):
    nx = dv.shape[0] // 2
    rows = dv.shape[1]
    me, core = idx[0], idx[1]
    x_copies = []
    for d, x in enumerate((x0, x1, x2, x3)):
        for q in range(x.shape[0]):
            at = pl.multiple_of(from_peer(idx, d, q) * 128, 128)
            copy = pltpu.make_async_copy(x.at[q], xs.at[:, pl.ds(at, 128)], x_sem.at[d * x.shape[0] + q])
            copy.start()
            x_copies.append(copy)
    deep = upv.shape[0] // nx
    up_copies = []
    for k in range(nx):
        chunk = pl.ds(k * deep, deep)
        up_copies.append(pltpu.make_async_copy(up.at[chunk], upv.at[chunk], up_sem.at[k]))
        up_copies[-1].start()
    d_copies = [
        pltpu.make_async_copy(own.at[pl.ds(0, rows)], dv.at[2 * me], d_sems.at[0]),
        pltpu.make_async_copy(own.at[pl.ds(rows, rows)], dv.at[2 * me + 1], d_sems.at[1]),
    ]
    for i, (by, mine, other) in enumerate(((1, m1, o1), (nx - 1, m2, o2), (2, m3, o3))):
        source = lax.rem(me + (nx - by), nx)
        d_copies.append(pltpu.make_async_copy(mine, dv.at[2 * source + core], d_sems.at[2 + 2 * i]))
        d_copies.append(pltpu.make_async_copy(other, dv.at[2 * source + 1 - core], d_sems.at[3 + 2 * i]))
    for copy in d_copies:
        copy.start()

    def wait_up(k):
        if k == 0:
            for copy in x_copies:
                copy.wait()
        up_copies[k].wait()

    def wait_down():
        for copy in d_copies:
            copy.wait()

    matmuls(idx, xs, upv, dv, ov, (u0, u1, u2, u3), out_sems, wait_up, wait_down, nx)


def second_kernel(
    idx, x0, x1, x2, x3, up, down, mixed, own_gain, own_bias, u0, u1, u2, u3, own, xs, xv, upv, dv, ov, gain, bias,
    x_sem, up_sem, d_sem, out_sems,
):
    nx = dv.shape[0] // 2
    nb = xv.shape[0]
    tokens = xs.shape[0]
    x_copies = []
    for d, x in enumerate((x0, x1, x2, x3)):
        for q in range(x.shape[0]):
            copy = pltpu.make_async_copy(x.at[q], xv.at[from_peer(idx, d, q)], x_sem.at[d * x.shape[0] + q])
            copy.start()
            x_copies.append(copy)
    up_copy = pltpu.make_async_copy(up, upv, up_sem)
    d_copy = pltpu.make_async_copy(down, dv, d_sem)
    up_copy.start()
    d_copy.start()
    for copy in x_copies:
        copy.wait()
    step = 64
    width = nb * 128
    for b in range(nb):
        t = xv[b, tokens : tokens + 8, :].astype(F32)
        gain[b : b + 1] = t[0:1] + t[1:2] + t[2:3]
        bias[b : b + 1] = t[3:4] + t[4:5] + t[5:6]

    def norm(i, carry):
        rows = pl.ds(pl.multiple_of(i * step, step), step)
        acc = jnp.zeros((step, 128), F32)
        for b in range(nb):
            acc = acc + xv[b, rows, :].astype(F32)
        mean = jnp.sum(acc, axis=1, keepdims=True) / width
        acc = jnp.zeros((step, 128), F32)
        for b in range(nb):
            d = xv[b, rows, :].astype(F32) - mean
            acc = acc + d * d
        scale = lax.rsqrt(jnp.sum(acc, axis=1, keepdims=True) / width + EPS)
        for b in range(nb):
            d = (xv[b, rows, :].astype(F32) - mean) * scale
            xs[rows, b * 128 : (b + 1) * 128] = (d * gain[b : b + 1] + bias[b : b + 1]).astype(BF)
        own[rows, :] = ((mixed[rows, :] - mean) * scale * own_gain[...] + own_bias[...]).astype(BF)
        return carry

    lax.fori_loop(0, tokens // step, norm, 0)

    def wait_up(k):
        if k == 0:
            up_copy.wait()

    matmuls(idx, xs, upv, dv, ov, (u0, u1, u2, u3), out_sems, wait_up, d_copy.wait, nx)


ANY = pl.BlockSpec(memory_space=pltpu.MemorySpace.HBM)
VMEM = pl.BlockSpec(memory_space=pltpu.MemorySpace.VMEM)
SMEM = pl.BlockSpec(memory_space=pltpu.MemorySpace.SMEM)


def first_ffn(idx, x, up, own, mine, others):
    tokens = x[0].shape[1]
    width, ff = up.shape
    nx, nb = lax.axis_size(X), NZ * NY
    return pl.pallas_call(
        first_kernel,
        out_shape=[jax.ShapeDtypeStruct((nb // 4, tokens, 128), BF)] * 4,
        in_specs=[SMEM] + [ANY] * 12,
        out_specs=[ANY] * 4,
        scratch_shapes=[
            pltpu.VMEM((tokens, width), BF),
            pltpu.VMEM((width, ff), BF),
            pltpu.VMEM((2 * nx, ff // 2, width // nx), BF),
            pltpu.VMEM((nb, tokens, 128), BF),
            pltpu.SemaphoreType.DMA((nb,)),
            pltpu.SemaphoreType.DMA((nx,)),
            pltpu.SemaphoreType.DMA((8,)),
            pltpu.SemaphoreType.DMA((nb,)),
        ],
        cost_estimate=pl.CostEstimate(flops=4 * tokens * width * ff, bytes_accessed=14 << 20, transcendentals=0),
        name="first_ffn",
    )(idx, *x, up, own, *mine, *others)


def second_ffn(idx, x, tokens, up, down, mixed, own_gain, own_bias):
    width, ff = up.shape
    nx, nb = lax.axis_size(X), NZ * NY
    return pl.pallas_call(
        second_kernel,
        out_shape=[jax.ShapeDtypeStruct((nb // 4, tokens, 128), BF)] * 4 + [jax.ShapeDtypeStruct((tokens, 128), BF)],
        in_specs=[SMEM] + [ANY] * 6 + [VMEM] * 3,
        out_specs=[ANY] * 4 + [VMEM],
        scratch_shapes=[
            pltpu.VMEM((tokens, width), BF),
            pltpu.VMEM((nb, *x[0].shape[1:]), BF),
            pltpu.VMEM((width, ff), BF),
            pltpu.VMEM((2 * nx, ff // 2, width // nx), BF),
            pltpu.VMEM((nb, tokens, 128), BF),
            pltpu.VMEM((nb, 128), F32),
            pltpu.VMEM((nb, 128), F32),
            pltpu.SemaphoreType.DMA((nb,)),
            pltpu.SemaphoreType.DMA,
            pltpu.SemaphoreType.DMA,
            pltpu.SemaphoreType.DMA((nb,)),
        ],
        cost_estimate=pl.CostEstimate(flops=4 * tokens * width * ff, bytes_accessed=14 << 20, transcendentals=0),
        name="second_ffn",
    )(idx, *x, up, down, mixed, own_gain, own_bias)


def body(
    stream,
    up_first,
    down_first,
    up_second,
    down_second,
    gain_first,
    bias_first,
    gain_second,
    bias_second,
):
    tokens = stream.shape[0]
    near, far = groups_of([lax.axis_size(axis) for axis in ALL])
    half = half_of(down_first)
    mine = [shift(half, X, by) for by in (1, -1, 2)]
    up_1 = lax.all_gather(half_of(up_first), (X, C), axis=0, tiled=True)
    x_far = far_to_all(stream, far)
    x_all = near_swap([x_far] * 4, near)
    others = [shift(m, C, 1) for m in mine]
    up_2 = lax.all_gather(half_of(up_second), (X, C), axis=0, tiled=True)
    down_2 = lax.all_gather(half_of(down_second), (X, C), axis=0, tiled=False)
    down_2 = down_2.reshape(-1, *half.shape)
    core = lax.axis_index(C)
    a, _ = place(lax.axis_index(Z), lax.axis_index(Y), core, NZ, NY)
    idx = jnp.stack([lax.axis_index(X), core, a]).astype(jnp.int32)
    parts = first_ffn(idx, x_all, up_1, down_first, mine, others)
    mixed = RESID * stream.astype(F32) + scattered_sum(parts, near, far)
    tail = jnp.stack(split3(gain_first) + split3(bias_first) + [jnp.zeros_like(gain_first)] * 2)
    mixed_all = gathered(jnp.concatenate([mixed, tail], axis=0).astype(BF), near, far)
    *parts, x = second_ffn(
        idx, mixed_all, tokens, up_2, down_2, mixed, gain_first[None], bias_first[None]
    )
    mixed = RESID * x.astype(F32) + scattered_sum(parts, near, far)
    width = mixed.shape[1] * lax.axis_size(RA)
    sums = jnp.concatenate([jnp.sum(mixed, axis=1), jnp.sum(mixed * mixed, axis=1)])
    sums = jnp.sum(stats_to_all(sums[None]), axis=0)[0]
    mean = sums[:tokens, None] / width
    var = sums[tokens:, None] / width - mean * mean
    return ((mixed - mean) * lax.rsqrt(var + EPS) * gain_second + bias_second).astype(BF)


def solution(mesh):
    torus = Mesh(mesh.devices.reshape(NZ, NY, mesh.shape["cb"], mesh.shape["dp"]), (Z, Y, X, C))
    in_specs = (
        P((X, C), RA),
        P(X, RA),
        P(RA, X),
        P(X, RA),
        P(RA, X),
        P(RA),
        P(RA),
        P(RA),
        P(RA),
    )
    out_specs = P((X, C), RA)

    return jax.shard_map(body, mesh=torus, in_specs=in_specs, out_specs=out_specs, check_vma=False)
```

time: 311 us -> 281 us (0.904)
  blocking collectives: 155 us -> 69.8 us
  waiting for transfers between devices: 79 us -> 118 us
  starting transfers between devices: 19.8 us -> 40.2 us
    all_to_all x5 -> x2, blocking collectives: 140 us -> 54.7 us  [far_swap(): return lax.all_to_all(blocks, ALL, 0, 0, axis_index_groups=far, tiled=True)]
    ppermute x0 -> x12, waiting for transfers between devices: none -> 56.8 us  [near_send(): lax.ppermute(blocks[d], ALL, near[d])]
    all_to_all x3 -> x2, waiting for transfers between devices: 43.1 us -> 23.7 us  [far_swap(): return lax.all_to_all(blocks, ALL, 0, 0, axis_index_groups=far, tiled=True)]
    ppermute x0 -> x12, starting transfers between devices: none -> 14.3 us  [near_send(): lax.ppermute(blocks[d], ALL, near[d])]
    reduce_sum x4 -> x2, other arithmetic: 6.38 us -> 0.21 us  [scattered_sum(): return jnp.sum(far_swap(some, far).astype(F32), axis=0)]
    all_to_all x3 -> x2, starting transfers between devices: 15.5 us -> 21.1 us  [far_swap(): return lax.all_to_all(blocks, ALL, 0, 0, axis_index_groups=far, tiled=True)]
    broadcast_in_dim x4 -> x2, local copies, waits for them, and re-layouts: 4.82 us -> 1.14 us  [far_to_all(): jnp.broadcast_to(block[None], (len(far[0]), *block.shape))]
    convert_element_type x1 -> x2, other arithmetic: 0.69 us -> 4.05 us  [scattered_sum(): some = sum((p.astype(F32) for p in near_swap(parts, near))).astype(BF)]
  transfers between devices with their start and end apart: 12 -> 23, of which waited for: 6 -> 13; matrix products, arithmetic and copies ran while one was open for 4% -> 3% of each run, Pallas kernels for 4% -> 4%
where the time goes in v1:
time: 281 us; the launch traced here: 279 us
  waiting for transfers between devices  118 us (42%)
  blocking collectives  69.8 us (25%)
  starting transfers between devices  40.2 us (14%)
  Pallas kernels  23.9 us (9%)
  between operations  13.3 us (5%)
  local copies, waits for them, and re-layouts  7.07 us (3%)
  other arithmetic  6.7 us (2%)
    ppermute x12, waiting for transfers between devices, near_send(): lax.ppermute(blocks[d], ALL, near[d])  56.8 us
    all_to_all x2, blocking collectives, far_swap(): return lax.all_to_all(blocks, ALL, 0, 0, axis_index_groups=far, tiled=True)  54.7 us
    ppermute x6, waiting for transfers between devices, shift(): return lax.ppermute(a, axis, [(i, (i + by) % n) for i in range(n)])  37.7 us
    all_to_all x2, waiting for transfers between devices, far_swap(): return lax.all_to_all(blocks, ALL, 0, 0, axis_index_groups=far, tiled=True)  23.7 us
    all_to_all x2, starting transfers between devices, far_swap(): return lax.all_to_all(blocks, ALL, 0, 0, axis_index_groups=far, tiled=True)  21.1 us
    all_to_all x1, blocking collectives, stats_to_all(): lax.all_to_all(jnp.broadcast_to(row[None], (n, *row.shape)), RA, 0, 0, ti...  15.1 us
    ppermute x12, starting transfers between devices, near_send(): lax.ppermute(blocks[d], ALL, near[d])  14.3 us
    pallas_call x1, Pallas kernels, second_ffn(): pl.pallas_call(second_kernel, out_shape=[jax.ShapeDtypeStruct((nb // 4, t...  13.9 us
  transfers between devices with their start and end apart: 23, of which 13 were waited for; matrix products, arithmetic and copies ran while one was open for 3% of the time, Pallas kernels for 4%

profile of v1, /device:TPU:2, one launch (start us, length us, event | category | flops | bytes accessed | tf_op | source)
XLA Modules:
  0.0 279.3 jit_solution(8957489017721756808)
XLA Ops:
  6.5 1.2 copy-done
  7.8 0.8 constant_dynamic-slice_fusion.3
  8.7 0.9 constant_dynamic-slice_fusion.1
  9.6 1.0 broadcast_in_dim.10
  10.6 11.1 %all-to-all-start = ((bf16[8,384,128]{2,1,0:T(8,128)(2,1)}), bf16[8,384,128]{2,1,0:T(8,128)(2,1)S(1)}, u32[]{:S(2)}, u32[]{:S(2)}) async-start(bf16[8,384,128]{2,1,0:T(8,128)(2,1)} %broadcast_in_dim.10), calls=%async_computation | async-start | bytes 1572864 | tf_op jit(solution)/shard_map/all_to_all | solution.py:41
  21.8 0.8 constant_dynamic-slice_fusion
  22.6 1.1 constant_dynamic-slice_fusion.2
  23.7 1.6 collective-permute-start.3
  25.3 0.5 collective-permute-start.4
  25.8 2.1 collective-permute-start.5
  28.0 21.8 %collective-permute-done.3.m1 = bf16[256,1024]{1,0:T(8,128)(2,1)} collective-permute-done((bf16[256,1024]{1,0:T(8,128)(2,1)S(1)}, bf16[256,1024]{1,0:T(8,128)(2,1)}, u32[]{:S(2)}, u32[]{:S(2)}) %collective-permute-start.3) | collective-permute-done | bytes 524320 | tf_op jit(solution)/shard_map/ppermute | solution.py:73
  49.7 1.0 collective-permute-start
  50.7 0.8 collective-permute-start.1
  51.5 1.8 collective-permute-start.2
  53.3 14.1 %collective-permute-done.5.m3 = bf16[256,1024]{1,0:T(8,128)(2,1)} collective-permute-done((bf16[256,1024]{1,0:T(8,128)(2,1)S(1)}, bf16[256,1024]{1,0:T(8,128)(2,1)}, u32[]{:S(2)}, u32[]{:S(2)}) %collective-permute-start.5) | collective-permute-done | bytes 524320 | tf_op jit(solution)/shard_map/ppermute | solution.py:73
  67.4 0.5 collective-permute-start.8
  67.9 0.6 pad_add_fusion.idx
  68.5 1.0 collective-permute-done.7.o2
  69.5 0.9 collective-permute-done.8.o3
  70.4 0.8 collective-permute-done.1.x2
  71.3 10.0 %first_ffn.1 = (bf16[8,384,128]{2,1,0:T(8,128)(2,1)}, bf16[8,384,128]{2,1,0:T(8,128)(2,1)}, bf16[8,384,128]{2,1,0:T(8,128)(2,1)}, bf16[8,384,128]{2,1,0:T(8,128)(2,1)}) custom-call(s32[3]{0:T(128)} %pad_add_fusion.idx, bf16[8,384,128]{2,1,0:T(8,128)(2,1)} %copy-done.2, bf16[8,384,128]{2,1,0:T(8,128)(2,1)} %copy-done.13, ...), custom_call_target="tpu_custom_call" | custom-call | flops 3221225472 | bytes 14680064 | tf_op jit(solution)/shard_map/first_ffn/pallas_call | solution.py:235
  81.3 1.6 collective-permute-start.10
  82.9 1.1 collective-permute-start.11
  84.0 0.9 collective-permute-start.9
  84.9 17.1 %collective-permute-done.10 = bf16[8,384,128]{2,1,0:T(8,128)(2,1)S(1)} collective-permute-done((bf16[8,384,128]{2,1,0:T(8,128)(2,1)}, bf16[8,384,128]{2,1,0:T(8,128)(2,1)S(1)}, u32[]{:S(2)}, u32[]{:S(2)}) %collective-permute-start.10) | collective-permute-done | bytes 786464 | tf_op jit(solution)/shard_map/ppermute | solution.py:49
  102.1 1.5 collective-permute-done.9
  103.6 2.5 add_convert_fusion.1
  106.1 10.0 %all-to-all-start.1 = ((bf16[8,384,128]{2,1,0:T(8,128)(2,1)}), bf16[8,384,128]{2,1,0:T(8,128)(2,1)S(1)}, u32[]{:S(2)}, u32[]{:S(2)}) async-start(bf16[8,384,128]{2,1,0:T(8,128)(2,1)} %add_convert_fusion.1), calls=%async_computation.1 | async-start | bytes 1572864 | tf_op jit(solution)/shard_map/all_to_all | solution.py:41
  116.1 23.7 %all-to-all-done.1 = bf16[8,384,128]{2,1,0:T(8,128)(2,1)S(1)} async-done(((bf16[8,384,128]{2,1,0:T(8,128)(2,1)}), bf16[8,384,128]{2,1,0:T(8,128)(2,1)S(1)}, u32[]{:S(2)}, u32[]{:S(2)}) %all-to-all-start.1) | async-done | bytes 786464 | tf_op jit(solution)/shard_map/all_to_all | solution.py:41
  139.9 0.7 fusion.11
  140.8 27.2 %all_to_all.25.x0 = bf16[8,392,128]{2,1,0:T(8,128)(2,1)S(1)} all-to-all(bf16[8,392,128]{2,1,0:T(8,128)(2,1)S(1)} %broadcast_in_dim.11), channel_id=1, replica_groups={{0,64,128,192,16,80,144,208},{81,145,209,17,65,129,193,1},{2,66,130,194..., dimensions={0} | all-to-all | bytes 1605632 | tf_op jit(solution)/shard_map/all_to_all | solution.py:41
  168.1 1.7 collective-permute-start.12
  169.7 1.9 collective-permute-start.13
  171.6 8.6 %collective-permute-done.12.x1 = bf16[8,392,128]{2,1,0:T(8,128)(2,1)S(1)} collective-permute-done((bf16[8,392,128]{2,1,0:T(8,128)(2,1)S(1)}, bf16[8,392,128]{2,1,0:T(8,128)(2,1)S(1)}, u32[]{:S(2)}, u32[]{:S(2)}) %collective-permute-start.12) | collective-permute-done | bytes 802848 | tf_op jit(solution)/shard_map/ppermute | solution.py:49
  180.2 10.3 %collective-permute-done.13.x2 = bf16[8,392,128]{2,1,0:T(8,128)(2,1)S(1)} collective-permute-done((bf16[8,392,128]{2,1,0:T(8,128)(2,1)S(1)}, bf16[8,392,128]{2,1,0:T(8,128)(2,1)S(1)}, u32[]{:S(2)}, u32[]{:S(2)}) %collective-permute-start.13) | collective-permute-done | bytes 802848 | tf_op jit(solution)/shard_map/ppermute | solution.py:49
  190.5 0.9 copy-done.12
  191.4 13.9 %second_ffn.1 = (bf16[8,384,128]{2,1,0:T(8,128)(2,1)}, bf16[8,384,128]{2,1,0:T(8,128)(2,1)}, bf16[8,384,128]{2,1,0:T(8,128)(2,1)}, bf16[8,384,128]{2,1,0:T(8,128)(2,1)}, bf16[384,128]{1,0:T(8,128)(2,1)}) custom-call(s32[3]{0:T(128)} %pad_add_fusion.idx, bf16[8,392,128]{2,1,0:T(8,128)(2,1)} %copy-done.1, bf16[8,392,128]{2,1,0:T(8,128)(2,1)} %copy-done.11, ...), custom_call_target="tpu_custom_call" | custom-call | flops 3221225472 | bytes 14680064 | tf_op jit(solution)/shard_map/second_ffn/pallas_call | solution.py:258
  205.3 0.6 collective-permute-start.15
  205.9 1.8 collective-permute-start.16
  207.7 1.1 collective-permute-start.17
  208.8 8.7 %collective-permute-done.15 = bf16[8,384,128]{2,1,0:T(8,128)(2,1)S(1)} collective-permute-done((bf16[8,384,128]{2,1,0:T(8,128)(2,1)}, bf16[8,384,128]{2,1,0:T(8,128)(2,1)S(1)}, u32[]{:S(2)}, u32[]{:S(2)}) %collective-permute-start.15) | collective-permute-done | bytes 786464 | tf_op jit(solution)/shard_map/ppermute | solution.py:49
  217.5 8.4 %collective-permute-done.16 = bf16[8,384,128]{2,1,0:T(8,128)(2,1)S(1)} collective-permute-done((bf16[8,384,128]{2,1,0:T(8,128)(2,1)}, bf16[8,384,128]{2,1,0:T(8,128)(2,1)S(1)}, u32[]{:S(2)}, u32[]{:S(2)}) %collective-permute-start.16) | collective-permute-done | bytes 786464 | tf_op jit(solution)/shard_map/ppermute | solution.py:49
  226.0 1.3 collective-permute-done.17
  227.3 1.5 add_convert_fusion
  228.9 27.5 %all_to_all.26 = bf16[8,384,128]{2,1,0:T(8,128)(2,1)S(1)} all-to-all(bf16[8,384,128]{2,1,0:T(8,128)(2,1)S(1)} %add_convert_fusion), channel_id=1, replica_groups={{0,64,128,192,16,80,144,208},{81,145,209,17,65,129,193,1},{2,66,130,194..., dimensions={0} | all-to-all | bytes 1572864 | tf_op jit(solution)/shard_map/all_to_all | solution.py:41
  256.5 0.2 fusion
  256.8 15.1 %all_to_all.27 = f32[32,1,768]{2,1,0:T(1,128)S(1)} all-to-all(f32[32,1,768]{2,1,0:T(1,128)S(1)} %broadcast_in_dim.14), channel_id=1, replica_groups=mesh['ra_0'=8,'ra_1'=4,'cb'=4,'dp'=2] {'ra_0','ra_1'}, dimensions={0} | all-to-all | bytes 196608 | tf_op jit(solution)/shard_map/all_to_all | solution.py:68
  272.0 0.8 add_convert_fusion.2
  (59 shorter events, 0.8 us)
Async XLA Ops:
  6.5 1.2 copy-start
  6.5 2.1 copy-start.5
  6.5 64.7 %all-gather.5.cloned.1.call-start = ((), (), s32[]{:S(2)}) async-start(), calls=%async_computation.5 | async-start | bytes 4718592 | tf_op jit(solution)/shard_map/all_gather | solution.py:296
  7.8 1.8 copy-start.3
  8.6 163.0 %all-gather.7.cloned.1.call-start = ((), (), s32[]{:S(2)}) async-start(), calls=%async_computation.6 | async-start | bytes 4718592 | tf_op jit(solution)/shard_map/all_gather | solution.py:300
  9.5 12.2 %copy-start.6 = (bf16[512,1024]{1,0:T(8,128)(2,1)S(1)}, bf16[512,1024]{1,0:T(8,128)(2,1)}, u32[]{:S(2)}) copy-start(bf16[512,1024]{1,0:T(8,128)(2,1)} %param.13) | copy-start | bytes 3145732
  10.6 39.1 %all-to-all-start = ((bf16[8,384,128]{2,1,0:T(8,128)(2,1)}), bf16[8,384,128]{2,1,0:T(8,128)(2,1)S(1)}, u32[]{:S(2)}, u32[]{:S(2)}) async-start(bf16[8,384,128]{2,1,0:T(8,128)(2,1)} %broadcast_in_dim.10), calls=%async_computation | async-start | bytes 1572864 | tf_op jit(solution)/shard_map/all_to_all | solution.py:41
  21.7 149.9 %all-gather.9.cloned.1.call-start = ((), (), s32[]{:S(2)}) async-start(), calls=%async_computation.7 | async-start | bytes 4718592 | tf_op jit(solution)/shard_map/all_gather | solution.py:301
  23.7 26.0 %collective-permute-start.3 = (bf16[256,1024]{1,0:T(8,128)(2,1)S(1)}, bf16[256,1024]{1,0:T(8,128)(2,1)}, u32[]{:S(2)}, u32[]{:S(2)}) collective-permute-start(bf16[256,1024]{1,0:T(8,128)(2,1)S(1)} %constant_dynamic-slice_fusion.2), channel_id=1, source_target_pairs={{0,2},{2,4},{4,6},{6,0},{1,3},{3,5},{5,7},{7,1},{8,10},{10,12},{12... | collective-permute-start | bytes 1572872 | tf_op jit(solution)/shard_map/ppermute | solution.py:73
  25.3 26.2 %collective-permute-start.4 = (bf16[256,1024]{1,0:T(8,128)(2,1)S(1)}, bf16[256,1024]{1,0:T(8,128)(2,1)}, u32[]{:S(2)}, u32[]{:S(2)}) collective-permute-start(bf16[256,1024]{1,0:T(8,128)(2,1)S(1)} %constant_dynamic-slice_fusion.2), channel_id=1, source_target_pairs={{0,6},{2,0},{4,2},{6,4},{1,7},{3,1},{5,3},{7,5},{8,14},{10,8},{12,... | collective-permute-start | bytes 1572872 | tf_op jit(solution)/shard_map/ppermute | solution.py:73
  25.8 41.6 %collective-permute-start.5 = (bf16[256,1024]{1,0:T(8,128)(2,1)S(1)}, bf16[256,1024]{1,0:T(8,128)(2,1)}, u32[]{:S(2)}, u32[]{:S(2)}) collective-permute-start(bf16[256,1024]{1,0:T(8,128)(2,1)S(1)} %constant_dynamic-slice_fusion.2), channel_id=1, source_target_pairs={{0,4},{2,6},{4,0},{6,2},{1,5},{3,7},{5,1},{7,3},{8,12},{10,14},{12... | collective-permute-start | bytes 1572872 | tf_op jit(solution)/shard_map/ppermute | solution.py:73
  49.7 17.7 %collective-permute-start.6 = (bf16[256,1024]{1,0:T(8,128)(2,1)}, bf16[256,1024]{1,0:T(8,128)(2,1)}, u32[]{:S(2)}, u32[]{:S(2)}) collective-permute-start(bf16[256,1024]{1,0:T(8,128)(2,1)} %collective-permute-done.3.m1), channel_id=1, source_target_pairs={{0,1},{1,0},{2,3},{3,2},{4,5},{5,4},{6,7},{7,6},{8,9},{9,8},{10,11... | collective-permute-start | bytes 1572872 | tf_op jit(solution)/shard_map/ppermute | solution.py:73
  49.7 21.5 %copy-start.2 = (bf16[8,384,128]{2,1,0:T(8,128)(2,1)}, bf16[8,384,128]{2,1,0:T(8,128)(2,1)S(1)}, u32[]{:S(2)}) copy-start(bf16[8,384,128]{2,1,0:T(8,128)(2,1)S(1)} %all-to-all-done.x0) | copy-start | bytes 2359300
  49.7 20.6 %collective-permute-start = (bf16[8,384,128]{2,1,0:T(8,128)(2,1)S(1)}, bf16[8,384,128]{2,1,0:T(8,128)(2,1)S(1)}, u32[]{:S(2)}, u32[]{:S(2)}) collective-permute-start(bf16[8,384,128]{2,1,0:T(8,128)(2,1)S(1)} %all-to-all-done.x0), channel_id=1, source_target_pairs={{0,32},{32,0},{8,40},{40,8},{249,25},{25,249},{225,1},{1,225},{2,3... | collective-permute-start | bytes 2359304 | tf_op jit(solution)/shard_map/ppermute | solution.py:49
  50.7 20.5 %collective-permute-start.1 = (bf16[8,384,128]{2,1,0:T(8,128)(2,1)S(1)}, bf16[8,384,128]{2,1,0:T(8,128)(2,1)}, u32[]{:S(2)}, u32[]{:S(2)}) collective-permute-start(bf16[8,384,128]{2,1,0:T(8,128)(2,1)S(1)} %all-to-all-done.x0), channel_id=1, source_target_pairs={{0,8},{32,40},{8,0},{40,32},{249,225},{25,1},{225,249},{1,25},{2,1... | collective-permute-start | bytes 2359304 | tf_op jit(solution)/shard_map/ppermute | solution.py:49
  51.5 19.7 %collective-permute-start.2 = (bf16[8,384,128]{2,1,0:T(8,128)(2,1)S(1)}, bf16[8,384,128]{2,1,0:T(8,128)(2,1)}, u32[]{:S(2)}, u32[]{:S(2)}) collective-permute-start(bf16[8,384,128]{2,1,0:T(8,128)(2,1)S(1)} %all-to-all-done.x0), channel_id=1, source_target_pairs={{0,40},{32,8},{8,32},{40,0},{249,1},{25,225},{225,25},{1,249},{2,4... | collective-permute-start | bytes 2359304 | tf_op jit(solution)/shard_map/ppermute | solution.py:49
  67.4 2.1 collective-permute-start.7
  67.4 3.0 %collective-permute-start.8 = (bf16[256,1024]{1,0:T(8,128)(2,1)}, bf16[256,1024]{1,0:T(8,128)(2,1)}, u32[]{:S(2)}, u32[]{:S(2)}) collective-permute-start(bf16[256,1024]{1,0:T(8,128)(2,1)} %collective-permute-done.5.m3), channel_id=1, source_target_pairs={{0,1},{1,0},{2,3},{3,2},{4,5},{5,4},{6,7},{7,6},{8,9},{9,8},{10,11... | collective-permute-start | bytes 1572872 | tf_op jit(solution)/shard_map/ppermute | solution.py:73
  69.5 1.7 copy-start.14
  70.4 0.9 copy-start.13
  81.3 20.7 %collective-permute-start.10 = (bf16[8,384,128]{2,1,0:T(8,128)(2,1)}, bf16[8,384,128]{2,1,0:T(8,128)(2,1)S(1)}, u32[]{:S(2)}, u32[]{:S(2)}) collective-permute-start(bf16[8,384,128]{2,1,0:T(8,128)(2,1)} %get-tuple-element.16), channel_id=1, source_target_pairs={{0,8},{32,40},{8,0},{40,32},{249,225},{25,1},{225,249},{1,25},{2,1... | collective-permute-start | bytes 2359304 | tf_op jit(solution)/shard_map/ppermute | solution.py:49
  82.9 19.1 %collective-permute-start.11 = (bf16[8,384,128]{2,1,0:T(8,128)(2,1)}, bf16[8,384,128]{2,1,0:T(8,128)(2,1)S(1)}, u32[]{:S(2)}, u32[]{:S(2)}) collective-permute-start(bf16[8,384,128]{2,1,0:T(8,128)(2,1)} %get-tuple-element.17), channel_id=1, source_target_pairs={{0,40},{32,8},{8,32},{40,0},{249,1},{25,225},{225,25},{1,249},{2,4... | collective-permute-start | bytes 2359304 | tf_op jit(solution)/shard_map/ppermute | solution.py:49
  84.0 19.5 %collective-permute-start.9 = (bf16[8,384,128]{2,1,0:T(8,128)(2,1)}, bf16[8,384,128]{2,1,0:T(8,128)(2,1)S(1)}, u32[]{:S(2)}, u32[]{:S(2)}) collective-permute-start(bf16[8,384,128]{2,1,0:T(8,128)(2,1)} %get-tuple-element.15), channel_id=1, source_target_pairs={{0,32},{32,0},{8,40},{40,8},{249,25},{25,249},{225,1},{1,225},{2,3... | collective-permute-start | bytes 2359304 | tf_op jit(solution)/shard_map/ppermute | solution.py:49
  106.1 10.0 %copy-start.9 = (f32[128]{0:T(128)S(1)}, f32[128]{0:T(128)}, u32[]{:S(2)}) copy-start(f32[128]{0:T(128)} %param.14) | copy-start | bytes 1540
  106.1 10.0 %copy-start.10 = (f32[128]{0:T(128)S(1)}, f32[128]{0:T(128)}, u32[]{:S(2)}) copy-start(f32[128]{0:T(128)} %param.15) | copy-start | bytes 1540
  106.1 33.7 %all-to-all-start.1 = ((bf16[8,384,128]{2,1,0:T(8,128)(2,1)}), bf16[8,384,128]{2,1,0:T(8,128)(2,1)S(1)}, u32[]{:S(2)}, u32[]{:S(2)}) async-start(bf16[8,384,128]{2,1,0:T(8,128)(2,1)} %add_convert_fusion.1), calls=%async_computation.1 | async-start | bytes 1572864 | tf_op jit(solution)/shard_map/all_to_all | solution.py:41
  168.1 22.4 %copy-start.1 = (bf16[8,392,128]{2,1,0:T(8,128)(2,1)}, bf16[8,392,128]{2,1,0:T(8,128)(2,1)S(1)}, u32[]{:S(2)}) copy-start(bf16[8,392,128]{2,1,0:T(8,128)(2,1)S(1)} %all_to_all.25.x0) | copy-start | bytes 2408452
  168.1 12.2 %collective-permute-start.12 = (bf16[8,392,128]{2,1,0:T(8,128)(2,1)S(1)}, bf16[8,392,128]{2,1,0:T(8,128)(2,1)S(1)}, u32[]{:S(2)}, u32[]{:S(2)}) collective-permute-start(bf16[8,392,128]{2,1,0:T(8,128)(2,1)S(1)} %all_to_all.25.x0), channel_id=1, source_target_pairs={{0,32},{32,0},{8,40},{40,8},{249,25},{25,249},{225,1},{1,225},{2,3... | collective-permute-start | bytes 2408456 | tf_op jit(solution)/shard_map/ppermute | solution.py:49
  169.7 20.8 %collective-permute-start.13 = (bf16[8,392,128]{2,1,0:T(8,128)(2,1)S(1)}, bf16[8,392,128]{2,1,0:T(8,128)(2,1)S(1)}, u32[]{:S(2)}, u32[]{:S(2)}) collective-permute-start(bf16[8,392,128]{2,1,0:T(8,128)(2,1)S(1)} %all_to_all.25.x0), channel_id=1, source_target_pairs={{0,8},{32,40},{8,0},{40,32},{249,225},{25,1},{225,249},{1,25},{2,1... | collective-permute-start | bytes 2408456 | tf_op jit(solution)/shard_map/ppermute | solution.py:49
  171.6 18.9 %collective-permute-start.14 = (bf16[8,392,128]{2,1,0:T(8,128)(2,1)S(1)}, bf16[8,392,128]{2,1,0:T(8,128)(2,1)}, u32[]{:S(2)}, u32[]{:S(2)}) collective-permute-start(bf16[8,392,128]{2,1,0:T(8,128)(2,1)S(1)} %all_to_all.25.x0), channel_id=1, source_target_pairs={{0,40},{32,8},{8,32},{40,0},{249,1},{25,225},{225,25},{1,249},{2,4... | collective-permute-start | bytes 2408456 | tf_op jit(solution)/shard_map/ppermute | solution.py:49
  180.2 10.3 %copy-start.11 = (bf16[8,392,128]{2,1,0:T(8,128)(2,1)}, bf16[8,392,128]{2,1,0:T(8,128)(2,1)S(1)}, u32[]{:S(2)}) copy-start(bf16[8,392,128]{2,1,0:T(8,128)(2,1)S(1)} %collective-permute-done.12.x1) | copy-start | bytes 2408452
  190.5 0.9 copy-start.12
  205.3 12.3 %collective-permute-start.15 = (bf16[8,384,128]{2,1,0:T(8,128)(2,1)}, bf16[8,384,128]{2,1,0:T(8,128)(2,1)S(1)}, u32[]{:S(2)}, u32[]{:S(2)}) collective-permute-start(bf16[8,384,128]{2,1,0:T(8,128)(2,1)} %get-tuple-element.20), channel_id=1, source_target_pairs={{0,32},{32,0},{8,40},{40,8},{249,25},{25,249},{225,1},{1,225},{2,3... | collective-permute-start | bytes 2359304 | tf_op jit(solution)/shard_map/ppermute | solution.py:49
  205.9 20.1 %collective-permute-start.16 = (bf16[8,384,128]{2,1,0:T(8,128)(2,1)}, bf16[8,384,128]{2,1,0:T(8,128)(2,1)S(1)}, u32[]{:S(2)}, u32[]{:S(2)}) collective-permute-start(bf16[8,384,128]{2,1,0:T(8,128)(2,1)} %get-tuple-element.21), channel_id=1, source_target_pairs={{0,8},{32,40},{8,0},{40,32},{249,225},{25,1},{225,249},{1,25},{2,1... | collective-permute-start | bytes 2359304 | tf_op jit(solution)/shard_map/ppermute | solution.py:49
  207.7 19.6 %collective-permute-start.17 = (bf16[8,384,128]{2,1,0:T(8,128)(2,1)}, bf16[8,384,128]{2,1,0:T(8,128)(2,1)S(1)}, u32[]{:S(2)}, u32[]{:S(2)}) collective-permute-start(bf16[8,384,128]{2,1,0:T(8,128)(2,1)} %get-tuple-element.22), channel_id=1, source_target_pairs={{0,40},{32,8},{8,32},{40,0},{249,1},{25,225},{225,25},{1,249},{2,4... | collective-permute-start | bytes 2359304 | tf_op jit(solution)/shard_map/ppermute | solution.py:49
  228.8 27.6 %copy-start.4 = (bf16[384,128]{1,0:T(8,128)(2,1)S(1)}, bf16[384,128]{1,0:T(8,128)(2,1)}, u32[]{:S(2)}) copy-start(bf16[384,128]{1,0:T(8,128)(2,1)} %get-tuple-element.18) | copy-start | bytes 294916
  228.8 43.1 %copy-start.7 = (f32[128]{0:T(128)S(1)}, f32[128]{0:T(128)}, u32[]{:S(2)}) copy-start(f32[128]{0:T(128)} %param.17) | copy-start | bytes 1540
  228.9 43.1 %copy-start.8 = (f32[128]{0:T(128)S(1)}, f32[128]{0:T(128)}, u32[]{:S(2)}) copy-start(f32[128]{0:T(128)} %param.16) | copy-start | bytes 1540
Sparse Core Ops, SparseCore 0:
  9.2 55.4 all-gather.4
  66.5 37.0 all-gather.6
  105.4 34.5 all-gather.8

commit v2 on v1

--- a/solution.py
+++ b/solution.py
@@ -17,12 +17,16 @@
 NZ, NY = 8, 4
 
 
-def place(z, y, core, nz, ny):
-    z, y = (z - core) % nz, (y - core) % ny
-    return (y % 2) * 2 + z % 2, (y // 2) * (nz // 2) + z // 2
-
-
-def groups_of(sizes):
+def place(z, y, core):
+    z, y = (z - core) % NZ, (y - core) % NY
+    return (y % 2) * 2 + z % 2, y // 2, z // 2
+
+
+def label(zh, p, core):
+    return (zh - core * (1 - p % 2)) % (NZ // 2)
+
+
+def pairs_of(sizes):
     nz, ny, nx, nc = sizes
     near, far = {}, {}
     for z in range(nz):
@@ -30,37 +34,33 @@
             for x in range(nx):
                 for c in range(nc):
                     at = ((z * ny + y) * nx + x) * nc + c
-                    a, b = place(z, y, c, nz, ny)
-                    near.setdefault((x, c, b), {})[a] = at
-                    far.setdefault((x, c, a), {})[b] = at
-    pairs = [[(g[a], g[a ^ d]) for g in near.values() for a in range(4)] for d in range(4)]
-    return pairs, [[m[i] for i in sorted(m)] for m in far.values()]
-
-
-def far_swap(blocks, far):
-    return lax.all_to_all(blocks, ALL, 0, 0, axis_index_groups=far, tiled=True)
-
-
-def far_to_all(block, far):
-    return far_swap(jnp.broadcast_to(block[None], (len(far[0]), *block.shape)), far)
-
-
-def near_send(blocks, near):
-    return [blocks[0]] + [lax.ppermute(blocks[d], ALL, near[d]) for d in (3, 1, 2)]
-
-
-def near_swap(blocks, near):
-    own, diagonal, one, two = near_send(blocks, near)
+                    p, yh, zh = place(z, y, c)
+                    near.setdefault((x, c, yh, zh), {})[p] = at
+                    far.setdefault((x, c, p), {})[yh * (nz // 2) + label(zh, p, c)] = at
+
+    def flips(groups, by):
+        return [(g[i], g[i ^ by]) for g in groups.values() for i in g]
+
+    return {
+        "near": [flips(near, d) for d in range(4)],
+        "mid": [flips(far, (e >> 1) * (nz // 2) + (e & 1)) for e in range(4)],
+        "last": flips(far, 2),
+    }
+
+
+def stage(blocks, pairs):
+    own, diagonal, one, two = [blocks[0]] + [lax.ppermute(blocks[d], ALL, pairs[d]) for d in (3, 1, 2)]
     return [own, one, two, diagonal]
 
 
-def gathered(block, near, far):
-    return near_swap([far_to_all(block, far)] * 4, near)
-
-
-def scattered_sum(parts, near, far):
-    some = sum(p.astype(F32) for p in near_swap(parts, near)).astype(BF)
-    return jnp.sum(far_swap(some, far).astype(F32), axis=0)
+def gathered(pair, pairs):
+    bundle = jnp.stack(stage([pair] * 4, pairs["mid"]))
+    return stage([bundle] * 4, pairs["near"])
+
+
+def scattered_sum(parts, pairs):
+    some = sum(p.astype(F32) for p in stage(parts, pairs["near"])).astype(BF)
+    return sum(p.astype(F32) for p in stage([some[e] for e in range(4)], pairs["mid"]))
 
 
 def stats_to_all(row):
@@ -84,19 +84,23 @@
     return [hi, mid, v - hi - mid]
 
 
-def from_peer(idx, d, q):
-    core, p = idx[1], idx[2] ^ d
-    z = ((q % (NZ // 2)) * 2 + (p & 1) + core) & (NZ - 1)
-    y = ((q // (NZ // 2)) * 2 + (p >> 1) + core) & (NY - 1)
+def from_peer(idx, d, e, g):
+    core, p, yh, zh = idx[1], idx[2] ^ d, idx[3], idx[4]
+    turn = core & (1 - (p & 1))
+    zh = ((((zh - turn) & (NZ // 2 - 1)) ^ (g * 2 + (e & 1))) + turn) & (NZ // 2 - 1)
+    z = (zh * 2 + (p & 1) + core) & (NZ - 1)
+    y = ((yh ^ (e >> 1)) * 2 + (p >> 1) + core) & (NY - 1)
     return z * NY + y
 
 
 def to_peer(idx, d, j, yh):
     core, p = idx[1], idx[2] ^ d
+    turn = core & (1 - (p & 1))
     zz = (p & 1) ^ core
     zh = (j - core * (1 - zz)) & (NZ // 2 - 1)
     y = (yh * 2 + (p >> 1) + core) & (NY - 1)
-    return (2 * j + zz) * NY + y, yh * (NZ // 2) + zh
+    flip = ((zh - turn) & (NZ // 2 - 1)) ^ ((idx[4] - turn) & (NZ // 2 - 1))
+    return (2 * j + zz) * NY + y, (flip & 1) + 2 * (yh ^ idx[3]), flip >> 1
 
 
 def matmuls(idx, xs, upv, dv, ov, outs, out_sems, wait_up, wait_down, nx):
@@ -119,9 +123,9 @@
             ov[2 * NY * j + i] = part[:, i * 128 : (i + 1) * 128]
         for d in range(4):
             for yh in range(NY // 2):
-                slot, q = to_peer(idx, d, j, yh)
+                slot, e, g = to_peer(idx, d, j, yh)
                 sem = out_sems.at[(d * nx + j) * 2 + yh]
-                copy = pltpu.make_async_copy(ov.at[slot], outs[d].at[q], sem)
+                copy = pltpu.make_async_copy(ov.at[slot], outs[d].at[e, g], sem)
                 copy.start()
                 copies.append(copy)
     for copy in copies:
@@ -136,9 +140,9 @@
     me, core = idx[0], idx[1]
     x_copies = []
     for d, x in enumerate((x0, x1, x2, x3)):
-        for q in range(x.shape[0]):
-            at = pl.multiple_of(from_peer(idx, d, q) * 128, 128)
-            copy = pltpu.make_async_copy(x.at[q], xs.at[:, pl.ds(at, 128)], x_sem.at[d * x.shape[0] + q])
+        for i in range(8):
+            at = pl.multiple_of(from_peer(idx, d, i // 2, i % 2) * 128, 128)
+            copy = pltpu.make_async_copy(x.at[i // 2, i % 2], xs.at[:, pl.ds(at, 128)], x_sem.at[d * 8 + i])
             copy.start()
             x_copies.append(copy)
     deep = upv.shape[0] // nx
@@ -180,8 +184,9 @@
     tokens = xs.shape[0]
     x_copies = []
     for d, x in enumerate((x0, x1, x2, x3)):
-        for q in range(x.shape[0]):
-            copy = pltpu.make_async_copy(x.at[q], xv.at[from_peer(idx, d, q)], x_sem.at[d * x.shape[0] + q])
+        for i in range(8):
+            to = xv.at[from_peer(idx, d, i // 2, i % 2)]
+            copy = pltpu.make_async_copy(x.at[i // 2, i % 2], to, x_sem.at[d * 8 + i])
             copy.start()
             x_copies.append(copy)
     up_copy = pltpu.make_async_copy(up, upv, up_sem)
@@ -200,14 +205,14 @@
     def norm(i, carry):
         rows = pl.ds(pl.multiple_of(i * step, step), step)
         acc = jnp.zeros((step, 128), F32)
+        squares = jnp.zeros((step, 128), F32)
         for b in range(nb):
-            acc = acc + xv[b, rows, :].astype(F32)
+            d = xv[b, rows, :].astype(F32)
+            acc = acc + d
+            squares = squares + d * d
         mean = jnp.sum(acc, axis=1, keepdims=True) / width
-        acc = jnp.zeros((step, 128), F32)
-        for b in range(nb):
-            d = xv[b, rows, :].astype(F32) - mean
-            acc = acc + d * d
-        scale = lax.rsqrt(jnp.sum(acc, axis=1, keepdims=True) / width + EPS)
+        var = jnp.sum(squares, axis=1, keepdims=True) / width - mean * mean
+        scale = lax.rsqrt(jnp.maximum(var, 0.0) + EPS)
         for b in range(nb):
             d = (xv[b, rows, :].astype(F32) - mean) * scale
             xs[rows, b * 128 : (b + 1) * 128] = (d * gain[b : b + 1] + bias[b : b + 1]).astype(BF)
@@ -229,12 +234,12 @@
 
 
 def first_ffn(idx, x, up, own, mine, others):
-    tokens = x[0].shape[1]
+    tokens = x[0].shape[2]
     width, ff = up.shape
     nx, nb = lax.axis_size(X), NZ * NY
     return pl.pallas_call(
         first_kernel,
-        out_shape=[jax.ShapeDtypeStruct((nb // 4, tokens, 128), BF)] * 4,
+        out_shape=[jax.ShapeDtypeStruct((4, nb // 16, tokens, 128), BF)] * 4,
         in_specs=[SMEM] + [ANY] * 12,
         out_specs=[ANY] * 4,
         scratch_shapes=[
@@ -257,12 +262,12 @@
     nx, nb = lax.axis_size(X), NZ * NY
     return pl.pallas_call(
         second_kernel,
-        out_shape=[jax.ShapeDtypeStruct((nb // 4, tokens, 128), BF)] * 4 + [jax.ShapeDtypeStruct((tokens, 128), BF)],
+        out_shape=[jax.ShapeDtypeStruct((4, nb // 16, tokens, 128), BF)] * 4 + [jax.ShapeDtypeStruct((tokens, 128), BF)],
         in_specs=[SMEM] + [ANY] * 6 + [VMEM] * 3,
         out_specs=[ANY] * 4 + [VMEM],
         scratch_shapes=[
             pltpu.VMEM((tokens, width), BF),
-            pltpu.VMEM((nb, *x[0].shape[1:]), BF),
+            pltpu.VMEM((nb, *x[0].shape[2:]), BF),
             pltpu.VMEM((width, ff), BF),
             pltpu.VMEM((2 * nx, ff // 2, width // nx), BF),
             pltpu.VMEM((nb, tokens, 128), BF),
@@ -290,27 +295,32 @@
     bias_second,
 ):
     tokens = stream.shape[0]
-    near, far = groups_of([lax.axis_size(axis) for axis in ALL])
+    pairs = pairs_of([lax.axis_size(axis) for axis in ALL])
+    pair = jnp.stack([stream, lax.ppermute(stream, ALL, pairs["last"])])
     half = half_of(down_first)
     mine = [shift(half, X, by) for by in (1, -1, 2)]
     up_1 = lax.all_gather(half_of(up_first), (X, C), axis=0, tiled=True)
-    x_far = far_to_all(stream, far)
-    x_all = near_swap([x_far] * 4, near)
+    x_all = gathered(pair, pairs)
     others = [shift(m, C, 1) for m in mine]
     up_2 = lax.all_gather(half_of(up_second), (X, C), axis=0, tiled=True)
     down_2 = lax.all_gather(half_of(down_second), (X, C), axis=0, tiled=False)
     down_2 = down_2.reshape(-1, *half.shape)
     core = lax.axis_index(C)
-    a, _ = place(lax.axis_index(Z), lax.axis_index(Y), core, NZ, NY)
-    idx = jnp.stack([lax.axis_index(X), core, a]).astype(jnp.int32)
+    p, yh, zh = place(lax.axis_index(Z), lax.axis_index(Y), core)
+    idx = jnp.stack([lax.axis_index(X), core, p, yh, zh]).astype(jnp.int32)
     parts = first_ffn(idx, x_all, up_1, down_first, mine, others)
-    mixed = RESID * stream.astype(F32) + scattered_sum(parts, near, far)
-    tail = jnp.stack(split3(gain_first) + split3(bias_first) + [jnp.zeros_like(gain_first)] * 2)
-    mixed_all = gathered(jnp.concatenate([mixed, tail], axis=0).astype(BF), near, far)
+    tail = jnp.stack(split3(gain_first) + split3(bias_first) + [jnp.zeros_like(gain_first)] * 2).astype(BF)
+    tails = jnp.stack([tail, lax.ppermute(tail, ALL, pairs["last"])])
+    some = scattered_sum(parts, pairs).astype(BF)
+    branch = some.astype(F32) + lax.ppermute(some, ALL, pairs["last"])[::-1].astype(F32)
+    mixed = RESID * pair.astype(F32) + branch
+    mixed_all = gathered(jnp.concatenate([mixed.astype(BF), tails], axis=1), pairs)
     *parts, x = second_ffn(
-        idx, mixed_all, tokens, up_2, down_2, mixed, gain_first[None], bias_first[None]
+        idx, mixed_all, tokens, up_2, down_2, mixed[0], gain_first[None], bias_first[None]
     )
-    mixed = RESID * x.astype(F32) + scattered_sum(parts, near, far)
+    some = scattered_sum(parts, pairs)
+    branch = some[0] + lax.ppermute(some[1].astype(BF), ALL, pairs["last"]).astype(F32)
+    mixed = RESID * x.astype(F32) + branch
     width = mixed.shape[1] * lax.axis_size(RA)
     sums = jnp.concatenate([jnp.sum(mixed, axis=1), jnp.sum(mixed * mixed, axis=1)])
     sums = jnp.sum(stats_to_all(sums[None]), axis=0)[0]

time: 281 us -> 249 us (0.89)
  blocking collectives: 69.8 us -> 17 us
  starting transfers between devices: 40.2 us -> 61.2 us
  waiting for transfers between devices: 118 us -> 124 us
    all_to_all x2 -> x0, blocking collectives: 54.7 us -> none  [far_swap(): return lax.all_to_all(blocks, ALL, 0, 0, axis_index_groups=far, tiled=True)]
    ppermute x12 -> x28, waiting for transfers between devices: 56.8 us -> 104 us  [the longest x24 90.7 us: stage(): lax.ppermute(blocks[d], ALL, pairs[d])]
    ppermute x12 -> x28, starting transfers between devices: 14.3 us -> 57.8 us  [the longest x24 40.9 us: stage(): lax.ppermute(blocks[d], ALL, pairs[d])]
    all_to_all x2 -> x0, waiting for transfers between devices: 23.7 us -> none  [far_swap(): return lax.all_to_all(blocks, ALL, 0, 0, axis_index_groups=far, tiled=True)]
    all_to_all x2 -> x0, starting transfers between devices: 21.1 us -> none  [far_swap(): return lax.all_to_all(blocks, ALL, 0, 0, axis_index_groups=far, tiled=True)]
    ppermute x6, waiting for transfers between devices: 37.7 us -> 19.8 us  [shift(): return lax.ppermute(a, axis, [(i, (i + by) % n) for i in range(n)])]
  transfers between devices with their start and end apart: 23 -> 37, of which waited for: 13 -> 25; matrix products, arithmetic and copies ran while one was open for 3% -> 2% of each run, Pallas kernels for 4% -> 4%
where the time goes in v2:
time: 249 us
  waiting for transfers between devices  124 us (50%)
  starting transfers between devices  61.2 us (25%)
  Pallas kernels  21.1 us (8%)
  blocking collectives  17 us (7%)
  between operations  13.4 us (5%)
  local copies, waits for them, and re-layouts  7.46 us (3%)
  other arithmetic  4.79 us (2%)
    ppermute x24, waiting for transfers between devices, stage(): lax.ppermute(blocks[d], ALL, pairs[d])  90.7 us
    ppermute x24, starting transfers between devices, stage(): lax.ppermute(blocks[d], ALL, pairs[d])  40.9 us
    ppermute x6, waiting for transfers between devices, shift(): return lax.ppermute(a, axis, [(i, (i + by) % n) for i in range(n)])  19.8 us
    all_to_all x1, blocking collectives, stats_to_all(): lax.all_to_all(jnp.broadcast_to(row[None], (n, *row.shape)), RA, 0, 0, ti...  17 us
    pallas_call x1, Pallas kernels, second_ffn(): pl.pallas_call(second_kernel, out_shape=[jax.ShapeDtypeStruct((4, nb // 1...  11.1 us
    pallas_call x1, Pallas kernels, first_ffn(): pl.pallas_call(first_kernel, out_shape=[jax.ShapeDtypeStruct((4, nb // 16...  10 us
    ppermute x1, starting transfers between devices, body(): pair = jnp.stack([stream, lax.ppermute(stream, ALL, pairs['last'])])  7.19 us
    ppermute x1, waiting for transfers between devices, body(): lax.ppermute(some[1].astype(BF), ALL, pairs['last']).astype(F32)  6.1 us
  transfers between devices with their start and end apart: 37, of which 25 were waited for; matrix products, arithmetic and copies ran while one was open for 2% of the time, Pallas kernels for 4%

profile of v2, /device:TPU:2, one launch (start us, length us, event | category | flops | bytes accessed | tf_op | source)
XLA Modules:
  0.0 248.9 jit_solution(12714411390365855186)
XLA Ops:
  6.5 1.2 copy-done
  11.0 1.6 collective-permute-start.7
  12.5 7.2 %collective-permute-start = (bf16[384,128]{1,0:T(8,128)(2,1)S(1)}, bf16[384,128]{1,0:T(8,128)(2,1)S(1)}, u32[]{:S(2)}, u32[]{:S(2)}) collective-permute-start(bf16[384,128]{1,0:T(8,128)(2,1)S(1)} %copy-done.3), channel_id=1, source_target_pairs={{0,128},{16,144},{64,192},{80,208},{128,0},{144,16},{192,64},{208,... | collective-permute-start | bytes 294920 | tf_op jit(solution)/shard_map/ppermute | solution.py:299
  20.3 3.0 %collective-permute-done = bf16[384,128]{1,0:T(8,128)(2,1)S(1)} collective-permute-done((bf16[384,128]{1,0:T(8,128)(2,1)S(1)}, bf16[384,128]{1,0:T(8,128)(2,1)S(1)}, u32[]{:S(2)}, u32[]{:S(2)}) %collective-permute-start) | collective-permute-done | bytes 98336 | tf_op jit(solution)/shard_map/ppermute | solution.py:299
  23.3 5.6 %collective-permute-start.3 = (bf16[2,384,128]{2,1,0:T(8,128)(2,1)S(1)}, bf16[2,384,128]{2,1,0:T(8,128)(2,1)S(1)}, u32[]{:S(2)}, u32[]{:S(2)}) collective-permute-start(bf16[2,384,128]{2,1,0:T(8,128)(2,1)S(1)} %get-tuple-element.38), channel_id=1, source_target_pairs={{0,80},{16,64},{64,16},{80,0},{128,208},{144,192},{192,144},{208,1... | collective-permute-start | bytes 589832 | tf_op jit(solution)/shard_map/ppermute | solution.py:52
  29.6 6.7 %collective-permute-done.3 = bf16[2,384,128]{2,1,0:T(8,128)(2,1)S(1)} collective-permute-done((bf16[2,384,128]{2,1,0:T(8,128)(2,1)S(1)}, bf16[2,384,128]{2,1,0:T(8,128)(2,1)S(1)}, u32[]{:S(2)}, u32[]{:S(2)}) %collective-permute-start.3) | collective-permute-done | bytes 196640 | tf_op jit(solution)/shard_map/ppermute | solution.py:52
  37.1 1.3 collective-permute-done.1
  39.0 2.5 %collective-permute-start.4 = (bf16[4,2,384,128]{3,2,1,0:T(8,128)(2,1)S(1)}, bf16[4,2,384,128]{3,2,1,0:T(8,128)(2,1)S(1)}, u32[]{:S(2)}, u32[]{:S(2)}) collective-permute-start(bf16[4,2,384,128]{3,2,1,0:T(8,128)(2,1)S(1)} %pad_maximum_fusion.1.x0), channel_id=1, source_target_pairs={{0,32},{8,40},{32,0},{40,8},{1,225},{25,249},{225,1},{249,25},{2,3... | collective-permute-start | bytes 2359304 | tf_op jit(solution)/shard_map/ppermute | solution.py:52
  43.1 18.6 %collective-permute-done.9.m3 = bf16[256,1024]{1,0:T(8,128)(2,1)} collective-permute-done((bf16[256,1024]{1,0:T(8,128)(2,1)S(1)}, bf16[256,1024]{1,0:T(8,128)(2,1)}, u32[]{:S(2)}, u32[]{:S(2)}) %collective-permute-start.9) | collective-permute-done | bytes 524320 | tf_op jit(solution)/shard_map/ppermute | solution.py:73
  63.9 0.9 collective-permute-done.12.o3
  65.7 10.0 %first_ffn.1 = (bf16[4,2,384,128]{3,2,1,0:T(8,128)(2,1)}, bf16[4,2,384,128]{3,2,1,0:T(8,128)(2,1)}, bf16[4,2,384,128]{3,2,1,0:T(8,128)(2,1)}, bf16[4,2,384,128]{3,2,1,0:T(8,128)(2,1)}) custom-call(s32[5]{0:T(128)} %stack.116.idx, bf16[4,2,384,128]{3,2,1,0:T(8,128)(2,1)} %copy-done.2, bf16[4,2,384,128]{3,2,1,0:T(8,128)(2,1)} %copy-done.13, ...), custom_call_target="tpu_custom_call" | custom-call | flops 3221225472 | bytes 14680064 | tf_op jit(solution)/shard_map/first_ffn/pallas_call | solution.py:240
  75.8 1.1 collective-permute-start.13
  76.9 1.6 collective-permute-start.14
  78.5 0.9 collective-permute-start.15
  79.4 8.7 %collective-permute-done.13 = bf16[4,2,384,128]{3,2,1,0:T(8,128)(2,1)S(1)} collective-permute-done((bf16[4,2,384,128]{3,2,1,0:T(8,128)(2,1)}, bf16[4,2,384,128]{3,2,1,0:T(8,128)(2,1)S(1)}, u32[]{:S(2)}, u32[]{:S(2)}) %collective-permute-start.13) | collective-permute-done | bytes 786464 | tf_op jit(solution)/shard_map/ppermute | solution.py:52
  88.1 8.6 %collective-permute-done.14 = bf16[4,2,384,128]{3,2,1,0:T(8,128)(2,1)S(1)} collective-permute-done((bf16[4,2,384,128]{3,2,1,0:T(8,128)(2,1)}, bf16[4,2,384,128]{3,2,1,0:T(8,128)(2,1)S(1)}, u32[]{:S(2)}, u32[]{:S(2)}) %collective-permute-start.14) | collective-permute-done | bytes 786464 | tf_op jit(solution)/shard_map/ppermute | solution.py:52
  97.5 1.5 add_convert_fusion.1
  99.1 1.5 collective-permute-start.16
  100.7 3.2 %collective-permute-start.17 = (bf16[2,384,128]{2,1,0:T(8,128)(2,1)S(1)}, bf16[2,384,128]{2,1,0:T(8,128)(2,1)S(1)}, u32[]{:S(2)}, u32[]{:S(2)}) collective-permute-start(bf16[2,384,128]{2,1,0:T(8,128)(2,1)S(1)} %get-tuple-element.34), channel_id=1, source_target_pairs={{0,16},{16,0},{64,80},{80,64},{128,144},{144,128},{192,208},{208,1... | collective-permute-start | bytes 589832 | tf_op jit(solution)/shard_map/ppermute | solution.py:52
  103.9 1.2 collective-permute-start.18
  105.1 2.2 collective-permute-done.16
  107.3 2.2 collective-permute-done.17
  109.5 5.6 %collective-permute-done.18 = bf16[2,384,128]{2,1,0:T(8,128)(2,1)S(1)} collective-permute-done((bf16[2,384,128]{2,1,0:T(8,128)(2,1)S(1)}, bf16[2,384,128]{2,1,0:T(8,128)(2,1)S(1)}, u32[]{:S(2)}, u32[]{:S(2)}) %collective-permute-start.18) | collective-permute-done | bytes 196640 | tf_op jit(solution)/shard_map/ppermute | solution.py:52
  115.2 2.4 collective-permute-start.19
  117.6 3.7 %collective-permute-start.20 = (bf16[8,128]{1,0:T(8,128)(2,1)S(1)}, bf16[8,128]{1,0:T(8,128)(2,1)S(1)}, u32[]{:S(2)}, u32[]{:S(2)}) collective-permute-start(bf16[8,128]{1,0:T(8,128)(2,1)S(1)} %stack.140), channel_id=1, source_target_pairs={{0,128},{16,144},{64,192},{80,208},{128,0},{144,16},{192,64},{208,... | collective-permute-start | bytes 6152 | tf_op jit(solution)/shard_map/ppermute | solution.py:313
  121.4 4.1 %collective-permute-done.19 = bf16[2,384,128]{2,1,0:T(8,128)(2,1)S(1)} collective-permute-done((bf16[2,384,128]{2,1,0:T(8,128)(2,1)S(1)}, bf16[2,384,128]{2,1,0:T(8,128)(2,1)S(1)}, u32[]{:S(2)}, u32[]{:S(2)}) %collective-permute-start.19) | collective-permute-done | bytes 196640 | tf_op jit(solution)/shard_map/ppermute | solution.py:315
  125.7 4.4 %collective-permute-start.21 = (bf16[2,392,128]{2,1,0:T(8,128)(2,1)S(1)}, bf16[2,392,128]{2,1,0:T(8,128)(2,1)S(1)}, u32[]{:S(2)}, u32[]{:S(2)}) collective-permute-start(bf16[2,392,128]{2,1,0:T(8,128)(2,1)S(1)} %get-tuple-element.36), channel_id=1, source_target_pairs={{0,64},{16,80},{64,0},{80,16},{128,192},{144,208},{192,128},{208,1... | collective-permute-start | bytes 602120 | tf_op jit(solution)/shard_map/ppermute | solution.py:52
  130.1 3.4 %collective-permute-start.22 = (bf16[2,392,128]{2,1,0:T(8,128)(2,1)S(1)}, bf16[2,392,128]{2,1,0:T(8,128)(2,1)S(1)}, u32[]{:S(2)}, u32[]{:S(2)}) collective-permute-start(bf16[2,392,128]{2,1,0:T(8,128)(2,1)S(1)} %get-tuple-element.36), channel_id=1, source_target_pairs={{0,16},{16,0},{64,80},{80,64},{128,144},{144,128},{192,208},{208,1... | collective-permute-start | bytes 602120 | tf_op jit(solution)/shard_map/ppermute | solution.py:52
  133.5 2.0 collective-permute-done.21
  135.5 5.5 %collective-permute-done.22 = bf16[2,392,128]{2,1,0:T(8,128)(2,1)S(1)} collective-permute-done((bf16[2,392,128]{2,1,0:T(8,128)(2,1)S(1)}, bf16[2,392,128]{2,1,0:T(8,128)(2,1)S(1)}, u32[]{:S(2)}, u32[]{:S(2)}) %collective-permute-start.22) | collective-permute-done | bytes 200736 | tf_op jit(solution)/shard_map/ppermute | solution.py:52
  141.0 4.5 %collective-permute-done.23 = bf16[2,392,128]{2,1,0:T(8,128)(2,1)S(1)} collective-permute-done((bf16[2,392,128]{2,1,0:T(8,128)(2,1)S(1)}, bf16[2,392,128]{2,1,0:T(8,128)(2,1)S(1)}, u32[]{:S(2)}, u32[]{:S(2)}) %collective-permute-start.23) | collective-permute-done | bytes 200736 | tf_op jit(solution)/shard_map/ppermute | solution.py:52
  145.6 0.9 collective-permute-start.24
  146.6 2.6 %collective-permute-start.26 = (bf16[4,2,392,128]{3,2,1,0:T(8,128)(2,1)S(1)}, bf16[4,2,392,128]{3,2,1,0:T(8,128)(2,1)}, u32[]{:S(2)}, u32[]{:S(2)}) collective-permute-start(bf16[4,2,392,128]{3,2,1,0:T(8,128)(2,1)S(1)} %pad_maximum_fusion.x0), channel_id=1, source_target_pairs={{0,40},{8,32},{32,8},{40,0},{1,249},{25,225},{225,25},{249,1},{2,4... | collective-permute-start | bytes 2408456 | tf_op jit(solution)/shard_map/ppermute | solution.py:52
  149.9 8.0 %collective-permute-done.24.x1 = bf16[4,2,392,128]{3,2,1,0:T(8,128)(2,1)S(1)} collective-permute-done((bf16[4,2,392,128]{3,2,1,0:T(8,128)(2,1)S(1)}, bf16[4,2,392,128]{3,2,1,0:T(8,128)(2,1)S(1)}, u32[]{:S(2)}, u32[]{:S(2)}) %collective-permute-start.24) | collective-permute-done | bytes 802848 | tf_op jit(solution)/shard_map/ppermute | solution.py:52
  157.8 9.5 %collective-permute-done.25.x2 = bf16[4,2,392,128]{3,2,1,0:T(8,128)(2,1)} collective-permute-done((bf16[4,2,392,128]{3,2,1,0:T(8,128)(2,1)S(1)}, bf16[4,2,392,128]{3,2,1,0:T(8,128)(2,1)}, u32[]{:S(2)}, u32[]{:S(2)}) %collective-permute-start.25) | collective-permute-done | bytes 802848 | tf_op jit(solution)/shard_map/ppermute | solution.py:52
  167.4 11.1 %second_ffn.1 = (bf16[4,2,384,128]{3,2,1,0:T(8,128)(2,1)}, bf16[4,2,384,128]{3,2,1,0:T(8,128)(2,1)}, bf16[4,2,384,128]{3,2,1,0:T(8,128)(2,1)}, bf16[4,2,384,128]{3,2,1,0:T(8,128)(2,1)}, bf16[384,128]{1,0:T(8,128)(2,1)}) custom-call(s32[5]{0:T(128)} %stack.116.idx, bf16[4,2,392,128]{3,2,1,0:T(8,128)(2,1)} %copy-done.1, bf16[4,2,392,128]{3,2,1,0:T(8,128)(2,1)} %copy-done.12, ...), custom_call_target="tpu_custom_call" | custom-call | flops 3221225472 | bytes 14680064 | tf_op jit(solution)/shard_map/second_ffn/pallas_call | solution.py:263
  178.5 1.3 collective-permute-start.27
  180.0 2.0 collective-permute-start.29
  182.1 8.7 %collective-permute-done.27 = bf16[4,2,384,128]{3,2,1,0:T(8,128)(2,1)S(1)} collective-permute-done((bf16[4,2,384,128]{3,2,1,0:T(8,128)(2,1)}, bf16[4,2,384,128]{3,2,1,0:T(8,128)(2,1)S(1)}, u32[]{:S(2)}, u32[]{:S(2)}) %collective-permute-start.27) | collective-permute-done | bytes 786464 | tf_op jit(solution)/shard_map/ppermute | solution.py:52
  190.8 9.6 %collective-permute-done.28 = bf16[4,2,384,128]{3,2,1,0:T(8,128)(2,1)S(1)} collective-permute-done((bf16[4,2,384,128]{3,2,1,0:T(8,128)(2,1)}, bf16[4,2,384,128]{3,2,1,0:T(8,128)(2,1)S(1)}, u32[]{:S(2)}, u32[]{:S(2)}) %collective-permute-start.28) | collective-permute-done | bytes 786464 | tf_op jit(solution)/shard_map/ppermute | solution.py:52
  200.4 1.5 add_convert_fusion
  202.3 1.3 collective-permute-start.31
  203.6 4.4 %collective-permute-start.32 = (bf16[2,384,128]{2,1,0:T(8,128)(2,1)S(1)}, bf16[2,384,128]{2,1,0:T(8,128)(2,1)S(1)}, u32[]{:S(2)}, u32[]{:S(2)}) collective-permute-start(bf16[2,384,128]{2,1,0:T(8,128)(2,1)S(1)} %get-tuple-element.30), channel_id=1, source_target_pairs={{0,80},{16,64},{64,16},{80,0},{128,208},{144,192},{192,144},{208,1... | collective-permute-start | bytes 589832 | tf_op jit(solution)/shard_map/ppermute | solution.py:52
  208.0 2.8 %collective-permute-done.30 = bf16[2,384,128]{2,1,0:T(8,128)(2,1)S(1)} collective-permute-done((bf16[2,384,128]{2,1,0:T(8,128)(2,1)S(1)}, bf16[2,384,128]{2,1,0:T(8,128)(2,1)S(1)}, u32[]{:S(2)}, u32[]{:S(2)}) %collective-permute-start.30) | collective-permute-done | bytes 196640 | tf_op jit(solution)/shard_map/ppermute | solution.py:52
  210.8 2.9 %collective-permute-done.31 = bf16[2,384,128]{2,1,0:T(8,128)(2,1)S(1)} collective-permute-done((bf16[2,384,128]{2,1,0:T(8,128)(2,1)S(1)}, bf16[2,384,128]{2,1,0:T(8,128)(2,1)S(1)}, u32[]{:S(2)}, u32[]{:S(2)}) %collective-permute-start.31) | collective-permute-done | bytes 196640 | tf_op jit(solution)/shard_map/ppermute | solution.py:52
  214.4 3.6 %collective-permute-start.33 = (bf16[384,128]{1,0:T(8,128)(2,1)S(1)}, bf16[384,128]{1,0:T(8,128)(2,1)S(1)}, u32[]{:S(2)}, u32[]{:S(2)}) collective-permute-start(bf16[384,128]{1,0:T(8,128)(2,1)S(1)} %fusion.7), channel_id=1, source_target_pairs={{0,128},{16,144},{64,192},{80,208},{128,0},{144,16},{192,64},{208,... | collective-permute-start | bytes 294920 | tf_op jit(solution)/shard_map/ppermute | solution.py:322
  218.0 6.1 %collective-permute-done.33 = bf16[384,128]{1,0:T(8,128)(2,1)S(1)} collective-permute-done((bf16[384,128]{1,0:T(8,128)(2,1)S(1)}, bf16[384,128]{1,0:T(8,128)(2,1)S(1)}, u32[]{:S(2)}, u32[]{:S(2)}) %collective-permute-start.33) | collective-permute-done | bytes 98336 | tf_op jit(solution)/shard_map/ppermute | solution.py:322
  224.4 17.0 %all_to_all.5 = f32[32,1,768]{2,1,0:T(1,128)S(1)} all-to-all(f32[32,1,768]{2,1,0:T(1,128)S(1)} %broadcast_in_dim.8), channel_id=1, replica_groups=mesh['ra_0'=8,'ra_1'=4,'cb'=4,'dp'=2] {'ra_0','ra_1'}, dimensions={0} | all-to-all | bytes 196608 | tf_op jit(solution)/shard_map/all_to_all | solution.py:68
  (95 shorter events, 15.0 us)
Async XLA Ops:
  6.5 2.1 copy-start.5
  6.5 58.3 %all-gather.5.cloned.1.call-start = ((), (), s32[]{:S(2)}) async-start(), calls=%async_computation.1 | async-start | bytes 4718592 | tf_op jit(solution)/shard_map/all_gather | solution.py:302
  8.6 141.2 %all-gather.7.cloned.1.call-start = ((), (), s32[]{:S(2)}) async-start(), calls=%async_computation.2 | async-start | bytes 4718592 | tf_op jit(solution)/shard_map/all_gather | solution.py:305
  9.5 3.0 %copy-start.3 = (bf16[384,128]{1,0:T(8,128)(2,1)S(1)}, bf16[384,128]{1,0:T(8,128)(2,1)}, u32[]{:S(2)}) copy-start(bf16[384,128]{1,0:T(8,128)(2,1)} %param.9) | copy-start | bytes 294916
  9.5 140.3 %all-gather.9.cloned.1.call-start = ((), (), s32[]{:S(2)}) async-start(), calls=%async_computation.3 | async-start | bytes 4718592 | tf_op jit(solution)/shard_map/all_gather | solution.py:306
  11.0 26.2 %collective-permute-start.7 = (bf16[256,1024]{1,0:T(8,128)(2,1)S(1)}, bf16[256,1024]{1,0:T(8,128)(2,1)S(1)}, u32[]{:S(2)}, u32[]{:S(2)}) collective-permute-start(bf16[256,1024]{1,0:T(8,128)(2,1)S(1)} %constant_dynamic-slice_fusion.2), channel_id=1, source_target_pairs={{0,2},{2,4},{4,6},{6,0},{1,3},{3,5},{5,7},{7,1},{8,10},{10,12},{12... | collective-permute-start | bytes 1572872 | tf_op jit(solution)/shard_map/ppermute | solution.py:73
  12.5 10.7 %collective-permute-start = (bf16[384,128]{1,0:T(8,128)(2,1)S(1)}, bf16[384,128]{1,0:T(8,128)(2,1)S(1)}, u32[]{:S(2)}, u32[]{:S(2)}) collective-permute-start(bf16[384,128]{1,0:T(8,128)(2,1)S(1)} %copy-done.3), channel_id=1, source_target_pairs={{0,128},{16,144},{64,192},{80,208},{128,0},{144,16},{192,64},{208,... | collective-permute-start | bytes 294920 | tf_op jit(solution)/shard_map/ppermute | solution.py:299
  19.7 22.5 %collective-permute-start.8 = (bf16[256,1024]{1,0:T(8,128)(2,1)S(1)}, bf16[256,1024]{1,0:T(8,128)(2,1)}, u32[]{:S(2)}, u32[]{:S(2)}) collective-permute-start(bf16[256,1024]{1,0:T(8,128)(2,1)S(1)} %constant_dynamic-slice_fusion.2), channel_id=1, source_target_pairs={{0,6},{2,0},{4,2},{6,4},{1,7},{3,1},{5,3},{7,5},{8,14},{10,8},{12,... | collective-permute-start | bytes 1572872 | tf_op jit(solution)/shard_map/ppermute | solution.py:73
  23.3 13.0 %collective-permute-start.3 = (bf16[2,384,128]{2,1,0:T(8,128)(2,1)S(1)}, bf16[2,384,128]{2,1,0:T(8,128)(2,1)S(1)}, u32[]{:S(2)}, u32[]{:S(2)}) collective-permute-start(bf16[2,384,128]{2,1,0:T(8,128)(2,1)S(1)} %get-tuple-element.38), channel_id=1, source_target_pairs={{0,80},{16,64},{64,16},{80,0},{128,208},{144,192},{192,144},{208,1... | collective-permute-start | bytes 589832 | tf_op jit(solution)/shard_map/ppermute | solution.py:52
  28.9 9.5 %collective-permute-start.1 = (bf16[2,384,128]{2,1,0:T(8,128)(2,1)S(1)}, bf16[2,384,128]{2,1,0:T(8,128)(2,1)S(1)}, u32[]{:S(2)}, u32[]{:S(2)}) collective-permute-start(bf16[2,384,128]{2,1,0:T(8,128)(2,1)S(1)} %get-tuple-element.38), channel_id=1, source_target_pairs={{0,64},{16,80},{64,0},{80,16},{128,192},{144,208},{192,128},{208,1... | collective-permute-start | bytes 589832 | tf_op jit(solution)/shard_map/ppermute | solution.py:52
  28.9 10.0 %collective-permute-start.2 = (bf16[2,384,128]{2,1,0:T(8,128)(2,1)S(1)}, bf16[2,384,128]{2,1,0:T(8,128)(2,1)S(1)}, u32[]{:S(2)}, u32[]{:S(2)}) collective-permute-start(bf16[2,384,128]{2,1,0:T(8,128)(2,1)S(1)} %get-tuple-element.38), channel_id=1, source_target_pairs={{0,16},{16,0},{64,80},{80,64},{128,144},{144,128},{192,208},{208,1... | collective-permute-start | bytes 589832 | tf_op jit(solution)/shard_map/ppermute | solution.py:52
  36.3 25.3 %collective-permute-start.9 = (bf16[256,1024]{1,0:T(8,128)(2,1)S(1)}, bf16[256,1024]{1,0:T(8,128)(2,1)}, u32[]{:S(2)}, u32[]{:S(2)}) collective-permute-start(bf16[256,1024]{1,0:T(8,128)(2,1)S(1)} %constant_dynamic-slice_fusion.2), channel_id=1, source_target_pairs={{0,4},{2,6},{4,0},{6,2},{1,5},{3,7},{5,1},{7,3},{8,12},{10,14},{12... | collective-permute-start | bytes 1572872 | tf_op jit(solution)/shard_map/ppermute | solution.py:73
  37.1 27.8 %copy-start.14 = (bf16[256,1024]{1,0:T(8,128)(2,1)}, bf16[256,1024]{1,0:T(8,128)(2,1)S(1)}, u32[]{:S(2)}) copy-start(bf16[256,1024]{1,0:T(8,128)(2,1)S(1)} %collective-permute-done.7.m1) | copy-start | bytes 1572868
  37.1 24.5 %collective-permute-start.10 = (bf16[256,1024]{1,0:T(8,128)(2,1)S(1)}, bf16[256,1024]{1,0:T(8,128)(2,1)S(1)}, u32[]{:S(2)}, u32[]{:S(2)}) collective-permute-start(bf16[256,1024]{1,0:T(8,128)(2,1)S(1)} %collective-permute-done.7.m1), channel_id=1, source_target_pairs={{0,1},{1,0},{2,3},{3,2},{4,5},{5,4},{6,7},{7,6},{8,9},{9,8},{10,11... | collective-permute-start | bytes 1572872 | tf_op jit(solution)/shard_map/ppermute | solution.py:73
  39.0 25.9 %copy-start.2 = (bf16[4,2,384,128]{3,2,1,0:T(8,128)(2,1)}, bf16[4,2,384,128]{3,2,1,0:T(8,128)(2,1)S(1)}, u32[]{:S(2)}) copy-start(bf16[4,2,384,128]{3,2,1,0:T(8,128)(2,1)S(1)} %pad_maximum_fusion.1.x0) | copy-start | bytes 2359300
  39.0 25.8 %collective-permute-start.4 = (bf16[4,2,384,128]{3,2,1,0:T(8,128)(2,1)S(1)}, bf16[4,2,384,128]{3,2,1,0:T(8,128)(2,1)S(1)}, u32[]{:S(2)}, u32[]{:S(2)}) collective-permute-start(bf16[4,2,384,128]{3,2,1,0:T(8,128)(2,1)S(1)} %pad_maximum_fusion.1.x0), channel_id=1, source_target_pairs={{0,32},{8,40},{32,0},{40,8},{1,225},{25,249},{225,1},{249,25},{2,3... | collective-permute-start | bytes 2359304 | tf_op jit(solution)/shard_map/ppermute | solution.py:52
  41.5 23.3 %collective-permute-start.5 = (bf16[4,2,384,128]{3,2,1,0:T(8,128)(2,1)S(1)}, bf16[4,2,384,128]{3,2,1,0:T(8,128)(2,1)}, u32[]{:S(2)}, u32[]{:S(2)}) collective-permute-start(bf16[4,2,384,128]{3,2,1,0:T(8,128)(2,1)S(1)} %pad_maximum_fusion.1.x0), channel_id=1, source_target_pairs={{0,8},{8,0},{32,40},{40,32},{1,25},{25,1},{225,249},{249,225},{2,1... | collective-permute-start | bytes 2359304 | tf_op jit(solution)/shard_map/ppermute | solution.py:52
  42.2 22.7 %collective-permute-start.6 = (bf16[4,2,384,128]{3,2,1,0:T(8,128)(2,1)S(1)}, bf16[4,2,384,128]{3,2,1,0:T(8,128)(2,1)}, u32[]{:S(2)}, u32[]{:S(2)}) collective-permute-start(bf16[4,2,384,128]{3,2,1,0:T(8,128)(2,1)S(1)} %pad_maximum_fusion.1.x0), channel_id=1, source_target_pairs={{0,40},{8,32},{32,8},{40,0},{1,249},{25,225},{225,25},{249,1},{2,4... | collective-permute-start | bytes 2359304 | tf_op jit(solution)/shard_map/ppermute | solution.py:52
  61.7 2.3 collective-permute-start.11
  62.5 2.4 collective-permute-start.12
  75.8 12.3 %collective-permute-start.13 = (bf16[4,2,384,128]{3,2,1,0:T(8,128)(2,1)}, bf16[4,2,384,128]{3,2,1,0:T(8,128)(2,1)S(1)}, u32[]{:S(2)}, u32[]{:S(2)}) collective-permute-start(bf16[4,2,384,128]{3,2,1,0:T(8,128)(2,1)} %get-tuple-element.15), channel_id=1, source_target_pairs={{0,32},{8,40},{32,0},{40,8},{1,225},{25,249},{225,1},{249,25},{2,3... | collective-permute-start | bytes 2359304 | tf_op jit(solution)/shard_map/ppermute | solution.py:52
  76.9 19.8 %collective-permute-start.14 = (bf16[4,2,384,128]{3,2,1,0:T(8,128)(2,1)}, bf16[4,2,384,128]{3,2,1,0:T(8,128)(2,1)S(1)}, u32[]{:S(2)}, u32[]{:S(2)}) collective-permute-start(bf16[4,2,384,128]{3,2,1,0:T(8,128)(2,1)} %get-tuple-element.16), channel_id=1, source_target_pairs={{0,8},{8,0},{32,40},{40,32},{1,25},{25,1},{225,249},{249,225},{2,1... | collective-permute-start | bytes 2359304 | tf_op jit(solution)/shard_map/ppermute | solution.py:52
  78.5 19.0 %collective-permute-start.15 = (bf16[4,2,384,128]{3,2,1,0:T(8,128)(2,1)}, bf16[4,2,384,128]{3,2,1,0:T(8,128)(2,1)S(1)}, u32[]{:S(2)}, u32[]{:S(2)}) collective-permute-start(bf16[4,2,384,128]{3,2,1,0:T(8,128)(2,1)} %get-tuple-element.17), channel_id=1, source_target_pairs={{0,40},{8,32},{32,8},{40,0},{1,249},{25,225},{225,25},{249,1},{2,4... | collective-permute-start | bytes 2359304 | tf_op jit(solution)/shard_map/ppermute | solution.py:52
  99.1 18.5 %copy-start.8 = (f32[128]{0:T(128)S(1)}, f32[128]{0:T(128)}, u32[]{:S(2)}) copy-start(f32[128]{0:T(128)} %param.15) | copy-start | bytes 1540
  99.1 18.5 %copy-start.9 = (f32[128]{0:T(128)S(1)}, f32[128]{0:T(128)}, u32[]{:S(2)}) copy-start(f32[128]{0:T(128)} %param.14) | copy-start | bytes 1540
  99.1 8.1 %collective-permute-start.16 = (bf16[2,384,128]{2,1,0:T(8,128)(2,1)S(1)}, bf16[2,384,128]{2,1,0:T(8,128)(2,1)S(1)}, u32[]{:S(2)}, u32[]{:S(2)}) collective-permute-start(bf16[2,384,128]{2,1,0:T(8,128)(2,1)S(1)} %get-tuple-element.32), channel_id=1, source_target_pairs={{0,64},{16,80},{64,0},{80,16},{128,192},{144,208},{192,128},{208,1... | collective-permute-start | bytes 589832 | tf_op jit(solution)/shard_map/ppermute | solution.py:52
  100.7 8.8 %collective-permute-start.17 = (bf16[2,384,128]{2,1,0:T(8,128)(2,1)S(1)}, bf16[2,384,128]{2,1,0:T(8,128)(2,1)S(1)}, u32[]{:S(2)}, u32[]{:S(2)}) collective-permute-start(bf16[2,384,128]{2,1,0:T(8,128)(2,1)S(1)} %get-tuple-element.34), channel_id=1, source_target_pairs={{0,16},{16,0},{64,80},{80,64},{128,144},{144,128},{192,208},{208,1... | collective-permute-start | bytes 589832 | tf_op jit(solution)/shard_map/ppermute | solution.py:52
  103.9 11.2 %collective-permute-start.18 = (bf16[2,384,128]{2,1,0:T(8,128)(2,1)S(1)}, bf16[2,384,128]{2,1,0:T(8,128)(2,1)S(1)}, u32[]{:S(2)}, u32[]{:S(2)}) collective-permute-start(bf16[2,384,128]{2,1,0:T(8,128)(2,1)S(1)} %get-tuple-element.33), channel_id=1, source_target_pairs={{0,80},{16,64},{64,16},{80,0},{128,208},{144,192},{192,144},{208,1... | collective-permute-start | bytes 589832 | tf_op jit(solution)/shard_map/ppermute | solution.py:52
  115.2 10.3 %collective-permute-start.19 = (bf16[2,384,128]{2,1,0:T(8,128)(2,1)S(1)}, bf16[2,384,128]{2,1,0:T(8,128)(2,1)S(1)}, u32[]{:S(2)}, u32[]{:S(2)}) collective-permute-start(bf16[2,384,128]{2,1,0:T(8,128)(2,1)S(1)} %fusion.4), channel_id=1, source_target_pairs={{0,128},{16,144},{64,192},{80,208},{128,0},{144,16},{192,64},{208,... | collective-permute-start | bytes 589832 | tf_op jit(solution)/shard_map/ppermute | solution.py:315
  117.6 8.0 %collective-permute-start.20 = (bf16[8,128]{1,0:T(8,128)(2,1)S(1)}, bf16[8,128]{1,0:T(8,128)(2,1)S(1)}, u32[]{:S(2)}, u32[]{:S(2)}) collective-permute-start(bf16[8,128]{1,0:T(8,128)(2,1)S(1)} %stack.140), channel_id=1, source_target_pairs={{0,128},{16,144},{64,192},{80,208},{128,0},{144,16},{192,64},{208,... | collective-permute-start | bytes 6152 | tf_op jit(solution)/shard_map/ppermute | solution.py:313
  125.7 9.8 %collective-permute-start.21 = (bf16[2,392,128]{2,1,0:T(8,128)(2,1)S(1)}, bf16[2,392,128]{2,1,0:T(8,128)(2,1)S(1)}, u32[]{:S(2)}, u32[]{:S(2)}) collective-permute-start(bf16[2,392,128]{2,1,0:T(8,128)(2,1)S(1)} %get-tuple-element.36), channel_id=1, source_target_pairs={{0,64},{16,80},{64,0},{80,16},{128,192},{144,208},{192,128},{208,1... | collective-permute-start | bytes 602120 | tf_op jit(solution)/shard_map/ppermute | solution.py:52
  130.1 10.9 %collective-permute-start.22 = (bf16[2,392,128]{2,1,0:T(8,128)(2,1)S(1)}, bf16[2,392,128]{2,1,0:T(8,128)(2,1)S(1)}, u32[]{:S(2)}, u32[]{:S(2)}) collective-permute-start(bf16[2,392,128]{2,1,0:T(8,128)(2,1)S(1)} %get-tuple-element.36), channel_id=1, source_target_pairs={{0,16},{16,0},{64,80},{80,64},{128,144},{144,128},{192,208},{208,1... | collective-permute-start | bytes 602120 | tf_op jit(solution)/shard_map/ppermute | solution.py:52
  133.5 12.0 %collective-permute-start.23 = (bf16[2,392,128]{2,1,0:T(8,128)(2,1)S(1)}, bf16[2,392,128]{2,1,0:T(8,128)(2,1)S(1)}, u32[]{:S(2)}, u32[]{:S(2)}) collective-permute-start(bf16[2,392,128]{2,1,0:T(8,128)(2,1)S(1)} %get-tuple-element.36), channel_id=1, source_target_pairs={{0,80},{16,64},{64,16},{80,0},{128,208},{144,192},{192,144},{208,1... | collective-permute-start | bytes 602120 | tf_op jit(solution)/shard_map/ppermute | solution.py:52
  145.6 21.8 %copy-start.1 = (bf16[4,2,392,128]{3,2,1,0:T(8,128)(2,1)}, bf16[4,2,392,128]{3,2,1,0:T(8,128)(2,1)S(1)}, u32[]{:S(2)}) copy-start(bf16[4,2,392,128]{3,2,1,0:T(8,128)(2,1)S(1)} %pad_maximum_fusion.x0) | copy-start | bytes 2408452
  145.6 12.3 %collective-permute-start.24 = (bf16[4,2,392,128]{3,2,1,0:T(8,128)(2,1)S(1)}, bf16[4,2,392,128]{3,2,1,0:T(8,128)(2,1)S(1)}, u32[]{:S(2)}, u32[]{:S(2)}) collective-permute-start(bf16[4,2,392,128]{3,2,1,0:T(8,128)(2,1)S(1)} %pad_maximum_fusion.x0), channel_id=1, source_target_pairs={{0,32},{8,40},{32,0},{40,8},{1,225},{25,249},{225,1},{249,25},{2,3... | collective-permute-start | bytes 2408456 | tf_op jit(solution)/shard_map/ppermute | solution.py:52
  146.5 20.9 %collective-permute-start.25 = (bf16[4,2,392,128]{3,2,1,0:T(8,128)(2,1)S(1)}, bf16[4,2,392,128]{3,2,1,0:T(8,128)(2,1)}, u32[]{:S(2)}, u32[]{:S(2)}) collective-permute-start(bf16[4,2,392,128]{3,2,1,0:T(8,128)(2,1)S(1)} %pad_maximum_fusion.x0), channel_id=1, source_target_pairs={{0,8},{8,0},{32,40},{40,32},{1,25},{25,1},{225,249},{249,225},{2,1... | collective-permute-start | bytes 2408456 | tf_op jit(solution)/shard_map/ppermute | solution.py:52
  146.6 20.8 %collective-permute-start.26 = (bf16[4,2,392,128]{3,2,1,0:T(8,128)(2,1)S(1)}, bf16[4,2,392,128]{3,2,1,0:T(8,128)(2,1)}, u32[]{:S(2)}, u32[]{:S(2)}) collective-permute-start(bf16[4,2,392,128]{3,2,1,0:T(8,128)(2,1)S(1)} %pad_maximum_fusion.x0), channel_id=1, source_target_pairs={{0,40},{8,32},{32,8},{40,0},{1,249},{25,225},{225,25},{249,1},{2,4... | collective-permute-start | bytes 2408456 | tf_op jit(solution)/shard_map/ppermute | solution.py:52
  157.8 9.5 %copy-start.12 = (bf16[4,2,392,128]{3,2,1,0:T(8,128)(2,1)}, bf16[4,2,392,128]{3,2,1,0:T(8,128)(2,1)S(1)}, u32[]{:S(2)}) copy-start(bf16[4,2,392,128]{3,2,1,0:T(8,128)(2,1)S(1)} %collective-permute-done.24.x1) | copy-start | bytes 2408452
  178.5 12.3 %collective-permute-start.27 = (bf16[4,2,384,128]{3,2,1,0:T(8,128)(2,1)}, bf16[4,2,384,128]{3,2,1,0:T(8,128)(2,1)S(1)}, u32[]{:S(2)}, u32[]{:S(2)}) collective-permute-start(bf16[4,2,384,128]{3,2,1,0:T(8,128)(2,1)} %get-tuple-element.20), channel_id=1, source_target_pairs={{0,32},{8,40},{32,0},{40,8},{1,225},{25,249},{225,1},{249,25},{2,3... | collective-permute-start | bytes 2359304 | tf_op jit(solution)/shard_map/ppermute | solution.py:52
  179.8 20.6 %collective-permute-start.28 = (bf16[4,2,384,128]{3,2,1,0:T(8,128)(2,1)}, bf16[4,2,384,128]{3,2,1,0:T(8,128)(2,1)S(1)}, u32[]{:S(2)}, u32[]{:S(2)}) collective-permute-start(bf16[4,2,384,128]{3,2,1,0:T(8,128)(2,1)} %get-tuple-element.21), channel_id=1, source_target_pairs={{0,8},{8,0},{32,40},{40,32},{1,25},{25,1},{225,249},{249,225},{2,1... | collective-permute-start | bytes 2359304 | tf_op jit(solution)/shard_map/ppermute | solution.py:52
  180.0 20.4 %collective-permute-start.29 = (bf16[4,2,384,128]{3,2,1,0:T(8,128)(2,1)}, bf16[4,2,384,128]{3,2,1,0:T(8,128)(2,1)S(1)}, u32[]{:S(2)}, u32[]{:S(2)}) collective-permute-start(bf16[4,2,384,128]{3,2,1,0:T(8,128)(2,1)} %get-tuple-element.22), channel_id=1, source_target_pairs={{0,40},{8,32},{32,8},{40,0},{1,249},{25,225},{225,25},{249,1},{2,4... | collective-permute-start | bytes 2359304 | tf_op jit(solution)/shard_map/ppermute | solution.py:52
  202.0 22.1 %copy-start.4 = (bf16[384,128]{1,0:T(8,128)(2,1)S(1)}, bf16[384,128]{1,0:T(8,128)(2,1)}, u32[]{:S(2)}) copy-start(bf16[384,128]{1,0:T(8,128)(2,1)} %get-tuple-element.18) | copy-start | bytes 294916
  202.0 39.6 %copy-start.10 = (f32[128]{0:T(128)S(1)}, f32[128]{0:T(128)}, u32[]{:S(2)}) copy-start(f32[128]{0:T(128)} %param.17) | copy-start | bytes 1540
  202.0 39.6 %copy-start.11 = (f32[128]{0:T(128)S(1)}, f32[128]{0:T(128)}, u32[]{:S(2)}) copy-start(f32[128]{0:T(128)} %param.16) | copy-start | bytes 1540
  202.0 8.8 %collective-permute-start.30 = (bf16[2,384,128]{2,1,0:T(8,128)(2,1)S(1)}, bf16[2,384,128]{2,1,0:T(8,128)(2,1)S(1)}, u32[]{:S(2)}, u32[]{:S(2)}) collective-permute-start(bf16[2,384,128]{2,1,0:T(8,128)(2,1)S(1)} %get-tuple-element.29), channel_id=1, source_target_pairs={{0,64},{16,80},{64,0},{80,16},{128,192},{144,208},{192,128},{208,1... | collective-permute-start | bytes 589832 | tf_op jit(solution)/shard_map/ppermute | solution.py:52
  202.3 11.4 %collective-permute-start.31 = (bf16[2,384,128]{2,1,0:T(8,128)(2,1)S(1)}, bf16[2,384,128]{2,1,0:T(8,128)(2,1)S(1)}, u32[]{:S(2)}, u32[]{:S(2)}) collective-permute-start(bf16[2,384,128]{2,1,0:T(8,128)(2,1)S(1)} %get-tuple-element.31), channel_id=1, source_target_pairs={{0,16},{16,0},{64,80},{80,64},{128,144},{144,128},{192,208},{208,1... | collective-permute-start | bytes 589832 | tf_op jit(solution)/shard_map/ppermute | solution.py:52
  203.6 10.7 %collective-permute-start.32 = (bf16[2,384,128]{2,1,0:T(8,128)(2,1)S(1)}, bf16[2,384,128]{2,1,0:T(8,128)(2,1)S(1)}, u32[]{:S(2)}, u32[]{:S(2)}) collective-permute-start(bf16[2,384,128]{2,1,0:T(8,128)(2,1)S(1)} %get-tuple-element.30), channel_id=1, source_target_pairs={{0,80},{16,64},{64,16},{80,0},{128,208},{144,192},{192,144},{208,1... | collective-permute-start | bytes 589832 | tf_op jit(solution)/shard_map/ppermute | solution.py:52
  214.4 9.7 %collective-permute-start.33 = (bf16[384,128]{1,0:T(8,128)(2,1)S(1)}, bf16[384,128]{1,0:T(8,128)(2,1)S(1)}, u32[]{:S(2)}, u32[]{:S(2)}) collective-permute-start(bf16[384,128]{1,0:T(8,128)(2,1)S(1)} %fusion.7), channel_id=1, source_target_pairs={{0,128},{16,144},{64,192},{80,208},{128,0},{144,16},{192,64},{208,... | collective-permute-start | bytes 294920 | tf_op jit(solution)/shard_map/ppermute | solution.py:322
  (5 other events, 6.2 us)
Sparse Core Ops, SparseCore 0:
  9.2 52.0 all-gather.4
  63.2 32.4 all-gather.6
  97.5 34.5 all-gather.8

commit v3 on v2

--- a/solution.py
+++ b/solution.py
@@ -78,6 +78,12 @@
     return lax.dynamic_slice_in_dim(w, lax.axis_index(C) * rows, rows, 0)
 
 
+def packed(up, down):
+    up, down = half_of(up), half_of(down)
+    width = up.shape[1]
+    return jnp.concatenate([up] + [down[:, i : i + width] for i in range(0, down.shape[1], width)], axis=0)
+
+
 def split3(v):
     hi = lax.reduce_precision(v, 8, 7)
     mid = lax.reduce_precision(v - hi, 8, 7)
@@ -103,18 +109,16 @@
     return (2 * j + zz) * NY + y, (flip & 1) + 2 * (yh ^ idx[3]), flip >> 1
 
 
-def matmuls(idx, xs, upv, dv, ov, outs, out_sems, wait_up, wait_down, nx):
-    deep = xs.shape[1] // nx
-    pre = None
-    for k in range(nx):
-        wait_up(k)
-        rows = slice(k * deep, (k + 1) * deep)
-        term = jnp.dot(xs[:, rows], upv[rows, :], preferred_element_type=F32)
-        pre = term if pre is None else pre + term
+def matmuls(idx, xs, upv, dv, ov, outs, out_sems, before_up, before_down):
+    nx = dv.shape[0] // 2
+    for copy in before_up:
+        copy.wait()
+    pre = jnp.dot(xs[...], upv[...], preferred_element_type=F32)
     hidden = jnp.square(jnp.maximum(pre, 0.0)).astype(BF)
     half = hidden.shape[1] // 2
     copies = []
-    wait_down()
+    for copy in before_down:
+        copy.wait()
     for j in range(nx):
         part = jnp.dot(hidden[:, :half], dv[2 * j], preferred_element_type=F32)
         part = part + jnp.dot(hidden[:, half:], dv[2 * j + 1], preferred_element_type=F32)
@@ -132,12 +136,41 @@
         copy.wait()
 
 
+def load_weights(idx, up, down, pieces, upv, dv, up_sems, d_sems):
+    nx = dv.shape[0] // 2
+    rows, wide = dv.shape[1:]
+    width = upv.shape[1]
+    deep = upv.shape[0] // nx
+    me, core = idx[0], idx[1]
+
+    def up_rows(source, half, count):
+        return upv.at[pl.ds(pl.multiple_of(source * deep + half * (deep // 2), deep // 2), count)]
+
+    ups = [pltpu.make_async_copy(up, up_rows(me, 0, deep), up_sems.at[0])]
+    downs = [pltpu.make_async_copy(down.at[pl.ds(i * rows, rows)], dv.at[2 * me + i], d_sems.at[i]) for i in range(2)]
+    for i, piece in enumerate(pieces):
+        by = (1, nx - 1, 2)[i % 3]
+        source = lax.rem(me + (nx - by), nx)
+        half = core if i < 3 else 1 - core
+        ups.append(
+            pltpu.make_async_copy(piece.at[pl.ds(0, deep // 2)], up_rows(source, half, deep // 2), up_sems.at[1 + i])
+        )
+        for k in range(wide // width):
+            downs.append(
+                pltpu.make_async_copy(
+                    piece.at[pl.ds(deep // 2 + k * rows, rows)],
+                    dv.at[2 * source + half, :, pl.ds(k * width, width)],
+                    d_sems.at[2 + 2 * i + k],
+                )
+            )
+    for copy in ups + downs:
+        copy.start()
+    return ups, downs
+
+
 def first_kernel(
-    idx, x0, x1, x2, x3, up, own, m1, m2, m3, o1, o2, o3, u0, u1, u2, u3, xs, upv, dv, ov, x_sem, up_sem, d_sems, out_sems
+    idx, x0, x1, x2, x3, up, down, m1, m2, m3, o1, o2, o3, u0, u1, u2, u3, xs, upv, dv, ov, x_sem, up_sems, d_sems, out_sems
 ):
-    nx = dv.shape[0] // 2
-    rows = dv.shape[1]
-    me, core = idx[0], idx[1]
     x_copies = []
     for d, x in enumerate((x0, x1, x2, x3)):
         for i in range(8):
@@ -145,41 +178,14 @@
             copy = pltpu.make_async_copy(x.at[i // 2, i % 2], xs.at[:, pl.ds(at, 128)], x_sem.at[d * 8 + i])
             copy.start()
             x_copies.append(copy)
-    deep = upv.shape[0] // nx
-    up_copies = []
-    for k in range(nx):
-        chunk = pl.ds(k * deep, deep)
-        up_copies.append(pltpu.make_async_copy(up.at[chunk], upv.at[chunk], up_sem.at[k]))
-        up_copies[-1].start()
-    d_copies = [
-        pltpu.make_async_copy(own.at[pl.ds(0, rows)], dv.at[2 * me], d_sems.at[0]),
-        pltpu.make_async_copy(own.at[pl.ds(rows, rows)], dv.at[2 * me + 1], d_sems.at[1]),
-    ]
-    for i, (by, mine, other) in enumerate(((1, m1, o1), (nx - 1, m2, o2), (2, m3, o3))):
-        source = lax.rem(me + (nx - by), nx)
-        d_copies.append(pltpu.make_async_copy(mine, dv.at[2 * source + core], d_sems.at[2 + 2 * i]))
-        d_copies.append(pltpu.make_async_copy(other, dv.at[2 * source + 1 - core], d_sems.at[3 + 2 * i]))
-    for copy in d_copies:
-        copy.start()
-
-    def wait_up(k):
-        if k == 0:
-            for copy in x_copies:
-                copy.wait()
-        up_copies[k].wait()
-
-    def wait_down():
-        for copy in d_copies:
-            copy.wait()
-
-    matmuls(idx, xs, upv, dv, ov, (u0, u1, u2, u3), out_sems, wait_up, wait_down, nx)
+    ups, downs = load_weights(idx, up, down, (m1, m2, m3, o1, o2, o3), upv, dv, up_sems, d_sems)
+    matmuls(idx, xs, upv, dv, ov, (u0, u1, u2, u3), out_sems, x_copies + ups, downs)
 
 
 def second_kernel(
-    idx, x0, x1, x2, x3, up, down, mixed, own_gain, own_bias, u0, u1, u2, u3, own, xs, xv, upv, dv, ov, gain, bias,
-    x_sem, up_sem, d_sem, out_sems,
+    idx, x0, x1, x2, x3, up, down, m1, m2, m3, o1, o2, o3, mixed, own_gain, own_bias, u0, u1, u2, u3, own,
+    xs, xv, upv, dv, ov, gain, bias, x_sem, up_sems, d_sems, out_sems,
 ):
-    nx = dv.shape[0] // 2
     nb = xv.shape[0]
     tokens = xs.shape[0]
     x_copies = []
@@ -189,10 +195,7 @@
             copy = pltpu.make_async_copy(x.at[i // 2, i % 2], to, x_sem.at[d * 8 + i])
             copy.start()
             x_copies.append(copy)
-    up_copy = pltpu.make_async_copy(up, upv, up_sem)
-    d_copy = pltpu.make_async_copy(down, dv, d_sem)
-    up_copy.start()
-    d_copy.start()
+    ups, downs = load_weights(idx, up, down, (m1, m2, m3, o1, o2, o3), upv, dv, up_sems, d_sems)
     for copy in x_copies:
         copy.wait()
     step = 64
@@ -221,11 +224,7 @@
 
     lax.fori_loop(0, tokens // step, norm, 0)
 
-    def wait_up(k):
-        if k == 0:
-            up_copy.wait()
-
-    matmuls(idx, xs, upv, dv, ov, (u0, u1, u2, u3), out_sems, wait_up, d_copy.wait, nx)
+    matmuls(idx, xs, upv, dv, ov, (u0, u1, u2, u3), out_sems, ups, downs)
 
 
 ANY = pl.BlockSpec(memory_space=pltpu.MemorySpace.HBM)
@@ -233,54 +232,30 @@
 SMEM = pl.BlockSpec(memory_space=pltpu.MemorySpace.SMEM)
 
 
-def first_ffn(idx, x, up, own, mine, others):
-    tokens = x[0].shape[2]
-    width, ff = up.shape
+def ffn(kernel, idx, x, tokens, up, down, pieces, extra, own_out, norm_scratch):
     nx, nb = lax.axis_size(X), NZ * NY
+    width, ff = up.shape[0] * nx, up.shape[1]
     return pl.pallas_call(
-        first_kernel,
-        out_shape=[jax.ShapeDtypeStruct((4, nb // 16, tokens, 128), BF)] * 4,
-        in_specs=[SMEM] + [ANY] * 12,
-        out_specs=[ANY] * 4,
-        scratch_shapes=[
-            pltpu.VMEM((tokens, width), BF),
+        kernel,
+        out_shape=[jax.ShapeDtypeStruct((4, nb // 16, tokens, 128), BF)] * 4 + own_out,
+        in_specs=[SMEM] + [ANY] * (6 + len(pieces)) + [VMEM] * len(extra),
+        out_specs=[ANY] * 4 + [VMEM] * len(own_out),
+        scratch_shapes=[pltpu.VMEM((tokens, width), BF)]
+        + norm_scratch[:1]
+        + [
             pltpu.VMEM((width, ff), BF),
             pltpu.VMEM((2 * nx, ff // 2, width // nx), BF),
             pltpu.VMEM((nb, tokens, 128), BF),
+        ]
+        + norm_scratch[1:]
+        + [
             pltpu.SemaphoreType.DMA((nb,)),
-            pltpu.SemaphoreType.DMA((nx,)),
-            pltpu.SemaphoreType.DMA((8,)),
+            pltpu.SemaphoreType.DMA((7,)),
+            pltpu.SemaphoreType.DMA((14,)),
             pltpu.SemaphoreType.DMA((nb,)),
         ],
         cost_estimate=pl.CostEstimate(flops=4 * tokens * width * ff, bytes_accessed=14 << 20, transcendentals=0),
-        name="first_ffn",
-    )(idx, *x, up, own, *mine, *others)
-
-
-def second_ffn(idx, x, tokens, up, down, mixed, own_gain, own_bias):
-    width, ff = up.shape
-    nx, nb = lax.axis_size(X), NZ * NY
-    return pl.pallas_call(
-        second_kernel,
-        out_shape=[jax.ShapeDtypeStruct((4, nb // 16, tokens, 128), BF)] * 4 + [jax.ShapeDtypeStruct((tokens, 128), BF)],
-        in_specs=[SMEM] + [ANY] * 6 + [VMEM] * 3,
-        out_specs=[ANY] * 4 + [VMEM],
-        scratch_shapes=[
-            pltpu.VMEM((tokens, width), BF),
-            pltpu.VMEM((nb, *x[0].shape[2:]), BF),
-            pltpu.VMEM((width, ff), BF),
-            pltpu.VMEM((2 * nx, ff // 2, width // nx), BF),
-            pltpu.VMEM((nb, tokens, 128), BF),
-            pltpu.VMEM((nb, 128), F32),
-            pltpu.VMEM((nb, 128), F32),
-            pltpu.SemaphoreType.DMA((nb,)),
-            pltpu.SemaphoreType.DMA,
-            pltpu.SemaphoreType.DMA,
-            pltpu.SemaphoreType.DMA((nb,)),
-        ],
-        cost_estimate=pl.CostEstimate(flops=4 * tokens * width * ff, bytes_accessed=14 << 20, transcendentals=0),
-        name="second_ffn",
-    )(idx, *x, up, down, mixed, own_gain, own_bias)
+    )(idx, *x, up, down, *pieces, *extra)
 
 
 def body(
@@ -297,26 +272,30 @@
     tokens = stream.shape[0]
     pairs = pairs_of([lax.axis_size(axis) for axis in ALL])
     pair = jnp.stack([stream, lax.ppermute(stream, ALL, pairs["last"])])
-    half = half_of(down_first)
-    mine = [shift(half, X, by) for by in (1, -1, 2)]
-    up_1 = lax.all_gather(half_of(up_first), (X, C), axis=0, tiled=True)
+    w = packed(up_first, down_first)
+    mine_1 = [shift(w, X, by) for by in (1, -1, 2)]
     x_all = gathered(pair, pairs)
-    others = [shift(m, C, 1) for m in mine]
-    up_2 = lax.all_gather(half_of(up_second), (X, C), axis=0, tiled=True)
-    down_2 = lax.all_gather(half_of(down_second), (X, C), axis=0, tiled=False)
-    down_2 = down_2.reshape(-1, *half.shape)
+    others_1 = [shift(m, C, 1) for m in mine_1]
+    w = packed(up_second, down_second)
+    mine_2 = [shift(w, X, by) for by in (1, -1, 2)]
     core = lax.axis_index(C)
     p, yh, zh = place(lax.axis_index(Z), lax.axis_index(Y), core)
     idx = jnp.stack([lax.axis_index(X), core, p, yh, zh]).astype(jnp.int32)
-    parts = first_ffn(idx, x_all, up_1, down_first, mine, others)
+    parts = ffn(first_kernel, idx, x_all, tokens, up_first, down_first, mine_1 + others_1, [], [], [])
     tail = jnp.stack(split3(gain_first) + split3(bias_first) + [jnp.zeros_like(gain_first)] * 2).astype(BF)
-    tails = jnp.stack([tail, lax.ppermute(tail, ALL, pairs["last"])])
-    some = scattered_sum(parts, pairs).astype(BF)
-    branch = some.astype(F32) + lax.ppermute(some, ALL, pairs["last"])[::-1].astype(F32)
-    mixed = RESID * pair.astype(F32) + branch
+    tails = jnp.broadcast_to(tail[None], (2, *tail.shape))
+    some = jnp.concatenate([scattered_sum(parts, pairs).astype(BF), tails], axis=1)
+    there = lax.ppermute(some, ALL, pairs["last"])[::-1]
+    mixed = RESID * pair.astype(F32) + some[:, :tokens].astype(F32) + there[:, :tokens].astype(F32)
+    tails = jnp.stack([tail, there[1, tokens:]])
     mixed_all = gathered(jnp.concatenate([mixed.astype(BF), tails], axis=1), pairs)
-    *parts, x = second_ffn(
-        idx, mixed_all, tokens, up_2, down_2, mixed[0], gain_first[None], bias_first[None]
+    others_2 = [shift(m, C, 1) for m in mine_2]
+    nb = NZ * NY
+    *parts, x = ffn(
+        second_kernel, idx, mixed_all, tokens, up_second, down_second, mine_2 + others_2,
+        [mixed[0], gain_first[None], bias_first[None]],
+        [jax.ShapeDtypeStruct((tokens, 128), BF)],
+        [pltpu.VMEM((nb, tokens + 8, 128), BF), pltpu.VMEM((nb, 128), F32), pltpu.VMEM((nb, 128), F32)],
     )
     some = scattered_sum(parts, pairs)
     branch = some[0] + lax.ppermute(some[1].astype(BF), ALL, pairs["last"]).astype(F32)

time: 249 us -> 266 us (1.068)
  waiting for transfers between devices: 124 us -> 151 us
  between operations: 13.4 us -> 0.35 us
  starting transfers between devices: 61.2 us -> 64.4 us
  Pallas kernels: 21.1 us -> 23.9 us
    ppermute x6 -> x12, waiting for transfers between devices: 19.8 us -> 35.4 us  [shift(): return lax.ppermute(a, axis, [(i, (i + by) % n) for i in range(n)])]
    ppermute x24, waiting for transfers between devices: 90.7 us -> 98.2 us  [stage(): lax.ppermute(blocks[d], ALL, pairs[d])]
    ppermute x6 -> x12, starting transfers between devices: 3.4 us -> 10.8 us  [shift(): return lax.ppermute(a, axis, [(i, (i + by) % n) for i in range(n)])]
    ppermute x2 -> x1, starting transfers between devices: 6.1 us -> 1.28 us  [body(): there = lax.ppermute(some, ALL, pairs['last'])[::-1]]
    ppermute x2 -> x1, waiting for transfers between devices: 4.09 us -> 8.56 us  [body(): there = lax.ppermute(some, ALL, pairs['last'])[::-1]]
    pallas_call x2, Pallas kernels: 21.1 us -> 23.9 us  [ffn(): pl.pallas_call(kernel, out_shape=[jax.ShapeDtypeStruct((4, nb // 16, toke...]
  transfers between devices with their start and end apart: 37 -> 39, of which waited for: 25 -> 25; matrix products, arithmetic and copies ran while one was open for 2% -> 1% of each run, Pallas kernels for 4% -> 0%
where the time goes in v3:
time: 266 us
  waiting for transfers between devices  151 us (57%)
  starting transfers between devices  64.4 us (24%)
  Pallas kernels  23.9 us (9%)
  blocking collectives  17 us (6%)
  local copies, waits for them, and re-layouts  5.43 us (2%)
  other arithmetic  3.83 us (1%)
    ppermute x24, waiting for transfers between devices, stage(): lax.ppermute(blocks[d], ALL, pairs[d])  98.2 us
    ppermute x24, starting transfers between devices, stage(): lax.ppermute(blocks[d], ALL, pairs[d])  42.8 us
    ppermute x12, waiting for transfers between devices, shift(): return lax.ppermute(a, axis, [(i, (i + by) % n) for i in range(n)])  35.4 us
    pallas_call x2, Pallas kernels, ffn(): pl.pallas_call(kernel, out_shape=[jax.ShapeDtypeStruct((4, nb // 16, toke...  23.9 us
    all_to_all x1, blocking collectives, stats_to_all(): lax.all_to_all(jnp.broadcast_to(row[None], (n, *row.shape)), RA, 0, 0, ti...  17 us
    ppermute x12, starting transfers between devices, shift(): return lax.ppermute(a, axis, [(i, (i + by) % n) for i in range(n)])  10.8 us
    ppermute x1, waiting for transfers between devices, body(): there = lax.ppermute(some, ALL, pairs['last'])[::-1]  8.56 us
    ppermute x1, waiting for transfers between devices, body(): lax.ppermute(some[1].astype(BF), ALL, pairs['last']).astype(F32)  7.51 us
  transfers between devices with their start and end apart: 39, of which 25 were waited for; matrix products, arithmetic and copies ran while one was open for 1% of the time, Pallas kernels for 0%

profile of v3, /device:TPU:2, one launch (start us, length us, event | category | flops | bytes accessed | tf_op | source)
XLA Modules:
  0.0 266.0 jit_solution(8384055665425844488)
XLA Ops:
  0.0 7.2 %collective-permute-start = (bf16[384,128]{1,0:T(8,128)(2,1)}, bf16[384,128]{1,0:T(8,128)(2,1)S(1)}, u32[]{:S(2)}, u32[]{:S(2)}) collective-permute-start(bf16[384,128]{1,0:T(8,128)(2,1)} %param.9), channel_id=1, source_target_pairs={{0,128},{16,144},{64,192},{80,208},{128,0},{144,16},{192,64},{208,... | collective-permute-start | bytes 294920 | tf_op jit(solution)/shard_map/ppermute | solution.py:274
  7.2 1.3 constant_dynamic-slice_fusion
  8.8 1.5 collective-permute-done
  10.3 6.6 %collective-permute-start.3 = (bf16[2,384,128]{2,1,0:T(8,128)(2,1)S(1)}, bf16[2,384,128]{2,1,0:T(8,128)(2,1)S(1)}, u32[]{:S(2)}, u32[]{:S(2)}) collective-permute-start(bf16[2,384,128]{2,1,0:T(8,128)(2,1)S(1)} %get-tuple-element.42), channel_id=1, source_target_pairs={{0,80},{16,64},{64,16},{80,0},{128,208},{144,192},{192,144},{208,1... | collective-permute-start | bytes 589832 | tf_op jit(solution)/shard_map/ppermute | solution.py:52
  17.0 1.6 collective-permute-start.7
  19.1 2.1 collective-permute-start.9
  21.2 1.9 collective-permute-done.3
  23.1 1.3 collective-permute-start.2
  24.3 4.9 %collective-permute-done.1 = bf16[2,384,128]{2,1,0:T(8,128)(2,1)S(1)} collective-permute-done((bf16[2,384,128]{2,1,0:T(8,128)(2,1)S(1)}, bf16[2,384,128]{2,1,0:T(8,128)(2,1)S(1)}, u32[]{:S(2)}, u32[]{:S(2)}) %collective-permute-start.1) | collective-permute-done | bytes 196640 | tf_op jit(solution)/shard_map/ppermute | solution.py:52
  29.3 1.8 collective-permute-done.2
  31.2 2.0 collective-permute-start.4
  33.2 9.4 %collective-permute-done.7.m1 = bf16[1024,512]{1,0:T(8,128)(2,1)} collective-permute-done((bf16[1024,512]{1,0:T(8,128)(2,1)S(1)}, bf16[1024,512]{1,0:T(8,128)(2,1)}, u32[]{:S(2)}, u32[]{:S(2)}) %collective-permute-start.7) | collective-permute-done | bytes 1048608 | tf_op jit(solution)/shard_map/ppermute | solution.py:73
  42.5 1.4 collective-permute-start.10
  44.5 22.9 %collective-permute-done.9.m3 = bf16[1024,512]{1,0:T(8,128)(2,1)} collective-permute-done((bf16[1024,512]{1,0:T(8,128)(2,1)S(1)}, bf16[1024,512]{1,0:T(8,128)(2,1)}, u32[]{:S(2)}, u32[]{:S(2)}) %collective-permute-start.9) | collective-permute-done | bytes 1048608 | tf_op jit(solution)/shard_map/ppermute | solution.py:73
  70.5 17.6 %collective-permute-done.5.x2 = bf16[4,2,384,128]{3,2,1,0:T(8,128)(2,1)} collective-permute-done((bf16[4,2,384,128]{3,2,1,0:T(8,128)(2,1)S(1)}, bf16[4,2,384,128]{3,2,1,0:T(8,128)(2,1)}, u32[]{:S(2)}, u32[]{:S(2)}) %collective-permute-start.5) | collective-permute-done | bytes 786464 | tf_op jit(solution)/shard_map/ppermute | solution.py:52
  88.1 10.3 %shard_map.91 = (bf16[4,2,384,128]{3,2,1,0:T(8,128)(2,1)}, bf16[4,2,384,128]{3,2,1,0:T(8,128)(2,1)}, bf16[4,2,384,128]{3,2,1,0:T(8,128)(2,1)}, bf16[4,2,384,128]{3,2,1,0:T(8,128)(2,1)}) custom-call(s32[5]{0:T(128)} %stack.106.idx, bf16[4,2,384,128]{3,2,1,0:T(8,128)(2,1)} %copy-done.1, bf16[4,2,384,128]{3,2,1,0:T(8,128)(2,1)} %copy-done.16, ...), custom_call_target="tpu_custom_call" | custom-call | flops 3221225472 | bytes 14680064 | tf_op jit(solution)/shard_map/pallas_call | solution.py:238
  99.3 2.7 %collective-permute-start.15 = (bf16[4,2,384,128]{3,2,1,0:T(8,128)(2,1)}, bf16[4,2,384,128]{3,2,1,0:T(8,128)(2,1)S(1)}, u32[]{:S(2)}, u32[]{:S(2)}) collective-permute-start(bf16[4,2,384,128]{3,2,1,0:T(8,128)(2,1)} %get-tuple-element.17), channel_id=1, source_target_pairs={{0,40},{8,32},{32,8},{40,0},{1,249},{25,225},{225,25},{249,1},{2,4... | collective-permute-start | bytes 2359304 | tf_op jit(solution)/shard_map/ppermute | solution.py:52
  102.2 2.0 collective-permute-start.27
  104.3 6.5 %collective-permute-done.13 = bf16[4,2,384,128]{3,2,1,0:T(8,128)(2,1)S(1)} collective-permute-done((bf16[4,2,384,128]{3,2,1,0:T(8,128)(2,1)}, bf16[4,2,384,128]{3,2,1,0:T(8,128)(2,1)S(1)}, u32[]{:S(2)}, u32[]{:S(2)}) %collective-permute-start.13) | collective-permute-done | bytes 786464 | tf_op jit(solution)/shard_map/ppermute | solution.py:52
  110.8 8.4 %collective-permute-done.15 = bf16[4,2,384,128]{3,2,1,0:T(8,128)(2,1)S(1)} collective-permute-done((bf16[4,2,384,128]{3,2,1,0:T(8,128)(2,1)}, bf16[4,2,384,128]{3,2,1,0:T(8,128)(2,1)S(1)}, u32[]{:S(2)}, u32[]{:S(2)}) %collective-permute-start.15) | collective-permute-done | bytes 786464 | tf_op jit(solution)/shard_map/ppermute | solution.py:52
  120.5 1.3 collective-permute-start.17
  121.8 4.0 %collective-permute-start.18 = (bf16[2,384,128]{2,1,0:T(8,128)(2,1)S(1)}, bf16[2,384,128]{2,1,0:T(8,128)(2,1)S(1)}, u32[]{:S(2)}, u32[]{:S(2)}) collective-permute-start(bf16[2,384,128]{2,1,0:T(8,128)(2,1)S(1)} %get-tuple-element.37), channel_id=1, source_target_pairs={{0,80},{16,64},{64,16},{80,0},{128,208},{144,192},{192,144},{208,1... | collective-permute-start | bytes 589832 | tf_op jit(solution)/shard_map/ppermute | solution.py:52
  125.8 1.5 collective-permute-done.26.m1
  127.4 1.5 collective-permute-start.28
  129.9 4.6 %collective-permute-done.18 = bf16[2,384,128]{2,1,0:T(8,128)(2,1)S(1)} collective-permute-done((bf16[2,384,128]{2,1,0:T(8,128)(2,1)S(1)}, bf16[2,384,128]{2,1,0:T(8,128)(2,1)S(1)}, u32[]{:S(2)}, u32[]{:S(2)}) %collective-permute-start.18) | collective-permute-done | bytes 196640 | tf_op jit(solution)/shard_map/ppermute | solution.py:52
  134.7 1.3 collective-permute-start.19
  136.0 8.6 %collective-permute-done.19 = bf16[2,392,128]{2,1,0:T(8,128)(2,1)S(1)} collective-permute-done((bf16[2,392,128]{2,1,0:T(8,128)(2,1)S(1)}, bf16[2,392,128]{2,1,0:T(8,128)(2,1)S(1)}, u32[]{:S(2)}, u32[]{:S(2)}) %collective-permute-start.19) | collective-permute-done | bytes 200736 | tf_op jit(solution)/shard_map/ppermute | solution.py:288
  144.7 5.9 %collective-permute-start.20 = (bf16[2,392,128]{2,1,0:T(8,128)(2,1)S(1)}, bf16[2,392,128]{2,1,0:T(8,128)(2,1)S(1)}, u32[]{:S(2)}, u32[]{:S(2)}) collective-permute-start(bf16[2,392,128]{2,1,0:T(8,128)(2,1)S(1)} %get-tuple-element.40), channel_id=1, source_target_pairs={{0,64},{16,80},{64,0},{80,16},{128,192},{144,208},{192,128},{208,1... | collective-permute-start | bytes 602120 | tf_op jit(solution)/shard_map/ppermute | solution.py:52
  150.8 3.0 %collective-permute-start.22 = (bf16[2,392,128]{2,1,0:T(8,128)(2,1)S(1)}, bf16[2,392,128]{2,1,0:T(8,128)(2,1)S(1)}, u32[]{:S(2)}, u32[]{:S(2)}) collective-permute-start(bf16[2,392,128]{2,1,0:T(8,128)(2,1)S(1)} %get-tuple-element.40), channel_id=1, source_target_pairs={{0,80},{16,64},{64,16},{80,0},{128,208},{144,192},{192,144},{208,1... | collective-permute-start | bytes 602120 | tf_op jit(solution)/shard_map/ppermute | solution.py:52
  153.8 1.2 collective-permute-done.28.m3
  155.0 2.0 collective-permute-done.20
  158.0 5.5 %collective-permute-done.22 = bf16[2,392,128]{2,1,0:T(8,128)(2,1)S(1)} collective-permute-done((bf16[2,392,128]{2,1,0:T(8,128)(2,1)S(1)}, bf16[2,392,128]{2,1,0:T(8,128)(2,1)S(1)}, u32[]{:S(2)}, u32[]{:S(2)}) %collective-permute-start.22) | collective-permute-done | bytes 200736 | tf_op jit(solution)/shard_map/ppermute | solution.py:52
  164.2 3.0 %collective-permute-start.25 = (bf16[4,2,392,128]{3,2,1,0:T(8,128)(2,1)S(1)}, bf16[4,2,392,128]{3,2,1,0:T(8,128)(2,1)S(1)}, u32[]{:S(2)}, u32[]{:S(2)}) collective-permute-start(bf16[4,2,392,128]{3,2,1,0:T(8,128)(2,1)S(1)} %pad_maximum_fusion.2.x0), channel_id=1, source_target_pairs={{0,40},{8,32},{32,8},{40,0},{1,249},{25,225},{225,25},{249,1},{2,4... | collective-permute-start | bytes 2408456 | tf_op jit(solution)/shard_map/ppermute | solution.py:52
  168.0 7.9 %collective-permute-done.23.x1 = bf16[4,2,392,128]{3,2,1,0:T(8,128)(2,1)S(1)} collective-permute-done((bf16[4,2,392,128]{3,2,1,0:T(8,128)(2,1)S(1)}, bf16[4,2,392,128]{3,2,1,0:T(8,128)(2,1)S(1)}, u32[]{:S(2)}, u32[]{:S(2)}) %collective-permute-start.23) | collective-permute-done | bytes 802848 | tf_op jit(solution)/shard_map/ppermute | solution.py:52
  175.9 9.1 %collective-permute-done.24.x2 = bf16[4,2,392,128]{3,2,1,0:T(8,128)(2,1)S(1)} collective-permute-done((bf16[4,2,392,128]{3,2,1,0:T(8,128)(2,1)S(1)}, bf16[4,2,392,128]{3,2,1,0:T(8,128)(2,1)S(1)}, u32[]{:S(2)}, u32[]{:S(2)}) %collective-permute-start.24) | collective-permute-done | bytes 802848 | tf_op jit(solution)/shard_map/ppermute | solution.py:52
  186.2 13.6 %shard_map.92 = (bf16[4,2,384,128]{3,2,1,0:T(8,128)(2,1)}, bf16[4,2,384,128]{3,2,1,0:T(8,128)(2,1)}, bf16[4,2,384,128]{3,2,1,0:T(8,128)(2,1)}, bf16[4,2,384,128]{3,2,1,0:T(8,128)(2,1)}, bf16[384,128]{1,0:T(8,128)(2,1)}) custom-call(s32[5]{0:T(128)} %stack.106.idx, bf16[4,2,392,128]{3,2,1,0:T(8,128)(2,1)} %copy-done, bf16[4,2,392,128]{3,2,1,0:T(8,128)(2,1)} %copy-done.13, ...), custom_call_target="tpu_custom_call" | custom-call | flops 3221225472 | bytes 14680064 | tf_op jit(solution)/shard_map/pallas_call | solution.py:238
  199.9 1.7 collective-permute-start.32
  201.7 1.7 collective-permute-start.34
  203.4 8.7 %collective-permute-done.32 = bf16[4,2,384,128]{3,2,1,0:T(8,128)(2,1)S(1)} collective-permute-done((bf16[4,2,384,128]{3,2,1,0:T(8,128)(2,1)}, bf16[4,2,384,128]{3,2,1,0:T(8,128)(2,1)S(1)}, u32[]{:S(2)}, u32[]{:S(2)}) %collective-permute-start.32) | collective-permute-done | bytes 786464 | tf_op jit(solution)/shard_map/ppermute | solution.py:52
  212.2 10.0 %collective-permute-done.33 = bf16[4,2,384,128]{3,2,1,0:T(8,128)(2,1)S(1)} collective-permute-done((bf16[4,2,384,128]{3,2,1,0:T(8,128)(2,1)}, bf16[4,2,384,128]{3,2,1,0:T(8,128)(2,1)S(1)}, u32[]{:S(2)}, u32[]{:S(2)}) %collective-permute-start.33) | collective-permute-done | bytes 786464 | tf_op jit(solution)/shard_map/ppermute | solution.py:52
  222.2 1.5 add_convert_fusion
  224.5 2.9 %collective-permute-start.36 = (bf16[2,384,128]{2,1,0:T(8,128)(2,1)S(1)}, bf16[2,384,128]{2,1,0:T(8,128)(2,1)S(1)}, u32[]{:S(2)}, u32[]{:S(2)}) collective-permute-start(bf16[2,384,128]{2,1,0:T(8,128)(2,1)S(1)} %get-tuple-element.35), channel_id=1, source_target_pairs={{0,16},{16,0},{64,80},{80,64},{128,144},{144,128},{192,208},{208,1... | collective-permute-start | bytes 589832 | tf_op jit(solution)/shard_map/ppermute | solution.py:52
  227.4 2.4 collective-permute-start.37
  229.8 4.9 %collective-permute-done.35 = bf16[2,384,128]{2,1,0:T(8,128)(2,1)S(1)} collective-permute-done((bf16[2,384,128]{2,1,0:T(8,128)(2,1)S(1)}, bf16[2,384,128]{2,1,0:T(8,128)(2,1)S(1)}, u32[]{:S(2)}, u32[]{:S(2)}) %collective-permute-start.35) | collective-permute-done | bytes 196640 | tf_op jit(solution)/shard_map/ppermute | solution.py:52
  234.6 3.2 %collective-permute-done.37 = bf16[2,384,128]{2,1,0:T(8,128)(2,1)S(1)} collective-permute-done((bf16[2,384,128]{2,1,0:T(8,128)(2,1)S(1)}, bf16[2,384,128]{2,1,0:T(8,128)(2,1)S(1)}, u32[]{:S(2)}, u32[]{:S(2)}) %collective-permute-start.37) | collective-permute-done | bytes 196640 | tf_op jit(solution)/shard_map/ppermute | solution.py:52
  237.9 2.4 collective-permute-start.38
  240.3 7.5 %collective-permute-done.38 = bf16[384,128]{1,0:T(8,128)(2,1)S(1)} collective-permute-done((bf16[384,128]{1,0:T(8,128)(2,1)S(1)}, bf16[384,128]{1,0:T(8,128)(2,1)S(1)}, u32[]{:S(2)}, u32[]{:S(2)}) %collective-permute-start.38) | collective-permute-done | bytes 98336 | tf_op jit(solution)/shard_map/ppermute | solution.py:301
  248.1 17.0 %all_to_all.5 = f32[32,1,768]{2,1,0:T(1,128)S(1)} all-to-all(f32[32,1,768]{2,1,0:T(1,128)S(1)} %broadcast_in_dim.11), channel_id=1, replica_groups=mesh['ra_0'=8,'ra_1'=4,'cb'=4,'dp'=2] {'ra_0','ra_1'}, dimensions={0} | all-to-all | bytes 196608 | tf_op jit(solution)/shard_map/all_to_all | solution.py:68
  (103 shorter events, 14.3 us)
Async XLA Ops:
  0.0 10.3 %collective-permute-start = (bf16[384,128]{1,0:T(8,128)(2,1)}, bf16[384,128]{1,0:T(8,128)(2,1)S(1)}, u32[]{:S(2)}, u32[]{:S(2)}) collective-permute-start(bf16[384,128]{1,0:T(8,128)(2,1)} %param.9), channel_id=1, source_target_pairs={{0,128},{16,144},{64,192},{80,208},{128,0},{144,16},{192,64},{208,... | collective-permute-start | bytes 294920 | tf_op jit(solution)/shard_map/ppermute | solution.py:274
  10.3 12.7 %collective-permute-start.3 = (bf16[2,384,128]{2,1,0:T(8,128)(2,1)S(1)}, bf16[2,384,128]{2,1,0:T(8,128)(2,1)S(1)}, u32[]{:S(2)}, u32[]{:S(2)}) collective-permute-start(bf16[2,384,128]{2,1,0:T(8,128)(2,1)S(1)} %get-tuple-element.42), channel_id=1, source_target_pairs={{0,80},{16,64},{64,16},{80,0},{128,208},{144,192},{192,144},{208,1... | collective-permute-start | bytes 589832 | tf_op jit(solution)/shard_map/ppermute | solution.py:52
  17.0 25.6 %collective-permute-start.7 = (bf16[1024,512]{1,0:T(8,128)(2,1)S(1)}, bf16[1024,512]{1,0:T(8,128)(2,1)}, u32[]{:S(2)}, u32[]{:S(2)}) collective-permute-start(bf16[1024,512]{1,0:T(8,128)(2,1)S(1)} %pad_maximum_fusion), channel_id=1, source_target_pairs={{0,2},{2,4},{4,6},{6,0},{1,3},{3,5},{5,7},{7,1},{8,10},{10,12},{12... | collective-permute-start | bytes 3145736 | tf_op jit(solution)/shard_map/ppermute | solution.py:73
  18.5 25.8 %collective-permute-start.8 = (bf16[1024,512]{1,0:T(8,128)(2,1)S(1)}, bf16[1024,512]{1,0:T(8,128)(2,1)}, u32[]{:S(2)}, u32[]{:S(2)}) collective-permute-start(bf16[1024,512]{1,0:T(8,128)(2,1)S(1)} %pad_maximum_fusion), channel_id=1, source_target_pairs={{0,6},{2,0},{4,2},{6,4},{1,7},{3,1},{5,3},{7,5},{8,14},{10,8},{12,... | collective-permute-start | bytes 3145736 | tf_op jit(solution)/shard_map/ppermute | solution.py:73
  19.1 48.3 %collective-permute-start.9 = (bf16[1024,512]{1,0:T(8,128)(2,1)S(1)}, bf16[1024,512]{1,0:T(8,128)(2,1)}, u32[]{:S(2)}, u32[]{:S(2)}) collective-permute-start(bf16[1024,512]{1,0:T(8,128)(2,1)S(1)} %pad_maximum_fusion), channel_id=1, source_target_pairs={{0,4},{2,6},{4,0},{6,2},{1,5},{3,7},{5,1},{7,3},{8,12},{10,14},{12... | collective-permute-start | bytes 3145736 | tf_op jit(solution)/shard_map/ppermute | solution.py:73
  21.2 8.1 %collective-permute-start.1 = (bf16[2,384,128]{2,1,0:T(8,128)(2,1)S(1)}, bf16[2,384,128]{2,1,0:T(8,128)(2,1)S(1)}, u32[]{:S(2)}, u32[]{:S(2)}) collective-permute-start(bf16[2,384,128]{2,1,0:T(8,128)(2,1)S(1)} %get-tuple-element.42), channel_id=1, source_target_pairs={{0,64},{16,80},{64,0},{80,16},{128,192},{144,208},{192,128},{208,1... | collective-permute-start | bytes 589832 | tf_op jit(solution)/shard_map/ppermute | solution.py:52
  23.1 8.0 %collective-permute-start.2 = (bf16[2,384,128]{2,1,0:T(8,128)(2,1)S(1)}, bf16[2,384,128]{2,1,0:T(8,128)(2,1)S(1)}, u32[]{:S(2)}, u32[]{:S(2)}) collective-permute-start(bf16[2,384,128]{2,1,0:T(8,128)(2,1)S(1)} %get-tuple-element.42), channel_id=1, source_target_pairs={{0,16},{16,0},{64,80},{80,64},{128,144},{144,128},{192,208},{208,1... | collective-permute-start | bytes 589832 | tf_op jit(solution)/shard_map/ppermute | solution.py:52
  31.2 57.0 %copy-start.1 = (bf16[4,2,384,128]{3,2,1,0:T(8,128)(2,1)}, bf16[4,2,384,128]{3,2,1,0:T(8,128)(2,1)S(1)}, u32[]{:S(2)}) copy-start(bf16[4,2,384,128]{3,2,1,0:T(8,128)(2,1)S(1)} %pad_maximum_fusion.3.x0) | copy-start | bytes 2359300
  31.2 37.1 %collective-permute-start.4 = (bf16[4,2,384,128]{3,2,1,0:T(8,128)(2,1)S(1)}, bf16[4,2,384,128]{3,2,1,0:T(8,128)(2,1)S(1)}, u32[]{:S(2)}, u32[]{:S(2)}) collective-permute-start(bf16[4,2,384,128]{3,2,1,0:T(8,128)(2,1)S(1)} %pad_maximum_fusion.3.x0), channel_id=1, source_target_pairs={{0,32},{8,40},{32,0},{40,8},{1,225},{25,249},{225,1},{249,25},{2,3... | collective-permute-start | bytes 2359304 | tf_op jit(solution)/shard_map/ppermute | solution.py:52
  42.5 45.6 %collective-permute-start.10 = (bf16[1024,512]{1,0:T(8,128)(2,1)}, bf16[1024,512]{1,0:T(8,128)(2,1)}, u32[]{:S(2)}, u32[]{:S(2)}) collective-permute-start(bf16[1024,512]{1,0:T(8,128)(2,1)} %collective-permute-done.7.m1), channel_id=1, source_target_pairs={{0,1},{1,0},{2,3},{3,2},{4,5},{5,4},{6,7},{7,6},{8,9},{9,8},{10,11... | collective-permute-start | bytes 3145736 | tf_op jit(solution)/shard_map/ppermute | solution.py:73
  44.3 43.8 %collective-permute-start.11 = (bf16[1024,512]{1,0:T(8,128)(2,1)}, bf16[1024,512]{1,0:T(8,128)(2,1)}, u32[]{:S(2)}, u32[]{:S(2)}) collective-permute-start(bf16[1024,512]{1,0:T(8,128)(2,1)} %collective-permute-done.8.m2), channel_id=1, source_target_pairs={{0,1},{1,0},{2,3},{3,2},{4,5},{5,4},{6,7},{7,6},{8,9},{9,8},{10,11... | collective-permute-start | bytes 3145736 | tf_op jit(solution)/shard_map/ppermute | solution.py:73
  67.4 20.7 %collective-permute-start.12 = (bf16[1024,512]{1,0:T(8,128)(2,1)}, bf16[1024,512]{1,0:T(8,128)(2,1)}, u32[]{:S(2)}, u32[]{:S(2)}) collective-permute-start(bf16[1024,512]{1,0:T(8,128)(2,1)} %collective-permute-done.9.m3), channel_id=1, source_target_pairs={{0,1},{1,0},{2,3},{3,2},{4,5},{5,4},{6,7},{7,6},{8,9},{9,8},{10,11... | collective-permute-start | bytes 3145736 | tf_op jit(solution)/shard_map/ppermute | solution.py:73
  67.6 20.5 %collective-permute-start.5 = (bf16[4,2,384,128]{3,2,1,0:T(8,128)(2,1)S(1)}, bf16[4,2,384,128]{3,2,1,0:T(8,128)(2,1)}, u32[]{:S(2)}, u32[]{:S(2)}) collective-permute-start(bf16[4,2,384,128]{3,2,1,0:T(8,128)(2,1)S(1)} %pad_maximum_fusion.3.x0), channel_id=1, source_target_pairs={{0,8},{8,0},{32,40},{40,32},{1,25},{25,1},{225,249},{249,225},{2,1... | collective-permute-start | bytes 2359304 | tf_op jit(solution)/shard_map/ppermute | solution.py:52
  69.2 18.9 %collective-permute-start.6 = (bf16[4,2,384,128]{3,2,1,0:T(8,128)(2,1)S(1)}, bf16[4,2,384,128]{3,2,1,0:T(8,128)(2,1)}, u32[]{:S(2)}, u32[]{:S(2)}) collective-permute-start(bf16[4,2,384,128]{3,2,1,0:T(8,128)(2,1)S(1)} %pad_maximum_fusion.3.x0), channel_id=1, source_target_pairs={{0,40},{8,32},{32,8},{40,0},{1,249},{25,225},{225,25},{249,1},{2,4... | collective-permute-start | bytes 2359304 | tf_op jit(solution)/shard_map/ppermute | solution.py:52
  70.5 31.6 %copy-start.6 = (bf16[1024,512]{1,0:T(8,128)(2,1)S(1)}, bf16[1024,512]{1,0:T(8,128)(2,1)}, u32[]{:S(2)}) copy-start(bf16[1024,512]{1,0:T(8,128)(2,1)} %up.3) | copy-start | bytes 3145732
  98.4 12.3 %collective-permute-start.13 = (bf16[4,2,384,128]{3,2,1,0:T(8,128)(2,1)}, bf16[4,2,384,128]{3,2,1,0:T(8,128)(2,1)S(1)}, u32[]{:S(2)}, u32[]{:S(2)}) collective-permute-start(bf16[4,2,384,128]{3,2,1,0:T(8,128)(2,1)} %get-tuple-element.15), channel_id=1, source_target_pairs={{0,32},{8,40},{32,0},{40,8},{1,225},{25,249},{225,1},{249,25},{2,3... | collective-permute-start | bytes 2359304 | tf_op jit(solution)/shard_map/ppermute | solution.py:52
  98.5 12.3 %collective-permute-start.14 = (bf16[4,2,384,128]{3,2,1,0:T(8,128)(2,1)}, bf16[4,2,384,128]{3,2,1,0:T(8,128)(2,1)S(1)}, u32[]{:S(2)}, u32[]{:S(2)}) collective-permute-start(bf16[4,2,384,128]{3,2,1,0:T(8,128)(2,1)} %get-tuple-element.16), channel_id=1, source_target_pairs={{0,8},{8,0},{32,40},{40,32},{1,25},{25,1},{225,249},{249,225},{2,1... | collective-permute-start | bytes 2359304 | tf_op jit(solution)/shard_map/ppermute | solution.py:52
  99.3 20.0 %collective-permute-start.15 = (bf16[4,2,384,128]{3,2,1,0:T(8,128)(2,1)}, bf16[4,2,384,128]{3,2,1,0:T(8,128)(2,1)S(1)}, u32[]{:S(2)}, u32[]{:S(2)}) collective-permute-start(bf16[4,2,384,128]{3,2,1,0:T(8,128)(2,1)} %get-tuple-element.17), channel_id=1, source_target_pairs={{0,40},{8,32},{32,8},{40,0},{1,249},{25,225},{225,25},{249,1},{2,4... | collective-permute-start | bytes 2359304 | tf_op jit(solution)/shard_map/ppermute | solution.py:52
  102.1 17.2 %copy-start.2 = (bf16[4,2,384,128]{3,2,1,0:T(8,128)(2,1)S(1)}, bf16[4,2,384,128]{3,2,1,0:T(8,128)(2,1)}, u32[]{:S(2)}) copy-start(bf16[4,2,384,128]{3,2,1,0:T(8,128)(2,1)} %get-tuple-element.14) | copy-start | bytes 2359300
  102.2 25.2 %collective-permute-start.26 = (bf16[1024,512]{1,0:T(8,128)(2,1)S(1)}, bf16[1024,512]{1,0:T(8,128)(2,1)}, u32[]{:S(2)}, u32[]{:S(2)}) collective-permute-start(bf16[1024,512]{1,0:T(8,128)(2,1)S(1)} %pad_maximum_fusion.1), channel_id=1, source_target_pairs={{0,2},{2,4},{4,6},{6,0},{1,3},{3,5},{5,7},{7,1},{8,10},{10,12},{12... | collective-permute-start | bytes 3145736 | tf_op jit(solution)/shard_map/ppermute | solution.py:73
  102.2 48.5 %collective-permute-start.27 = (bf16[1024,512]{1,0:T(8,128)(2,1)S(1)}, bf16[1024,512]{1,0:T(8,128)(2,1)}, u32[]{:S(2)}, u32[]{:S(2)}) collective-permute-start(bf16[1024,512]{1,0:T(8,128)(2,1)S(1)} %pad_maximum_fusion.1), channel_id=1, source_target_pairs={{0,6},{2,0},{4,2},{6,4},{1,7},{3,1},{5,3},{7,5},{8,14},{10,8},{12,... | collective-permute-start | bytes 3145736 | tf_op jit(solution)/shard_map/ppermute | solution.py:73
  119.8 9.1 %collective-permute-start.16 = (bf16[2,384,128]{2,1,0:T(8,128)(2,1)S(1)}, bf16[2,384,128]{2,1,0:T(8,128)(2,1)S(1)}, u32[]{:S(2)}, u32[]{:S(2)}) collective-permute-start(bf16[2,384,128]{2,1,0:T(8,128)(2,1)S(1)} %get-tuple-element.36), channel_id=1, source_target_pairs={{0,64},{16,80},{64,0},{80,16},{128,192},{144,208},{192,128},{208,1... | collective-permute-start | bytes 589832 | tf_op jit(solution)/shard_map/ppermute | solution.py:52
  120.5 9.4 %collective-permute-start.17 = (bf16[2,384,128]{2,1,0:T(8,128)(2,1)S(1)}, bf16[2,384,128]{2,1,0:T(8,128)(2,1)S(1)}, u32[]{:S(2)}, u32[]{:S(2)}) collective-permute-start(bf16[2,384,128]{2,1,0:T(8,128)(2,1)S(1)} %get-tuple-element.38), channel_id=1, source_target_pairs={{0,16},{16,0},{64,80},{80,64},{128,144},{144,128},{192,208},{208,1... | collective-permute-start | bytes 589832 | tf_op jit(solution)/shard_map/ppermute | solution.py:52
  121.8 12.7 %collective-permute-start.18 = (bf16[2,384,128]{2,1,0:T(8,128)(2,1)S(1)}, bf16[2,384,128]{2,1,0:T(8,128)(2,1)S(1)}, u32[]{:S(2)}, u32[]{:S(2)}) collective-permute-start(bf16[2,384,128]{2,1,0:T(8,128)(2,1)S(1)} %get-tuple-element.37), channel_id=1, source_target_pairs={{0,80},{16,64},{64,16},{80,0},{128,208},{144,192},{192,144},{208,1... | collective-permute-start | bytes 589832 | tf_op jit(solution)/shard_map/ppermute | solution.py:52
  127.4 27.6 %collective-permute-start.28 = (bf16[1024,512]{1,0:T(8,128)(2,1)S(1)}, bf16[1024,512]{1,0:T(8,128)(2,1)}, u32[]{:S(2)}, u32[]{:S(2)}) collective-permute-start(bf16[1024,512]{1,0:T(8,128)(2,1)S(1)} %pad_maximum_fusion.1), channel_id=1, source_target_pairs={{0,4},{2,6},{4,0},{6,2},{1,5},{3,7},{5,1},{7,3},{8,12},{10,14},{12... | collective-permute-start | bytes 3145736 | tf_op jit(solution)/shard_map/ppermute | solution.py:73
  128.9 35.4 %collective-permute-start.29 = (bf16[1024,512]{1,0:T(8,128)(2,1)}, bf16[1024,512]{1,0:T(8,128)(2,1)}, u32[]{:S(2)}, u32[]{:S(2)}) collective-permute-start(bf16[1024,512]{1,0:T(8,128)(2,1)} %collective-permute-done.26.m1), channel_id=1, source_target_pairs={{0,1},{1,0},{2,3},{3,2},{4,5},{5,4},{6,7},{7,6},{8,9},{9,8},{10,11... | collective-permute-start | bytes 3145736 | tf_op jit(solution)/shard_map/ppermute | solution.py:73
  134.7 9.9 %collective-permute-start.19 = (bf16[2,392,128]{2,1,0:T(8,128)(2,1)S(1)}, bf16[2,392,128]{2,1,0:T(8,128)(2,1)S(1)}, u32[]{:S(2)}, u32[]{:S(2)}) collective-permute-start(bf16[2,392,128]{2,1,0:T(8,128)(2,1)S(1)} %pad_maximum_fusion.4), channel_id=1, source_target_pairs={{0,128},{16,144},{64,192},{80,208},{128,0},{144,16},{192,64},{208,... | collective-permute-start | bytes 602120 | tf_op jit(solution)/shard_map/ppermute | solution.py:288
  144.7 12.3 %collective-permute-start.20 = (bf16[2,392,128]{2,1,0:T(8,128)(2,1)S(1)}, bf16[2,392,128]{2,1,0:T(8,128)(2,1)S(1)}, u32[]{:S(2)}, u32[]{:S(2)}) collective-permute-start(bf16[2,392,128]{2,1,0:T(8,128)(2,1)S(1)} %get-tuple-element.40), channel_id=1, source_target_pairs={{0,64},{16,80},{64,0},{80,16},{128,192},{144,208},{192,128},{208,1... | collective-permute-start | bytes 602120 | tf_op jit(solution)/shard_map/ppermute | solution.py:52
  150.7 7.3 %collective-permute-start.21 = (bf16[2,392,128]{2,1,0:T(8,128)(2,1)S(1)}, bf16[2,392,128]{2,1,0:T(8,128)(2,1)S(1)}, u32[]{:S(2)}, u32[]{:S(2)}) collective-permute-start(bf16[2,392,128]{2,1,0:T(8,128)(2,1)S(1)} %get-tuple-element.40), channel_id=1, source_target_pairs={{0,16},{16,0},{64,80},{80,64},{128,144},{144,128},{192,208},{208,1... | collective-permute-start | bytes 602120 | tf_op jit(solution)/shard_map/ppermute | solution.py:52
  150.8 12.8 %collective-permute-start.22 = (bf16[2,392,128]{2,1,0:T(8,128)(2,1)S(1)}, bf16[2,392,128]{2,1,0:T(8,128)(2,1)S(1)}, u32[]{:S(2)}, u32[]{:S(2)}) collective-permute-start(bf16[2,392,128]{2,1,0:T(8,128)(2,1)S(1)} %get-tuple-element.40), channel_id=1, source_target_pairs={{0,80},{16,64},{64,16},{80,0},{128,208},{144,192},{192,144},{208,1... | collective-permute-start | bytes 602120 | tf_op jit(solution)/shard_map/ppermute | solution.py:52
  154.9 13.0 %collective-permute-start.30 = (bf16[1024,512]{1,0:T(8,128)(2,1)}, bf16[1024,512]{1,0:T(8,128)(2,1)S(1)}, u32[]{:S(2)}, u32[]{:S(2)}) collective-permute-start(bf16[1024,512]{1,0:T(8,128)(2,1)} %collective-permute-done.27.m2), channel_id=1, source_target_pairs={{0,1},{1,0},{2,3},{3,2},{4,5},{5,4},{6,7},{7,6},{8,9},{9,8},{10,11... | collective-permute-start | bytes 3145736 | tf_op jit(solution)/shard_map/ppermute | solution.py:73
  157.1 10.9 %collective-permute-start.31 = (bf16[1024,512]{1,0:T(8,128)(2,1)}, bf16[1024,512]{1,0:T(8,128)(2,1)S(1)}, u32[]{:S(2)}, u32[]{:S(2)}) collective-permute-start(bf16[1024,512]{1,0:T(8,128)(2,1)} %collective-permute-done.28.m3), channel_id=1, source_target_pairs={{0,1},{1,0},{2,3},{3,2},{4,5},{5,4},{6,7},{7,6},{8,9},{9,8},{10,11... | collective-permute-start | bytes 3145736 | tf_op jit(solution)/shard_map/ppermute | solution.py:73
  163.7 22.5 %copy-start = (bf16[4,2,392,128]{3,2,1,0:T(8,128)(2,1)}, bf16[4,2,392,128]{3,2,1,0:T(8,128)(2,1)S(1)}, u32[]{:S(2)}) copy-start(bf16[4,2,392,128]{3,2,1,0:T(8,128)(2,1)S(1)} %pad_maximum_fusion.2.x0) | copy-start | bytes 2408452
  163.7 12.3 %collective-permute-start.23 = (bf16[4,2,392,128]{3,2,1,0:T(8,128)(2,1)S(1)}, bf16[4,2,392,128]{3,2,1,0:T(8,128)(2,1)S(1)}, u32[]{:S(2)}, u32[]{:S(2)}) collective-permute-start(bf16[4,2,392,128]{3,2,1,0:T(8,128)(2,1)S(1)} %pad_maximum_fusion.2.x0), channel_id=1, source_target_pairs={{0,32},{8,40},{32,0},{40,8},{1,225},{25,249},{225,1},{249,25},{2,3... | collective-permute-start | bytes 2408456 | tf_op jit(solution)/shard_map/ppermute | solution.py:52
  164.2 20.8 %collective-permute-start.24 = (bf16[4,2,392,128]{3,2,1,0:T(8,128)(2,1)S(1)}, bf16[4,2,392,128]{3,2,1,0:T(8,128)(2,1)S(1)}, u32[]{:S(2)}, u32[]{:S(2)}) collective-permute-start(bf16[4,2,392,128]{3,2,1,0:T(8,128)(2,1)S(1)} %pad_maximum_fusion.2.x0), channel_id=1, source_target_pairs={{0,8},{8,0},{32,40},{40,32},{1,25},{25,1},{225,249},{249,225},{2,1... | collective-permute-start | bytes 2408456 | tf_op jit(solution)/shard_map/ppermute | solution.py:52
  164.2 20.8 %collective-permute-start.25 = (bf16[4,2,392,128]{3,2,1,0:T(8,128)(2,1)S(1)}, bf16[4,2,392,128]{3,2,1,0:T(8,128)(2,1)S(1)}, u32[]{:S(2)}, u32[]{:S(2)}) collective-permute-start(bf16[4,2,392,128]{3,2,1,0:T(8,128)(2,1)S(1)} %pad_maximum_fusion.2.x0), channel_id=1, source_target_pairs={{0,40},{8,32},{32,8},{40,0},{1,249},{25,225},{225,25},{249,1},{2,4... | collective-permute-start | bytes 2408456 | tf_op jit(solution)/shard_map/ppermute | solution.py:52
  168.0 18.2 %copy-start.11 = (bf16[1024,512]{1,0:T(8,128)(2,1)}, bf16[1024,512]{1,0:T(8,128)(2,1)S(1)}, u32[]{:S(2)}) copy-start(bf16[1024,512]{1,0:T(8,128)(2,1)S(1)} %collective-permute-done.30.o2) | copy-start | bytes 3145732
  168.0 18.2 %copy-start.12 = (bf16[1024,512]{1,0:T(8,128)(2,1)}, bf16[1024,512]{1,0:T(8,128)(2,1)S(1)}, u32[]{:S(2)}) copy-start(bf16[1024,512]{1,0:T(8,128)(2,1)S(1)} %collective-permute-done.31.o3) | copy-start | bytes 3145732
  199.9 12.3 %collective-permute-start.32 = (bf16[4,2,384,128]{3,2,1,0:T(8,128)(2,1)}, bf16[4,2,384,128]{3,2,1,0:T(8,128)(2,1)S(1)}, u32[]{:S(2)}, u32[]{:S(2)}) collective-permute-start(bf16[4,2,384,128]{3,2,1,0:T(8,128)(2,1)} %get-tuple-element.20), channel_id=1, source_target_pairs={{0,32},{8,40},{32,0},{40,8},{1,225},{25,249},{225,1},{249,25},{2,3... | collective-permute-start | bytes 2359304 | tf_op jit(solution)/shard_map/ppermute | solution.py:52
  201.5 20.6 %collective-permute-start.33 = (bf16[4,2,384,128]{3,2,1,0:T(8,128)(2,1)}, bf16[4,2,384,128]{3,2,1,0:T(8,128)(2,1)S(1)}, u32[]{:S(2)}, u32[]{:S(2)}) collective-permute-start(bf16[4,2,384,128]{3,2,1,0:T(8,128)(2,1)} %get-tuple-element.21), channel_id=1, source_target_pairs={{0,8},{8,0},{32,40},{40,32},{1,25},{25,1},{225,249},{249,225},{2,1... | collective-permute-start | bytes 2359304 | tf_op jit(solution)/shard_map/ppermute | solution.py:52
  201.7 20.5 %collective-permute-start.34 = (bf16[4,2,384,128]{3,2,1,0:T(8,128)(2,1)}, bf16[4,2,384,128]{3,2,1,0:T(8,128)(2,1)S(1)}, u32[]{:S(2)}, u32[]{:S(2)}) collective-permute-start(bf16[4,2,384,128]{3,2,1,0:T(8,128)(2,1)} %get-tuple-element.22), channel_id=1, source_target_pairs={{0,40},{8,32},{32,8},{40,0},{1,249},{25,225},{225,25},{249,1},{2,4... | collective-permute-start | bytes 2359304 | tf_op jit(solution)/shard_map/ppermute | solution.py:52
  223.7 24.1 %copy-start.4 = (bf16[384,128]{1,0:T(8,128)(2,1)S(1)}, bf16[384,128]{1,0:T(8,128)(2,1)}, u32[]{:S(2)}) copy-start(bf16[384,128]{1,0:T(8,128)(2,1)} %get-tuple-element.18) | copy-start | bytes 294916
  223.8 10.9 %collective-permute-start.35 = (bf16[2,384,128]{2,1,0:T(8,128)(2,1)S(1)}, bf16[2,384,128]{2,1,0:T(8,128)(2,1)S(1)}, u32[]{:S(2)}, u32[]{:S(2)}) collective-permute-start(bf16[2,384,128]{2,1,0:T(8,128)(2,1)S(1)} %get-tuple-element.33), channel_id=1, source_target_pairs={{0,64},{16,80},{64,0},{80,16},{128,192},{144,208},{192,128},{208,1... | collective-permute-start | bytes 589832 | tf_op jit(solution)/shard_map/ppermute | solution.py:52
  224.5 10.2 %collective-permute-start.36 = (bf16[2,384,128]{2,1,0:T(8,128)(2,1)S(1)}, bf16[2,384,128]{2,1,0:T(8,128)(2,1)S(1)}, u32[]{:S(2)}, u32[]{:S(2)}) collective-permute-start(bf16[2,384,128]{2,1,0:T(8,128)(2,1)S(1)} %get-tuple-element.35), channel_id=1, source_target_pairs={{0,16},{16,0},{64,80},{80,64},{128,144},{144,128},{192,208},{208,1... | collective-permute-start | bytes 589832 | tf_op jit(solution)/shard_map/ppermute | solution.py:52
  227.4 37.8 %copy-start.9 = (f32[128]{0:T(128)S(1)}, f32[128]{0:T(128)}, u32[]{:S(2)}) copy-start(f32[128]{0:T(128)} %param.17) | copy-start | bytes 1540
  227.4 37.8 %copy-start.10 = (f32[128]{0:T(128)S(1)}, f32[128]{0:T(128)}, u32[]{:S(2)}) copy-start(f32[128]{0:T(128)} %param.16) | copy-start | bytes 1540
  227.4 10.4 %collective-permute-start.37 = (bf16[2,384,128]{2,1,0:T(8,128)(2,1)S(1)}, bf16[2,384,128]{2,1,0:T(8,128)(2,1)S(1)}, u32[]{:S(2)}, u32[]{:S(2)}) collective-permute-start(bf16[2,384,128]{2,1,0:T(8,128)(2,1)S(1)} %get-tuple-element.34), channel_id=1, source_target_pairs={{0,80},{16,64},{64,16},{80,0},{128,208},{144,192},{192,144},{208,1... | collective-permute-start | bytes 589832 | tf_op jit(solution)/shard_map/ppermute | solution.py:52
  237.9 9.9 %collective-permute-start.38 = (bf16[384,128]{1,0:T(8,128)(2,1)S(1)}, bf16[384,128]{1,0:T(8,128)(2,1)S(1)}, u32[]{:S(2)}, u32[]{:S(2)}) collective-permute-start(bf16[384,128]{1,0:T(8,128)(2,1)S(1)} %fusion.7), channel_id=1, source_target_pairs={{0,128},{16,144},{64,192},{80,208},{128,0},{144,16},{192,64},{208,... | collective-permute-start | bytes 294920 | tf_op jit(solution)/shard_map/ppermute | solution.py:301
  (8 other events, 27.4 us)

commit v4 on v3

--- a/solution.py
+++ b/solution.py
@@ -49,7 +49,8 @@
 
 
 def stage(blocks, pairs):
-    own, diagonal, one, two = [blocks[0]] + [lax.ppermute(blocks[d], ALL, pairs[d]) for d in (3, 1, 2)]
+    got = {d: lax.ppermute(blocks[d], ALL, pairs[d]) for d in (1, 2, 3)}
+    own, diagonal, one, two = blocks[0], got[3], got[1], got[2]
     return [own, one, two, diagonal]
 
 
@@ -148,17 +149,16 @@
 
     ups = [pltpu.make_async_copy(up, up_rows(me, 0, deep), up_sems.at[0])]
     downs = [pltpu.make_async_copy(down.at[pl.ds(i * rows, rows)], dv.at[2 * me + i], d_sems.at[i]) for i in range(2)]
-    for i, piece in enumerate(pieces):
-        by = (1, nx - 1, 2)[i % 3]
+    for i, (piece, by, same) in enumerate(pieces):
         source = lax.rem(me + (nx - by), nx)
-        half = core if i < 3 else 1 - core
-        ups.append(
-            pltpu.make_async_copy(piece.at[pl.ds(0, deep // 2)], up_rows(source, half, deep // 2), up_sems.at[1 + i])
-        )
+        half = core if same else 1 - core
+        if not isinstance(piece, tuple):
+            piece = (piece.at[pl.ds(0, deep // 2)], piece.at[pl.ds(deep // 2, deep // 2)])
+        ups.append(pltpu.make_async_copy(piece[0], up_rows(source, half, deep // 2), up_sems.at[1 + i]))
         for k in range(wide // width):
             downs.append(
                 pltpu.make_async_copy(
-                    piece.at[pl.ds(deep // 2 + k * rows, rows)],
+                    piece[1].at[pl.ds(k * rows, rows)],
                     dv.at[2 * source + half, :, pl.ds(k * width, width)],
                     d_sems.at[2 + 2 * i + k],
                 )
@@ -169,7 +169,7 @@
 
 
 def first_kernel(
-    idx, x0, x1, x2, x3, up, down, m1, m2, m3, o1, o2, o3, u0, u1, u2, u3, xs, upv, dv, ov, x_sem, up_sems, d_sems, out_sems
+    idx, x0, x1, x2, x3, up, down, m1, m3, fu, fd, o1, o3, pu, pd, u0, u1, u2, u3, xs, upv, dv, ov, x_sem, up_sems, d_sems, out_sems
 ):
     x_copies = []
     for d, x in enumerate((x0, x1, x2, x3)):
@@ -178,7 +178,8 @@
             copy = pltpu.make_async_copy(x.at[i // 2, i % 2], xs.at[:, pl.ds(at, 128)], x_sem.at[d * 8 + i])
             copy.start()
             x_copies.append(copy)
-    ups, downs = load_weights(idx, up, down, (m1, m2, m3, o1, o2, o3), upv, dv, up_sems, d_sems)
+    pieces = [(m1, 1, True), (m3, 3, True), ((fu, fd), 2, True), (o1, 1, False), (o3, 3, False), ((pu, pd), 2, False)]
+    ups, downs = load_weights(idx, up, down, pieces, upv, dv, up_sems, d_sems)
     matmuls(idx, xs, upv, dv, ov, (u0, u1, u2, u3), out_sems, x_copies + ups, downs)
 
 
@@ -195,7 +196,8 @@
             copy = pltpu.make_async_copy(x.at[i // 2, i % 2], to, x_sem.at[d * 8 + i])
             copy.start()
             x_copies.append(copy)
-    ups, downs = load_weights(idx, up, down, (m1, m2, m3, o1, o2, o3), upv, dv, up_sems, d_sems)
+    pieces = [(m1, 1, True), (m2, 3, True), (m3, 2, True), (o1, 1, False), (o2, 3, False), (o3, 2, False)]
+    ups, downs = load_weights(idx, up, down, pieces, upv, dv, up_sems, d_sems)
     for copy in x_copies:
         copy.wait()
     step = 64
@@ -273,8 +275,10 @@
     pairs = pairs_of([lax.axis_size(axis) for axis in ALL])
     pair = jnp.stack([stream, lax.ppermute(stream, ALL, pairs["last"])])
     w = packed(up_first, down_first)
-    mine_1 = [shift(w, X, by) for by in (1, -1, 2)]
+    left, right = shift(w, X, 1), shift(w, X, -1)
     x_all = gathered(pair, pairs)
+    cut = w.shape[0] // 2
+    mine_1 = [left, right, shift(left[:cut], X, 1), shift(right[cut:], X, -1)]
     others_1 = [shift(m, C, 1) for m in mine_1]
     w = packed(up_second, down_second)
     mine_2 = [shift(w, X, by) for by in (1, -1, 2)]

time: 266 us -> 245 us (0.921)
  waiting for transfers between devices: 151 us -> 117 us
  starting transfers between devices: 64.4 us -> 74.2 us
    ppermute x24, waiting for transfers between devices: 98.2 us -> 78.8 us  [stage(): got = {d: lax.ppermute(blocks[d], ALL, pairs[d]) for d in (1, 2, 3)}]
    ppermute x12 -> x14, waiting for transfers between devices: 35.4 us -> 26.1 us  [shift(): return lax.ppermute(a, axis, [(i, (i + by) % n) for i in range(n)])]
    ppermute x1, starting transfers between devices: 1.28 us -> 7.26 us  [body(): there = lax.ppermute(some, ALL, pairs['last'])[::-1]]
    ppermute x1, waiting for transfers between devices: 8.56 us -> 4.4 us  [body(): there = lax.ppermute(some, ALL, pairs['last'])[::-1]]
    ppermute x24, starting transfers between devices: 42.8 us -> 45.6 us  [stage(): got = {d: lax.ppermute(blocks[d], ALL, pairs[d]) for d in (1, 2, 3)}]
    ppermute x12 -> x14, starting transfers between devices: 10.8 us -> 12.1 us  [shift(): return lax.ppermute(a, axis, [(i, (i + by) % n) for i in range(n)])]
  transfers between devices with their start and end apart: 39 -> 41, of which waited for: 25 -> 25; matrix products, arithmetic and copies ran while one was open for 1% -> 2% of each run, Pallas kernels for 0% -> 0%
where the time goes in v4:
time: 245 us; the launch traced here: 243 us
  waiting for transfers between devices  117 us (48%)
  starting transfers between devices  74.2 us (30%)
  Pallas kernels  24 us (10%)
  blocking collectives  17.7 us (7%)
  local copies, waits for them, and re-layouts  5.59 us (2%)
  other arithmetic  3.83 us (2%)
    ppermute x24, waiting for transfers between devices, stage(): got = {d: lax.ppermute(blocks[d], ALL, pairs[d]) for d in (1, 2, 3)}  78.8 us
    ppermute x24, starting transfers between devices, stage(): got = {d: lax.ppermute(blocks[d], ALL, pairs[d]) for d in (1, 2, 3)}  45.6 us
    ppermute x14, waiting for transfers between devices, shift(): return lax.ppermute(a, axis, [(i, (i + by) % n) for i in range(n)])  26.1 us
    pallas_call x2, Pallas kernels, ffn(): pl.pallas_call(kernel, out_shape=[jax.ShapeDtypeStruct((4, nb // 16, toke...  24 us
    all_to_all x1, blocking collectives, stats_to_all(): lax.all_to_all(jnp.broadcast_to(row[None], (n, *row.shape)), RA, 0, 0, ti...  17.7 us
    ppermute x14, starting transfers between devices, shift(): return lax.ppermute(a, axis, [(i, (i + by) % n) for i in range(n)])  12.1 us
    ppermute x1, starting transfers between devices, body(): there = lax.ppermute(some, ALL, pairs['last'])[::-1]  7.26 us
    ppermute x1, starting transfers between devices, body(): pair = jnp.stack([stream, lax.ppermute(stream, ALL, pairs['last'])])  7.19 us
  transfers between devices with their start and end apart: 41, of which 25 were waited for; matrix products, arithmetic and copies ran while one was open for 2% of the time, Pallas kernels for 0%

profile of v4, /device:TPU:2, one launch (start us, length us, event | category | flops | bytes accessed | tf_op | source)
XLA Modules:
  0.0 243.2 jit_solution(14686787935915024478)
XLA Ops:
  0.0 7.2 %collective-permute-start = (bf16[384,128]{1,0:T(8,128)(2,1)}, bf16[384,128]{1,0:T(8,128)(2,1)S(1)}, u32[]{:S(2)}, u32[]{:S(2)}) collective-permute-start(bf16[384,128]{1,0:T(8,128)(2,1)} %param.9), channel_id=1, source_target_pairs={{0,128},{16,144},{64,192},{80,208},{128,0},{144,16},{192,64},{208,... | collective-permute-start | bytes 294920 | tf_op jit(solution)/shard_map/ppermute | solution.py:276
  7.2 1.3 constant_dynamic-slice_fusion
  8.8 1.5 collective-permute-done
  10.3 6.6 %collective-permute-start.3 = (bf16[2,384,128]{2,1,0:T(8,128)(2,1)S(1)}, bf16[2,384,128]{2,1,0:T(8,128)(2,1)S(1)}, u32[]{:S(2)}, u32[]{:S(2)}) collective-permute-start(bf16[2,384,128]{2,1,0:T(8,128)(2,1)S(1)} %get-tuple-element.42), channel_id=1, source_target_pairs={{0,80},{16,64},{64,16},{80,0},{128,208},{144,192},{192,144},{208,1... | collective-permute-start | bytes 589832 | tf_op jit(solution)/shard_map/ppermute | solution.py:52
  17.6 1.6 collective-permute-start.7
  19.7 4.5 %collective-permute-done.3 = bf16[2,384,128]{2,1,0:T(8,128)(2,1)S(1)} collective-permute-done((bf16[2,384,128]{2,1,0:T(8,128)(2,1)S(1)}, bf16[2,384,128]{2,1,0:T(8,128)(2,1)S(1)}, u32[]{:S(2)}, u32[]{:S(2)}) %collective-permute-start.3) | collective-permute-done | bytes 196640 | tf_op jit(solution)/shard_map/ppermute | solution.py:52
  24.2 1.5 collective-permute-done.1
  25.8 1.5 collective-permute-done.2
  27.3 1.7 collective-permute-start.4
  30.0 13.4 %collective-permute-done.7.m1 = bf16[1024,512]{1,0:T(8,128)(2,1)S(1)} collective-permute-done((bf16[1024,512]{1,0:T(8,128)(2,1)S(1)}, bf16[1024,512]{1,0:T(8,128)(2,1)S(1)}, u32[]{:S(2)}, u32[]{:S(2)}) %collective-permute-start.7) | collective-permute-done | bytes 1048608 | tf_op jit(solution)/shard_map/ppermute | solution.py:74
  43.4 1.6 collective-permute-start.9
  47.5 2.0 collective-permute-start.6
  49.5 8.4 %collective-permute-done.9.fu = bf16[512,512]{1,0:T(8,128)(2,1)S(1)} collective-permute-done((bf16[512,512]{1,0:T(8,128)(2,1)S(1)}, bf16[512,512]{1,0:T(8,128)(2,1)S(1)}, u32[]{:S(2)}, u32[]{:S(2)}) %collective-permute-start.9) | collective-permute-done | bytes 524320 | tf_op jit(solution)/shard_map/ppermute | solution.py:74
  57.9 2.5 %collective-permute-done.10.fd = bf16[512,512]{1,0:T(8,128)(2,1)} collective-permute-done((bf16[512,512]{1,0:T(8,128)(2,1)S(1)}, bf16[512,512]{1,0:T(8,128)(2,1)}, u32[]{:S(2)}, u32[]{:S(2)}) %collective-permute-start.10) | collective-permute-done | bytes 524320 | tf_op jit(solution)/shard_map/ppermute | solution.py:74
  61.3 1.5 collective-permute-done.14.pd
  62.7 10.4 %shard_map.91 = (bf16[4,2,384,128]{3,2,1,0:T(8,128)(2,1)}, bf16[4,2,384,128]{3,2,1,0:T(8,128)(2,1)}, bf16[4,2,384,128]{3,2,1,0:T(8,128)(2,1)}, bf16[4,2,384,128]{3,2,1,0:T(8,128)(2,1)}) custom-call(s32[5]{0:T(128)} %stack.106.idx, bf16[4,2,384,128]{3,2,1,0:T(8,128)(2,1)} %copy-done.1, bf16[4,2,384,128]{3,2,1,0:T(8,128)(2,1)} %copy-done.17, ...), custom_call_target="tpu_custom_call" | custom-call | flops 3221225472 | bytes 14680064 | tf_op jit(solution)/shard_map/pallas_call | solution.py:240
  75.1 1.6 collective-permute-start.17
  76.8 1.3 collective-permute-start.28
  78.9 6.5 %collective-permute-done.15 = bf16[4,2,384,128]{3,2,1,0:T(8,128)(2,1)S(1)} collective-permute-done((bf16[4,2,384,128]{3,2,1,0:T(8,128)(2,1)}, bf16[4,2,384,128]{3,2,1,0:T(8,128)(2,1)S(1)}, u32[]{:S(2)}, u32[]{:S(2)}) %collective-permute-start.15) | collective-permute-done | bytes 786464 | tf_op jit(solution)/shard_map/ppermute | solution.py:52
  85.4 9.3 %collective-permute-done.16 = bf16[4,2,384,128]{3,2,1,0:T(8,128)(2,1)S(1)} collective-permute-done((bf16[4,2,384,128]{3,2,1,0:T(8,128)(2,1)}, bf16[4,2,384,128]{3,2,1,0:T(8,128)(2,1)S(1)}, u32[]{:S(2)}, u32[]{:S(2)}) %collective-permute-start.16) | collective-permute-done | bytes 786464 | tf_op jit(solution)/shard_map/ppermute | solution.py:52
  95.4 2.9 %collective-permute-start.19 = (bf16[2,384,128]{2,1,0:T(8,128)(2,1)S(1)}, bf16[2,384,128]{2,1,0:T(8,128)(2,1)S(1)}, u32[]{:S(2)}, u32[]{:S(2)}) collective-permute-start(bf16[2,384,128]{2,1,0:T(8,128)(2,1)S(1)} %get-tuple-element.38), channel_id=1, source_target_pairs={{0,16},{16,0},{64,80},{80,64},{128,144},{144,128},{192,208},{208,1... | collective-permute-start | bytes 589832 | tf_op jit(solution)/shard_map/ppermute | solution.py:52
  98.2 3.0 %collective-permute-start.20 = (bf16[2,384,128]{2,1,0:T(8,128)(2,1)S(1)}, bf16[2,384,128]{2,1,0:T(8,128)(2,1)S(1)}, u32[]{:S(2)}, u32[]{:S(2)}) collective-permute-start(bf16[2,384,128]{2,1,0:T(8,128)(2,1)S(1)} %get-tuple-element.37), channel_id=1, source_target_pairs={{0,80},{16,64},{64,16},{80,0},{128,208},{144,192},{192,144},{208,1... | collective-permute-start | bytes 589832 | tf_op jit(solution)/shard_map/ppermute | solution.py:52
  101.3 4.5 %collective-permute-start.30 = (bf16[1024,512]{1,0:T(8,128)(2,1)S(1)}, bf16[1024,512]{1,0:T(8,128)(2,1)}, u32[]{:S(2)}, u32[]{:S(2)}) collective-permute-start(bf16[1024,512]{1,0:T(8,128)(2,1)S(1)} %pad_maximum_fusion.1), channel_id=1, source_target_pairs={{0,4},{2,6},{4,0},{6,2},{1,5},{3,7},{5,1},{7,3},{8,12},{10,14},{12... | collective-permute-start | bytes 3145736 | tf_op jit(solution)/shard_map/ppermute | solution.py:74
  107.8 7.3 %collective-permute-start.21 = (bf16[2,392,128]{2,1,0:T(8,128)(2,1)S(1)}, bf16[2,392,128]{2,1,0:T(8,128)(2,1)S(1)}, u32[]{:S(2)}, u32[]{:S(2)}) collective-permute-start(bf16[2,392,128]{2,1,0:T(8,128)(2,1)S(1)} %pad_maximum_fusion.4), channel_id=1, source_target_pairs={{0,128},{16,144},{64,192},{80,208},{128,0},{144,16},{192,64},{208,... | collective-permute-start | bytes 602120 | tf_op jit(solution)/shard_map/ppermute | solution.py:292
  115.1 4.4 %collective-permute-done.21 = bf16[2,392,128]{2,1,0:T(8,128)(2,1)S(1)} collective-permute-done((bf16[2,392,128]{2,1,0:T(8,128)(2,1)S(1)}, bf16[2,392,128]{2,1,0:T(8,128)(2,1)S(1)}, u32[]{:S(2)}, u32[]{:S(2)}) %collective-permute-start.21) | collective-permute-done | bytes 200736 | tf_op jit(solution)/shard_map/ppermute | solution.py:292
  119.7 7.5 %collective-permute-start.22 = (bf16[2,392,128]{2,1,0:T(8,128)(2,1)S(1)}, bf16[2,392,128]{2,1,0:T(8,128)(2,1)S(1)}, u32[]{:S(2)}, u32[]{:S(2)}) collective-permute-start(bf16[2,392,128]{2,1,0:T(8,128)(2,1)S(1)} %get-tuple-element.40), channel_id=1, source_target_pairs={{0,64},{16,80},{64,0},{80,16},{128,192},{144,208},{192,128},{208,1... | collective-permute-start | bytes 602120 | tf_op jit(solution)/shard_map/ppermute | solution.py:52
  127.2 1.3 collective-permute-start.23
  128.5 2.3 collective-permute-start.24
  130.8 1.8 collective-permute-done.22
  132.6 2.3 collective-permute-done.23
  134.9 4.9 %collective-permute-done.24 = bf16[2,392,128]{2,1,0:T(8,128)(2,1)S(1)} collective-permute-done((bf16[2,392,128]{2,1,0:T(8,128)(2,1)S(1)}, bf16[2,392,128]{2,1,0:T(8,128)(2,1)S(1)}, u32[]{:S(2)}, u32[]{:S(2)}) %collective-permute-start.24) | collective-permute-done | bytes 200736 | tf_op jit(solution)/shard_map/ppermute | solution.py:52
  140.0 3.4 %collective-permute-start.26 = (bf16[4,2,392,128]{3,2,1,0:T(8,128)(2,1)S(1)}, bf16[4,2,392,128]{3,2,1,0:T(8,128)(2,1)S(1)}, u32[]{:S(2)}, u32[]{:S(2)}) collective-permute-start(bf16[4,2,392,128]{3,2,1,0:T(8,128)(2,1)S(1)} %pad_maximum_fusion.2.x0), channel_id=1, source_target_pairs={{0,8},{8,0},{32,40},{40,32},{1,25},{25,1},{225,249},{249,225},{2,1... | collective-permute-start | bytes 2408456 | tf_op jit(solution)/shard_map/ppermute | solution.py:52
  144.2 8.0 %collective-permute-done.25.x1 = bf16[4,2,392,128]{3,2,1,0:T(8,128)(2,1)S(1)} collective-permute-done((bf16[4,2,392,128]{3,2,1,0:T(8,128)(2,1)S(1)}, bf16[4,2,392,128]{3,2,1,0:T(8,128)(2,1)S(1)}, u32[]{:S(2)}, u32[]{:S(2)}) %collective-permute-start.25) | collective-permute-done | bytes 802848 | tf_op jit(solution)/shard_map/ppermute | solution.py:52
  152.2 10.0 %collective-permute-done.26.x2 = bf16[4,2,392,128]{3,2,1,0:T(8,128)(2,1)S(1)} collective-permute-done((bf16[4,2,392,128]{3,2,1,0:T(8,128)(2,1)S(1)}, bf16[4,2,392,128]{3,2,1,0:T(8,128)(2,1)S(1)}, u32[]{:S(2)}, u32[]{:S(2)}) %collective-permute-start.26) | collective-permute-done | bytes 802848 | tf_op jit(solution)/shard_map/ppermute | solution.py:52
  163.4 13.7 %shard_map.92 = (bf16[4,2,384,128]{3,2,1,0:T(8,128)(2,1)}, bf16[4,2,384,128]{3,2,1,0:T(8,128)(2,1)}, bf16[4,2,384,128]{3,2,1,0:T(8,128)(2,1)}, bf16[4,2,384,128]{3,2,1,0:T(8,128)(2,1)}, bf16[384,128]{1,0:T(8,128)(2,1)}) custom-call(s32[5]{0:T(128)} %stack.106.idx, bf16[4,2,392,128]{3,2,1,0:T(8,128)(2,1)} %copy-done, bf16[4,2,392,128]{3,2,1,0:T(8,128)(2,1)} %copy-done.14, ...), custom_call_target="tpu_custom_call" | custom-call | flops 3221225472 | bytes 14680064 | tf_op jit(solution)/shard_map/pallas_call | solution.py:240
  179.2 1.4 collective-permute-start.36
  180.6 8.7 %collective-permute-done.34 = bf16[4,2,384,128]{3,2,1,0:T(8,128)(2,1)S(1)} collective-permute-done((bf16[4,2,384,128]{3,2,1,0:T(8,128)(2,1)}, bf16[4,2,384,128]{3,2,1,0:T(8,128)(2,1)S(1)}, u32[]{:S(2)}, u32[]{:S(2)}) %collective-permute-start.34) | collective-permute-done | bytes 786464 | tf_op jit(solution)/shard_map/ppermute | solution.py:52
  189.3 8.2 %collective-permute-done.35 = bf16[4,2,384,128]{3,2,1,0:T(8,128)(2,1)S(1)} collective-permute-done((bf16[4,2,384,128]{3,2,1,0:T(8,128)(2,1)}, bf16[4,2,384,128]{3,2,1,0:T(8,128)(2,1)S(1)}, u32[]{:S(2)}, u32[]{:S(2)}) %collective-permute-start.35) | collective-permute-done | bytes 786464 | tf_op jit(solution)/shard_map/ppermute | solution.py:52
  197.5 1.7 collective-permute-done.36
  199.2 1.5 add_convert_fusion
  200.8 2.0 collective-permute-start.37
  203.9 2.9 %collective-permute-start.39 = (bf16[2,384,128]{2,1,0:T(8,128)(2,1)S(1)}, bf16[2,384,128]{2,1,0:T(8,128)(2,1)S(1)}, u32[]{:S(2)}, u32[]{:S(2)}) collective-permute-start(bf16[2,384,128]{2,1,0:T(8,128)(2,1)S(1)} %get-tuple-element.34), channel_id=1, source_target_pairs={{0,80},{16,64},{64,16},{80,0},{128,208},{144,192},{192,144},{208,1... | collective-permute-start | bytes 589832 | tf_op jit(solution)/shard_map/ppermute | solution.py:52
  206.8 2.2 collective-permute-done.37
  209.0 5.3 %collective-permute-done.38 = bf16[2,384,128]{2,1,0:T(8,128)(2,1)S(1)} collective-permute-done((bf16[2,384,128]{2,1,0:T(8,128)(2,1)S(1)}, bf16[2,384,128]{2,1,0:T(8,128)(2,1)S(1)}, u32[]{:S(2)}, u32[]{:S(2)}) %collective-permute-start.38) | collective-permute-done | bytes 196640 | tf_op jit(solution)/shard_map/ppermute | solution.py:52
  214.3 1.4 collective-permute-done.39
  215.7 2.0 collective-permute-start.40
  217.8 6.6 %collective-permute-done.40 = bf16[384,128]{1,0:T(8,128)(2,1)S(1)} collective-permute-done((bf16[384,128]{1,0:T(8,128)(2,1)S(1)}, bf16[384,128]{1,0:T(8,128)(2,1)S(1)}, u32[]{:S(2)}, u32[]{:S(2)}) %collective-permute-start.40) | collective-permute-done | bytes 98336 | tf_op jit(solution)/shard_map/ppermute | solution.py:305
  224.6 17.7 %all_to_all.5 = f32[32,1,768]{2,1,0:T(1,128)S(1)} all-to-all(f32[32,1,768]{2,1,0:T(1,128)S(1)} %broadcast_in_dim.11), channel_id=1, replica_groups=mesh['ra_0'=8,'ra_1'=4,'cb'=4,'dp'=2] {'ra_0','ra_1'}, dimensions={0} | all-to-all | bytes 196608 | tf_op jit(solution)/shard_map/all_to_all | solution.py:69
  (115 shorter events, 18.4 us)
Async XLA Ops:
  0.0 10.3 %collective-permute-start = (bf16[384,128]{1,0:T(8,128)(2,1)}, bf16[384,128]{1,0:T(8,128)(2,1)S(1)}, u32[]{:S(2)}, u32[]{:S(2)}) collective-permute-start(bf16[384,128]{1,0:T(8,128)(2,1)} %param.9), channel_id=1, source_target_pairs={{0,128},{16,144},{64,192},{80,208},{128,0},{144,16},{192,64},{208,... | collective-permute-start | bytes 294920 | tf_op jit(solution)/shard_map/ppermute | solution.py:276
  10.3 13.9 %collective-permute-start.3 = (bf16[2,384,128]{2,1,0:T(8,128)(2,1)S(1)}, bf16[2,384,128]{2,1,0:T(8,128)(2,1)S(1)}, u32[]{:S(2)}, u32[]{:S(2)}) collective-permute-start(bf16[2,384,128]{2,1,0:T(8,128)(2,1)S(1)} %get-tuple-element.42), channel_id=1, source_target_pairs={{0,80},{16,64},{64,16},{80,0},{128,208},{144,192},{192,144},{208,1... | collective-permute-start | bytes 589832 | tf_op jit(solution)/shard_map/ppermute | solution.py:52
  16.9 8.9 %collective-permute-start.1 = (bf16[2,384,128]{2,1,0:T(8,128)(2,1)S(1)}, bf16[2,384,128]{2,1,0:T(8,128)(2,1)S(1)}, u32[]{:S(2)}, u32[]{:S(2)}) collective-permute-start(bf16[2,384,128]{2,1,0:T(8,128)(2,1)S(1)} %get-tuple-element.42), channel_id=1, source_target_pairs={{0,64},{16,80},{64,0},{80,16},{128,192},{144,208},{192,128},{208,1... | collective-permute-start | bytes 589832 | tf_op jit(solution)/shard_map/ppermute | solution.py:52
  16.9 10.3 %collective-permute-start.2 = (bf16[2,384,128]{2,1,0:T(8,128)(2,1)S(1)}, bf16[2,384,128]{2,1,0:T(8,128)(2,1)S(1)}, u32[]{:S(2)}, u32[]{:S(2)}) collective-permute-start(bf16[2,384,128]{2,1,0:T(8,128)(2,1)S(1)} %get-tuple-element.42), channel_id=1, source_target_pairs={{0,16},{16,0},{64,80},{80,64},{128,144},{144,128},{192,208},{208,1... | collective-permute-start | bytes 589832 | tf_op jit(solution)/shard_map/ppermute | solution.py:52
  17.6 25.7 %collective-permute-start.7 = (bf16[1024,512]{1,0:T(8,128)(2,1)S(1)}, bf16[1024,512]{1,0:T(8,128)(2,1)S(1)}, u32[]{:S(2)}, u32[]{:S(2)}) collective-permute-start(bf16[1024,512]{1,0:T(8,128)(2,1)S(1)} %pad_maximum_fusion), channel_id=1, source_target_pairs={{0,2},{2,4},{4,6},{6,0},{1,3},{3,5},{5,7},{7,1},{8,10},{10,12},{12... | collective-permute-start | bytes 3145736 | tf_op jit(solution)/shard_map/ppermute | solution.py:74
  19.2 26.1 %collective-permute-start.8 = (bf16[1024,512]{1,0:T(8,128)(2,1)S(1)}, bf16[1024,512]{1,0:T(8,128)(2,1)}, u32[]{:S(2)}, u32[]{:S(2)}) collective-permute-start(bf16[1024,512]{1,0:T(8,128)(2,1)S(1)} %pad_maximum_fusion), channel_id=1, source_target_pairs={{0,6},{2,0},{4,2},{6,4},{1,7},{3,1},{5,3},{7,5},{8,14},{10,8},{12,... | collective-permute-start | bytes 3145736 | tf_op jit(solution)/shard_map/ppermute | solution.py:74
  27.3 20.1 %copy-start.1 = (bf16[4,2,384,128]{3,2,1,0:T(8,128)(2,1)}, bf16[4,2,384,128]{3,2,1,0:T(8,128)(2,1)S(1)}, u32[]{:S(2)}) copy-start(bf16[4,2,384,128]{3,2,1,0:T(8,128)(2,1)S(1)} %pad_maximum_fusion.3.x0) | copy-start | bytes 2359300
  27.3 19.6 %collective-permute-start.4 = (bf16[4,2,384,128]{3,2,1,0:T(8,128)(2,1)S(1)}, bf16[4,2,384,128]{3,2,1,0:T(8,128)(2,1)S(1)}, u32[]{:S(2)}, u32[]{:S(2)}) collective-permute-start(bf16[4,2,384,128]{3,2,1,0:T(8,128)(2,1)S(1)} %pad_maximum_fusion.3.x0), channel_id=1, source_target_pairs={{0,32},{8,40},{32,0},{40,8},{1,225},{25,249},{225,1},{249,25},{2,3... | collective-permute-start | bytes 2359304 | tf_op jit(solution)/shard_map/ppermute | solution.py:52
  29.1 18.4 %collective-permute-start.5 = (bf16[4,2,384,128]{3,2,1,0:T(8,128)(2,1)S(1)}, bf16[4,2,384,128]{3,2,1,0:T(8,128)(2,1)S(1)}, u32[]{:S(2)}, u32[]{:S(2)}) collective-permute-start(bf16[4,2,384,128]{3,2,1,0:T(8,128)(2,1)S(1)} %pad_maximum_fusion.3.x0), channel_id=1, source_target_pairs={{0,8},{8,0},{32,40},{40,32},{1,25},{25,1},{225,249},{249,225},{2,1... | collective-permute-start | bytes 2359304 | tf_op jit(solution)/shard_map/ppermute | solution.py:52
  43.4 14.5 %collective-permute-start.9 = (bf16[512,512]{1,0:T(8,128)(2,1)S(1)}, bf16[512,512]{1,0:T(8,128)(2,1)S(1)}, u32[]{:S(2)}, u32[]{:S(2)}) collective-permute-start(bf16[512,512]{1,0:T(8,128)(2,1)S(1)} %slice.92), channel_id=1, source_target_pairs={{0,2},{2,4},{4,6},{6,0},{1,3},{3,5},{5,7},{7,1},{8,10},{10,12},{12... | collective-permute-start | bytes 1572872 | tf_op jit(solution)/shard_map/ppermute | solution.py:74
  46.3 14.1 %collective-permute-start.10 = (bf16[512,512]{1,0:T(8,128)(2,1)S(1)}, bf16[512,512]{1,0:T(8,128)(2,1)}, u32[]{:S(2)}, u32[]{:S(2)}) collective-permute-start(bf16[512,512]{1,0:T(8,128)(2,1)S(1)} %slice.93), channel_id=1, source_target_pairs={{0,6},{2,0},{4,2},{6,4},{1,7},{3,1},{5,3},{7,5},{8,14},{10,8},{12,... | collective-permute-start | bytes 1572872 | tf_op jit(solution)/shard_map/ppermute | solution.py:74
  46.9 15.8 %collective-permute-start.11 = (bf16[1024,512]{1,0:T(8,128)(2,1)S(1)}, bf16[1024,512]{1,0:T(8,128)(2,1)}, u32[]{:S(2)}, u32[]{:S(2)}) collective-permute-start(bf16[1024,512]{1,0:T(8,128)(2,1)S(1)} %collective-permute-done.7.m1), channel_id=1, source_target_pairs={{0,1},{1,0},{2,3},{3,2},{4,5},{5,4},{6,7},{7,6},{8,9},{9,8},{10,11... | collective-permute-start | bytes 3145736 | tf_op jit(solution)/shard_map/ppermute | solution.py:74
  47.0 15.8 %collective-permute-start.12 = (bf16[1024,512]{1,0:T(8,128)(2,1)}, bf16[1024,512]{1,0:T(8,128)(2,1)}, u32[]{:S(2)}, u32[]{:S(2)}) collective-permute-start(bf16[1024,512]{1,0:T(8,128)(2,1)} %collective-permute-done.8.m3), channel_id=1, source_target_pairs={{0,1},{1,0},{2,3},{3,2},{4,5},{5,4},{6,7},{7,6},{8,9},{9,8},{10,11... | collective-permute-start | bytes 3145736 | tf_op jit(solution)/shard_map/ppermute | solution.py:74
  47.5 13.8 %collective-permute-start.6 = (bf16[4,2,384,128]{3,2,1,0:T(8,128)(2,1)S(1)}, bf16[4,2,384,128]{3,2,1,0:T(8,128)(2,1)}, u32[]{:S(2)}, u32[]{:S(2)}) collective-permute-start(bf16[4,2,384,128]{3,2,1,0:T(8,128)(2,1)S(1)} %pad_maximum_fusion.3.x0), channel_id=1, source_target_pairs={{0,40},{8,32},{32,8},{40,0},{1,249},{25,225},{225,25},{249,1},{2,4... | collective-permute-start | bytes 2359304 | tf_op jit(solution)/shard_map/ppermute | solution.py:52
  57.9 3.3 %collective-permute-start.13 = (bf16[512,512]{1,0:T(8,128)(2,1)S(1)}, bf16[512,512]{1,0:T(8,128)(2,1)}, u32[]{:S(2)}, u32[]{:S(2)}) collective-permute-start(bf16[512,512]{1,0:T(8,128)(2,1)S(1)} %collective-permute-done.9.fu), channel_id=1, source_target_pairs={{0,1},{1,0},{2,3},{3,2},{4,5},{5,4},{6,7},{7,6},{8,9},{9,8},{10,11... | collective-permute-start | bytes 1572872 | tf_op jit(solution)/shard_map/ppermute | solution.py:74
  60.5 2.3 collective-permute-start.14
  73.1 12.3 %collective-permute-start.15 = (bf16[4,2,384,128]{3,2,1,0:T(8,128)(2,1)}, bf16[4,2,384,128]{3,2,1,0:T(8,128)(2,1)S(1)}, u32[]{:S(2)}, u32[]{:S(2)}) collective-permute-start(bf16[4,2,384,128]{3,2,1,0:T(8,128)(2,1)} %get-tuple-element.15), channel_id=1, source_target_pairs={{0,32},{8,40},{32,0},{40,8},{1,225},{25,249},{225,1},{249,25},{2,3... | collective-permute-start | bytes 2359304 | tf_op jit(solution)/shard_map/ppermute | solution.py:52
  74.1 20.6 %collective-permute-start.16 = (bf16[4,2,384,128]{3,2,1,0:T(8,128)(2,1)}, bf16[4,2,384,128]{3,2,1,0:T(8,128)(2,1)S(1)}, u32[]{:S(2)}, u32[]{:S(2)}) collective-permute-start(bf16[4,2,384,128]{3,2,1,0:T(8,128)(2,1)} %get-tuple-element.16), channel_id=1, source_target_pairs={{0,8},{8,0},{32,40},{40,32},{1,25},{25,1},{225,249},{249,225},{2,1... | collective-permute-start | bytes 2359304 | tf_op jit(solution)/shard_map/ppermute | solution.py:52
  75.1 19.7 %collective-permute-start.17 = (bf16[4,2,384,128]{3,2,1,0:T(8,128)(2,1)}, bf16[4,2,384,128]{3,2,1,0:T(8,128)(2,1)S(1)}, u32[]{:S(2)}, u32[]{:S(2)}) collective-permute-start(bf16[4,2,384,128]{3,2,1,0:T(8,128)(2,1)} %get-tuple-element.17), channel_id=1, source_target_pairs={{0,40},{8,32},{32,8},{40,0},{1,249},{25,225},{225,25},{249,1},{2,4... | collective-permute-start | bytes 2359304 | tf_op jit(solution)/shard_map/ppermute | solution.py:52
  76.8 24.5 %collective-permute-start.28 = (bf16[1024,512]{1,0:T(8,128)(2,1)S(1)}, bf16[1024,512]{1,0:T(8,128)(2,1)}, u32[]{:S(2)}, u32[]{:S(2)}) collective-permute-start(bf16[1024,512]{1,0:T(8,128)(2,1)S(1)} %pad_maximum_fusion.1), channel_id=1, source_target_pairs={{0,2},{2,4},{4,6},{6,0},{1,3},{3,5},{5,7},{7,1},{8,10},{10,12},{12... | collective-permute-start | bytes 3145736 | tf_op jit(solution)/shard_map/ppermute | solution.py:74
  78.1 50.4 %collective-permute-start.29 = (bf16[1024,512]{1,0:T(8,128)(2,1)S(1)}, bf16[1024,512]{1,0:T(8,128)(2,1)}, u32[]{:S(2)}, u32[]{:S(2)}) collective-permute-start(bf16[1024,512]{1,0:T(8,128)(2,1)S(1)} %pad_maximum_fusion.1), channel_id=1, source_target_pairs={{0,6},{2,0},{4,2},{6,4},{1,7},{3,1},{5,3},{7,5},{8,14},{10,8},{12,... | collective-permute-start | bytes 3145736 | tf_op jit(solution)/shard_map/ppermute | solution.py:74
  95.3 10.6 %collective-permute-start.18 = (bf16[2,384,128]{2,1,0:T(8,128)(2,1)S(1)}, bf16[2,384,128]{2,1,0:T(8,128)(2,1)S(1)}, u32[]{:S(2)}, u32[]{:S(2)}) collective-permute-start(bf16[2,384,128]{2,1,0:T(8,128)(2,1)S(1)} %get-tuple-element.36), channel_id=1, source_target_pairs={{0,64},{16,80},{64,0},{80,16},{128,192},{144,208},{192,128},{208,1... | collective-permute-start | bytes 589832 | tf_op jit(solution)/shard_map/ppermute | solution.py:52
  95.4 11.2 %collective-permute-start.19 = (bf16[2,384,128]{2,1,0:T(8,128)(2,1)S(1)}, bf16[2,384,128]{2,1,0:T(8,128)(2,1)S(1)}, u32[]{:S(2)}, u32[]{:S(2)}) collective-permute-start(bf16[2,384,128]{2,1,0:T(8,128)(2,1)S(1)} %get-tuple-element.38), channel_id=1, source_target_pairs={{0,16},{16,0},{64,80},{80,64},{128,144},{144,128},{192,208},{208,1... | collective-permute-start | bytes 589832 | tf_op jit(solution)/shard_map/ppermute | solution.py:52
  98.2 9.5 %collective-permute-start.20 = (bf16[2,384,128]{2,1,0:T(8,128)(2,1)S(1)}, bf16[2,384,128]{2,1,0:T(8,128)(2,1)S(1)}, u32[]{:S(2)}, u32[]{:S(2)}) collective-permute-start(bf16[2,384,128]{2,1,0:T(8,128)(2,1)S(1)} %get-tuple-element.37), channel_id=1, source_target_pairs={{0,80},{16,64},{64,16},{80,0},{128,208},{144,192},{192,144},{208,1... | collective-permute-start | bytes 589832 | tf_op jit(solution)/shard_map/ppermute | solution.py:52
  101.3 29.5 %collective-permute-start.30 = (bf16[1024,512]{1,0:T(8,128)(2,1)S(1)}, bf16[1024,512]{1,0:T(8,128)(2,1)}, u32[]{:S(2)}, u32[]{:S(2)}) collective-permute-start(bf16[1024,512]{1,0:T(8,128)(2,1)S(1)} %pad_maximum_fusion.1), channel_id=1, source_target_pairs={{0,4},{2,6},{4,0},{6,2},{1,5},{3,7},{5,1},{7,3},{8,12},{10,14},{12... | collective-permute-start | bytes 3145736 | tf_op jit(solution)/shard_map/ppermute | solution.py:74
  105.8 37.6 %collective-permute-start.31 = (bf16[1024,512]{1,0:T(8,128)(2,1)}, bf16[1024,512]{1,0:T(8,128)(2,1)}, u32[]{:S(2)}, u32[]{:S(2)}) collective-permute-start(bf16[1024,512]{1,0:T(8,128)(2,1)} %collective-permute-done.28.m1), channel_id=1, source_target_pairs={{0,1},{1,0},{2,3},{3,2},{4,5},{5,4},{6,7},{7,6},{8,9},{9,8},{10,11... | collective-permute-start | bytes 3145736 | tf_op jit(solution)/shard_map/ppermute | solution.py:74
  107.8 11.7 %collective-permute-start.21 = (bf16[2,392,128]{2,1,0:T(8,128)(2,1)S(1)}, bf16[2,392,128]{2,1,0:T(8,128)(2,1)S(1)}, u32[]{:S(2)}, u32[]{:S(2)}) collective-permute-start(bf16[2,392,128]{2,1,0:T(8,128)(2,1)S(1)} %pad_maximum_fusion.4), channel_id=1, source_target_pairs={{0,128},{16,144},{64,192},{80,208},{128,0},{144,16},{192,64},{208,... | collective-permute-start | bytes 602120 | tf_op jit(solution)/shard_map/ppermute | solution.py:292
  119.7 12.9 %collective-permute-start.22 = (bf16[2,392,128]{2,1,0:T(8,128)(2,1)S(1)}, bf16[2,392,128]{2,1,0:T(8,128)(2,1)S(1)}, u32[]{:S(2)}, u32[]{:S(2)}) collective-permute-start(bf16[2,392,128]{2,1,0:T(8,128)(2,1)S(1)} %get-tuple-element.40), channel_id=1, source_target_pairs={{0,64},{16,80},{64,0},{80,16},{128,192},{144,208},{192,128},{208,1... | collective-permute-start | bytes 602120 | tf_op jit(solution)/shard_map/ppermute | solution.py:52
  127.2 7.7 %collective-permute-start.23 = (bf16[2,392,128]{2,1,0:T(8,128)(2,1)S(1)}, bf16[2,392,128]{2,1,0:T(8,128)(2,1)S(1)}, u32[]{:S(2)}, u32[]{:S(2)}) collective-permute-start(bf16[2,392,128]{2,1,0:T(8,128)(2,1)S(1)} %get-tuple-element.40), channel_id=1, source_target_pairs={{0,16},{16,0},{64,80},{80,64},{128,144},{144,128},{192,208},{208,1... | collective-permute-start | bytes 602120 | tf_op jit(solution)/shard_map/ppermute | solution.py:52
  128.5 11.3 %collective-permute-start.24 = (bf16[2,392,128]{2,1,0:T(8,128)(2,1)S(1)}, bf16[2,392,128]{2,1,0:T(8,128)(2,1)S(1)}, u32[]{:S(2)}, u32[]{:S(2)}) collective-permute-start(bf16[2,392,128]{2,1,0:T(8,128)(2,1)S(1)} %get-tuple-element.40), channel_id=1, source_target_pairs={{0,80},{16,64},{64,16},{80,0},{128,208},{144,192},{192,144},{208,1... | collective-permute-start | bytes 602120 | tf_op jit(solution)/shard_map/ppermute | solution.py:52
  130.8 13.4 %collective-permute-start.32 = (bf16[1024,512]{1,0:T(8,128)(2,1)}, bf16[1024,512]{1,0:T(8,128)(2,1)S(1)}, u32[]{:S(2)}, u32[]{:S(2)}) collective-permute-start(bf16[1024,512]{1,0:T(8,128)(2,1)} %collective-permute-done.29.m2), channel_id=1, source_target_pairs={{0,1},{1,0},{2,3},{3,2},{4,5},{5,4},{6,7},{7,6},{8,9},{9,8},{10,11... | collective-permute-start | bytes 3145736 | tf_op jit(solution)/shard_map/ppermute | solution.py:74
  132.6 11.6 %collective-permute-start.33 = (bf16[1024,512]{1,0:T(8,128)(2,1)}, bf16[1024,512]{1,0:T(8,128)(2,1)S(1)}, u32[]{:S(2)}, u32[]{:S(2)}) collective-permute-start(bf16[1024,512]{1,0:T(8,128)(2,1)} %collective-permute-done.30.m3), channel_id=1, source_target_pairs={{0,1},{1,0},{2,3},{3,2},{4,5},{5,4},{6,7},{7,6},{8,9},{9,8},{10,11... | collective-permute-start | bytes 3145736 | tf_op jit(solution)/shard_map/ppermute | solution.py:74
  139.9 23.4 %copy-start = (bf16[4,2,392,128]{3,2,1,0:T(8,128)(2,1)}, bf16[4,2,392,128]{3,2,1,0:T(8,128)(2,1)S(1)}, u32[]{:S(2)}) copy-start(bf16[4,2,392,128]{3,2,1,0:T(8,128)(2,1)S(1)} %pad_maximum_fusion.2.x0) | copy-start | bytes 2408452
  139.9 12.3 %collective-permute-start.25 = (bf16[4,2,392,128]{3,2,1,0:T(8,128)(2,1)S(1)}, bf16[4,2,392,128]{3,2,1,0:T(8,128)(2,1)S(1)}, u32[]{:S(2)}, u32[]{:S(2)}) collective-permute-start(bf16[4,2,392,128]{3,2,1,0:T(8,128)(2,1)S(1)} %pad_maximum_fusion.2.x0), channel_id=1, source_target_pairs={{0,32},{8,40},{32,0},{40,8},{1,225},{25,249},{225,1},{249,25},{2,3... | collective-permute-start | bytes 2408456 | tf_op jit(solution)/shard_map/ppermute | solution.py:52
  140.0 22.1 %collective-permute-start.26 = (bf16[4,2,392,128]{3,2,1,0:T(8,128)(2,1)S(1)}, bf16[4,2,392,128]{3,2,1,0:T(8,128)(2,1)S(1)}, u32[]{:S(2)}, u32[]{:S(2)}) collective-permute-start(bf16[4,2,392,128]{3,2,1,0:T(8,128)(2,1)S(1)} %pad_maximum_fusion.2.x0), channel_id=1, source_target_pairs={{0,8},{8,0},{32,40},{40,32},{1,25},{25,1},{225,249},{249,225},{2,1... | collective-permute-start | bytes 2408456 | tf_op jit(solution)/shard_map/ppermute | solution.py:52
  143.4 18.7 %collective-permute-start.27 = (bf16[4,2,392,128]{3,2,1,0:T(8,128)(2,1)S(1)}, bf16[4,2,392,128]{3,2,1,0:T(8,128)(2,1)S(1)}, u32[]{:S(2)}, u32[]{:S(2)}) collective-permute-start(bf16[4,2,392,128]{3,2,1,0:T(8,128)(2,1)S(1)} %pad_maximum_fusion.2.x0), channel_id=1, source_target_pairs={{0,40},{8,32},{32,8},{40,0},{1,249},{25,225},{225,25},{249,1},{2,4... | collective-permute-start | bytes 2408456 | tf_op jit(solution)/shard_map/ppermute | solution.py:52
  144.2 19.2 %copy-start.12 = (bf16[1024,512]{1,0:T(8,128)(2,1)}, bf16[1024,512]{1,0:T(8,128)(2,1)S(1)}, u32[]{:S(2)}) copy-start(bf16[1024,512]{1,0:T(8,128)(2,1)S(1)} %collective-permute-done.32.o2) | copy-start | bytes 3145732
  144.2 19.1 %copy-start.13 = (bf16[1024,512]{1,0:T(8,128)(2,1)}, bf16[1024,512]{1,0:T(8,128)(2,1)S(1)}, u32[]{:S(2)}) copy-start(bf16[1024,512]{1,0:T(8,128)(2,1)S(1)} %collective-permute-done.33.o3) | copy-start | bytes 3145732
  177.0 12.3 %collective-permute-start.34 = (bf16[4,2,384,128]{3,2,1,0:T(8,128)(2,1)}, bf16[4,2,384,128]{3,2,1,0:T(8,128)(2,1)S(1)}, u32[]{:S(2)}, u32[]{:S(2)}) collective-permute-start(bf16[4,2,384,128]{3,2,1,0:T(8,128)(2,1)} %get-tuple-element.20), channel_id=1, source_target_pairs={{0,32},{8,40},{32,0},{40,8},{1,225},{25,249},{225,1},{249,25},{2,3... | collective-permute-start | bytes 2359304 | tf_op jit(solution)/shard_map/ppermute | solution.py:52
  178.3 19.3 %collective-permute-start.35 = (bf16[4,2,384,128]{3,2,1,0:T(8,128)(2,1)}, bf16[4,2,384,128]{3,2,1,0:T(8,128)(2,1)S(1)}, u32[]{:S(2)}, u32[]{:S(2)}) collective-permute-start(bf16[4,2,384,128]{3,2,1,0:T(8,128)(2,1)} %get-tuple-element.21), channel_id=1, source_target_pairs={{0,8},{8,0},{32,40},{40,32},{1,25},{25,1},{225,249},{249,225},{2,1... | collective-permute-start | bytes 2359304 | tf_op jit(solution)/shard_map/ppermute | solution.py:52
  179.2 20.0 %collective-permute-start.36 = (bf16[4,2,384,128]{3,2,1,0:T(8,128)(2,1)}, bf16[4,2,384,128]{3,2,1,0:T(8,128)(2,1)S(1)}, u32[]{:S(2)}, u32[]{:S(2)}) collective-permute-start(bf16[4,2,384,128]{3,2,1,0:T(8,128)(2,1)} %get-tuple-element.22), channel_id=1, source_target_pairs={{0,40},{8,32},{32,8},{40,0},{1,249},{25,225},{225,25},{249,1},{2,4... | collective-permute-start | bytes 2359304 | tf_op jit(solution)/shard_map/ppermute | solution.py:52
  200.8 23.6 %copy-start.4 = (bf16[384,128]{1,0:T(8,128)(2,1)S(1)}, bf16[384,128]{1,0:T(8,128)(2,1)}, u32[]{:S(2)}) copy-start(bf16[384,128]{1,0:T(8,128)(2,1)} %get-tuple-element.18) | copy-start | bytes 294916
  200.8 8.1 %collective-permute-start.37 = (bf16[2,384,128]{2,1,0:T(8,128)(2,1)S(1)}, bf16[2,384,128]{2,1,0:T(8,128)(2,1)S(1)}, u32[]{:S(2)}, u32[]{:S(2)}) collective-permute-start(bf16[2,384,128]{2,1,0:T(8,128)(2,1)S(1)} %get-tuple-element.33), channel_id=1, source_target_pairs={{0,64},{16,80},{64,0},{80,16},{128,192},{144,208},{192,128},{208,1... | collective-permute-start | bytes 589832 | tf_op jit(solution)/shard_map/ppermute | solution.py:52
  202.8 11.5 %collective-permute-start.38 = (bf16[2,384,128]{2,1,0:T(8,128)(2,1)S(1)}, bf16[2,384,128]{2,1,0:T(8,128)(2,1)S(1)}, u32[]{:S(2)}, u32[]{:S(2)}) collective-permute-start(bf16[2,384,128]{2,1,0:T(8,128)(2,1)S(1)} %get-tuple-element.35), channel_id=1, source_target_pairs={{0,16},{16,0},{64,80},{80,64},{128,144},{144,128},{192,208},{208,1... | collective-permute-start | bytes 589832 | tf_op jit(solution)/shard_map/ppermute | solution.py:52
  203.9 38.5 %copy-start.10 = (f32[128]{0:T(128)S(1)}, f32[128]{0:T(128)}, u32[]{:S(2)}) copy-start(f32[128]{0:T(128)} %param.17) | copy-start | bytes 1540
  203.9 38.5 %copy-start.11 = (f32[128]{0:T(128)S(1)}, f32[128]{0:T(128)}, u32[]{:S(2)}) copy-start(f32[128]{0:T(128)} %param.16) | copy-start | bytes 1540
  203.9 11.7 %collective-permute-start.39 = (bf16[2,384,128]{2,1,0:T(8,128)(2,1)S(1)}, bf16[2,384,128]{2,1,0:T(8,128)(2,1)S(1)}, u32[]{:S(2)}, u32[]{:S(2)}) collective-permute-start(bf16[2,384,128]{2,1,0:T(8,128)(2,1)S(1)} %get-tuple-element.34), channel_id=1, source_target_pairs={{0,80},{16,64},{64,16},{80,0},{128,208},{144,192},{192,144},{208,1... | collective-permute-start | bytes 589832 | tf_op jit(solution)/shard_map/ppermute | solution.py:52
  215.7 8.6 %collective-permute-start.40 = (bf16[384,128]{1,0:T(8,128)(2,1)S(1)}, bf16[384,128]{1,0:T(8,128)(2,1)S(1)}, u32[]{:S(2)}, u32[]{:S(2)}) collective-permute-start(bf16[384,128]{1,0:T(8,128)(2,1)S(1)} %fusion.7), channel_id=1, source_target_pairs={{0,128},{16,144},{64,192},{80,208},{128,0},{144,16},{192,64},{208,... | collective-permute-start | bytes 294920 | tf_op jit(solution)/shard_map/ppermute | solution.py:305
  (13 other events, 95.7 us)

commit v5 on v4

--- a/solution.py
+++ b/solution.py
@@ -110,123 +110,104 @@
     return (2 * j + zz) * NY + y, (flip & 1) + 2 * (yh ^ idx[3]), flip >> 1
 
 
-def matmuls(idx, xs, upv, dv, ov, outs, out_sems, before_up, before_down):
-    nx = dv.shape[0] // 2
-    for copy in before_up:
-        copy.wait()
-    pre = jnp.dot(xs[...], upv[...], preferred_element_type=F32)
+def matmuls(idx, xs, up, down, pieces, hv, ov, outs):
+    nx = 1 + len(pieces)
+    me, core = idx[0], idx[1]
+    per = xs.shape[0] // nx
+    wide = hv.shape[2]
+
+    def features(first, count):
+        return jnp.concatenate([xs[first + k] for k in range(count)], axis=1)
+
+    pre = jnp.dot(features(per * me, per), up[...], preferred_element_type=F32)
+    for by, mine, other in pieces:
+        source = lax.rem(me + (nx - by), nx)
+        for half, piece in ((core, mine), (1 - core, other)):
+            rows = features(per * source + per // 2 * half, per // 2)
+            pre = pre + jnp.dot(rows, piece(0, per // 2 * 128), preferred_element_type=F32)
     hidden = jnp.square(jnp.maximum(pre, 0.0)).astype(BF)
-    half = hidden.shape[1] // 2
-    copies = []
-    for copy in before_down:
-        copy.wait()
-    for j in range(nx):
-        part = jnp.dot(hidden[:, :half], dv[2 * j], preferred_element_type=F32)
-        part = part + jnp.dot(hidden[:, half:], dv[2 * j + 1], preferred_element_type=F32)
+    for half in range(2):
+        hv[half] = hidden[:, half * wide : (half + 1) * wide]
+
+    def emit(j, at, part):
         part = part.astype(BF)
-        for i in range(2 * NY):
-            ov[2 * NY * j + i] = part[:, i * 128 : (i + 1) * 128]
+        for i in range(part.shape[1] // 128):
+            ov[per * j + at + i] = part[:, i * 128 : (i + 1) * 128]
+
+    def send(j):
         for d in range(4):
             for yh in range(NY // 2):
                 slot, e, g = to_peer(idx, d, j, yh)
-                sem = out_sems.at[(d * nx + j) * 2 + yh]
-                copy = pltpu.make_async_copy(ov.at[slot], outs[d].at[e, g], sem)
-                copy.start()
-                copies.append(copy)
-    for copy in copies:
-        copy.wait()
-
-
-def load_weights(idx, up, down, pieces, upv, dv, up_sems, d_sems):
-    nx = dv.shape[0] // 2
-    rows, wide = dv.shape[1:]
-    width = upv.shape[1]
-    deep = upv.shape[0] // nx
-    me, core = idx[0], idx[1]
-
-    def up_rows(source, half, count):
-        return upv.at[pl.ds(pl.multiple_of(source * deep + half * (deep // 2), deep // 2), count)]
-
-    ups = [pltpu.make_async_copy(up, up_rows(me, 0, deep), up_sems.at[0])]
-    downs = [pltpu.make_async_copy(down.at[pl.ds(i * rows, rows)], dv.at[2 * me + i], d_sems.at[i]) for i in range(2)]
-    for i, (piece, by, same) in enumerate(pieces):
+                outs[d][e, g] = ov[slot]
+
+    part = jnp.dot(hv[0], down[:wide], preferred_element_type=F32)
+    emit(me, 0, part + jnp.dot(hv[1], down[wide:], preferred_element_type=F32))
+    send(me)
+    for by, mine, other in pieces:
         source = lax.rem(me + (nx - by), nx)
-        half = core if same else 1 - core
-        if not isinstance(piece, tuple):
-            piece = (piece.at[pl.ds(0, deep // 2)], piece.at[pl.ds(deep // 2, deep // 2)])
-        ups.append(pltpu.make_async_copy(piece[0], up_rows(source, half, deep // 2), up_sems.at[1 + i]))
-        for k in range(wide // width):
-            downs.append(
-                pltpu.make_async_copy(
-                    piece[1].at[pl.ds(k * rows, rows)],
-                    dv.at[2 * source + half, :, pl.ds(k * width, width)],
-                    d_sems.at[2 + 2 * i + k],
-                )
-            )
-    for copy in ups + downs:
-        copy.start()
-    return ups, downs
+        for k in range(2):
+            first = per // 2 * 128 + k * wide
+            part = jnp.dot(hv[core], mine(first, wide), preferred_element_type=F32)
+            part = part + jnp.dot(hv[1 - core], other(first, wide), preferred_element_type=F32)
+            emit(source, k * per // 2, part)
+        send(source)
+
+
+def whole(ref):
+    return lambda first, count: ref[first : first + count]
+
+
+def split(top, low):
+    cut = top.shape[0]
+    return lambda first, count: top[first : first + count] if first < cut else low[first - cut : first - cut + count]
 
 
 def first_kernel(
-    idx, x0, x1, x2, x3, up, down, m1, m3, fu, fd, o1, o3, pu, pd, u0, u1, u2, u3, xs, upv, dv, ov, x_sem, up_sems, d_sems, out_sems
+    idx, x0, x1, x2, x3, up, down, m1, m3, fu, fd, o1, o3, pu, pd, u0, u1, u2, u3, xs, hv, ov
 ):
-    x_copies = []
     for d, x in enumerate((x0, x1, x2, x3)):
         for i in range(8):
-            at = pl.multiple_of(from_peer(idx, d, i // 2, i % 2) * 128, 128)
-            copy = pltpu.make_async_copy(x.at[i // 2, i % 2], xs.at[:, pl.ds(at, 128)], x_sem.at[d * 8 + i])
-            copy.start()
-            x_copies.append(copy)
-    pieces = [(m1, 1, True), (m3, 3, True), ((fu, fd), 2, True), (o1, 1, False), (o3, 3, False), ((pu, pd), 2, False)]
-    ups, downs = load_weights(idx, up, down, pieces, upv, dv, up_sems, d_sems)
-    matmuls(idx, xs, upv, dv, ov, (u0, u1, u2, u3), out_sems, x_copies + ups, downs)
+            xs[from_peer(idx, d, i // 2, i % 2)] = x[i // 2, i % 2]
+    pieces = [(1, whole(m1), whole(o1)), (3, whole(m3), whole(o3)), (2, split(fu, fd), split(pu, pd))]
+    matmuls(idx, xs, up, down, pieces, hv, ov, (u0, u1, u2, u3))
 
 
 def second_kernel(
     idx, x0, x1, x2, x3, up, down, m1, m2, m3, o1, o2, o3, mixed, own_gain, own_bias, u0, u1, u2, u3, own,
-    xs, xv, upv, dv, ov, gain, bias, x_sem, up_sems, d_sems, out_sems,
+    xs, gain, bias, hv, ov,
 ):
-    nb = xv.shape[0]
-    tokens = xs.shape[0]
-    x_copies = []
+    nb, tokens = xs.shape[:2]
+    step = 64
+    width = nb * 128
+    blocks = []
     for d, x in enumerate((x0, x1, x2, x3)):
         for i in range(8):
-            to = xv.at[from_peer(idx, d, i // 2, i % 2)]
-            copy = pltpu.make_async_copy(x.at[i // 2, i % 2], to, x_sem.at[d * 8 + i])
-            copy.start()
-            x_copies.append(copy)
-    pieces = [(m1, 1, True), (m2, 3, True), (m3, 2, True), (o1, 1, False), (o2, 3, False), (o3, 2, False)]
-    ups, downs = load_weights(idx, up, down, pieces, upv, dv, up_sems, d_sems)
-    for copy in x_copies:
-        copy.wait()
-    step = 64
-    width = nb * 128
-    for b in range(nb):
-        t = xv[b, tokens : tokens + 8, :].astype(F32)
-        gain[b : b + 1] = t[0:1] + t[1:2] + t[2:3]
-        bias[b : b + 1] = t[3:4] + t[4:5] + t[5:6]
+            b = from_peer(idx, d, i // 2, i % 2)
+            blocks.append((x, i // 2, i % 2, b))
+            t = x[i // 2, i % 2, tokens : tokens + 8, :].astype(F32)
+            gain[pl.ds(b, 1)] = t[0:1] + t[1:2] + t[2:3]
+            bias[pl.ds(b, 1)] = t[3:4] + t[4:5] + t[5:6]
 
     def norm(i, carry):
         rows = pl.ds(pl.multiple_of(i * step, step), step)
         acc = jnp.zeros((step, 128), F32)
         squares = jnp.zeros((step, 128), F32)
-        for b in range(nb):
-            d = xv[b, rows, :].astype(F32)
-            acc = acc + d
-            squares = squares + d * d
+        for x, e, g, b in blocks:
+            v = x[e, g, rows, :].astype(F32)
+            acc = acc + v
+            squares = squares + v * v
         mean = jnp.sum(acc, axis=1, keepdims=True) / width
         var = jnp.sum(squares, axis=1, keepdims=True) / width - mean * mean
         scale = lax.rsqrt(jnp.maximum(var, 0.0) + EPS)
-        for b in range(nb):
-            d = (xv[b, rows, :].astype(F32) - mean) * scale
-            xs[rows, b * 128 : (b + 1) * 128] = (d * gain[b : b + 1] + bias[b : b + 1]).astype(BF)
+        for x, e, g, b in blocks:
+            v = (x[e, g, rows, :].astype(F32) - mean) * scale
+            xs[b, rows, :] = (v * gain[pl.ds(b, 1)] + bias[pl.ds(b, 1)]).astype(BF)
         own[rows, :] = ((mixed[rows, :] - mean) * scale * own_gain[...] + own_bias[...]).astype(BF)
         return carry
 
     lax.fori_loop(0, tokens // step, norm, 0)
-
-    matmuls(idx, xs, upv, dv, ov, (u0, u1, u2, u3), out_sems, ups, downs)
+    pieces = [(1, whole(m1), whole(o1)), (3, whole(m2), whole(o2)), (2, whole(m3), whole(o3))]
+    matmuls(idx, xs, up, down, pieces, hv, ov, (u0, u1, u2, u3))
 
 
 ANY = pl.BlockSpec(memory_space=pltpu.MemorySpace.HBM)
@@ -237,27 +218,21 @@
 def ffn(kernel, idx, x, tokens, up, down, pieces, extra, own_out, norm_scratch):
     nx, nb = lax.axis_size(X), NZ * NY
     width, ff = up.shape[0] * nx, up.shape[1]
+    near = [pltpu.with_memory_space_constraint(a, pltpu.MemorySpace.VMEM) for a in (*x, up, down, *pieces)]
     return pl.pallas_call(
         kernel,
-        out_shape=[jax.ShapeDtypeStruct((4, nb // 16, tokens, 128), BF)] * 4 + own_out,
-        in_specs=[SMEM] + [ANY] * (6 + len(pieces)) + [VMEM] * len(extra),
-        out_specs=[ANY] * 4 + [VMEM] * len(own_out),
-        scratch_shapes=[pltpu.VMEM((tokens, width), BF)]
-        + norm_scratch[:1]
+        out_shape=[pltpu.VMEM((4, nb // 16, tokens, 128), BF)] * 4 + own_out,
+        in_specs=[SMEM] + [VMEM] * (len(near) + len(extra)),
+        out_specs=[VMEM] * (4 + len(own_out)),
+        scratch_shapes=[pltpu.VMEM((nb, tokens, 128), BF)]
+        + norm_scratch
         + [
-            pltpu.VMEM((width, ff), BF),
-            pltpu.VMEM((2 * nx, ff // 2, width // nx), BF),
+            pltpu.VMEM((2, tokens, ff // 2), BF),
             pltpu.VMEM((nb, tokens, 128), BF),
-        ]
-        + norm_scratch[1:]
-        + [
-            pltpu.SemaphoreType.DMA((nb,)),
-            pltpu.SemaphoreType.DMA((7,)),
-            pltpu.SemaphoreType.DMA((14,)),
-            pltpu.SemaphoreType.DMA((nb,)),
         ],
+        compiler_params=pltpu.CompilerParams(vmem_limit_bytes=28 << 20),
         cost_estimate=pl.CostEstimate(flops=4 * tokens * width * ff, bytes_accessed=14 << 20, transcendentals=0),
-    )(idx, *x, up, down, *pieces, *extra)
+    )(idx, *near, *extra)
 
 
 def body(
@@ -298,8 +273,8 @@
     *parts, x = ffn(
         second_kernel, idx, mixed_all, tokens, up_second, down_second, mine_2 + others_2,
         [mixed[0], gain_first[None], bias_first[None]],
-        [jax.ShapeDtypeStruct((tokens, 128), BF)],
-        [pltpu.VMEM((nb, tokens + 8, 128), BF), pltpu.VMEM((nb, 128), F32), pltpu.VMEM((nb, 128), F32)],
+        [pltpu.VMEM((tokens, 128), BF)],
+        [pltpu.VMEM((nb, 128), F32), pltpu.VMEM((nb, 128), F32)],
     )
     some = scattered_sum(parts, pairs)
     branch = some[0] + lax.ppermute(some[1].astype(BF), ALL, pairs["last"]).astype(F32)

time: 245 us -> 238 us (0.971)
  Pallas kernels: 24 us -> 14.3 us
  local copies, waits for them, and re-layouts: 5.59 us -> 9.85 us
  starting transfers between devices: 74.2 us -> 71.3 us
    pallas_call x2, Pallas kernels: 24 us -> 14.3 us  [ffn(): pl.pallas_call(kernel, out_shape=[pltpu.VMEM((4, nb // 16, tokens, 128),...]
    unnamed x40 -> x38, local copies, waits for them, and re-layouts: 1.46 us -> 6.53 us
    ppermute x1, waiting for transfers between devices: 4.4 us -> 8.26 us  [body(): there = lax.ppermute(some, ALL, pairs['last'])[::-1]]
    ppermute x1, starting transfers between devices: 7.26 us -> 3.56 us  [body(): there = lax.ppermute(some, ALL, pairs['last'])[::-1]]
    ppermute x14, waiting for transfers between devices: 26.1 us -> 23.3 us  [shift(): return lax.ppermute(a, axis, [(i, (i + by) % n) for i in range(n)])]
    ppermute x24, starting transfers between devices: 45.6 us -> 42.8 us  [stage(): got = {d: lax.ppermute(blocks[d], ALL, pairs[d]) for d in (1, 2, 3)}]
  transfers between devices with their start and end apart: 41 -> 41, of which waited for: 25 -> 26; matrix products, arithmetic and copies ran while one was open for 2% -> 3% of each run, Pallas kernels for 0% -> 0%
where the time goes in v5:
time: 238 us; the launch traced here: 237 us
  waiting for transfers between devices  119 us (50%)
  starting transfers between devices  71.3 us (30%)
  blocking collectives  17.6 us (7%)
  Pallas kernels  14.3 us (6%)
  local copies, waits for them, and re-layouts  9.85 us (4%)
  other arithmetic  4.82 us (2%)
    ppermute x24, waiting for transfers between devices, stage(): got = {d: lax.ppermute(blocks[d], ALL, pairs[d]) for d in (1, 2, 3)}  80.9 us
    ppermute x24, starting transfers between devices, stage(): got = {d: lax.ppermute(blocks[d], ALL, pairs[d]) for d in (1, 2, 3)}  42.8 us
    ppermute x14, waiting for transfers between devices, shift(): return lax.ppermute(a, axis, [(i, (i + by) % n) for i in range(n)])  23.3 us
    all_to_all x1, blocking collectives, stats_to_all(): lax.all_to_all(jnp.broadcast_to(row[None], (n, *row.shape)), RA, 0, 0, ti...  17.6 us
    pallas_call x2, Pallas kernels, ffn(): pl.pallas_call(kernel, out_shape=[pltpu.VMEM((4, nb // 16, tokens, 128),...  14.3 us
    ppermute x14, starting transfers between devices, shift(): return lax.ppermute(a, axis, [(i, (i + by) % n) for i in range(n)])  14.3 us
    ppermute x1, waiting for transfers between devices, body(): there = lax.ppermute(some, ALL, pairs['last'])[::-1]  8.26 us
    ppermute x1, starting transfers between devices, body(): pair = jnp.stack([stream, lax.ppermute(stream, ALL, pairs['last'])])  7.19 us
  transfers between devices with their start and end apart: 41, of which 26 were waited for; matrix products, arithmetic and copies ran while one was open for 3% of the time, Pallas kernels for 0%

profile of v5, /device:TPU:2, one launch (start us, length us, event | category | flops | bytes accessed | tf_op | source)
XLA Modules:
  0.0 236.7 jit_solution(2514103453546960892)
XLA Ops:
  0.0 7.2 %collective-permute-start = (bf16[384,128]{1,0:T(8,128)(2,1)}, bf16[384,128]{1,0:T(8,128)(2,1)S(1)}, u32[]{:S(2)}, u32[]{:S(2)}) collective-permute-start(bf16[384,128]{1,0:T(8,128)(2,1)} %param.9), channel_id=1, source_target_pairs={{0,128},{16,144},{64,192},{80,208},{128,0},{144,16},{192,64},{208,... | collective-permute-start | bytes 294920 | tf_op jit(solution)/shard_map/ppermute | solution.py:251
  7.2 2.1 constant_dynamic-slice_fusion
  10.3 6.6 %collective-permute-start.3 = (bf16[2,384,128]{2,1,0:T(8,128)(2,1)S(1)}, bf16[2,384,128]{2,1,0:T(8,128)(2,1)S(1)}, u32[]{:S(2)}, u32[]{:S(2)}) collective-permute-start(bf16[2,384,128]{2,1,0:T(8,128)(2,1)S(1)} %get-tuple-element.42), channel_id=1, source_target_pairs={{0,80},{16,64},{64,16},{80,0},{128,208},{144,192},{192,144},{208,1... | collective-permute-start | bytes 589832 | tf_op jit(solution)/shard_map/ppermute | solution.py:52
  17.6 1.6 collective-permute-start.7
  19.7 4.5 %collective-permute-done.3 = bf16[2,384,128]{2,1,0:T(8,128)(2,1)S(1)} collective-permute-done((bf16[2,384,128]{2,1,0:T(8,128)(2,1)S(1)}, bf16[2,384,128]{2,1,0:T(8,128)(2,1)S(1)}, u32[]{:S(2)}, u32[]{:S(2)}) %collective-permute-start.3) | collective-permute-done | bytes 196640 | tf_op jit(solution)/shard_map/ppermute | solution.py:52
  24.2 1.6 collective-permute-done.1
  25.8 1.4 collective-permute-done.2
  27.3 1.7 collective-permute-start.4
  30.0 13.4 %collective-permute-done.7.m1 = bf16[1024,512]{1,0:T(8,128)(2,1)S(1)} collective-permute-done((bf16[1024,512]{1,0:T(8,128)(2,1)S(1)}, bf16[1024,512]{1,0:T(8,128)(2,1)S(1)}, u32[]{:S(2)}, u32[]{:S(2)}) %collective-permute-start.7) | collective-permute-done | bytes 1048608 | tf_op jit(solution)/shard_map/ppermute | solution.py:74
  43.4 1.6 collective-permute-start.9
  48.1 2.0 collective-permute-start.6
  50.1 7.7 %collective-permute-done.9.fu = bf16[512,512]{1,0:T(8,128)(2,1)S(1)} collective-permute-done((bf16[512,512]{1,0:T(8,128)(2,1)S(1)}, bf16[512,512]{1,0:T(8,128)(2,1)S(1)}, u32[]{:S(2)}, u32[]{:S(2)}) %collective-permute-start.9) | collective-permute-done | bytes 524320 | tf_op jit(solution)/shard_map/ppermute | solution.py:74
  57.8 1.5 collective-permute-done.10.fd
  59.4 1.7 collective-permute-done.6.x3
  66.3 6.4 %shard_map.91 = (bf16[4,2,384,128]{3,2,1,0:T(8,128)(2,1)S(1)}, bf16[4,2,384,128]{3,2,1,0:T(8,128)(2,1)S(1)}, bf16[4,2,384,128]{3,2,1,0:T(8,128)(2,1)S(1)}, bf16[4,2,384,128]{3,2,1,0:T(8,128)(2,1)S(1)}) custom-call(s32[5]{0:T(128)S(1)} %stack.106.idx, bf16[4,2,384,128]{3,2,1,0:T(8,128)(2,1)S(1)} %pad_maximum_fusion.3.x0, ...), custom_call_target="tpu_custom_call" | custom-call | flops 3221225472 | bytes 14680064 | tf_op jit(solution)/shard_map/pallas_call | solution.py:222
  74.9 1.4 collective-permute-start.17
  78.6 1.3 collective-permute-start.29
  79.9 4.9 %collective-permute-done.15 = bf16[4,2,384,128]{3,2,1,0:T(8,128)(2,1)S(1)} collective-permute-done((bf16[4,2,384,128]{3,2,1,0:T(8,128)(2,1)S(1)}, bf16[4,2,384,128]{3,2,1,0:T(8,128)(2,1)S(1)}, u32[]{:S(2)}, u32[]{:S(2)}) %collective-permute-start.15) | collective-permute-done | bytes 786464 | tf_op jit(solution)/shard_map/ppermute | solution.py:52
  84.8 9.3 %collective-permute-done.16 = bf16[4,2,384,128]{3,2,1,0:T(8,128)(2,1)S(1)} collective-permute-done((bf16[4,2,384,128]{3,2,1,0:T(8,128)(2,1)S(1)}, bf16[4,2,384,128]{3,2,1,0:T(8,128)(2,1)S(1)}, u32[]{:S(2)}, u32[]{:S(2)}) %collective-permute-start.16) | collective-permute-done | bytes 786464 | tf_op jit(solution)/shard_map/ppermute | solution.py:52
  96.4 2.9 %collective-permute-start.19 = (bf16[2,384,128]{2,1,0:T(8,128)(2,1)S(1)}, bf16[2,384,128]{2,1,0:T(8,128)(2,1)}, u32[]{:S(2)}, u32[]{:S(2)}) collective-permute-start(bf16[2,384,128]{2,1,0:T(8,128)(2,1)S(1)} %get-tuple-element.38), channel_id=1, source_target_pairs={{0,16},{16,0},{64,80},{80,64},{128,144},{144,128},{192,208},{208,1... | collective-permute-start | bytes 589832 | tf_op jit(solution)/shard_map/ppermute | solution.py:52
  99.3 1.9 collective-permute-start.20
  101.3 5.1 %collective-permute-start.30 = (bf16[1024,512]{1,0:T(8,128)(2,1)}, bf16[1024,512]{1,0:T(8,128)(2,1)}, u32[]{:S(2)}, u32[]{:S(2)}) collective-permute-start(bf16[1024,512]{1,0:T(8,128)(2,1)} %pad_maximum_fusion.1), channel_id=1, source_target_pairs={{0,4},{2,6},{4,0},{6,2},{1,5},{3,7},{5,1},{7,3},{8,12},{10,14},{12... | collective-permute-start | bytes 3145736 | tf_op jit(solution)/shard_map/ppermute | solution.py:74
  107.6 4.1 %collective-permute-done.20 = bf16[2,384,128]{2,1,0:T(8,128)(2,1)} collective-permute-done((bf16[2,384,128]{2,1,0:T(8,128)(2,1)S(1)}, bf16[2,384,128]{2,1,0:T(8,128)(2,1)}, u32[]{:S(2)}, u32[]{:S(2)}) %collective-permute-start.20) | collective-permute-done | bytes 196640 | tf_op jit(solution)/shard_map/ppermute | solution.py:52
  112.9 3.6 %collective-permute-start.21 = (bf16[2,392,128]{2,1,0:T(8,128)(2,1)S(1)}, bf16[2,392,128]{2,1,0:T(8,128)(2,1)S(1)}, u32[]{:S(2)}, u32[]{:S(2)}) collective-permute-start(bf16[2,392,128]{2,1,0:T(8,128)(2,1)S(1)} %pad_maximum_fusion.4), channel_id=1, source_target_pairs={{0,128},{16,144},{64,192},{80,208},{128,0},{144,16},{192,64},{208,... | collective-permute-start | bytes 602120 | tf_op jit(solution)/shard_map/ppermute | solution.py:267
  116.5 8.3 %collective-permute-done.21 = bf16[2,392,128]{2,1,0:T(8,128)(2,1)S(1)} collective-permute-done((bf16[2,392,128]{2,1,0:T(8,128)(2,1)S(1)}, bf16[2,392,128]{2,1,0:T(8,128)(2,1)S(1)}, u32[]{:S(2)}, u32[]{:S(2)}) %collective-permute-start.21) | collective-permute-done | bytes 200736 | tf_op jit(solution)/shard_map/ppermute | solution.py:267
  125.0 4.1 %collective-permute-start.22 = (bf16[2,392,128]{2,1,0:T(8,128)(2,1)S(1)}, bf16[2,392,128]{2,1,0:T(8,128)(2,1)S(1)}, u32[]{:S(2)}, u32[]{:S(2)}) collective-permute-start(bf16[2,392,128]{2,1,0:T(8,128)(2,1)S(1)} %get-tuple-element.40), channel_id=1, source_target_pairs={{0,64},{16,80},{64,0},{80,16},{128,192},{144,208},{192,128},{208,1... | collective-permute-start | bytes 602120 | tf_op jit(solution)/shard_map/ppermute | solution.py:52
  129.1 1.4 collective-permute-start.23
  130.5 2.3 collective-permute-start.24
  133.5 1.9 collective-permute-done.22
  135.4 1.3 collective-permute-done.23
  136.7 4.6 %collective-permute-done.24 = bf16[2,392,128]{2,1,0:T(8,128)(2,1)S(1)} collective-permute-done((bf16[2,392,128]{2,1,0:T(8,128)(2,1)S(1)}, bf16[2,392,128]{2,1,0:T(8,128)(2,1)S(1)}, u32[]{:S(2)}, u32[]{:S(2)}) %collective-permute-start.24) | collective-permute-done | bytes 200736 | tf_op jit(solution)/shard_map/ppermute | solution.py:52
  141.6 1.8 collective-permute-start.26
  143.4 1.7 collective-permute-start.27
  145.1 8.6 %collective-permute-done.25.x1 = bf16[4,2,392,128]{3,2,1,0:T(8,128)(2,1)S(1)} collective-permute-done((bf16[4,2,392,128]{3,2,1,0:T(8,128)(2,1)S(1)}, bf16[4,2,392,128]{3,2,1,0:T(8,128)(2,1)S(1)}, u32[]{:S(2)}, u32[]{:S(2)}) %collective-permute-start.25) | collective-permute-done | bytes 802848 | tf_op jit(solution)/shard_map/ppermute | solution.py:52
  153.7 8.0 %collective-permute-done.26.x2 = bf16[4,2,392,128]{3,2,1,0:T(8,128)(2,1)S(1)} collective-permute-done((bf16[4,2,392,128]{3,2,1,0:T(8,128)(2,1)S(1)}, bf16[4,2,392,128]{3,2,1,0:T(8,128)(2,1)S(1)}, u32[]{:S(2)}, u32[]{:S(2)}) %collective-permute-start.26) | collective-permute-done | bytes 802848 | tf_op jit(solution)/shard_map/ppermute | solution.py:52
  161.7 1.8 collective-permute-done.27.x3
  163.5 7.9 %shard_map.92 = (bf16[4,2,384,128]{3,2,1,0:T(8,128)(2,1)S(1)}, bf16[4,2,384,128]{3,2,1,0:T(8,128)(2,1)S(1)}, bf16[4,2,384,128]{3,2,1,0:T(8,128)(2,1)S(1)}, bf16[...) custom-call(s32[5]{0:T(128)S(1)} %stack.106.idx, bf16[4,2,392,128]{3,2,1,0:T(8,128)(2,1)S(1)} %pad_maximum_fusion.2.x0, ...), custom_call_target="tpu_custom_call" | custom-call | flops 3221225472 | bytes 14680064 | tf_op jit(solution)/shard_map/pallas_call | solution.py:222
  172.4 1.7 collective-permute-start.35
  175.0 8.5 %collective-permute-done.34 = bf16[4,2,384,128]{3,2,1,0:T(8,128)(2,1)S(1)} collective-permute-done((bf16[4,2,384,128]{3,2,1,0:T(8,128)(2,1)S(1)}, bf16[4,2,384,128]{3,2,1,0:T(8,128)(2,1)S(1)}, u32[]{:S(2)}, u32[]{:S(2)}) %collective-permute-start.34) | collective-permute-done | bytes 786464 | tf_op jit(solution)/shard_map/ppermute | solution.py:52
  183.5 9.3 %collective-permute-done.35 = bf16[4,2,384,128]{3,2,1,0:T(8,128)(2,1)S(1)} collective-permute-done((bf16[4,2,384,128]{3,2,1,0:T(8,128)(2,1)S(1)}, bf16[4,2,384,128]{3,2,1,0:T(8,128)(2,1)S(1)}, u32[]{:S(2)}, u32[]{:S(2)}) %collective-permute-start.35) | collective-permute-done | bytes 786464 | tf_op jit(solution)/shard_map/ppermute | solution.py:52
  193.3 3.5 %collective-permute-start.37 = (bf16[2,384,128]{2,1,0:T(8,128)(2,1)S(1)}, bf16[2,384,128]{2,1,0:T(8,128)(2,1)S(1)}, u32[]{:S(2)}, u32[]{:S(2)}) collective-permute-start(bf16[2,384,128]{2,1,0:T(8,128)(2,1)S(1)} %get-tuple-element.33), channel_id=1, source_target_pairs={{0,64},{16,80},{64,0},{80,16},{128,192},{144,208},{192,128},{208,1... | collective-permute-start | bytes 589832 | tf_op jit(solution)/shard_map/ppermute | solution.py:52
  198.1 1.8 collective-permute-start.39
  199.9 2.8 %collective-permute-done.37 = bf16[2,384,128]{2,1,0:T(8,128)(2,1)S(1)} collective-permute-done((bf16[2,384,128]{2,1,0:T(8,128)(2,1)S(1)}, bf16[2,384,128]{2,1,0:T(8,128)(2,1)S(1)}, u32[]{:S(2)}, u32[]{:S(2)}) %collective-permute-start.37) | collective-permute-done | bytes 196640 | tf_op jit(solution)/shard_map/ppermute | solution.py:52
  202.7 2.3 collective-permute-done.38
  205.0 4.2 %collective-permute-done.39 = bf16[2,384,128]{2,1,0:T(8,128)(2,1)S(1)} collective-permute-done((bf16[2,384,128]{2,1,0:T(8,128)(2,1)S(1)}, bf16[2,384,128]{2,1,0:T(8,128)(2,1)S(1)}, u32[]{:S(2)}, u32[]{:S(2)}) %collective-permute-start.39) | collective-permute-done | bytes 196640 | tf_op jit(solution)/shard_map/ppermute | solution.py:52
  209.3 3.5 %collective-permute-start.40 = (bf16[384,128]{1,0:T(8,128)(2,1)S(1)}, bf16[384,128]{1,0:T(8,128)(2,1)S(1)}, u32[]{:S(2)}, u32[]{:S(2)}) collective-permute-start(bf16[384,128]{1,0:T(8,128)(2,1)S(1)} %fusion.7), channel_id=1, source_target_pairs={{0,128},{16,144},{64,192},{80,208},{128,0},{144,16},{192,64},{208,... | collective-permute-start | bytes 294920 | tf_op jit(solution)/shard_map/ppermute | solution.py:280
  212.8 5.2 %collective-permute-done.40 = bf16[384,128]{1,0:T(8,128)(2,1)S(1)} collective-permute-done((bf16[384,128]{1,0:T(8,128)(2,1)S(1)}, bf16[384,128]{1,0:T(8,128)(2,1)S(1)}, u32[]{:S(2)}, u32[]{:S(2)}) %collective-permute-start.40) | collective-permute-done | bytes 98336 | tf_op jit(solution)/shard_map/ppermute | solution.py:280
  218.2 17.6 %all_to_all.5 = f32[32,1,768]{2,1,0:T(1,128)S(1)} all-to-all(f32[32,1,768]{2,1,0:T(1,128)S(1)} %broadcast_in_dim.11), channel_id=1, replica_groups=mesh['ra_0'=8,'ra_1'=4,'cb'=4,'dp'=2] {'ra_0','ra_1'}, dimensions={0} | all-to-all | bytes 196608 | tf_op jit(solution)/shard_map/all_to_all | solution.py:69
  (113 shorter events, 26.9 us)
Async XLA Ops:
  0.0 10.3 %collective-permute-start = (bf16[384,128]{1,0:T(8,128)(2,1)}, bf16[384,128]{1,0:T(8,128)(2,1)S(1)}, u32[]{:S(2)}, u32[]{:S(2)}) collective-permute-start(bf16[384,128]{1,0:T(8,128)(2,1)} %param.9), channel_id=1, source_target_pairs={{0,128},{16,144},{64,192},{80,208},{128,0},{144,16},{192,64},{208,... | collective-permute-start | bytes 294920 | tf_op jit(solution)/shard_map/ppermute | solution.py:251
  10.3 7.3 %copy-start.15 = (bf16[384,128]{1,0:T(8,128)(2,1)}, bf16[384,128]{1,0:T(8,128)(2,1)S(1)}, u32[]{:S(2)}) copy-start(bf16[384,128]{1,0:T(8,128)(2,1)S(1)} %collective-permute-done) | copy-start | bytes 294916
  10.3 13.9 %collective-permute-start.3 = (bf16[2,384,128]{2,1,0:T(8,128)(2,1)S(1)}, bf16[2,384,128]{2,1,0:T(8,128)(2,1)S(1)}, u32[]{:S(2)}, u32[]{:S(2)}) collective-permute-start(bf16[2,384,128]{2,1,0:T(8,128)(2,1)S(1)} %get-tuple-element.42), channel_id=1, source_target_pairs={{0,80},{16,64},{64,16},{80,0},{128,208},{144,192},{192,144},{208,1... | collective-permute-start | bytes 589832 | tf_op jit(solution)/shard_map/ppermute | solution.py:52
  16.9 9.0 %collective-permute-start.1 = (bf16[2,384,128]{2,1,0:T(8,128)(2,1)S(1)}, bf16[2,384,128]{2,1,0:T(8,128)(2,1)S(1)}, u32[]{:S(2)}, u32[]{:S(2)}) collective-permute-start(bf16[2,384,128]{2,1,0:T(8,128)(2,1)S(1)} %get-tuple-element.42), channel_id=1, source_target_pairs={{0,64},{16,80},{64,0},{80,16},{128,192},{144,208},{192,128},{208,1... | collective-permute-start | bytes 589832 | tf_op jit(solution)/shard_map/ppermute | solution.py:52
  16.9 10.3 %collective-permute-start.2 = (bf16[2,384,128]{2,1,0:T(8,128)(2,1)S(1)}, bf16[2,384,128]{2,1,0:T(8,128)(2,1)S(1)}, u32[]{:S(2)}, u32[]{:S(2)}) collective-permute-start(bf16[2,384,128]{2,1,0:T(8,128)(2,1)S(1)} %get-tuple-element.42), channel_id=1, source_target_pairs={{0,16},{16,0},{64,80},{80,64},{128,144},{144,128},{192,208},{208,1... | collective-permute-start | bytes 589832 | tf_op jit(solution)/shard_map/ppermute | solution.py:52
  17.6 25.7 %collective-permute-start.7 = (bf16[1024,512]{1,0:T(8,128)(2,1)S(1)}, bf16[1024,512]{1,0:T(8,128)(2,1)S(1)}, u32[]{:S(2)}, u32[]{:S(2)}) collective-permute-start(bf16[1024,512]{1,0:T(8,128)(2,1)S(1)} %pad_maximum_fusion), channel_id=1, source_target_pairs={{0,2},{2,4},{4,6},{6,0},{1,3},{3,5},{5,7},{7,1},{8,10},{10,12},{12... | collective-permute-start | bytes 3145736 | tf_op jit(solution)/shard_map/ppermute | solution.py:74
  19.2 25.9 %collective-permute-start.8 = (bf16[1024,512]{1,0:T(8,128)(2,1)S(1)}, bf16[1024,512]{1,0:T(8,128)(2,1)S(1)}, u32[]{:S(2)}, u32[]{:S(2)}) collective-permute-start(bf16[1024,512]{1,0:T(8,128)(2,1)S(1)} %pad_maximum_fusion), channel_id=1, source_target_pairs={{0,6},{2,0},{4,2},{6,4},{1,7},{3,1},{5,3},{7,5},{8,14},{10,8},{12,... | collective-permute-start | bytes 3145736 | tf_op jit(solution)/shard_map/ppermute | solution.py:74
  27.3 18.5 %collective-permute-start.4 = (bf16[4,2,384,128]{3,2,1,0:T(8,128)(2,1)S(1)}, bf16[4,2,384,128]{3,2,1,0:T(8,128)(2,1)S(1)}, u32[]{:S(2)}, u32[]{:S(2)}) collective-permute-start(bf16[4,2,384,128]{3,2,1,0:T(8,128)(2,1)S(1)} %pad_maximum_fusion.3.x0), channel_id=1, source_target_pairs={{0,32},{8,40},{32,0},{40,8},{1,225},{25,249},{225,1},{249,25},{2,3... | collective-permute-start | bytes 2359304 | tf_op jit(solution)/shard_map/ppermute | solution.py:52
  29.0 18.1 %collective-permute-start.5 = (bf16[4,2,384,128]{3,2,1,0:T(8,128)(2,1)S(1)}, bf16[4,2,384,128]{3,2,1,0:T(8,128)(2,1)S(1)}, u32[]{:S(2)}, u32[]{:S(2)}) collective-permute-start(bf16[4,2,384,128]{3,2,1,0:T(8,128)(2,1)S(1)} %pad_maximum_fusion.3.x0), channel_id=1, source_target_pairs={{0,8},{8,0},{32,40},{40,32},{1,25},{25,1},{225,249},{249,225},{2,1... | collective-permute-start | bytes 2359304 | tf_op jit(solution)/shard_map/ppermute | solution.py:52
  43.4 14.4 %collective-permute-start.9 = (bf16[512,512]{1,0:T(8,128)(2,1)S(1)}, bf16[512,512]{1,0:T(8,128)(2,1)S(1)}, u32[]{:S(2)}, u32[]{:S(2)}) collective-permute-start(bf16[512,512]{1,0:T(8,128)(2,1)S(1)} %slice.92), channel_id=1, source_target_pairs={{0,2},{2,4},{4,6},{6,0},{1,3},{3,5},{5,7},{7,1},{8,10},{10,12},{12... | collective-permute-start | bytes 1572872 | tf_op jit(solution)/shard_map/ppermute | solution.py:74
  45.2 14.1 %collective-permute-start.10 = (bf16[512,512]{1,0:T(8,128)(2,1)S(1)}, bf16[512,512]{1,0:T(8,128)(2,1)}, u32[]{:S(2)}, u32[]{:S(2)}) collective-permute-start(bf16[512,512]{1,0:T(8,128)(2,1)S(1)} %slice.93), channel_id=1, source_target_pairs={{0,6},{2,0},{4,2},{6,4},{1,7},{3,1},{5,3},{7,5},{8,14},{10,8},{12,... | collective-permute-start | bytes 1572872 | tf_op jit(solution)/shard_map/ppermute | solution.py:74
  45.8 15.8 %collective-permute-start.11 = (bf16[1024,512]{1,0:T(8,128)(2,1)S(1)}, bf16[1024,512]{1,0:T(8,128)(2,1)}, u32[]{:S(2)}, u32[]{:S(2)}) collective-permute-start(bf16[1024,512]{1,0:T(8,128)(2,1)S(1)} %collective-permute-done.7.m1), channel_id=1, source_target_pairs={{0,1},{1,0},{2,3},{3,2},{4,5},{5,4},{6,7},{7,6},{8,9},{9,8},{10,11... | collective-permute-start | bytes 3145736 | tf_op jit(solution)/shard_map/ppermute | solution.py:74
  46.7 14.9 %collective-permute-start.12 = (bf16[1024,512]{1,0:T(8,128)(2,1)S(1)}, bf16[1024,512]{1,0:T(8,128)(2,1)}, u32[]{:S(2)}, u32[]{:S(2)}) collective-permute-start(bf16[1024,512]{1,0:T(8,128)(2,1)S(1)} %collective-permute-done.8.m3), channel_id=1, source_target_pairs={{0,1},{1,0},{2,3},{3,2},{4,5},{5,4},{6,7},{7,6},{8,9},{9,8},{10,11... | collective-permute-start | bytes 3145736 | tf_op jit(solution)/shard_map/ppermute | solution.py:74
  48.1 13.0 %collective-permute-start.6 = (bf16[4,2,384,128]{3,2,1,0:T(8,128)(2,1)S(1)}, bf16[4,2,384,128]{3,2,1,0:T(8,128)(2,1)}, u32[]{:S(2)}, u32[]{:S(2)}) collective-permute-start(bf16[4,2,384,128]{3,2,1,0:T(8,128)(2,1)S(1)} %pad_maximum_fusion.3.x0), channel_id=1, source_target_pairs={{0,40},{8,32},{32,8},{40,0},{1,249},{25,225},{225,25},{249,1},{2,4... | collective-permute-start | bytes 2359304 | tf_op jit(solution)/shard_map/ppermute | solution.py:52
  57.8 3.3 %collective-permute-start.13 = (bf16[512,512]{1,0:T(8,128)(2,1)S(1)}, bf16[512,512]{1,0:T(8,128)(2,1)}, u32[]{:S(2)}, u32[]{:S(2)}) collective-permute-start(bf16[512,512]{1,0:T(8,128)(2,1)S(1)} %collective-permute-done.9.fu), channel_id=1, source_target_pairs={{0,1},{1,0},{2,3},{3,2},{4,5},{5,4},{6,7},{7,6},{8,9},{9,8},{10,11... | collective-permute-start | bytes 1572872 | tf_op jit(solution)/shard_map/ppermute | solution.py:74
  59.3 2.3 collective-permute-start.14
  66.3 10.0 %copy-start.2 = (bf16[1024,512]{1,0:T(8,128)(2,1)S(1)}, bf16[1024,512]{1,0:T(8,128)(2,1)}, u32[]{:S(2)}) copy-start(bf16[1024,512]{1,0:T(8,128)(2,1)} %up.3) | copy-start | bytes 3145732
  72.7 12.1 %collective-permute-start.15 = (bf16[4,2,384,128]{3,2,1,0:T(8,128)(2,1)S(1)}, bf16[4,2,384,128]{3,2,1,0:T(8,128)(2,1)S(1)}, u32[]{:S(2)}, u32[]{:S(2)}) collective-permute-start(bf16[4,2,384,128]{3,2,1,0:T(8,128)(2,1)S(1)} %get-tuple-element.15), channel_id=1, source_target_pairs={{0,32},{8,40},{32,0},{40,8},{1,225},{25,249},{225,1},{249,25},{2,3... | collective-permute-start | bytes 2359304 | tf_op jit(solution)/shard_map/ppermute | solution.py:52
  73.7 20.4 %collective-permute-start.16 = (bf16[4,2,384,128]{3,2,1,0:T(8,128)(2,1)S(1)}, bf16[4,2,384,128]{3,2,1,0:T(8,128)(2,1)S(1)}, u32[]{:S(2)}, u32[]{:S(2)}) collective-permute-start(bf16[4,2,384,128]{3,2,1,0:T(8,128)(2,1)S(1)} %get-tuple-element.16), channel_id=1, source_target_pairs={{0,8},{8,0},{32,40},{40,32},{1,25},{25,1},{225,249},{249,225},{2,1... | collective-permute-start | bytes 2359304 | tf_op jit(solution)/shard_map/ppermute | solution.py:52
  74.9 19.2 %collective-permute-start.17 = (bf16[4,2,384,128]{3,2,1,0:T(8,128)(2,1)S(1)}, bf16[4,2,384,128]{3,2,1,0:T(8,128)(2,1)S(1)}, u32[]{:S(2)}, u32[]{:S(2)}) collective-permute-start(bf16[4,2,384,128]{3,2,1,0:T(8,128)(2,1)S(1)} %get-tuple-element.17), channel_id=1, source_target_pairs={{0,40},{8,32},{32,8},{40,0},{1,249},{25,225},{225,25},{249,1},{2,4... | collective-permute-start | bytes 2359304 | tf_op jit(solution)/shard_map/ppermute | solution.py:52
  77.4 23.8 %collective-permute-start.28 = (bf16[1024,512]{1,0:T(8,128)(2,1)}, bf16[1024,512]{1,0:T(8,128)(2,1)S(1)}, u32[]{:S(2)}, u32[]{:S(2)}) collective-permute-start(bf16[1024,512]{1,0:T(8,128)(2,1)} %pad_maximum_fusion.1), channel_id=1, source_target_pairs={{0,2},{2,4},{4,6},{6,0},{1,3},{3,5},{5,7},{7,1},{8,10},{10,12},{12... | collective-permute-start | bytes 3145736 | tf_op jit(solution)/shard_map/ppermute | solution.py:74
  78.6 51.9 %collective-permute-start.29 = (bf16[1024,512]{1,0:T(8,128)(2,1)}, bf16[1024,512]{1,0:T(8,128)(2,1)S(1)}, u32[]{:S(2)}, u32[]{:S(2)}) collective-permute-start(bf16[1024,512]{1,0:T(8,128)(2,1)} %pad_maximum_fusion.1), channel_id=1, source_target_pairs={{0,6},{2,0},{4,2},{6,4},{1,7},{3,1},{5,3},{7,5},{8,14},{10,8},{12,... | collective-permute-start | bytes 3145736 | tf_op jit(solution)/shard_map/ppermute | solution.py:74
  95.3 29.5 %copy-start.16 = (bf16[384,128]{1,0:T(8,128)(2,1)S(1)}, bf16[384,128]{1,0:T(8,128)(2,1)}, u32[]{:S(2)}) copy-start(bf16[384,128]{1,0:T(8,128)(2,1)} %copy-done.15) | copy-start | bytes 294916
  95.3 11.1 %collective-permute-start.18 = (bf16[2,384,128]{2,1,0:T(8,128)(2,1)}, bf16[2,384,128]{2,1,0:T(8,128)(2,1)}, u32[]{:S(2)}, u32[]{:S(2)}) collective-permute-start(bf16[2,384,128]{2,1,0:T(8,128)(2,1)} %get-tuple-element.36), channel_id=1, source_target_pairs={{0,64},{16,80},{64,0},{80,16},{128,192},{144,208},{192,128},{208,1... | collective-permute-start | bytes 589832 | tf_op jit(solution)/shard_map/ppermute | solution.py:52
  96.4 11.2 %collective-permute-start.19 = (bf16[2,384,128]{2,1,0:T(8,128)(2,1)S(1)}, bf16[2,384,128]{2,1,0:T(8,128)(2,1)}, u32[]{:S(2)}, u32[]{:S(2)}) collective-permute-start(bf16[2,384,128]{2,1,0:T(8,128)(2,1)S(1)} %get-tuple-element.38), channel_id=1, source_target_pairs={{0,16},{16,0},{64,80},{80,64},{128,144},{144,128},{192,208},{208,1... | collective-permute-start | bytes 589832 | tf_op jit(solution)/shard_map/ppermute | solution.py:52
  99.3 12.4 %collective-permute-start.20 = (bf16[2,384,128]{2,1,0:T(8,128)(2,1)S(1)}, bf16[2,384,128]{2,1,0:T(8,128)(2,1)}, u32[]{:S(2)}, u32[]{:S(2)}) collective-permute-start(bf16[2,384,128]{2,1,0:T(8,128)(2,1)S(1)} %get-tuple-element.37), channel_id=1, source_target_pairs={{0,80},{16,64},{64,16},{80,0},{128,208},{144,192},{192,144},{208,1... | collective-permute-start | bytes 589832 | tf_op jit(solution)/shard_map/ppermute | solution.py:52
  101.3 31.5 %collective-permute-start.30 = (bf16[1024,512]{1,0:T(8,128)(2,1)}, bf16[1024,512]{1,0:T(8,128)(2,1)}, u32[]{:S(2)}, u32[]{:S(2)}) collective-permute-start(bf16[1024,512]{1,0:T(8,128)(2,1)} %pad_maximum_fusion.1), channel_id=1, source_target_pairs={{0,4},{2,6},{4,0},{6,2},{1,5},{3,7},{5,1},{7,3},{8,12},{10,14},{12... | collective-permute-start | bytes 3145736 | tf_op jit(solution)/shard_map/ppermute | solution.py:74
  106.4 37.0 %collective-permute-start.31 = (bf16[1024,512]{1,0:T(8,128)(2,1)S(1)}, bf16[1024,512]{1,0:T(8,128)(2,1)}, u32[]{:S(2)}, u32[]{:S(2)}) collective-permute-start(bf16[1024,512]{1,0:T(8,128)(2,1)S(1)} %collective-permute-done.28.m1), channel_id=1, source_target_pairs={{0,1},{1,0},{2,3},{3,2},{4,5},{5,4},{6,7},{7,6},{8,9},{9,8},{10,11... | collective-permute-start | bytes 3145736 | tf_op jit(solution)/shard_map/ppermute | solution.py:74
  112.9 11.9 %collective-permute-start.21 = (bf16[2,392,128]{2,1,0:T(8,128)(2,1)S(1)}, bf16[2,392,128]{2,1,0:T(8,128)(2,1)S(1)}, u32[]{:S(2)}, u32[]{:S(2)}) collective-permute-start(bf16[2,392,128]{2,1,0:T(8,128)(2,1)S(1)} %pad_maximum_fusion.4), channel_id=1, source_target_pairs={{0,128},{16,144},{64,192},{80,208},{128,0},{144,16},{192,64},{208,... | collective-permute-start | bytes 602120 | tf_op jit(solution)/shard_map/ppermute | solution.py:267
  124.9 38.6 %copy-start.5 = (bf16[512,1024]{1,0:T(8,128)(2,1)S(1)}, bf16[512,1024]{1,0:T(8,128)(2,1)}, u32[]{:S(2)}) copy-start(bf16[512,1024]{1,0:T(8,128)(2,1)} %down.3) | copy-start | bytes 3145732
  125.0 38.5 %copy-start.3 = (bf16[1024,512]{1,0:T(8,128)(2,1)S(1)}, bf16[1024,512]{1,0:T(8,128)(2,1)}, u32[]{:S(2)}) copy-start(bf16[1024,512]{1,0:T(8,128)(2,1)} %up.3) | copy-start | bytes 3145732
  125.0 10.4 %collective-permute-start.22 = (bf16[2,392,128]{2,1,0:T(8,128)(2,1)S(1)}, bf16[2,392,128]{2,1,0:T(8,128)(2,1)S(1)}, u32[]{:S(2)}, u32[]{:S(2)}) collective-permute-start(bf16[2,392,128]{2,1,0:T(8,128)(2,1)S(1)} %get-tuple-element.40), channel_id=1, source_target_pairs={{0,64},{16,80},{64,0},{80,16},{128,192},{144,208},{192,128},{208,1... | collective-permute-start | bytes 602120 | tf_op jit(solution)/shard_map/ppermute | solution.py:52
  129.1 7.6 %collective-permute-start.23 = (bf16[2,392,128]{2,1,0:T(8,128)(2,1)S(1)}, bf16[2,392,128]{2,1,0:T(8,128)(2,1)S(1)}, u32[]{:S(2)}, u32[]{:S(2)}) collective-permute-start(bf16[2,392,128]{2,1,0:T(8,128)(2,1)S(1)} %get-tuple-element.40), channel_id=1, source_target_pairs={{0,16},{16,0},{64,80},{80,64},{128,144},{144,128},{192,208},{208,1... | collective-permute-start | bytes 602120 | tf_op jit(solution)/shard_map/ppermute | solution.py:52
  130.5 10.8 %collective-permute-start.24 = (bf16[2,392,128]{2,1,0:T(8,128)(2,1)S(1)}, bf16[2,392,128]{2,1,0:T(8,128)(2,1)S(1)}, u32[]{:S(2)}, u32[]{:S(2)}) collective-permute-start(bf16[2,392,128]{2,1,0:T(8,128)(2,1)S(1)} %get-tuple-element.40), channel_id=1, source_target_pairs={{0,80},{16,64},{64,16},{80,0},{128,208},{144,192},{192,144},{208,1... | collective-permute-start | bytes 602120 | tf_op jit(solution)/shard_map/ppermute | solution.py:52
  132.8 12.3 %collective-permute-start.32 = (bf16[1024,512]{1,0:T(8,128)(2,1)S(1)}, bf16[1024,512]{1,0:T(8,128)(2,1)S(1)}, u32[]{:S(2)}, u32[]{:S(2)}) collective-permute-start(bf16[1024,512]{1,0:T(8,128)(2,1)S(1)} %collective-permute-done.29.m2), channel_id=1, source_target_pairs={{0,1},{1,0},{2,3},{3,2},{4,5},{5,4},{6,7},{7,6},{8,9},{9,8},{10,11... | collective-permute-start | bytes 3145736 | tf_op jit(solution)/shard_map/ppermute | solution.py:74
  135.4 9.7 %collective-permute-start.33 = (bf16[1024,512]{1,0:T(8,128)(2,1)}, bf16[1024,512]{1,0:T(8,128)(2,1)S(1)}, u32[]{:S(2)}, u32[]{:S(2)}) collective-permute-start(bf16[1024,512]{1,0:T(8,128)(2,1)} %collective-permute-done.30.m3), channel_id=1, source_target_pairs={{0,1},{1,0},{2,3},{3,2},{4,5},{5,4},{6,7},{7,6},{8,9},{9,8},{10,11... | collective-permute-start | bytes 3145736 | tf_op jit(solution)/shard_map/ppermute | solution.py:74
  141.5 12.3 %collective-permute-start.25 = (bf16[4,2,392,128]{3,2,1,0:T(8,128)(2,1)S(1)}, bf16[4,2,392,128]{3,2,1,0:T(8,128)(2,1)S(1)}, u32[]{:S(2)}, u32[]{:S(2)}) collective-permute-start(bf16[4,2,392,128]{3,2,1,0:T(8,128)(2,1)S(1)} %pad_maximum_fusion.2.x0), channel_id=1, source_target_pairs={{0,32},{8,40},{32,0},{40,8},{1,225},{25,249},{225,1},{249,25},{2,3... | collective-permute-start | bytes 2408456 | tf_op jit(solution)/shard_map/ppermute | solution.py:52
  141.6 20.1 %collective-permute-start.26 = (bf16[4,2,392,128]{3,2,1,0:T(8,128)(2,1)S(1)}, bf16[4,2,392,128]{3,2,1,0:T(8,128)(2,1)S(1)}, u32[]{:S(2)}, u32[]{:S(2)}) collective-permute-start(bf16[4,2,392,128]{3,2,1,0:T(8,128)(2,1)S(1)} %pad_maximum_fusion.2.x0), channel_id=1, source_target_pairs={{0,8},{8,0},{32,40},{40,32},{1,25},{25,1},{225,249},{249,225},{2,1... | collective-permute-start | bytes 2408456 | tf_op jit(solution)/shard_map/ppermute | solution.py:52
  143.4 20.1 %collective-permute-start.27 = (bf16[4,2,392,128]{3,2,1,0:T(8,128)(2,1)S(1)}, bf16[4,2,392,128]{3,2,1,0:T(8,128)(2,1)S(1)}, u32[]{:S(2)}, u32[]{:S(2)}) collective-permute-start(bf16[4,2,392,128]{3,2,1,0:T(8,128)(2,1)S(1)} %pad_maximum_fusion.2.x0), channel_id=1, source_target_pairs={{0,40},{8,32},{32,8},{40,0},{1,249},{25,225},{225,25},{249,1},{2,4... | collective-permute-start | bytes 2408456 | tf_op jit(solution)/shard_map/ppermute | solution.py:52
  171.5 12.1 %collective-permute-start.34 = (bf16[4,2,384,128]{3,2,1,0:T(8,128)(2,1)S(1)}, bf16[4,2,384,128]{3,2,1,0:T(8,128)(2,1)S(1)}, u32[]{:S(2)}, u32[]{:S(2)}) collective-permute-start(bf16[4,2,384,128]{3,2,1,0:T(8,128)(2,1)S(1)} %get-tuple-element.20), channel_id=1, source_target_pairs={{0,32},{8,40},{32,0},{40,8},{1,225},{25,249},{225,1},{249,25},{2,3... | collective-permute-start | bytes 2359304 | tf_op jit(solution)/shard_map/ppermute | solution.py:52
  172.4 20.4 %collective-permute-start.35 = (bf16[4,2,384,128]{3,2,1,0:T(8,128)(2,1)S(1)}, bf16[4,2,384,128]{3,2,1,0:T(8,128)(2,1)S(1)}, u32[]{:S(2)}, u32[]{:S(2)}) collective-permute-start(bf16[4,2,384,128]{3,2,1,0:T(8,128)(2,1)S(1)} %get-tuple-element.21), channel_id=1, source_target_pairs={{0,8},{8,0},{32,40},{40,32},{1,25},{25,1},{225,249},{249,225},{2,1... | collective-permute-start | bytes 2359304 | tf_op jit(solution)/shard_map/ppermute | solution.py:52
  174.2 18.7 %collective-permute-start.36 = (bf16[4,2,384,128]{3,2,1,0:T(8,128)(2,1)S(1)}, bf16[4,2,384,128]{3,2,1,0:T(8,128)(2,1)S(1)}, u32[]{:S(2)}, u32[]{:S(2)}) collective-permute-start(bf16[4,2,384,128]{3,2,1,0:T(8,128)(2,1)S(1)} %get-tuple-element.22), channel_id=1, source_target_pairs={{0,40},{8,32},{32,8},{40,0},{1,249},{25,225},{225,25},{249,1},{2,4... | collective-permute-start | bytes 2359304 | tf_op jit(solution)/shard_map/ppermute | solution.py:52
  193.3 9.3 %collective-permute-start.37 = (bf16[2,384,128]{2,1,0:T(8,128)(2,1)S(1)}, bf16[2,384,128]{2,1,0:T(8,128)(2,1)S(1)}, u32[]{:S(2)}, u32[]{:S(2)}) collective-permute-start(bf16[2,384,128]{2,1,0:T(8,128)(2,1)S(1)} %get-tuple-element.33), channel_id=1, source_target_pairs={{0,64},{16,80},{64,0},{80,16},{128,192},{144,208},{192,128},{208,1... | collective-permute-start | bytes 589832 | tf_op jit(solution)/shard_map/ppermute | solution.py:52
  196.8 8.2 %collective-permute-start.38 = (bf16[2,384,128]{2,1,0:T(8,128)(2,1)S(1)}, bf16[2,384,128]{2,1,0:T(8,128)(2,1)S(1)}, u32[]{:S(2)}, u32[]{:S(2)}) collective-permute-start(bf16[2,384,128]{2,1,0:T(8,128)(2,1)S(1)} %get-tuple-element.35), channel_id=1, source_target_pairs={{0,16},{16,0},{64,80},{80,64},{128,144},{144,128},{192,208},{208,1... | collective-permute-start | bytes 589832 | tf_op jit(solution)/shard_map/ppermute | solution.py:52
  198.1 37.8 %copy-start.17 = (f32[128]{0:T(128)S(1)}, f32[128]{0:T(128)}, u32[]{:S(2)}) copy-start(f32[128]{0:T(128)} %param.17) | copy-start | bytes 1540
  198.1 37.8 %copy-start.18 = (f32[128]{0:T(128)S(1)}, f32[128]{0:T(128)}, u32[]{:S(2)}) copy-start(f32[128]{0:T(128)} %param.16) | copy-start | bytes 1540
  198.1 11.1 %collective-permute-start.39 = (bf16[2,384,128]{2,1,0:T(8,128)(2,1)S(1)}, bf16[2,384,128]{2,1,0:T(8,128)(2,1)S(1)}, u32[]{:S(2)}, u32[]{:S(2)}) collective-permute-start(bf16[2,384,128]{2,1,0:T(8,128)(2,1)S(1)} %get-tuple-element.34), channel_id=1, source_target_pairs={{0,80},{16,64},{64,16},{80,0},{128,208},{144,192},{192,144},{208,1... | collective-permute-start | bytes 589832 | tf_op jit(solution)/shard_map/ppermute | solution.py:52
  209.3 8.6 %collective-permute-start.40 = (bf16[384,128]{1,0:T(8,128)(2,1)S(1)}, bf16[384,128]{1,0:T(8,128)(2,1)S(1)}, u32[]{:S(2)}, u32[]{:S(2)}) collective-permute-start(bf16[384,128]{1,0:T(8,128)(2,1)S(1)} %fusion.7), channel_id=1, source_target_pairs={{0,128},{16,144},{64,192},{80,208},{128,0},{144,16},{192,64},{208,... | collective-permute-start | bytes 294920 | tf_op jit(solution)/shard_map/ppermute | solution.py:280
  (12 other events, 30.2 us)

commit v6 on v5

--- a/solution.py
+++ b/solution.py
@@ -110,7 +110,7 @@
     return (2 * j + zz) * NY + y, (flip & 1) + 2 * (yh ^ idx[3]), flip >> 1
 
 
-def matmuls(idx, xs, up, down, pieces, hv, ov, outs):
+def matmuls(idx, xs, up, down, copies, pieces, hv, ov, outs):
     nx = 1 + len(pieces)
     me, core = idx[0], idx[1]
     per = xs.shape[0] // nx
@@ -119,12 +119,16 @@
     def features(first, count):
         return jnp.concatenate([xs[first + k] for k in range(count)], axis=1)
 
-    pre = jnp.dot(features(per * me, per), up[...], preferred_element_type=F32)
+    pre = None
     for by, mine, other in pieces:
         source = lax.rem(me + (nx - by), nx)
         for half, piece in ((core, mine), (1 - core, other)):
             rows = features(per * source + per // 2 * half, per // 2)
-            pre = pre + jnp.dot(rows, piece(0, per // 2 * 128), preferred_element_type=F32)
+            term = jnp.dot(rows, piece(0, per // 2 * 128), preferred_element_type=F32)
+            pre = term if pre is None else pre + term
+    for copy in copies:
+        copy.wait()
+    pre = pre + jnp.dot(features(per * me, per), up[...], preferred_element_type=F32)
     hidden = jnp.square(jnp.maximum(pre, 0.0)).astype(BF)
     for half in range(2):
         hv[half] = hidden[:, half * wide : (half + 1) * wide]
@@ -153,6 +157,13 @@
         send(source)
 
 
+def fetch(up, down, upv, dv, sems):
+    copies = [pltpu.make_async_copy(up, upv, sems.at[0]), pltpu.make_async_copy(down, dv, sems.at[1])]
+    for copy in copies:
+        copy.start()
+    return copies
+
+
 def whole(ref):
     return lambda first, count: ref[first : first + count]
 
@@ -163,19 +174,21 @@
 
 
 def first_kernel(
-    idx, x0, x1, x2, x3, up, down, m1, m3, fu, fd, o1, o3, pu, pd, u0, u1, u2, u3, xs, hv, ov
+    idx, x0, x1, x2, x3, up, down, m1, m3, fu, fd, o1, o3, pu, pd, u0, u1, u2, u3, xs, hv, ov, upv, dv, sems
 ):
+    copies = fetch(up, down, upv, dv, sems)
     for d, x in enumerate((x0, x1, x2, x3)):
         for i in range(8):
             xs[from_peer(idx, d, i // 2, i % 2)] = x[i // 2, i % 2]
     pieces = [(1, whole(m1), whole(o1)), (3, whole(m3), whole(o3)), (2, split(fu, fd), split(pu, pd))]
-    matmuls(idx, xs, up, down, pieces, hv, ov, (u0, u1, u2, u3))
+    matmuls(idx, xs, upv, dv, copies, pieces, hv, ov, (u0, u1, u2, u3))
 
 
 def second_kernel(
     idx, x0, x1, x2, x3, up, down, m1, m2, m3, o1, o2, o3, mixed, own_gain, own_bias, u0, u1, u2, u3, own,
-    xs, gain, bias, hv, ov,
+    xs, gain, bias, hv, ov, upv, dv, sems,
 ):
+    copies = fetch(up, down, upv, dv, sems)
     nb, tokens = xs.shape[:2]
     step = 64
     width = nb * 128
@@ -207,7 +220,7 @@
 
     lax.fori_loop(0, tokens // step, norm, 0)
     pieces = [(1, whole(m1), whole(o1)), (3, whole(m2), whole(o2)), (2, whole(m3), whole(o3))]
-    matmuls(idx, xs, up, down, pieces, hv, ov, (u0, u1, u2, u3))
+    matmuls(idx, xs, upv, dv, copies, pieces, hv, ov, (u0, u1, u2, u3))
 
 
 ANY = pl.BlockSpec(memory_space=pltpu.MemorySpace.HBM)
@@ -218,21 +231,25 @@
 def ffn(kernel, idx, x, tokens, up, down, pieces, extra, own_out, norm_scratch):
     nx, nb = lax.axis_size(X), NZ * NY
     width, ff = up.shape[0] * nx, up.shape[1]
-    near = [pltpu.with_memory_space_constraint(a, pltpu.MemorySpace.VMEM) for a in (*x, up, down, *pieces)]
+    near = [pltpu.with_memory_space_constraint(a, pltpu.MemorySpace.VMEM) for a in (*x, *pieces)]
+    far = [pltpu.with_memory_space_constraint(a, pltpu.MemorySpace.HBM) for a in (up, down)]
     return pl.pallas_call(
         kernel,
         out_shape=[pltpu.VMEM((4, nb // 16, tokens, 128), BF)] * 4 + own_out,
-        in_specs=[SMEM] + [VMEM] * (len(near) + len(extra)),
+        in_specs=[SMEM] + [VMEM] * 4 + [ANY] * 2 + [VMEM] * (len(pieces) + len(extra)),
         out_specs=[VMEM] * (4 + len(own_out)),
         scratch_shapes=[pltpu.VMEM((nb, tokens, 128), BF)]
         + norm_scratch
         + [
             pltpu.VMEM((2, tokens, ff // 2), BF),
             pltpu.VMEM((nb, tokens, 128), BF),
+            pltpu.VMEM(up.shape, BF),
+            pltpu.VMEM(down.shape, BF),
+            pltpu.SemaphoreType.DMA((2,)),
         ],
         compiler_params=pltpu.CompilerParams(vmem_limit_bytes=28 << 20),
         cost_estimate=pl.CostEstimate(flops=4 * tokens * width * ff, bytes_accessed=14 << 20, transcendentals=0),
-    )(idx, *near, *extra)
+    )(idx, *near[:4], *far, *near[4:], *extra)
 
 
 def body(

time: 238 us -> 237 us (level)
  local copies, waits for them, and re-layouts: 9.85 us -> 7.42 us
    unnamed x38 -> x30, local copies, waits for them, and re-layouts: 6.53 us -> 4.08 us
where the time goes in v6:
time: 237 us; the launch traced here: 235 us
  waiting for transfers between devices  119 us (50%)
  starting transfers between devices  70.6 us (30%)
  blocking collectives  17.2 us (7%)
  Pallas kernels  15.6 us (7%)
  local copies, waits for them, and re-layouts  7.42 us (3%)
  other arithmetic  4.82 us (2%)
    ppermute x24, waiting for transfers between devices, stage(): got = {d: lax.ppermute(blocks[d], ALL, pairs[d]) for d in (1, 2, 3)}  80.8 us
    ppermute x24, starting transfers between devices, stage(): got = {d: lax.ppermute(blocks[d], ALL, pairs[d]) for d in (1, 2, 3)}  42.8 us
    ppermute x14, waiting for transfers between devices, shift(): return lax.ppermute(a, axis, [(i, (i + by) % n) for i in range(n)])  23.2 us
    all_to_all x1, blocking collectives, stats_to_all(): lax.all_to_all(jnp.broadcast_to(row[None], (n, *row.shape)), RA, 0, 0, ti...  17.2 us
    pallas_call x2, Pallas kernels, ffn(): pl.pallas_call(kernel, out_shape=[pltpu.VMEM((4, nb // 16, tokens, 128),...  15.6 us
    ppermute x14, starting transfers between devices, shift(): return lax.ppermute(a, axis, [(i, (i + by) % n) for i in range(n)])  14.5 us
    ppermute x1, waiting for transfers between devices, body(): there = lax.ppermute(some, ALL, pairs['last'])[::-1]  8.24 us
    ppermute x1, starting transfers between devices, body(): pair = jnp.stack([stream, lax.ppermute(stream, ALL, pairs['last'])])  7.19 us
  transfers between devices with their start and end apart: 41, of which 26 were waited for; matrix products, arithmetic and copies ran while one was open for 3% of the time, Pallas kernels for 0%

profile of v6, /device:TPU:2, one launch (start us, length us, event | category | flops | bytes accessed | tf_op | source)
XLA Modules:
  0.0 235.4 jit_solution(1652025146156153111)
XLA Ops:
  0.0 7.2 %collective-permute-start = (bf16[384,128]{1,0:T(8,128)(2,1)}, bf16[384,128]{1,0:T(8,128)(2,1)S(1)}, u32[]{:S(2)}, u32[]{:S(2)}) collective-permute-start(bf16[384,128]{1,0:T(8,128)(2,1)} %param.9), channel_id=1, source_target_pairs={{0,128},{16,144},{64,192},{80,208},{128,0},{144,16},{192,64},{208,... | collective-permute-start | bytes 294920 | tf_op jit(solution)/shard_map/ppermute | solution.py:268
  7.2 2.1 constant_dynamic-slice_fusion
  10.3 6.6 %collective-permute-start.3 = (bf16[2,384,128]{2,1,0:T(8,128)(2,1)S(1)}, bf16[2,384,128]{2,1,0:T(8,128)(2,1)S(1)}, u32[]{:S(2)}, u32[]{:S(2)}) collective-permute-start(bf16[2,384,128]{2,1,0:T(8,128)(2,1)S(1)} %get-tuple-element.42), channel_id=1, source_target_pairs={{0,80},{16,64},{64,16},{80,0},{128,208},{144,192},{192,144},{208,1... | collective-permute-start | bytes 589832 | tf_op jit(solution)/shard_map/ppermute | solution.py:52
  17.6 1.6 collective-permute-start.7
  19.7 4.5 %collective-permute-done.3 = bf16[2,384,128]{2,1,0:T(8,128)(2,1)S(1)} collective-permute-done((bf16[2,384,128]{2,1,0:T(8,128)(2,1)S(1)}, bf16[2,384,128]{2,1,0:T(8,128)(2,1)S(1)}, u32[]{:S(2)}, u32[]{:S(2)}) %collective-permute-start.3) | collective-permute-done | bytes 196640 | tf_op jit(solution)/shard_map/ppermute | solution.py:52
  24.2 1.6 collective-permute-done.1
  25.8 1.4 collective-permute-done.2
  27.3 1.7 collective-permute-start.4
  30.0 13.4 %collective-permute-done.7.m1 = bf16[1024,512]{1,0:T(8,128)(2,1)S(1)} collective-permute-done((bf16[1024,512]{1,0:T(8,128)(2,1)S(1)}, bf16[1024,512]{1,0:T(8,128)(2,1)S(1)}, u32[]{:S(2)}, u32[]{:S(2)}) %collective-permute-start.7) | collective-permute-done | bytes 1048608 | tf_op jit(solution)/shard_map/ppermute | solution.py:74
  43.4 1.6 collective-permute-start.9
  48.1 2.0 collective-permute-start.6
  50.1 7.7 %collective-permute-done.9.fu = bf16[512,512]{1,0:T(8,128)(2,1)S(1)} collective-permute-done((bf16[512,512]{1,0:T(8,128)(2,1)S(1)}, bf16[512,512]{1,0:T(8,128)(2,1)S(1)}, u32[]{:S(2)}, u32[]{:S(2)}) %collective-permute-start.9) | collective-permute-done | bytes 524320 | tf_op jit(solution)/shard_map/ppermute | solution.py:74
  57.8 1.5 collective-permute-done.10.fd
  59.4 1.7 collective-permute-done.6.x3
  63.8 7.6 %shard_map.91 = (bf16[4,2,384,128]{3,2,1,0:T(8,128)(2,1)S(1)}, bf16[4,2,384,128]{3,2,1,0:T(8,128)(2,1)S(1)}, bf16[4,2,384,128]{3,2,1,0:T(8,128)(2,1)S(1)}, bf16[4,2,384,128]{3,2,1,0:T(8,128)(2,1)S(1)}) custom-call(s32[5]{0:T(128)S(1)} %stack.106.idx, bf16[4,2,384,128]{3,2,1,0:T(8,128)(2,1)S(1)} %pad_maximum_fusion.3.x0, ...), custom_call_target="tpu_custom_call" | custom-call | flops 3221225472 | bytes 14680064 | tf_op jit(solution)/shard_map/pallas_call | solution.py:236
  73.7 1.4 collective-permute-start.17
  77.4 1.3 collective-permute-start.29
  78.7 4.9 %collective-permute-done.15 = bf16[4,2,384,128]{3,2,1,0:T(8,128)(2,1)S(1)} collective-permute-done((bf16[4,2,384,128]{3,2,1,0:T(8,128)(2,1)S(1)}, bf16[4,2,384,128]{3,2,1,0:T(8,128)(2,1)S(1)}, u32[]{:S(2)}, u32[]{:S(2)}) %collective-permute-start.15) | collective-permute-done | bytes 786464 | tf_op jit(solution)/shard_map/ppermute | solution.py:52
  83.5 9.3 %collective-permute-done.16 = bf16[4,2,384,128]{3,2,1,0:T(8,128)(2,1)S(1)} collective-permute-done((bf16[4,2,384,128]{3,2,1,0:T(8,128)(2,1)S(1)}, bf16[4,2,384,128]{3,2,1,0:T(8,128)(2,1)S(1)}, u32[]{:S(2)}, u32[]{:S(2)}) %collective-permute-start.16) | collective-permute-done | bytes 786464 | tf_op jit(solution)/shard_map/ppermute | solution.py:52
  95.2 2.9 %collective-permute-start.19 = (bf16[2,384,128]{2,1,0:T(8,128)(2,1)S(1)}, bf16[2,384,128]{2,1,0:T(8,128)(2,1)}, u32[]{:S(2)}, u32[]{:S(2)}) collective-permute-start(bf16[2,384,128]{2,1,0:T(8,128)(2,1)S(1)} %get-tuple-element.38), channel_id=1, source_target_pairs={{0,16},{16,0},{64,80},{80,64},{128,144},{144,128},{192,208},{208,1... | collective-permute-start | bytes 589832 | tf_op jit(solution)/shard_map/ppermute | solution.py:52
  98.1 1.9 collective-permute-start.20
  100.0 5.1 %collective-permute-start.30 = (bf16[1024,512]{1,0:T(8,128)(2,1)}, bf16[1024,512]{1,0:T(8,128)(2,1)}, u32[]{:S(2)}, u32[]{:S(2)}) collective-permute-start(bf16[1024,512]{1,0:T(8,128)(2,1)} %pad_maximum_fusion.1), channel_id=1, source_target_pairs={{0,4},{2,6},{4,0},{6,2},{1,5},{3,7},{5,1},{7,3},{8,12},{10,14},{12... | collective-permute-start | bytes 3145736 | tf_op jit(solution)/shard_map/ppermute | solution.py:74
  105.2 1.3 collective-permute-start.31
  106.5 4.0 %collective-permute-done.20 = bf16[2,384,128]{2,1,0:T(8,128)(2,1)} collective-permute-done((bf16[2,384,128]{2,1,0:T(8,128)(2,1)S(1)}, bf16[2,384,128]{2,1,0:T(8,128)(2,1)}, u32[]{:S(2)}, u32[]{:S(2)}) %collective-permute-start.20) | collective-permute-done | bytes 196640 | tf_op jit(solution)/shard_map/ppermute | solution.py:52
  111.8 3.5 %collective-permute-start.21 = (bf16[2,392,128]{2,1,0:T(8,128)(2,1)S(1)}, bf16[2,392,128]{2,1,0:T(8,128)(2,1)S(1)}, u32[]{:S(2)}, u32[]{:S(2)}) collective-permute-start(bf16[2,392,128]{2,1,0:T(8,128)(2,1)S(1)} %pad_maximum_fusion.4), channel_id=1, source_target_pairs={{0,128},{16,144},{64,192},{80,208},{128,0},{144,16},{192,64},{208,... | collective-permute-start | bytes 602120 | tf_op jit(solution)/shard_map/ppermute | solution.py:284
  115.4 8.2 %collective-permute-done.21 = bf16[2,392,128]{2,1,0:T(8,128)(2,1)S(1)} collective-permute-done((bf16[2,392,128]{2,1,0:T(8,128)(2,1)S(1)}, bf16[2,392,128]{2,1,0:T(8,128)(2,1)S(1)}, u32[]{:S(2)}, u32[]{:S(2)}) %collective-permute-start.21) | collective-permute-done | bytes 200736 | tf_op jit(solution)/shard_map/ppermute | solution.py:284
  123.8 4.1 %collective-permute-start.22 = (bf16[2,392,128]{2,1,0:T(8,128)(2,1)S(1)}, bf16[2,392,128]{2,1,0:T(8,128)(2,1)S(1)}, u32[]{:S(2)}, u32[]{:S(2)}) collective-permute-start(bf16[2,392,128]{2,1,0:T(8,128)(2,1)S(1)} %get-tuple-element.40), channel_id=1, source_target_pairs={{0,64},{16,80},{64,0},{80,16},{128,192},{144,208},{192,128},{208,1... | collective-permute-start | bytes 602120 | tf_op jit(solution)/shard_map/ppermute | solution.py:52
  127.9 1.2 collective-permute-start.23
  129.1 2.3 collective-permute-start.24
  132.1 2.1 collective-permute-done.22
  134.2 1.3 collective-permute-done.23
  135.5 4.3 %collective-permute-done.24 = bf16[2,392,128]{2,1,0:T(8,128)(2,1)S(1)} collective-permute-done((bf16[2,392,128]{2,1,0:T(8,128)(2,1)S(1)}, bf16[2,392,128]{2,1,0:T(8,128)(2,1)S(1)}, u32[]{:S(2)}, u32[]{:S(2)}) %collective-permute-start.24) | collective-permute-done | bytes 200736 | tf_op jit(solution)/shard_map/ppermute | solution.py:52
  140.0 2.1 collective-permute-start.26
  142.2 1.4 collective-permute-start.27
  143.6 8.6 %collective-permute-done.25.x1 = bf16[4,2,392,128]{3,2,1,0:T(8,128)(2,1)S(1)} collective-permute-done((bf16[4,2,392,128]{3,2,1,0:T(8,128)(2,1)S(1)}, bf16[4,2,392,128]{3,2,1,0:T(8,128)(2,1)S(1)}, u32[]{:S(2)}, u32[]{:S(2)}) %collective-permute-start.25) | collective-permute-done | bytes 802848 | tf_op jit(solution)/shard_map/ppermute | solution.py:52
  152.2 8.3 %collective-permute-done.26.x2 = bf16[4,2,392,128]{3,2,1,0:T(8,128)(2,1)S(1)} collective-permute-done((bf16[4,2,392,128]{3,2,1,0:T(8,128)(2,1)S(1)}, bf16[4,2,392,128]{3,2,1,0:T(8,128)(2,1)S(1)}, u32[]{:S(2)}, u32[]{:S(2)}) %collective-permute-start.26) | collective-permute-done | bytes 802848 | tf_op jit(solution)/shard_map/ppermute | solution.py:52
  160.5 1.8 collective-permute-done.27.x3
  162.3 8.0 %shard_map.92 = (bf16[4,2,384,128]{3,2,1,0:T(8,128)(2,1)S(1)}, bf16[4,2,384,128]{3,2,1,0:T(8,128)(2,1)S(1)}, bf16[4,2,384,128]{3,2,1,0:T(8,128)(2,1)S(1)}, bf16[...) custom-call(s32[5]{0:T(128)S(1)} %stack.106.idx, bf16[4,2,392,128]{3,2,1,0:T(8,128)(2,1)S(1)} %pad_maximum_fusion.2.x0, ...), custom_call_target="tpu_custom_call" | custom-call | flops 3221225472 | bytes 14680064 | tf_op jit(solution)/shard_map/pallas_call | solution.py:236
  170.9 2.0 collective-permute-start.35
  173.9 8.5 %collective-permute-done.34 = bf16[4,2,384,128]{3,2,1,0:T(8,128)(2,1)S(1)} collective-permute-done((bf16[4,2,384,128]{3,2,1,0:T(8,128)(2,1)S(1)}, bf16[4,2,384,128]{3,2,1,0:T(8,128)(2,1)S(1)}, u32[]{:S(2)}, u32[]{:S(2)}) %collective-permute-start.34) | collective-permute-done | bytes 786464 | tf_op jit(solution)/shard_map/ppermute | solution.py:52
  182.4 9.0 %collective-permute-done.35 = bf16[4,2,384,128]{3,2,1,0:T(8,128)(2,1)S(1)} collective-permute-done((bf16[4,2,384,128]{3,2,1,0:T(8,128)(2,1)S(1)}, bf16[4,2,384,128]{3,2,1,0:T(8,128)(2,1)S(1)}, u32[]{:S(2)}, u32[]{:S(2)}) %collective-permute-start.35) | collective-permute-done | bytes 786464 | tf_op jit(solution)/shard_map/ppermute | solution.py:52
  191.8 3.7 %collective-permute-start.37 = (bf16[2,384,128]{2,1,0:T(8,128)(2,1)S(1)}, bf16[2,384,128]{2,1,0:T(8,128)(2,1)S(1)}, u32[]{:S(2)}, u32[]{:S(2)}) collective-permute-start(bf16[2,384,128]{2,1,0:T(8,128)(2,1)S(1)} %get-tuple-element.33), channel_id=1, source_target_pairs={{0,64},{16,80},{64,0},{80,16},{128,192},{144,208},{192,128},{208,1... | collective-permute-start | bytes 589832 | tf_op jit(solution)/shard_map/ppermute | solution.py:52
  196.6 2.0 collective-permute-start.39
  198.6 2.8 %collective-permute-done.37 = bf16[2,384,128]{2,1,0:T(8,128)(2,1)S(1)} collective-permute-done((bf16[2,384,128]{2,1,0:T(8,128)(2,1)S(1)}, bf16[2,384,128]{2,1,0:T(8,128)(2,1)S(1)}, u32[]{:S(2)}, u32[]{:S(2)}) %collective-permute-start.37) | collective-permute-done | bytes 196640 | tf_op jit(solution)/shard_map/ppermute | solution.py:52
  201.3 5.7 %collective-permute-done.38 = bf16[2,384,128]{2,1,0:T(8,128)(2,1)S(1)} collective-permute-done((bf16[2,384,128]{2,1,0:T(8,128)(2,1)S(1)}, bf16[2,384,128]{2,1,0:T(8,128)(2,1)S(1)}, u32[]{:S(2)}, u32[]{:S(2)}) %collective-permute-start.38) | collective-permute-done | bytes 196640 | tf_op jit(solution)/shard_map/ppermute | solution.py:52
  208.2 2.6 %collective-permute-start.40 = (bf16[384,128]{1,0:T(8,128)(2,1)S(1)}, bf16[384,128]{1,0:T(8,128)(2,1)S(1)}, u32[]{:S(2)}, u32[]{:S(2)}) collective-permute-start(bf16[384,128]{1,0:T(8,128)(2,1)S(1)} %fusion.7), channel_id=1, source_target_pairs={{0,128},{16,144},{64,192},{80,208},{128,0},{144,16},{192,64},{208,... | collective-permute-start | bytes 294920 | tf_op jit(solution)/shard_map/ppermute | solution.py:297
  210.8 6.2 %collective-permute-done.40 = bf16[384,128]{1,0:T(8,128)(2,1)S(1)} collective-permute-done((bf16[384,128]{1,0:T(8,128)(2,1)S(1)}, bf16[384,128]{1,0:T(8,128)(2,1)S(1)}, u32[]{:S(2)}, u32[]{:S(2)}) %collective-permute-start.40) | collective-permute-done | bytes 98336 | tf_op jit(solution)/shard_map/ppermute | solution.py:297
  217.2 17.2 %all_to_all.5 = f32[32,1,768]{2,1,0:T(1,128)S(1)} all-to-all(f32[32,1,768]{2,1,0:T(1,128)S(1)} %broadcast_in_dim.11), channel_id=1, replica_groups=mesh['ra_0'=8,'ra_1'=4,'cb'=4,'dp'=2] {'ra_0','ra_1'}, dimensions={0} | all-to-all | bytes 196608 | tf_op jit(solution)/shard_map/all_to_all | solution.py:69
  (105 shorter events, 23.9 us)
Async XLA Ops:
  0.0 10.3 %collective-permute-start = (bf16[384,128]{1,0:T(8,128)(2,1)}, bf16[384,128]{1,0:T(8,128)(2,1)S(1)}, u32[]{:S(2)}, u32[]{:S(2)}) collective-permute-start(bf16[384,128]{1,0:T(8,128)(2,1)} %param.9), channel_id=1, source_target_pairs={{0,128},{16,144},{64,192},{80,208},{128,0},{144,16},{192,64},{208,... | collective-permute-start | bytes 294920 | tf_op jit(solution)/shard_map/ppermute | solution.py:268
  10.3 7.3 %copy-start.9 = (bf16[384,128]{1,0:T(8,128)(2,1)}, bf16[384,128]{1,0:T(8,128)(2,1)S(1)}, u32[]{:S(2)}) copy-start(bf16[384,128]{1,0:T(8,128)(2,1)S(1)} %collective-permute-done) | copy-start | bytes 294916
  10.3 13.9 %collective-permute-start.3 = (bf16[2,384,128]{2,1,0:T(8,128)(2,1)S(1)}, bf16[2,384,128]{2,1,0:T(8,128)(2,1)S(1)}, u32[]{:S(2)}, u32[]{:S(2)}) collective-permute-start(bf16[2,384,128]{2,1,0:T(8,128)(2,1)S(1)} %get-tuple-element.42), channel_id=1, source_target_pairs={{0,80},{16,64},{64,16},{80,0},{128,208},{144,192},{192,144},{208,1... | collective-permute-start | bytes 589832 | tf_op jit(solution)/shard_map/ppermute | solution.py:52
  16.9 9.0 %collective-permute-start.1 = (bf16[2,384,128]{2,1,0:T(8,128)(2,1)S(1)}, bf16[2,384,128]{2,1,0:T(8,128)(2,1)S(1)}, u32[]{:S(2)}, u32[]{:S(2)}) collective-permute-start(bf16[2,384,128]{2,1,0:T(8,128)(2,1)S(1)} %get-tuple-element.42), channel_id=1, source_target_pairs={{0,64},{16,80},{64,0},{80,16},{128,192},{144,208},{192,128},{208,1... | collective-permute-start | bytes 589832 | tf_op jit(solution)/shard_map/ppermute | solution.py:52
  16.9 10.3 %collective-permute-start.2 = (bf16[2,384,128]{2,1,0:T(8,128)(2,1)S(1)}, bf16[2,384,128]{2,1,0:T(8,128)(2,1)S(1)}, u32[]{:S(2)}, u32[]{:S(2)}) collective-permute-start(bf16[2,384,128]{2,1,0:T(8,128)(2,1)S(1)} %get-tuple-element.42), channel_id=1, source_target_pairs={{0,16},{16,0},{64,80},{80,64},{128,144},{144,128},{192,208},{208,1... | collective-permute-start | bytes 589832 | tf_op jit(solution)/shard_map/ppermute | solution.py:52
  17.6 25.7 %collective-permute-start.7 = (bf16[1024,512]{1,0:T(8,128)(2,1)S(1)}, bf16[1024,512]{1,0:T(8,128)(2,1)S(1)}, u32[]{:S(2)}, u32[]{:S(2)}) collective-permute-start(bf16[1024,512]{1,0:T(8,128)(2,1)S(1)} %pad_maximum_fusion), channel_id=1, source_target_pairs={{0,2},{2,4},{4,6},{6,0},{1,3},{3,5},{5,7},{7,1},{8,10},{10,12},{12... | collective-permute-start | bytes 3145736 | tf_op jit(solution)/shard_map/ppermute | solution.py:74
  19.2 25.9 %collective-permute-start.8 = (bf16[1024,512]{1,0:T(8,128)(2,1)S(1)}, bf16[1024,512]{1,0:T(8,128)(2,1)S(1)}, u32[]{:S(2)}, u32[]{:S(2)}) collective-permute-start(bf16[1024,512]{1,0:T(8,128)(2,1)S(1)} %pad_maximum_fusion), channel_id=1, source_target_pairs={{0,6},{2,0},{4,2},{6,4},{1,7},{3,1},{5,3},{7,5},{8,14},{10,8},{12,... | collective-permute-start | bytes 3145736 | tf_op jit(solution)/shard_map/ppermute | solution.py:74
  27.3 18.5 %collective-permute-start.4 = (bf16[4,2,384,128]{3,2,1,0:T(8,128)(2,1)S(1)}, bf16[4,2,384,128]{3,2,1,0:T(8,128)(2,1)S(1)}, u32[]{:S(2)}, u32[]{:S(2)}) collective-permute-start(bf16[4,2,384,128]{3,2,1,0:T(8,128)(2,1)S(1)} %pad_maximum_fusion.3.x0), channel_id=1, source_target_pairs={{0,32},{8,40},{32,0},{40,8},{1,225},{25,249},{225,1},{249,25},{2,3... | collective-permute-start | bytes 2359304 | tf_op jit(solution)/shard_map/ppermute | solution.py:52
  29.0 18.1 %collective-permute-start.5 = (bf16[4,2,384,128]{3,2,1,0:T(8,128)(2,1)S(1)}, bf16[4,2,384,128]{3,2,1,0:T(8,128)(2,1)S(1)}, u32[]{:S(2)}, u32[]{:S(2)}) collective-permute-start(bf16[4,2,384,128]{3,2,1,0:T(8,128)(2,1)S(1)} %pad_maximum_fusion.3.x0), channel_id=1, source_target_pairs={{0,8},{8,0},{32,40},{40,32},{1,25},{25,1},{225,249},{249,225},{2,1... | collective-permute-start | bytes 2359304 | tf_op jit(solution)/shard_map/ppermute | solution.py:52
  43.4 14.4 %collective-permute-start.9 = (bf16[512,512]{1,0:T(8,128)(2,1)S(1)}, bf16[512,512]{1,0:T(8,128)(2,1)S(1)}, u32[]{:S(2)}, u32[]{:S(2)}) collective-permute-start(bf16[512,512]{1,0:T(8,128)(2,1)S(1)} %slice.92), channel_id=1, source_target_pairs={{0,2},{2,4},{4,6},{6,0},{1,3},{3,5},{5,7},{7,1},{8,10},{10,12},{12... | collective-permute-start | bytes 1572872 | tf_op jit(solution)/shard_map/ppermute | solution.py:74
  45.2 14.1 %collective-permute-start.10 = (bf16[512,512]{1,0:T(8,128)(2,1)S(1)}, bf16[512,512]{1,0:T(8,128)(2,1)}, u32[]{:S(2)}, u32[]{:S(2)}) collective-permute-start(bf16[512,512]{1,0:T(8,128)(2,1)S(1)} %slice.93), channel_id=1, source_target_pairs={{0,6},{2,0},{4,2},{6,4},{1,7},{3,1},{5,3},{7,5},{8,14},{10,8},{12,... | collective-permute-start | bytes 1572872 | tf_op jit(solution)/shard_map/ppermute | solution.py:74
  45.8 15.8 %collective-permute-start.11 = (bf16[1024,512]{1,0:T(8,128)(2,1)S(1)}, bf16[1024,512]{1,0:T(8,128)(2,1)}, u32[]{:S(2)}, u32[]{:S(2)}) collective-permute-start(bf16[1024,512]{1,0:T(8,128)(2,1)S(1)} %collective-permute-done.7.m1), channel_id=1, source_target_pairs={{0,1},{1,0},{2,3},{3,2},{4,5},{5,4},{6,7},{7,6},{8,9},{9,8},{10,11... | collective-permute-start | bytes 3145736 | tf_op jit(solution)/shard_map/ppermute | solution.py:74
  46.7 14.9 %collective-permute-start.12 = (bf16[1024,512]{1,0:T(8,128)(2,1)S(1)}, bf16[1024,512]{1,0:T(8,128)(2,1)}, u32[]{:S(2)}, u32[]{:S(2)}) collective-permute-start(bf16[1024,512]{1,0:T(8,128)(2,1)S(1)} %collective-permute-done.8.m3), channel_id=1, source_target_pairs={{0,1},{1,0},{2,3},{3,2},{4,5},{5,4},{6,7},{7,6},{8,9},{9,8},{10,11... | collective-permute-start | bytes 3145736 | tf_op jit(solution)/shard_map/ppermute | solution.py:74
  48.1 13.0 %collective-permute-start.6 = (bf16[4,2,384,128]{3,2,1,0:T(8,128)(2,1)S(1)}, bf16[4,2,384,128]{3,2,1,0:T(8,128)(2,1)}, u32[]{:S(2)}, u32[]{:S(2)}) collective-permute-start(bf16[4,2,384,128]{3,2,1,0:T(8,128)(2,1)S(1)} %pad_maximum_fusion.3.x0), channel_id=1, source_target_pairs={{0,40},{8,32},{32,8},{40,0},{1,249},{25,225},{225,25},{249,1},{2,4... | collective-permute-start | bytes 2359304 | tf_op jit(solution)/shard_map/ppermute | solution.py:52
  57.8 3.3 %collective-permute-start.13 = (bf16[512,512]{1,0:T(8,128)(2,1)S(1)}, bf16[512,512]{1,0:T(8,128)(2,1)}, u32[]{:S(2)}, u32[]{:S(2)}) collective-permute-start(bf16[512,512]{1,0:T(8,128)(2,1)S(1)} %collective-permute-done.9.fu), channel_id=1, source_target_pairs={{0,1},{1,0},{2,3},{3,2},{4,5},{5,4},{6,7},{7,6},{8,9},{9,8},{10,11... | collective-permute-start | bytes 1572872 | tf_op jit(solution)/shard_map/ppermute | solution.py:74
  59.3 2.3 collective-permute-start.14
  63.8 11.2 %copy-start.12 = (bf16[1024,512]{1,0:T(8,128)(2,1)S(1)}, bf16[1024,512]{1,0:T(8,128)(2,1)}, u32[]{:S(2)}) copy-start(bf16[1024,512]{1,0:T(8,128)(2,1)} %up.3) | copy-start | bytes 3145732
  71.5 12.1 %collective-permute-start.15 = (bf16[4,2,384,128]{3,2,1,0:T(8,128)(2,1)S(1)}, bf16[4,2,384,128]{3,2,1,0:T(8,128)(2,1)S(1)}, u32[]{:S(2)}, u32[]{:S(2)}) collective-permute-start(bf16[4,2,384,128]{3,2,1,0:T(8,128)(2,1)S(1)} %get-tuple-element.15), channel_id=1, source_target_pairs={{0,32},{8,40},{32,0},{40,8},{1,225},{25,249},{225,1},{249,25},{2,3... | collective-permute-start | bytes 2359304 | tf_op jit(solution)/shard_map/ppermute | solution.py:52
  72.5 20.4 %collective-permute-start.16 = (bf16[4,2,384,128]{3,2,1,0:T(8,128)(2,1)S(1)}, bf16[4,2,384,128]{3,2,1,0:T(8,128)(2,1)S(1)}, u32[]{:S(2)}, u32[]{:S(2)}) collective-permute-start(bf16[4,2,384,128]{3,2,1,0:T(8,128)(2,1)S(1)} %get-tuple-element.16), channel_id=1, source_target_pairs={{0,8},{8,0},{32,40},{40,32},{1,25},{25,1},{225,249},{249,225},{2,1... | collective-permute-start | bytes 2359304 | tf_op jit(solution)/shard_map/ppermute | solution.py:52
  73.7 19.2 %collective-permute-start.17 = (bf16[4,2,384,128]{3,2,1,0:T(8,128)(2,1)S(1)}, bf16[4,2,384,128]{3,2,1,0:T(8,128)(2,1)S(1)}, u32[]{:S(2)}, u32[]{:S(2)}) collective-permute-start(bf16[4,2,384,128]{3,2,1,0:T(8,128)(2,1)S(1)} %get-tuple-element.17), channel_id=1, source_target_pairs={{0,40},{8,32},{32,8},{40,0},{1,249},{25,225},{225,25},{249,1},{2,4... | collective-permute-start | bytes 2359304 | tf_op jit(solution)/shard_map/ppermute | solution.py:52
  76.2 23.9 %collective-permute-start.28 = (bf16[1024,512]{1,0:T(8,128)(2,1)}, bf16[1024,512]{1,0:T(8,128)(2,1)S(1)}, u32[]{:S(2)}, u32[]{:S(2)}) collective-permute-start(bf16[1024,512]{1,0:T(8,128)(2,1)} %pad_maximum_fusion.1), channel_id=1, source_target_pairs={{0,2},{2,4},{4,6},{6,0},{1,3},{3,5},{5,7},{7,1},{8,10},{10,12},{12... | collective-permute-start | bytes 3145736 | tf_op jit(solution)/shard_map/ppermute | solution.py:74
  77.4 51.8 %collective-permute-start.29 = (bf16[1024,512]{1,0:T(8,128)(2,1)}, bf16[1024,512]{1,0:T(8,128)(2,1)S(1)}, u32[]{:S(2)}, u32[]{:S(2)}) collective-permute-start(bf16[1024,512]{1,0:T(8,128)(2,1)} %pad_maximum_fusion.1), channel_id=1, source_target_pairs={{0,6},{2,0},{4,2},{6,4},{1,7},{3,1},{5,3},{7,5},{8,14},{10,8},{12,... | collective-permute-start | bytes 3145736 | tf_op jit(solution)/shard_map/ppermute | solution.py:74
  93.3 6.7 %copy-start = (f32[128]{0:T(128)S(1)}, f32[128]{0:T(128)}, u32[]{:S(2)}) copy-start(f32[128]{0:T(128)} %param.15) | copy-start | bytes 1540
  93.3 6.7 %copy-start.1 = (f32[128]{0:T(128)S(1)}, f32[128]{0:T(128)}, u32[]{:S(2)}) copy-start(f32[128]{0:T(128)} %param.14) | copy-start | bytes 1540
  94.1 29.6 %copy-start.10 = (bf16[384,128]{1,0:T(8,128)(2,1)S(1)}, bf16[384,128]{1,0:T(8,128)(2,1)}, u32[]{:S(2)}) copy-start(bf16[384,128]{1,0:T(8,128)(2,1)} %copy-done.9) | copy-start | bytes 294916
  94.1 11.1 %collective-permute-start.18 = (bf16[2,384,128]{2,1,0:T(8,128)(2,1)}, bf16[2,384,128]{2,1,0:T(8,128)(2,1)}, u32[]{:S(2)}, u32[]{:S(2)}) collective-permute-start(bf16[2,384,128]{2,1,0:T(8,128)(2,1)} %get-tuple-element.36), channel_id=1, source_target_pairs={{0,64},{16,80},{64,0},{80,16},{128,192},{144,208},{192,128},{208,1... | collective-permute-start | bytes 589832 | tf_op jit(solution)/shard_map/ppermute | solution.py:52
  95.2 11.3 %collective-permute-start.19 = (bf16[2,384,128]{2,1,0:T(8,128)(2,1)S(1)}, bf16[2,384,128]{2,1,0:T(8,128)(2,1)}, u32[]{:S(2)}, u32[]{:S(2)}) collective-permute-start(bf16[2,384,128]{2,1,0:T(8,128)(2,1)S(1)} %get-tuple-element.38), channel_id=1, source_target_pairs={{0,16},{16,0},{64,80},{80,64},{128,144},{144,128},{192,208},{208,1... | collective-permute-start | bytes 589832 | tf_op jit(solution)/shard_map/ppermute | solution.py:52
  98.1 12.4 %collective-permute-start.20 = (bf16[2,384,128]{2,1,0:T(8,128)(2,1)S(1)}, bf16[2,384,128]{2,1,0:T(8,128)(2,1)}, u32[]{:S(2)}, u32[]{:S(2)}) collective-permute-start(bf16[2,384,128]{2,1,0:T(8,128)(2,1)S(1)} %get-tuple-element.37), channel_id=1, source_target_pairs={{0,80},{16,64},{64,16},{80,0},{128,208},{144,192},{192,144},{208,1... | collective-permute-start | bytes 589832 | tf_op jit(solution)/shard_map/ppermute | solution.py:52
  100.0 31.4 %collective-permute-start.30 = (bf16[1024,512]{1,0:T(8,128)(2,1)}, bf16[1024,512]{1,0:T(8,128)(2,1)}, u32[]{:S(2)}, u32[]{:S(2)}) collective-permute-start(bf16[1024,512]{1,0:T(8,128)(2,1)} %pad_maximum_fusion.1), channel_id=1, source_target_pairs={{0,4},{2,6},{4,0},{6,2},{1,5},{3,7},{5,1},{7,3},{8,12},{10,14},{12... | collective-permute-start | bytes 3145736 | tf_op jit(solution)/shard_map/ppermute | solution.py:74
  105.2 37.0 %collective-permute-start.31 = (bf16[1024,512]{1,0:T(8,128)(2,1)S(1)}, bf16[1024,512]{1,0:T(8,128)(2,1)}, u32[]{:S(2)}, u32[]{:S(2)}) collective-permute-start(bf16[1024,512]{1,0:T(8,128)(2,1)S(1)} %collective-permute-done.28.m1), channel_id=1, source_target_pairs={{0,1},{1,0},{2,3},{3,2},{4,5},{5,4},{6,7},{7,6},{8,9},{9,8},{10,11... | collective-permute-start | bytes 3145736 | tf_op jit(solution)/shard_map/ppermute | solution.py:74
  111.8 11.8 %collective-permute-start.21 = (bf16[2,392,128]{2,1,0:T(8,128)(2,1)S(1)}, bf16[2,392,128]{2,1,0:T(8,128)(2,1)S(1)}, u32[]{:S(2)}, u32[]{:S(2)}) collective-permute-start(bf16[2,392,128]{2,1,0:T(8,128)(2,1)S(1)} %pad_maximum_fusion.4), channel_id=1, source_target_pairs={{0,128},{16,144},{64,192},{80,208},{128,0},{144,16},{192,64},{208,... | collective-permute-start | bytes 602120 | tf_op jit(solution)/shard_map/ppermute | solution.py:284
  123.8 10.4 %collective-permute-start.22 = (bf16[2,392,128]{2,1,0:T(8,128)(2,1)S(1)}, bf16[2,392,128]{2,1,0:T(8,128)(2,1)S(1)}, u32[]{:S(2)}, u32[]{:S(2)}) collective-permute-start(bf16[2,392,128]{2,1,0:T(8,128)(2,1)S(1)} %get-tuple-element.40), channel_id=1, source_target_pairs={{0,64},{16,80},{64,0},{80,16},{128,192},{144,208},{192,128},{208,1... | collective-permute-start | bytes 602120 | tf_op jit(solution)/shard_map/ppermute | solution.py:52
  127.9 7.6 %collective-permute-start.23 = (bf16[2,392,128]{2,1,0:T(8,128)(2,1)S(1)}, bf16[2,392,128]{2,1,0:T(8,128)(2,1)S(1)}, u32[]{:S(2)}, u32[]{:S(2)}) collective-permute-start(bf16[2,392,128]{2,1,0:T(8,128)(2,1)S(1)} %get-tuple-element.40), channel_id=1, source_target_pairs={{0,16},{16,0},{64,80},{80,64},{128,144},{144,128},{192,208},{208,1... | collective-permute-start | bytes 602120 | tf_op jit(solution)/shard_map/ppermute | solution.py:52
  129.1 10.7 %collective-permute-start.24 = (bf16[2,392,128]{2,1,0:T(8,128)(2,1)S(1)}, bf16[2,392,128]{2,1,0:T(8,128)(2,1)S(1)}, u32[]{:S(2)}, u32[]{:S(2)}) collective-permute-start(bf16[2,392,128]{2,1,0:T(8,128)(2,1)S(1)} %get-tuple-element.40), channel_id=1, source_target_pairs={{0,80},{16,64},{64,16},{80,0},{128,208},{144,192},{192,144},{208,1... | collective-permute-start | bytes 602120 | tf_op jit(solution)/shard_map/ppermute | solution.py:52
  131.4 12.2 %collective-permute-start.32 = (bf16[1024,512]{1,0:T(8,128)(2,1)S(1)}, bf16[1024,512]{1,0:T(8,128)(2,1)S(1)}, u32[]{:S(2)}, u32[]{:S(2)}) collective-permute-start(bf16[1024,512]{1,0:T(8,128)(2,1)S(1)} %collective-permute-done.29.m2), channel_id=1, source_target_pairs={{0,1},{1,0},{2,3},{3,2},{4,5},{5,4},{6,7},{7,6},{8,9},{9,8},{10,11... | collective-permute-start | bytes 3145736 | tf_op jit(solution)/shard_map/ppermute | solution.py:74
  134.2 9.4 %collective-permute-start.33 = (bf16[1024,512]{1,0:T(8,128)(2,1)}, bf16[1024,512]{1,0:T(8,128)(2,1)S(1)}, u32[]{:S(2)}, u32[]{:S(2)}) collective-permute-start(bf16[1024,512]{1,0:T(8,128)(2,1)} %collective-permute-done.30.m3), channel_id=1, source_target_pairs={{0,1},{1,0},{2,3},{3,2},{4,5},{5,4},{6,7},{7,6},{8,9},{9,8},{10,11... | collective-permute-start | bytes 3145736 | tf_op jit(solution)/shard_map/ppermute | solution.py:74
  139.9 12.3 %collective-permute-start.25 = (bf16[4,2,392,128]{3,2,1,0:T(8,128)(2,1)S(1)}, bf16[4,2,392,128]{3,2,1,0:T(8,128)(2,1)S(1)}, u32[]{:S(2)}, u32[]{:S(2)}) collective-permute-start(bf16[4,2,392,128]{3,2,1,0:T(8,128)(2,1)S(1)} %pad_maximum_fusion.2.x0), channel_id=1, source_target_pairs={{0,32},{8,40},{32,0},{40,8},{1,225},{25,249},{225,1},{249,25},{2,3... | collective-permute-start | bytes 2408456 | tf_op jit(solution)/shard_map/ppermute | solution.py:52
  140.0 20.4 %collective-permute-start.26 = (bf16[4,2,392,128]{3,2,1,0:T(8,128)(2,1)S(1)}, bf16[4,2,392,128]{3,2,1,0:T(8,128)(2,1)S(1)}, u32[]{:S(2)}, u32[]{:S(2)}) collective-permute-start(bf16[4,2,392,128]{3,2,1,0:T(8,128)(2,1)S(1)} %pad_maximum_fusion.2.x0), channel_id=1, source_target_pairs={{0,8},{8,0},{32,40},{40,32},{1,25},{25,1},{225,249},{249,225},{2,1... | collective-permute-start | bytes 2408456 | tf_op jit(solution)/shard_map/ppermute | solution.py:52
  142.2 20.1 %collective-permute-start.27 = (bf16[4,2,392,128]{3,2,1,0:T(8,128)(2,1)S(1)}, bf16[4,2,392,128]{3,2,1,0:T(8,128)(2,1)S(1)}, u32[]{:S(2)}, u32[]{:S(2)}) collective-permute-start(bf16[4,2,392,128]{3,2,1,0:T(8,128)(2,1)S(1)} %pad_maximum_fusion.2.x0), channel_id=1, source_target_pairs={{0,40},{8,32},{32,8},{40,0},{1,249},{25,225},{225,25},{249,1},{2,4... | collective-permute-start | bytes 2408456 | tf_op jit(solution)/shard_map/ppermute | solution.py:52
  170.3 12.1 %collective-permute-start.34 = (bf16[4,2,384,128]{3,2,1,0:T(8,128)(2,1)S(1)}, bf16[4,2,384,128]{3,2,1,0:T(8,128)(2,1)S(1)}, u32[]{:S(2)}, u32[]{:S(2)}) collective-permute-start(bf16[4,2,384,128]{3,2,1,0:T(8,128)(2,1)S(1)} %get-tuple-element.20), channel_id=1, source_target_pairs={{0,32},{8,40},{32,0},{40,8},{1,225},{25,249},{225,1},{249,25},{2,3... | collective-permute-start | bytes 2359304 | tf_op jit(solution)/shard_map/ppermute | solution.py:52
  170.9 20.4 %collective-permute-start.35 = (bf16[4,2,384,128]{3,2,1,0:T(8,128)(2,1)S(1)}, bf16[4,2,384,128]{3,2,1,0:T(8,128)(2,1)S(1)}, u32[]{:S(2)}, u32[]{:S(2)}) collective-permute-start(bf16[4,2,384,128]{3,2,1,0:T(8,128)(2,1)S(1)} %get-tuple-element.21), channel_id=1, source_target_pairs={{0,8},{8,0},{32,40},{40,32},{1,25},{25,1},{225,249},{249,225},{2,1... | collective-permute-start | bytes 2359304 | tf_op jit(solution)/shard_map/ppermute | solution.py:52
  173.0 18.4 %collective-permute-start.36 = (bf16[4,2,384,128]{3,2,1,0:T(8,128)(2,1)S(1)}, bf16[4,2,384,128]{3,2,1,0:T(8,128)(2,1)S(1)}, u32[]{:S(2)}, u32[]{:S(2)}) collective-permute-start(bf16[4,2,384,128]{3,2,1,0:T(8,128)(2,1)S(1)} %get-tuple-element.22), channel_id=1, source_target_pairs={{0,40},{8,32},{32,8},{40,0},{1,249},{25,225},{225,25},{249,1},{2,4... | collective-permute-start | bytes 2359304 | tf_op jit(solution)/shard_map/ppermute | solution.py:52
  191.8 9.5 %collective-permute-start.37 = (bf16[2,384,128]{2,1,0:T(8,128)(2,1)S(1)}, bf16[2,384,128]{2,1,0:T(8,128)(2,1)S(1)}, u32[]{:S(2)}, u32[]{:S(2)}) collective-permute-start(bf16[2,384,128]{2,1,0:T(8,128)(2,1)S(1)} %get-tuple-element.33), channel_id=1, source_target_pairs={{0,64},{16,80},{64,0},{80,16},{128,192},{144,208},{192,128},{208,1... | collective-permute-start | bytes 589832 | tf_op jit(solution)/shard_map/ppermute | solution.py:52
  195.5 11.5 %collective-permute-start.38 = (bf16[2,384,128]{2,1,0:T(8,128)(2,1)S(1)}, bf16[2,384,128]{2,1,0:T(8,128)(2,1)S(1)}, u32[]{:S(2)}, u32[]{:S(2)}) collective-permute-start(bf16[2,384,128]{2,1,0:T(8,128)(2,1)S(1)} %get-tuple-element.35), channel_id=1, source_target_pairs={{0,16},{16,0},{64,80},{80,64},{128,144},{144,128},{192,208},{208,1... | collective-permute-start | bytes 589832 | tf_op jit(solution)/shard_map/ppermute | solution.py:52
  196.6 38.0 %copy-start.13 = (f32[128]{0:T(128)S(1)}, f32[128]{0:T(128)}, u32[]{:S(2)}) copy-start(f32[128]{0:T(128)} %param.17) | copy-start | bytes 1540
  196.6 38.0 %copy-start.14 = (f32[128]{0:T(128)S(1)}, f32[128]{0:T(128)}, u32[]{:S(2)}) copy-start(f32[128]{0:T(128)} %param.16) | copy-start | bytes 1540
  196.6 11.5 %collective-permute-start.39 = (bf16[2,384,128]{2,1,0:T(8,128)(2,1)S(1)}, bf16[2,384,128]{2,1,0:T(8,128)(2,1)S(1)}, u32[]{:S(2)}, u32[]{:S(2)}) collective-permute-start(bf16[2,384,128]{2,1,0:T(8,128)(2,1)S(1)} %get-tuple-element.34), channel_id=1, source_target_pairs={{0,80},{16,64},{64,16},{80,0},{128,208},{144,192},{192,144},{208,1... | collective-permute-start | bytes 589832 | tf_op jit(solution)/shard_map/ppermute | solution.py:52
  208.2 8.7 %collective-permute-start.40 = (bf16[384,128]{1,0:T(8,128)(2,1)S(1)}, bf16[384,128]{1,0:T(8,128)(2,1)S(1)}, u32[]{:S(2)}, u32[]{:S(2)}) collective-permute-start(bf16[384,128]{1,0:T(8,128)(2,1)S(1)} %fusion.7), channel_id=1, source_target_pairs={{0,128},{16,144},{64,192},{80,208},{128,0},{144,16},{192,64},{208,... | collective-permute-start | bytes 294920 | tf_op jit(solution)/shard_map/ppermute | solution.py:297
  (8 other events, 14.4 us)

commit v7 on v6

--- a/solution.py
+++ b/solution.py
@@ -60,8 +60,16 @@
 
 
 def scattered_sum(parts, pairs):
-    some = sum(p.astype(F32) for p in stage(parts, pairs["near"])).astype(BF)
-    return sum(p.astype(F32) for p in stage([some[e] for e in range(4)], pairs["mid"]))
+    def near_sum(some):
+        return sum(p.astype(F32) for p in stage(some, pairs["near"])).astype(BF)
+
+    def flip(block, e):
+        return lax.ppermute(block, ALL, pairs["mid"][e]).astype(F32)
+
+    high = near_sum(parts[4:])
+    low = near_sum(parts[:4])
+    far = flip(high[0], 2) + flip(high[1], 3)
+    return low[0].astype(F32) + flip(low[1], 1) + far
 
 
 def stats_to_all(row):
@@ -140,9 +148,9 @@
 
     def send(j):
         for d in range(4):
-            for yh in range(NY // 2):
-                slot, e, g = to_peer(idx, d, j, yh)
-                outs[d][e, g] = ov[slot]
+            for f in range(2):
+                slot, e, g = to_peer(idx, d, j, idx[3] ^ f)
+                outs[4 * f + d][e & 1, g] = ov[slot]
 
     part = jnp.dot(hv[0], down[:wide], preferred_element_type=F32)
     emit(me, 0, part + jnp.dot(hv[1], down[wide:], preferred_element_type=F32))
@@ -174,18 +182,18 @@
 
 
 def first_kernel(
-    idx, x0, x1, x2, x3, up, down, m1, m3, fu, fd, o1, o3, pu, pd, u0, u1, u2, u3, xs, hv, ov, upv, dv, sems
+    idx, x0, x1, x2, x3, up, down, m1, m3, fu, fd, o1, o3, pu, pd, u0, u1, u2, u3, v0, v1, v2, v3, xs, hv, ov, upv, dv, sems
 ):
     copies = fetch(up, down, upv, dv, sems)
     for d, x in enumerate((x0, x1, x2, x3)):
         for i in range(8):
             xs[from_peer(idx, d, i // 2, i % 2)] = x[i // 2, i % 2]
     pieces = [(1, whole(m1), whole(o1)), (3, whole(m3), whole(o3)), (2, split(fu, fd), split(pu, pd))]
-    matmuls(idx, xs, upv, dv, copies, pieces, hv, ov, (u0, u1, u2, u3))
+    matmuls(idx, xs, upv, dv, copies, pieces, hv, ov, (u0, u1, u2, u3, v0, v1, v2, v3))
 
 
 def second_kernel(
-    idx, x0, x1, x2, x3, up, down, m1, m2, m3, o1, o2, o3, mixed, own_gain, own_bias, u0, u1, u2, u3, own,
+    idx, x0, x1, x2, x3, up, down, m1, m2, m3, others, mixed, own_gain, own_bias, u0, u1, u2, u3, v0, v1, v2, v3, own,
     xs, gain, bias, hv, ov, upv, dv, sems,
 ):
     copies = fetch(up, down, upv, dv, sems)
@@ -219,8 +227,8 @@
         return carry
 
     lax.fori_loop(0, tokens // step, norm, 0)
-    pieces = [(1, whole(m1), whole(o1)), (3, whole(m2), whole(o2)), (2, whole(m3), whole(o3))]
-    matmuls(idx, xs, upv, dv, copies, pieces, hv, ov, (u0, u1, u2, u3))
+    pieces = [(by, whole(m), whole(others.at[k])) for k, (by, m) in enumerate(((1, m1), (3, m2), (2, m3)))]
+    matmuls(idx, xs, upv, dv, copies, pieces, hv, ov, (u0, u1, u2, u3, v0, v1, v2, v3))
 
 
 ANY = pl.BlockSpec(memory_space=pltpu.MemorySpace.HBM)
@@ -235,9 +243,9 @@
     far = [pltpu.with_memory_space_constraint(a, pltpu.MemorySpace.HBM) for a in (up, down)]
     return pl.pallas_call(
         kernel,
-        out_shape=[pltpu.VMEM((4, nb // 16, tokens, 128), BF)] * 4 + own_out,
+        out_shape=[pltpu.VMEM((2, nb // 16, tokens, 128), BF)] * 8 + own_out,
         in_specs=[SMEM] + [VMEM] * 4 + [ANY] * 2 + [VMEM] * (len(pieces) + len(extra)),
-        out_specs=[VMEM] * (4 + len(own_out)),
+        out_specs=[VMEM] * (8 + len(own_out)),
         scratch_shapes=[pltpu.VMEM((nb, tokens, 128), BF)]
         + norm_scratch
         + [
@@ -285,7 +293,7 @@
     mixed = RESID * pair.astype(F32) + some[:, :tokens].astype(F32) + there[:, :tokens].astype(F32)
     tails = jnp.stack([tail, there[1, tokens:]])
     mixed_all = gathered(jnp.concatenate([mixed.astype(BF), tails], axis=1), pairs)
-    others_2 = [shift(m, C, 1) for m in mine_2]
+    others_2 = [shift(jnp.stack(mine_2), C, 1)]
     nb = NZ * NY
     *parts, x = ffn(
         second_kernel, idx, mixed_all, tokens, up_second, down_second, mine_2 + others_2,

time: 237 us -> 270 us (1.14)
  waiting for transfers between devices: 119 us -> 138 us
  local copies, waits for them, and re-layouts: 7.42 us -> 24.5 us
  starting transfers between devices: 70.6 us -> 66.6 us
  other arithmetic: 4.82 us -> 8.19 us
    ppermute x0 -> x6, waiting for transfers between devices: none -> 17.3 us  [flip(): return lax.ppermute(block, ALL, pairs['mid'][e]).astype(F32)]
    ppermute x24, waiting for transfers between devices: 80.8 us -> 65.6 us  [stage(): got = {d: lax.ppermute(blocks[d], ALL, pairs[d]) for d in (1, 2, 3)}]
    unnamed x30 -> x46, local copies, waits for them, and re-layouts: 4.08 us -> 14.8 us
    ppermute x24, starting transfers between devices: 42.8 us -> 32.3 us  [stage(): got = {d: lax.ppermute(blocks[d], ALL, pairs[d]) for d in (1, 2, 3)}]
    ppermute x14 -> x12, waiting for transfers between devices: 23.2 us -> 33.3 us  [shift(): return lax.ppermute(a, axis, [(i, (i + by) % n) for i in range(n)])]
    ppermute x0 -> x6, starting transfers between devices: none -> 8.24 us  [flip(): return lax.ppermute(block, ALL, pairs['mid'][e]).astype(F32)]
    ppermute x14 -> x12, starting transfers between devices: 14.5 us -> 15.2 us  [shift(): return lax.ppermute(a, axis, [(i, (i + by) % n) for i in range(n)])]
  transfers between devices with their start and end apart: 41 -> 45, of which waited for: 26 -> 26; matrix products, arithmetic and copies ran while one was open for 3% -> 5% of each run, Pallas kernels for 0% -> 3%
where the time goes in v7:
time: 270 us; the launch traced here: 268 us
  waiting for transfers between devices  138 us (51%)
  starting transfers between devices  66.6 us (25%)
  local copies, waits for them, and re-layouts  24.5 us (9%)
  Pallas kernels  16 us (6%)
  blocking collectives  14.5 us (5%)
  other arithmetic  8.19 us (3%)
    ppermute x24, waiting for transfers between devices, stage(): got = {d: lax.ppermute(blocks[d], ALL, pairs[d]) for d in (1, 2, 3)}  65.6 us
    ppermute x12, waiting for transfers between devices, shift(): return lax.ppermute(a, axis, [(i, (i + by) % n) for i in range(n)])  33.3 us
    ppermute x24, starting transfers between devices, stage(): got = {d: lax.ppermute(blocks[d], ALL, pairs[d]) for d in (1, 2, 3)}  32.3 us
    ppermute x6, waiting for transfers between devices, flip(): return lax.ppermute(block, ALL, pairs['mid'][e]).astype(F32)  17.3 us
    pallas_call x2, Pallas kernels, ffn(): pl.pallas_call(kernel, out_shape=[pltpu.VMEM((2, nb // 16, tokens, 128),...  16 us
    ppermute x12, starting transfers between devices, shift(): return lax.ppermute(a, axis, [(i, (i + by) % n) for i in range(n)])  15.2 us
    unnamed x46, local copies, waits for them, and re-layouts  14.8 us
    all_to_all x1, blocking collectives, stats_to_all(): lax.all_to_all(jnp.broadcast_to(row[None], (n, *row.shape)), RA, 0, 0, ti...  14.5 us
  transfers between devices with their start and end apart: 45, of which 26 were waited for; matrix products, arithmetic and copies ran while one was open for 5% of the time, Pallas kernels for 3%

profile of v7, /device:TPU:2, one launch (start us, length us, event | category | flops | bytes accessed | tf_op | source)
XLA Modules:
  0.0 268.2 jit_solution(1452149905619649391)
XLA Ops:
  2.5 1.6 collective-permute-start.7
  4.9 6.9 %collective-permute-start = (bf16[384,128]{1,0:T(8,128)(2,1)S(1)}, bf16[384,128]{1,0:T(8,128)(2,1)S(1)}, u32[]{:S(2)}, u32[]{:S(2)}) collective-permute-start(bf16[384,128]{1,0:T(8,128)(2,1)S(1)} %copy-done.19), channel_id=1, source_target_pairs={{0,128},{16,144},{64,192},{80,208},{128,0},{144,16},{192,64},{208,... | collective-permute-start | bytes 294920 | tf_op jit(solution)/shard_map/ppermute | solution.py:276
  11.8 3.3 %collective-permute-done = bf16[384,128]{1,0:T(8,128)(2,1)S(1)} collective-permute-done((bf16[384,128]{1,0:T(8,128)(2,1)S(1)}, bf16[384,128]{1,0:T(8,128)(2,1)S(1)}, u32[]{:S(2)}, u32[]{:S(2)}) %collective-permute-start) | collective-permute-done | bytes 98336 | tf_op jit(solution)/shard_map/ppermute | solution.py:276
  15.1 5.6 %collective-permute-start.3 = (bf16[2,384,128]{2,1,0:T(8,128)(2,1)S(1)}, bf16[2,384,128]{2,1,0:T(8,128)(2,1)S(1)}, u32[]{:S(2)}, u32[]{:S(2)}) collective-permute-start(bf16[2,384,128]{2,1,0:T(8,128)(2,1)S(1)} %get-tuple-element.56), channel_id=1, source_target_pairs={{0,80},{16,64},{64,16},{80,0},{128,208},{144,192},{192,144},{208,1... | collective-permute-start | bytes 589832 | tf_op jit(solution)/shard_map/ppermute | solution.py:52
  21.4 5.8 %collective-permute-done.3 = bf16[2,384,128]{2,1,0:T(8,128)(2,1)S(1)} collective-permute-done((bf16[2,384,128]{2,1,0:T(8,128)(2,1)S(1)}, bf16[2,384,128]{2,1,0:T(8,128)(2,1)S(1)}, u32[]{:S(2)}, u32[]{:S(2)}) %collective-permute-start.3) | collective-permute-done | bytes 196640 | tf_op jit(solution)/shard_map/ppermute | solution.py:52
  27.1 3.0 %collective-permute-done.1 = bf16[2,384,128]{2,1,0:T(8,128)(2,1)S(1)} collective-permute-done((bf16[2,384,128]{2,1,0:T(8,128)(2,1)S(1)}, bf16[2,384,128]{2,1,0:T(8,128)(2,1)S(1)}, u32[]{:S(2)}, u32[]{:S(2)}) %collective-permute-start.1) | collective-permute-done | bytes 196640 | tf_op jit(solution)/shard_map/ppermute | solution.py:52
  30.8 1.8 collective-permute-start.4
  34.4 1.6 collective-permute-start.9
  38.7 7.7 %collective-permute-done.9.fu = bf16[512,512]{1,0:T(8,128)(2,1)S(1)} collective-permute-done((bf16[512,512]{1,0:T(8,128)(2,1)S(1)}, bf16[512,512]{1,0:T(8,128)(2,1)S(1)}, u32[]{:S(2)}, u32[]{:S(2)}) %collective-permute-start.9) | collective-permute-done | bytes 524320 | tf_op jit(solution)/shard_map/ppermute | solution.py:82
  46.4 3.0 %collective-permute-start.13 = (bf16[512,512]{1,0:T(8,128)(2,1)S(1)}, bf16[512,512]{1,0:T(8,128)(2,1)S(1)}, u32[]{:S(2)}, u32[]{:S(2)}) collective-permute-start(bf16[512,512]{1,0:T(8,128)(2,1)S(1)} %collective-permute-done.9.fu), channel_id=1, source_target_pairs={{0,1},{1,0},{2,3},{3,2},{4,5},{5,4},{6,7},{7,6},{8,9},{9,8},{10,11... | collective-permute-start | bytes 1572872 | tf_op jit(solution)/shard_map/ppermute | solution.py:82
  50.2 1.8 collective-permute-start.14
  57.5 1.5 collective-permute-start.31
  61.2 3.0 %collective-permute-start.33 = (bf16[1024,512]{1,0:T(8,128)(2,1)}, bf16[1024,512]{1,0:T(8,128)(2,1)S(1)}, u32[]{:S(2)}, u32[]{:S(2)}) collective-permute-start(bf16[1024,512]{1,0:T(8,128)(2,1)} %pad_maximum_fusion.2), channel_id=1, source_target_pairs={{0,4},{2,6},{4,0},{6,2},{1,5},{3,7},{5,1},{7,3},{8,12},{10,14},{12... | collective-permute-start | bytes 3145736 | tf_op jit(solution)/shard_map/ppermute | solution.py:82
  73.0 7.6 %shard_map.91 = (bf16[2,2,384,128]{3,2,1,0:T(8,128)(2,1)S(1)}, bf16[2,2,384,128]{3,2,1,0:T(8,128)(2,1)S(1)}, bf16[2,2,384,128]{3,2,1,0:T(8,128)(2,1)S(1)}, bf16[...) custom-call(s32[5]{0:T(128)S(1)} %stack.118.idx, ...), custom_call_target="tpu_custom_call" | custom-call | flops 3221225472 | bytes 14680064 | tf_op jit(solution)/shard_map/pallas_call | solution.py:244
  82.4 1.4 collective-permute-done.31.m1
  85.2 23.6 %collective-permute-done.33.m3 = bf16[1024,512]{1,0:T(8,128)(2,1)S(1)} collective-permute-done((bf16[1024,512]{1,0:T(8,128)(2,1)}, bf16[1024,512]{1,0:T(8,128)(2,1)S(1)}, u32[]{:S(2)}, u32[]{:S(2)}) %collective-permute-start.33) | collective-permute-done | bytes 1048608 | tf_op jit(solution)/shard_map/ppermute | solution.py:82
  108.8 2.0 pad_maximum_fusion
  111.4 1.6 collective-permute-start.20
  114.5 2.7 %collective-permute-start.18 = (bf16[2,384,128]{2,1,0:T(8,128)(2,1)S(1)}, bf16[2,384,128]{2,1,0:T(8,128)(2,1)}, u32[]{:S(2)}, u32[]{:S(2)}) collective-permute-start(bf16[2,384,128]{2,1,0:T(8,128)(2,1)S(1)} %slice_bitcast_fusion.8), channel_id=1, source_target_pairs={{0,64},{16,80},{64,0},{80,16},{128,192},{144,208},{192,128},{208,1... | collective-permute-start | bytes 589832 | tf_op jit(solution)/shard_map/ppermute | solution.py:67
  119.4 8.3 %collective-permute-done.21 = bf16[2,2,384,128]{3,2,1,0:T(8,128)(2,1)S(1)} collective-permute-done((bf16[2,2,384,128]{3,2,1,0:T(8,128)(2,1)S(1)}, bf16[2,2,384,128]{3,2,1,0:T(8,128)(2,1)S(1)}, u32[]{:S(2)}, u32[]{:S(2)}) %collective-permute-start.21) | collective-permute-done | bytes 393248 | tf_op jit(solution)/shard_map/ppermute | solution.py:52
  128.8 2.7 %collective-permute-start.22 = (bf16[2,384,128]{2,1,0:T(8,128)(2,1)}, bf16[2,384,128]{2,1,0:T(8,128)(2,1)}, u32[]{:S(2)}, u32[]{:S(2)}) collective-permute-start(bf16[2,384,128]{2,1,0:T(8,128)(2,1)} %get-tuple-element.51), channel_id=1, source_target_pairs={{0,16},{16,0},{64,80},{80,64},{128,144},{144,128},{192,208},{208,1... | collective-permute-start | bytes 589832 | tf_op jit(solution)/shard_map/ppermute | solution.py:67
  134.0 4.8 %collective-permute-done.22 = bf16[2,384,128]{2,1,0:T(8,128)(2,1)} collective-permute-done((bf16[2,384,128]{2,1,0:T(8,128)(2,1)}, bf16[2,384,128]{2,1,0:T(8,128)(2,1)}, u32[]{:S(2)}, u32[]{:S(2)}) %collective-permute-start.22) | collective-permute-done | bytes 196640 | tf_op jit(solution)/shard_map/ppermute | solution.py:67
  138.8 3.1 %collective-permute-done.23 = bf16[2,384,128]{2,1,0:T(8,128)(2,1)} collective-permute-done((bf16[2,384,128]{2,1,0:T(8,128)(2,1)}, bf16[2,384,128]{2,1,0:T(8,128)(2,1)}, u32[]{:S(2)}, u32[]{:S(2)}) %collective-permute-start.23) | collective-permute-done | bytes 196640 | tf_op jit(solution)/shard_map/ppermute | solution.py:67
  142.0 1.3 fusion.2
  144.0 2.7 %collective-permute-start.24 = (bf16[2,392,128]{2,1,0:T(8,128)(2,1)}, bf16[2,392,128]{2,1,0:T(8,128)(2,1)}, u32[]{:S(2)}, u32[]{:S(2)}) collective-permute-start(bf16[2,392,128]{2,1,0:T(8,128)(2,1)} %pad_maximum_fusion.5), channel_id=1, source_target_pairs={{0,128},{16,144},{64,192},{80,208},{128,0},{144,16},{192,64},{208,... | collective-permute-start | bytes 602120 | tf_op jit(solution)/shard_map/ppermute | solution.py:292
  148.0 10.2 %collective-permute-done.24 = bf16[2,392,128]{2,1,0:T(8,128)(2,1)} collective-permute-done((bf16[2,392,128]{2,1,0:T(8,128)(2,1)}, bf16[2,392,128]{2,1,0:T(8,128)(2,1)}, u32[]{:S(2)}, u32[]{:S(2)}) %collective-permute-start.24) | collective-permute-done | bytes 200736 | tf_op jit(solution)/shard_map/ppermute | solution.py:292
  160.1 3.0 %collective-permute-start.26 = (bf16[2,392,128]{2,1,0:T(8,128)(2,1)S(1)}, bf16[2,392,128]{2,1,0:T(8,128)(2,1)S(1)}, u32[]{:S(2)}, u32[]{:S(2)}) collective-permute-start(bf16[2,392,128]{2,1,0:T(8,128)(2,1)S(1)} %get-tuple-element.54), channel_id=1, source_target_pairs={{0,16},{16,0},{64,80},{80,64},{128,144},{144,128},{192,208},{208,1... | collective-permute-start | bytes 602120 | tf_op jit(solution)/shard_map/ppermute | solution.py:52
  163.1 2.9 %collective-permute-start.27 = (bf16[2,392,128]{2,1,0:T(8,128)(2,1)S(1)}, bf16[2,392,128]{2,1,0:T(8,128)(2,1)S(1)}, u32[]{:S(2)}, u32[]{:S(2)}) collective-permute-start(bf16[2,392,128]{2,1,0:T(8,128)(2,1)S(1)} %get-tuple-element.54), channel_id=1, source_target_pairs={{0,80},{16,64},{64,16},{80,0},{128,208},{144,192},{192,144},{208,1... | collective-permute-start | bytes 602120 | tf_op jit(solution)/shard_map/ppermute | solution.py:52
  166.0 2.2 collective-permute-done.25
  168.1 4.4 %collective-permute-done.26 = bf16[2,392,128]{2,1,0:T(8,128)(2,1)S(1)} collective-permute-done((bf16[2,392,128]{2,1,0:T(8,128)(2,1)S(1)}, bf16[2,392,128]{2,1,0:T(8,128)(2,1)S(1)}, u32[]{:S(2)}, u32[]{:S(2)}) %collective-permute-start.26) | collective-permute-done | bytes 200736 | tf_op jit(solution)/shard_map/ppermute | solution.py:52
  172.5 3.6 %collective-permute-done.27 = bf16[2,392,128]{2,1,0:T(8,128)(2,1)S(1)} collective-permute-done((bf16[2,392,128]{2,1,0:T(8,128)(2,1)S(1)}, bf16[2,392,128]{2,1,0:T(8,128)(2,1)S(1)}, u32[]{:S(2)}, u32[]{:S(2)}) %collective-permute-start.27) | collective-permute-done | bytes 200736 | tf_op jit(solution)/shard_map/ppermute | solution.py:52
  176.5 3.4 %collective-permute-start.30 = (bf16[4,2,392,128]{3,2,1,0:T(8,128)(2,1)S(1)}, bf16[4,2,392,128]{3,2,1,0:T(8,128)(2,1)S(1)}, u32[]{:S(2)}, u32[]{:S(2)}) collective-permute-start(bf16[4,2,392,128]{3,2,1,0:T(8,128)(2,1)S(1)} %pad_maximum_fusion.3.x0), channel_id=1, source_target_pairs={{0,40},{8,32},{32,8},{40,0},{1,249},{25,225},{225,25},{249,1},{2,4... | collective-permute-start | bytes 2408456 | tf_op jit(solution)/shard_map/ppermute | solution.py:52
  179.9 8.7 %collective-permute-done.28.x1 = bf16[4,2,392,128]{3,2,1,0:T(8,128)(2,1)S(1)} collective-permute-done((bf16[4,2,392,128]{3,2,1,0:T(8,128)(2,1)S(1)}, bf16[4,2,392,128]{3,2,1,0:T(8,128)(2,1)S(1)}, u32[]{:S(2)}, u32[]{:S(2)}) %collective-permute-start.28) | collective-permute-done | bytes 802848 | tf_op jit(solution)/shard_map/ppermute | solution.py:52
  188.5 8.7 %collective-permute-done.29.x2 = bf16[4,2,392,128]{3,2,1,0:T(8,128)(2,1)S(1)} collective-permute-done((bf16[4,2,392,128]{3,2,1,0:T(8,128)(2,1)S(1)}, bf16[4,2,392,128]{3,2,1,0:T(8,128)(2,1)S(1)}, u32[]{:S(2)}, u32[]{:S(2)}) %collective-permute-start.29) | collective-permute-done | bytes 802848 | tf_op jit(solution)/shard_map/ppermute | solution.py:52
  197.2 8.3 %shard_map.92 = (bf16[2,2,384,128]{3,2,1,0:T(8,128)(2,1)S(1)}, bf16[2,2,384,128]{3,2,1,0:T(8,128)(2,1)S(1)}, bf16[2,2,384,128]{3,2,1,0:T(8,128)(2,1)S(1)}, bf16[...) custom-call(s32[5]{0:T(128)S(1)} %stack.118.idx, ...), custom_call_target="tpu_custom_call" | custom-call | flops 3221225472 | bytes 14680064 | tf_op jit(solution)/shard_map/pallas_call | solution.py:244
  205.6 2.0 collective-permute-start.35
  207.6 1.6 collective-permute-start.37
  209.2 1.9 collective-permute-start.39
  211.1 2.4 collective-permute-done.35
  213.4 1.4 collective-permute-start.41
  214.8 4.8 %collective-permute-done.36 = bf16[2,2,384,128]{3,2,1,0:T(8,128)(2,1)S(1)} collective-permute-done((bf16[2,2,384,128]{3,2,1,0:T(8,128)(2,1)S(1)}, bf16[2,2,384,128]{3,2,1,0:T(8,128)(2,1)S(1)}, u32[]{:S(2)}, u32[]{:S(2)}) %collective-permute-start.36) | collective-permute-done | bytes 393248 | tf_op jit(solution)/shard_map/ppermute | solution.py:52
  220.1 1.8 collective-permute-done.39
  221.9 1.9 collective-permute-done.40
  223.8 7.4 %collective-permute-done.41 = bf16[2,2,384,128]{3,2,1,0:T(8,128)(2,1)S(1)} collective-permute-done((bf16[2,2,384,128]{3,2,1,0:T(8,128)(2,1)S(1)}, bf16[2,2,384,128]{3,2,1,0:T(8,128)(2,1)S(1)}, u32[]{:S(2)}, u32[]{:S(2)}) %collective-permute-start.41) | collective-permute-done | bytes 393248 | tf_op jit(solution)/shard_map/ppermute | solution.py:52
  231.9 1.4 collective-permute-start.43
  233.3 9.4 %collective-permute-done.42 = bf16[2,384,128]{2,1,0:T(8,128)(2,1)S(1)} collective-permute-done((bf16[2,384,128]{2,1,0:T(8,128)(2,1)S(1)}, bf16[2,384,128]{2,1,0:T(8,128)(2,1)S(1)}, u32[]{:S(2)}, u32[]{:S(2)}) %collective-permute-start.42) | collective-permute-done | bytes 196640 | tf_op jit(solution)/shard_map/ppermute | solution.py:67
  244.1 8.4 %collective-permute-done.44 = bf16[384,128]{1,0:T(8,128)(2,1)S(1)} collective-permute-done((bf16[384,128]{1,0:T(8,128)(2,1)S(1)}, bf16[384,128]{1,0:T(8,128)(2,1)S(1)}, u32[]{:S(2)}, u32[]{:S(2)}) %collective-permute-start.44) | collective-permute-done | bytes 98336 | tf_op jit(solution)/shard_map/ppermute | solution.py:305
  252.7 14.5 %all_to_all.5 = f32[32,1,768]{2,1,0:T(1,128)S(1)} all-to-all(f32[32,1,768]{2,1,0:T(1,128)S(1)} %broadcast_in_dim.11), channel_id=1, replica_groups=mesh['ra_0'=8,'ra_1'=4,'cb'=4,'dp'=2] {'ra_0','ra_1'}, dimensions={0} | all-to-all | bytes 196608 | tf_op jit(solution)/shard_map/all_to_all | solution.py:77
  (134 shorter events, 45.5 us)
Async XLA Ops:
  2.5 30.8 %collective-permute-start.7 = (bf16[1024,512]{1,0:T(8,128)(2,1)S(1)}, bf16[1024,512]{1,0:T(8,128)(2,1)}, u32[]{:S(2)}, u32[]{:S(2)}) collective-permute-start(bf16[1024,512]{1,0:T(8,128)(2,1)S(1)} %pad_maximum_fusion.1), channel_id=1, source_target_pairs={{0,2},{2,4},{4,6},{6,0},{1,3},{3,5},{5,7},{7,1},{8,10},{10,12},{12... | collective-permute-start | bytes 3145736 | tf_op jit(solution)/shard_map/ppermute | solution.py:82
  4.0 31.9 %collective-permute-start.8 = (bf16[1024,512]{1,0:T(8,128)(2,1)S(1)}, bf16[1024,512]{1,0:T(8,128)(2,1)}, u32[]{:S(2)}, u32[]{:S(2)}) collective-permute-start(bf16[1024,512]{1,0:T(8,128)(2,1)S(1)} %pad_maximum_fusion.1), channel_id=1, source_target_pairs={{0,6},{2,0},{4,2},{6,4},{1,7},{3,1},{5,3},{7,5},{8,14},{10,8},{12,... | collective-permute-start | bytes 3145736 | tf_op jit(solution)/shard_map/ppermute | solution.py:82
  4.9 10.2 %collective-permute-start = (bf16[384,128]{1,0:T(8,128)(2,1)S(1)}, bf16[384,128]{1,0:T(8,128)(2,1)S(1)}, u32[]{:S(2)}, u32[]{:S(2)}) collective-permute-start(bf16[384,128]{1,0:T(8,128)(2,1)S(1)} %copy-done.19), channel_id=1, source_target_pairs={{0,128},{16,144},{64,192},{80,208},{128,0},{144,16},{192,64},{208,... | collective-permute-start | bytes 294920 | tf_op jit(solution)/shard_map/ppermute | solution.py:276
  15.0 40.4 %copy-start.20 = (bf16[1024,512]{1,0:T(8,128)(2,1)S(1)}, bf16[1024,512]{1,0:T(8,128)(2,1)}, u32[]{:S(2)}) copy-start(bf16[1024,512]{1,0:T(8,128)(2,1)} %up.3) | copy-start | bytes 3145732
  15.1 12.0 %collective-permute-start.3 = (bf16[2,384,128]{2,1,0:T(8,128)(2,1)S(1)}, bf16[2,384,128]{2,1,0:T(8,128)(2,1)S(1)}, u32[]{:S(2)}, u32[]{:S(2)}) collective-permute-start(bf16[2,384,128]{2,1,0:T(8,128)(2,1)S(1)} %get-tuple-element.56), channel_id=1, source_target_pairs={{0,80},{16,64},{64,16},{80,0},{128,208},{144,192},{192,144},{208,1... | collective-permute-start | bytes 589832 | tf_op jit(solution)/shard_map/ppermute | solution.py:52
  20.7 9.4 %collective-permute-start.1 = (bf16[2,384,128]{2,1,0:T(8,128)(2,1)S(1)}, bf16[2,384,128]{2,1,0:T(8,128)(2,1)S(1)}, u32[]{:S(2)}, u32[]{:S(2)}) collective-permute-start(bf16[2,384,128]{2,1,0:T(8,128)(2,1)S(1)} %get-tuple-element.56), channel_id=1, source_target_pairs={{0,64},{16,80},{64,0},{80,16},{128,192},{144,208},{192,128},{208,1... | collective-permute-start | bytes 589832 | tf_op jit(solution)/shard_map/ppermute | solution.py:52
  20.7 9.9 %collective-permute-start.2 = (bf16[2,384,128]{2,1,0:T(8,128)(2,1)S(1)}, bf16[2,384,128]{2,1,0:T(8,128)(2,1)S(1)}, u32[]{:S(2)}, u32[]{:S(2)}) collective-permute-start(bf16[2,384,128]{2,1,0:T(8,128)(2,1)S(1)} %get-tuple-element.56), channel_id=1, source_target_pairs={{0,16},{16,0},{64,80},{80,64},{128,144},{144,128},{192,208},{208,1... | collective-permute-start | bytes 589832 | tf_op jit(solution)/shard_map/ppermute | solution.py:52
  30.8 22.0 %collective-permute-start.4 = (bf16[4,2,384,128]{3,2,1,0:T(8,128)(2,1)S(1)}, bf16[4,2,384,128]{3,2,1,0:T(8,128)(2,1)S(1)}, u32[]{:S(2)}, u32[]{:S(2)}) collective-permute-start(bf16[4,2,384,128]{3,2,1,0:T(8,128)(2,1)S(1)} %pad_maximum_fusion.4.x0), channel_id=1, source_target_pairs={{0,32},{8,40},{32,0},{40,8},{1,225},{25,249},{225,1},{249,25},{2,3... | collective-permute-start | bytes 2359304 | tf_op jit(solution)/shard_map/ppermute | solution.py:52
  32.6 21.1 %collective-permute-start.5 = (bf16[4,2,384,128]{3,2,1,0:T(8,128)(2,1)S(1)}, bf16[4,2,384,128]{3,2,1,0:T(8,128)(2,1)S(1)}, u32[]{:S(2)}, u32[]{:S(2)}) collective-permute-start(bf16[4,2,384,128]{3,2,1,0:T(8,128)(2,1)S(1)} %pad_maximum_fusion.4.x0), channel_id=1, source_target_pairs={{0,8},{8,0},{32,40},{40,32},{1,25},{25,1},{225,249},{249,225},{2,1... | collective-permute-start | bytes 2359304 | tf_op jit(solution)/shard_map/ppermute | solution.py:52
  34.4 12.0 %collective-permute-start.9 = (bf16[512,512]{1,0:T(8,128)(2,1)S(1)}, bf16[512,512]{1,0:T(8,128)(2,1)S(1)}, u32[]{:S(2)}, u32[]{:S(2)}) collective-permute-start(bf16[512,512]{1,0:T(8,128)(2,1)S(1)} %slice.92), channel_id=1, source_target_pairs={{0,2},{2,4},{4,6},{6,0},{1,3},{3,5},{5,7},{7,1},{8,10},{10,12},{12... | collective-permute-start | bytes 1572872 | tf_op jit(solution)/shard_map/ppermute | solution.py:82
  37.0 13.1 %collective-permute-start.10 = (bf16[512,512]{1,0:T(8,128)(2,1)S(1)}, bf16[512,512]{1,0:T(8,128)(2,1)S(1)}, u32[]{:S(2)}, u32[]{:S(2)}) collective-permute-start(bf16[512,512]{1,0:T(8,128)(2,1)S(1)} %slice.93), channel_id=1, source_target_pairs={{0,6},{2,0},{4,2},{6,4},{1,7},{3,1},{5,3},{7,5},{8,14},{10,8},{12,... | collective-permute-start | bytes 1572872 | tf_op jit(solution)/shard_map/ppermute | solution.py:82
  37.6 18.9 %collective-permute-start.6 = (bf16[4,2,384,128]{3,2,1,0:T(8,128)(2,1)S(1)}, bf16[4,2,384,128]{3,2,1,0:T(8,128)(2,1)S(1)}, u32[]{:S(2)}, u32[]{:S(2)}) collective-permute-start(bf16[4,2,384,128]{3,2,1,0:T(8,128)(2,1)S(1)} %pad_maximum_fusion.4.x0), channel_id=1, source_target_pairs={{0,40},{8,32},{32,8},{40,0},{1,249},{25,225},{225,25},{249,1},{2,4... | collective-permute-start | bytes 2359304 | tf_op jit(solution)/shard_map/ppermute | solution.py:52
  46.4 12.7 %collective-permute-start.13 = (bf16[512,512]{1,0:T(8,128)(2,1)S(1)}, bf16[512,512]{1,0:T(8,128)(2,1)S(1)}, u32[]{:S(2)}, u32[]{:S(2)}) collective-permute-start(bf16[512,512]{1,0:T(8,128)(2,1)S(1)} %collective-permute-done.9.fu), channel_id=1, source_target_pairs={{0,1},{1,0},{2,3},{3,2},{4,5},{5,4},{6,7},{7,6},{8,9},{9,8},{10,11... | collective-permute-start | bytes 1572872 | tf_op jit(solution)/shard_map/ppermute | solution.py:82
  50.2 10.2 %collective-permute-start.14 = (bf16[512,512]{1,0:T(8,128)(2,1)S(1)}, bf16[512,512]{1,0:T(8,128)(2,1)S(1)}, u32[]{:S(2)}, u32[]{:S(2)}) collective-permute-start(bf16[512,512]{1,0:T(8,128)(2,1)S(1)} %collective-permute-done.10.fd), channel_id=1, source_target_pairs={{0,1},{1,0},{2,3},{3,2},{4,5},{5,4},{6,7},{7,6},{8,9},{9,8},{10,11... | collective-permute-start | bytes 1572872 | tf_op jit(solution)/shard_map/ppermute | solution.py:82
  53.7 10.6 %collective-permute-start.11 = (bf16[1024,512]{1,0:T(8,128)(2,1)}, bf16[1024,512]{1,0:T(8,128)(2,1)}, u32[]{:S(2)}, u32[]{:S(2)}) collective-permute-start(bf16[1024,512]{1,0:T(8,128)(2,1)} %collective-permute-done.7.m1), channel_id=1, source_target_pairs={{0,1},{1,0},{2,3},{3,2},{4,5},{5,4},{6,7},{7,6},{8,9},{9,8},{10,11... | collective-permute-start | bytes 3145736 | tf_op jit(solution)/shard_map/ppermute | solution.py:82
  54.7 9.6 %collective-permute-start.12 = (bf16[1024,512]{1,0:T(8,128)(2,1)}, bf16[1024,512]{1,0:T(8,128)(2,1)}, u32[]{:S(2)}, u32[]{:S(2)}) collective-permute-start(bf16[1024,512]{1,0:T(8,128)(2,1)} %collective-permute-done.8.m3), channel_id=1, source_target_pairs={{0,1},{1,0},{2,3},{3,2},{4,5},{5,4},{6,7},{7,6},{8,9},{9,8},{10,11... | collective-permute-start | bytes 3145736 | tf_op jit(solution)/shard_map/ppermute | solution.py:82
  57.5 26.2 %collective-permute-start.31 = (bf16[1024,512]{1,0:T(8,128)(2,1)}, bf16[1024,512]{1,0:T(8,128)(2,1)S(1)}, u32[]{:S(2)}, u32[]{:S(2)}) collective-permute-start(bf16[1024,512]{1,0:T(8,128)(2,1)} %pad_maximum_fusion.2), channel_id=1, source_target_pairs={{0,2},{2,4},{4,6},{6,0},{1,3},{3,5},{5,7},{7,1},{8,10},{10,12},{12... | collective-permute-start | bytes 3145736 | tf_op jit(solution)/shard_map/ppermute | solution.py:82
  59.9 25.3 %collective-permute-start.32 = (bf16[1024,512]{1,0:T(8,128)(2,1)}, bf16[1024,512]{1,0:T(8,128)(2,1)S(1)}, u32[]{:S(2)}, u32[]{:S(2)}) collective-permute-start(bf16[1024,512]{1,0:T(8,128)(2,1)} %pad_maximum_fusion.2), channel_id=1, source_target_pairs={{0,6},{2,0},{4,2},{6,4},{1,7},{3,1},{5,3},{7,5},{8,14},{10,8},{12,... | collective-permute-start | bytes 3145736 | tf_op jit(solution)/shard_map/ppermute | solution.py:82
  61.2 47.6 %collective-permute-start.33 = (bf16[1024,512]{1,0:T(8,128)(2,1)}, bf16[1024,512]{1,0:T(8,128)(2,1)S(1)}, u32[]{:S(2)}, u32[]{:S(2)}) collective-permute-start(bf16[1024,512]{1,0:T(8,128)(2,1)} %pad_maximum_fusion.2), channel_id=1, source_target_pairs={{0,4},{2,6},{4,0},{6,2},{1,5},{3,7},{5,1},{7,3},{8,12},{10,14},{12... | collective-permute-start | bytes 3145736 | tf_op jit(solution)/shard_map/ppermute | solution.py:82
  80.6 30.8 %collective-permute-start.15 = (bf16[2,2,384,128]{3,2,1,0:T(8,128)(2,1)S(1)}, bf16[2,2,384,128]{3,2,1,0:T(8,128)(2,1)S(1)}, u32[]{:S(2)}, u32[]{:S(2)}) collective-permute-start(bf16[2,2,384,128]{3,2,1,0:T(8,128)(2,1)S(1)} %get-tuple-element.23), channel_id=1, source_target_pairs={{0,32},{8,40},{32,0},{40,8},{1,225},{25,249},{225,1},{249,25},{2,3... | collective-permute-start | bytes 1179656 | tf_op jit(solution)/shard_map/ppermute | solution.py:52
  81.3 31.7 %collective-permute-start.16 = (bf16[2,2,384,128]{3,2,1,0:T(8,128)(2,1)S(1)}, bf16[2,2,384,128]{3,2,1,0:T(8,128)(2,1)S(1)}, u32[]{:S(2)}, u32[]{:S(2)}) collective-permute-start(bf16[2,2,384,128]{3,2,1,0:T(8,128)(2,1)S(1)} %get-tuple-element.24), channel_id=1, source_target_pairs={{0,8},{8,0},{32,40},{40,32},{1,25},{25,1},{225,249},{249,225},{2,1... | collective-permute-start | bytes 1179656 | tf_op jit(solution)/shard_map/ppermute | solution.py:52
  83.8 30.5 %collective-permute-start.17 = (bf16[2,2,384,128]{3,2,1,0:T(8,128)(2,1)S(1)}, bf16[2,2,384,128]{3,2,1,0:T(8,128)(2,1)S(1)}, u32[]{:S(2)}, u32[]{:S(2)}) collective-permute-start(bf16[2,2,384,128]{3,2,1,0:T(8,128)(2,1)S(1)} %get-tuple-element.25), channel_id=1, source_target_pairs={{0,40},{8,32},{32,8},{40,0},{1,249},{25,225},{225,25},{249,1},{2,4... | collective-permute-start | bytes 1179656 | tf_op jit(solution)/shard_map/ppermute | solution.py:52
  110.8 86.5 %collective-permute-start.34 = (bf16[3,1024,512]{2,1,0:T(8,128)(2,1)}, bf16[3,1024,512]{2,1,0:T(8,128)(2,1)}, u32[]{:S(2)}, u32[]{:S(2)}) collective-permute-start(bf16[3,1024,512]{2,1,0:T(8,128)(2,1)} %pad_maximum_fusion), channel_id=1, source_target_pairs={{0,1},{1,0},{2,3},{3,2},{4,5},{5,4},{6,7},{7,6},{8,9},{9,8},{10,11... | collective-permute-start | bytes 9437192 | tf_op jit(solution)/shard_map/ppermute | solution.py:82
  110.8 7.8 %collective-permute-start.19 = (bf16[2,2,384,128]{3,2,1,0:T(8,128)(2,1)S(1)}, bf16[2,2,384,128]{3,2,1,0:T(8,128)(2,1)S(1)}, u32[]{:S(2)}, u32[]{:S(2)}) collective-permute-start(bf16[2,2,384,128]{3,2,1,0:T(8,128)(2,1)S(1)} %get-tuple-element.27), channel_id=1, source_target_pairs={{0,32},{8,40},{32,0},{40,8},{1,225},{25,249},{225,1},{249,25},{2,3... | collective-permute-start | bytes 1179656 | tf_op jit(solution)/shard_map/ppermute | solution.py:52
  111.4 8.0 %collective-permute-start.20 = (bf16[2,2,384,128]{3,2,1,0:T(8,128)(2,1)S(1)}, bf16[2,2,384,128]{3,2,1,0:T(8,128)(2,1)S(1)}, u32[]{:S(2)}, u32[]{:S(2)}) collective-permute-start(bf16[2,2,384,128]{3,2,1,0:T(8,128)(2,1)S(1)} %get-tuple-element.28), channel_id=1, source_target_pairs={{0,8},{8,0},{32,40},{40,32},{1,25},{25,1},{225,249},{249,225},{2,1... | collective-permute-start | bytes 1179656 | tf_op jit(solution)/shard_map/ppermute | solution.py:52
  113.0 14.7 %collective-permute-start.21 = (bf16[2,2,384,128]{3,2,1,0:T(8,128)(2,1)S(1)}, bf16[2,2,384,128]{3,2,1,0:T(8,128)(2,1)S(1)}, u32[]{:S(2)}, u32[]{:S(2)}) collective-permute-start(bf16[2,2,384,128]{3,2,1,0:T(8,128)(2,1)S(1)} %get-tuple-element.29), channel_id=1, source_target_pairs={{0,40},{8,32},{32,8},{40,0},{1,249},{25,225},{225,25},{249,1},{2,4... | collective-permute-start | bytes 1179656 | tf_op jit(solution)/shard_map/ppermute | solution.py:52
  114.5 19.5 %collective-permute-start.18 = (bf16[2,384,128]{2,1,0:T(8,128)(2,1)S(1)}, bf16[2,384,128]{2,1,0:T(8,128)(2,1)}, u32[]{:S(2)}, u32[]{:S(2)}) collective-permute-start(bf16[2,384,128]{2,1,0:T(8,128)(2,1)S(1)} %slice_bitcast_fusion.8), channel_id=1, source_target_pairs={{0,64},{16,80},{64,0},{80,16},{128,192},{144,208},{192,128},{208,1... | collective-permute-start | bytes 589832 | tf_op jit(solution)/shard_map/ppermute | solution.py:67
  128.8 10.0 %collective-permute-start.22 = (bf16[2,384,128]{2,1,0:T(8,128)(2,1)}, bf16[2,384,128]{2,1,0:T(8,128)(2,1)}, u32[]{:S(2)}, u32[]{:S(2)}) collective-permute-start(bf16[2,384,128]{2,1,0:T(8,128)(2,1)} %get-tuple-element.51), channel_id=1, source_target_pairs={{0,16},{16,0},{64,80},{80,64},{128,144},{144,128},{192,208},{208,1... | collective-permute-start | bytes 589832 | tf_op jit(solution)/shard_map/ppermute | solution.py:67
  131.5 10.5 %collective-permute-start.23 = (bf16[2,384,128]{2,1,0:T(8,128)(2,1)}, bf16[2,384,128]{2,1,0:T(8,128)(2,1)}, u32[]{:S(2)}, u32[]{:S(2)}) collective-permute-start(bf16[2,384,128]{2,1,0:T(8,128)(2,1)} %get-tuple-element.52), channel_id=1, source_target_pairs={{0,80},{16,64},{64,16},{80,0},{128,208},{144,192},{192,144},{208,1... | collective-permute-start | bytes 589832 | tf_op jit(solution)/shard_map/ppermute | solution.py:67
  144.0 14.2 %collective-permute-start.24 = (bf16[2,392,128]{2,1,0:T(8,128)(2,1)}, bf16[2,392,128]{2,1,0:T(8,128)(2,1)}, u32[]{:S(2)}, u32[]{:S(2)}) collective-permute-start(bf16[2,392,128]{2,1,0:T(8,128)(2,1)} %pad_maximum_fusion.5), channel_id=1, source_target_pairs={{0,128},{16,144},{64,192},{80,208},{128,0},{144,16},{192,64},{208,... | collective-permute-start | bytes 602120 | tf_op jit(solution)/shard_map/ppermute | solution.py:292
  160.0 8.2 %collective-permute-start.25 = (bf16[2,392,128]{2,1,0:T(8,128)(2,1)S(1)}, bf16[2,392,128]{2,1,0:T(8,128)(2,1)S(1)}, u32[]{:S(2)}, u32[]{:S(2)}) collective-permute-start(bf16[2,392,128]{2,1,0:T(8,128)(2,1)S(1)} %get-tuple-element.54), channel_id=1, source_target_pairs={{0,64},{16,80},{64,0},{80,16},{128,192},{144,208},{192,128},{208,1... | collective-permute-start | bytes 602120 | tf_op jit(solution)/shard_map/ppermute | solution.py:52
  160.1 12.4 %collective-permute-start.26 = (bf16[2,392,128]{2,1,0:T(8,128)(2,1)S(1)}, bf16[2,392,128]{2,1,0:T(8,128)(2,1)S(1)}, u32[]{:S(2)}, u32[]{:S(2)}) collective-permute-start(bf16[2,392,128]{2,1,0:T(8,128)(2,1)S(1)} %get-tuple-element.54), channel_id=1, source_target_pairs={{0,16},{16,0},{64,80},{80,64},{128,144},{144,128},{192,208},{208,1... | collective-permute-start | bytes 602120 | tf_op jit(solution)/shard_map/ppermute | solution.py:52
  163.1 13.1 %collective-permute-start.27 = (bf16[2,392,128]{2,1,0:T(8,128)(2,1)S(1)}, bf16[2,392,128]{2,1,0:T(8,128)(2,1)S(1)}, u32[]{:S(2)}, u32[]{:S(2)}) collective-permute-start(bf16[2,392,128]{2,1,0:T(8,128)(2,1)S(1)} %get-tuple-element.54), channel_id=1, source_target_pairs={{0,80},{16,64},{64,16},{80,0},{128,208},{144,192},{192,144},{208,1... | collective-permute-start | bytes 602120 | tf_op jit(solution)/shard_map/ppermute | solution.py:52
  176.3 12.3 %collective-permute-start.28 = (bf16[4,2,392,128]{3,2,1,0:T(8,128)(2,1)S(1)}, bf16[4,2,392,128]{3,2,1,0:T(8,128)(2,1)S(1)}, u32[]{:S(2)}, u32[]{:S(2)}) collective-permute-start(bf16[4,2,392,128]{3,2,1,0:T(8,128)(2,1)S(1)} %pad_maximum_fusion.3.x0), channel_id=1, source_target_pairs={{0,32},{8,40},{32,0},{40,8},{1,225},{25,249},{225,1},{249,25},{2,3... | collective-permute-start | bytes 2408456 | tf_op jit(solution)/shard_map/ppermute | solution.py:52
  176.4 20.9 %collective-permute-start.29 = (bf16[4,2,392,128]{3,2,1,0:T(8,128)(2,1)S(1)}, bf16[4,2,392,128]{3,2,1,0:T(8,128)(2,1)S(1)}, u32[]{:S(2)}, u32[]{:S(2)}) collective-permute-start(bf16[4,2,392,128]{3,2,1,0:T(8,128)(2,1)S(1)} %pad_maximum_fusion.3.x0), channel_id=1, source_target_pairs={{0,8},{8,0},{32,40},{40,32},{1,25},{25,1},{225,249},{249,225},{2,1... | collective-permute-start | bytes 2408456 | tf_op jit(solution)/shard_map/ppermute | solution.py:52
  176.5 20.8 %collective-permute-start.30 = (bf16[4,2,392,128]{3,2,1,0:T(8,128)(2,1)S(1)}, bf16[4,2,392,128]{3,2,1,0:T(8,128)(2,1)S(1)}, u32[]{:S(2)}, u32[]{:S(2)}) collective-permute-start(bf16[4,2,392,128]{3,2,1,0:T(8,128)(2,1)S(1)} %pad_maximum_fusion.3.x0), channel_id=1, source_target_pairs={{0,40},{8,32},{32,8},{40,0},{1,249},{25,225},{225,25},{249,1},{2,4... | collective-permute-start | bytes 2408456 | tf_op jit(solution)/shard_map/ppermute | solution.py:52
  205.6 7.9 %collective-permute-start.35 = (bf16[2,2,384,128]{3,2,1,0:T(8,128)(2,1)S(1)}, bf16[2,2,384,128]{3,2,1,0:T(8,128)(2,1)S(1)}, u32[]{:S(2)}, u32[]{:S(2)}) collective-permute-start(bf16[2,2,384,128]{3,2,1,0:T(8,128)(2,1)S(1)} %get-tuple-element.32), channel_id=1, source_target_pairs={{0,32},{8,40},{32,0},{40,8},{1,225},{25,249},{225,1},{249,25},{2,3... | collective-permute-start | bytes 1179656 | tf_op jit(solution)/shard_map/ppermute | solution.py:52
  207.6 12.0 %collective-permute-start.36 = (bf16[2,2,384,128]{3,2,1,0:T(8,128)(2,1)S(1)}, bf16[2,2,384,128]{3,2,1,0:T(8,128)(2,1)S(1)}, u32[]{:S(2)}, u32[]{:S(2)}) collective-permute-start(bf16[2,2,384,128]{3,2,1,0:T(8,128)(2,1)S(1)} %get-tuple-element.33), channel_id=1, source_target_pairs={{0,8},{8,0},{32,40},{40,32},{1,25},{25,1},{225,249},{249,225},{2,1... | collective-permute-start | bytes 1179656 | tf_op jit(solution)/shard_map/ppermute | solution.py:52
  207.6 12.0 %collective-permute-start.37 = (bf16[2,2,384,128]{3,2,1,0:T(8,128)(2,1)S(1)}, bf16[2,2,384,128]{3,2,1,0:T(8,128)(2,1)S(1)}, u32[]{:S(2)}, u32[]{:S(2)}) collective-permute-start(bf16[2,2,384,128]{3,2,1,0:T(8,128)(2,1)S(1)} %get-tuple-element.34), channel_id=1, source_target_pairs={{0,40},{8,32},{32,8},{40,0},{1,249},{25,225},{225,25},{249,1},{2,4... | collective-permute-start | bytes 1179656 | tf_op jit(solution)/shard_map/ppermute | solution.py:52
  209.2 12.8 %collective-permute-start.39 = (bf16[2,2,384,128]{3,2,1,0:T(8,128)(2,1)S(1)}, bf16[2,2,384,128]{3,2,1,0:T(8,128)(2,1)S(1)}, u32[]{:S(2)}, u32[]{:S(2)}) collective-permute-start(bf16[2,2,384,128]{3,2,1,0:T(8,128)(2,1)S(1)} %get-tuple-element.36), channel_id=1, source_target_pairs={{0,32},{8,40},{32,0},{40,8},{1,225},{25,249},{225,1},{249,25},{2,3... | collective-permute-start | bytes 1179656 | tf_op jit(solution)/shard_map/ppermute | solution.py:52
  211.1 12.7 %collective-permute-start.40 = (bf16[2,2,384,128]{3,2,1,0:T(8,128)(2,1)S(1)}, bf16[2,2,384,128]{3,2,1,0:T(8,128)(2,1)S(1)}, u32[]{:S(2)}, u32[]{:S(2)}) collective-permute-start(bf16[2,2,384,128]{3,2,1,0:T(8,128)(2,1)S(1)} %get-tuple-element.37), channel_id=1, source_target_pairs={{0,8},{8,0},{32,40},{40,32},{1,25},{25,1},{225,249},{249,225},{2,1... | collective-permute-start | bytes 1179656 | tf_op jit(solution)/shard_map/ppermute | solution.py:52
  213.4 17.7 %collective-permute-start.41 = (bf16[2,2,384,128]{3,2,1,0:T(8,128)(2,1)S(1)}, bf16[2,2,384,128]{3,2,1,0:T(8,128)(2,1)S(1)}, u32[]{:S(2)}, u32[]{:S(2)}) collective-permute-start(bf16[2,2,384,128]{3,2,1,0:T(8,128)(2,1)S(1)} %get-tuple-element.38), channel_id=1, source_target_pairs={{0,40},{8,32},{32,8},{40,0},{1,249},{25,225},{225,25},{249,1},{2,4... | collective-permute-start | bytes 1179656 | tf_op jit(solution)/shard_map/ppermute | solution.py:52
  219.8 13.5 %collective-permute-start.38 = (bf16[2,384,128]{2,1,0:T(8,128)(2,1)S(1)}, bf16[2,384,128]{2,1,0:T(8,128)(2,1)S(1)}, u32[]{:S(2)}, u32[]{:S(2)}) collective-permute-start(bf16[2,384,128]{2,1,0:T(8,128)(2,1)S(1)} %slice_bitcast_fusion.3), channel_id=1, source_target_pairs={{0,64},{16,80},{64,0},{80,16},{128,192},{144,208},{192,128},{208,1... | collective-permute-start | bytes 589832 | tf_op jit(solution)/shard_map/ppermute | solution.py:67
  231.2 36.2 %copy-start.21 = (f32[128]{0:T(128)S(1)}, f32[128]{0:T(128)}, u32[]{:S(2)}) copy-start(f32[128]{0:T(128)} %param.17) | copy-start | bytes 1540
  231.2 36.3 %copy-start.22 = (f32[128]{0:T(128)S(1)}, f32[128]{0:T(128)}, u32[]{:S(2)}) copy-start(f32[128]{0:T(128)} %param.16) | copy-start | bytes 1540
  231.4 11.3 %collective-permute-start.42 = (bf16[2,384,128]{2,1,0:T(8,128)(2,1)S(1)}, bf16[2,384,128]{2,1,0:T(8,128)(2,1)S(1)}, u32[]{:S(2)}, u32[]{:S(2)}) collective-permute-start(bf16[2,384,128]{2,1,0:T(8,128)(2,1)S(1)} %get-tuple-element.49), channel_id=1, source_target_pairs={{0,16},{16,0},{64,80},{80,64},{128,144},{144,128},{192,208},{208,1... | collective-permute-start | bytes 589832 | tf_op jit(solution)/shard_map/ppermute | solution.py:67
  231.9 10.8 %collective-permute-start.43 = (bf16[2,384,128]{2,1,0:T(8,128)(2,1)S(1)}, bf16[2,384,128]{2,1,0:T(8,128)(2,1)S(1)}, u32[]{:S(2)}, u32[]{:S(2)}) collective-permute-start(bf16[2,384,128]{2,1,0:T(8,128)(2,1)S(1)} %get-tuple-element.50), channel_id=1, source_target_pairs={{0,80},{16,64},{64,16},{80,0},{128,208},{144,192},{192,144},{208,1... | collective-permute-start | bytes 589832 | tf_op jit(solution)/shard_map/ppermute | solution.py:67
  242.8 9.7 %collective-permute-start.44 = (bf16[384,128]{1,0:T(8,128)(2,1)S(1)}, bf16[384,128]{1,0:T(8,128)(2,1)S(1)}, u32[]{:S(2)}, u32[]{:S(2)}) collective-permute-start(bf16[384,128]{1,0:T(8,128)(2,1)S(1)} %fusion.5), channel_id=1, source_target_pairs={{0,128},{16,144},{64,192},{80,208},{128,0},{144,16},{192,64},{208,... | collective-permute-start | bytes 294920 | tf_op jit(solution)/shard_map/ppermute | solution.py:305
  (20 other events, 93.3 us)

commit v8 on v7

--- a/solution.py
+++ b/solution.py
@@ -66,6 +66,9 @@
     def flip(block, e):
         return lax.ppermute(block, ALL, pairs["mid"][e]).astype(F32)
 
+    if len(parts) == 4:
+        some = near_sum(parts)
+        return sum(p.astype(F32) for p in stage([some[e] for e in range(4)], pairs["mid"]))
     high = near_sum(parts[4:])
     low = near_sum(parts[:4])
     far = flip(high[0], 2) + flip(high[1], 3)
@@ -150,7 +153,10 @@
         for d in range(4):
             for f in range(2):
                 slot, e, g = to_peer(idx, d, j, idx[3] ^ f)
-                outs[4 * f + d][e & 1, g] = ov[slot]
+                if len(outs) == 4:
+                    outs[d][e, g] = ov[slot]
+                else:
+                    outs[4 * f + d][e & 1, g] = ov[slot]
 
     part = jnp.dot(hv[0], down[:wide], preferred_element_type=F32)
     emit(me, 0, part + jnp.dot(hv[1], down[wide:], preferred_element_type=F32))
@@ -182,14 +188,14 @@
 
 
 def first_kernel(
-    idx, x0, x1, x2, x3, up, down, m1, m3, fu, fd, o1, o3, pu, pd, u0, u1, u2, u3, v0, v1, v2, v3, xs, hv, ov, upv, dv, sems
+    idx, x0, x1, x2, x3, up, down, m1, m3, fu, fd, o1, o3, pu, pd, u0, u1, u2, u3, xs, hv, ov, upv, dv, sems
 ):
     copies = fetch(up, down, upv, dv, sems)
     for d, x in enumerate((x0, x1, x2, x3)):
         for i in range(8):
             xs[from_peer(idx, d, i // 2, i % 2)] = x[i // 2, i % 2]
     pieces = [(1, whole(m1), whole(o1)), (3, whole(m3), whole(o3)), (2, split(fu, fd), split(pu, pd))]
-    matmuls(idx, xs, upv, dv, copies, pieces, hv, ov, (u0, u1, u2, u3, v0, v1, v2, v3))
+    matmuls(idx, xs, upv, dv, copies, pieces, hv, ov, (u0, u1, u2, u3))
 
 
 def second_kernel(
@@ -237,15 +243,15 @@
 
 
 def ffn(kernel, idx, x, tokens, up, down, pieces, extra, own_out, norm_scratch):
-    nx, nb = lax.axis_size(X), NZ * NY
+    nx, nb, cuts = lax.axis_size(X), NZ * NY, 1 + len(own_out)
     width, ff = up.shape[0] * nx, up.shape[1]
     near = [pltpu.with_memory_space_constraint(a, pltpu.MemorySpace.VMEM) for a in (*x, *pieces)]
     far = [pltpu.with_memory_space_constraint(a, pltpu.MemorySpace.HBM) for a in (up, down)]
     return pl.pallas_call(
         kernel,
-        out_shape=[pltpu.VMEM((2, nb // 16, tokens, 128), BF)] * 8 + own_out,
+        out_shape=[pltpu.VMEM((4 // cuts, nb // 16, tokens, 128), BF)] * (4 * cuts) + own_out,
         in_specs=[SMEM] + [VMEM] * 4 + [ANY] * 2 + [VMEM] * (len(pieces) + len(extra)),
-        out_specs=[VMEM] * (8 + len(own_out)),
+        out_specs=[VMEM] * (4 * cuts + len(own_out)),
         scratch_shapes=[pltpu.VMEM((nb, tokens, 128), BF)]
         + norm_scratch
         + [

time: 270 us -> 271 us (level)
  the two profiles are of different devices: /device:TPU:2 before, /device:TPU:32 now
where the time goes in v8:
time: 271 us
  starting transfers between devices  107 us (39%)
  waiting for transfers between devices  96.6 us (36%)
  local copies, waits for them, and re-layouts  23.8 us (9%)
  blocking collectives  19.1 us (7%)
  Pallas kernels  16 us (6%)
  other arithmetic  8.17 us (3%)
    ppermute x24, waiting for transfers between devices, stage(): got = {d: lax.ppermute(blocks[d], ALL, pairs[d]) for d in (1, 2, 3)}  77.3 us
    ppermute x24, starting transfers between devices, stage(): got = {d: lax.ppermute(blocks[d], ALL, pairs[d]) for d in (1, 2, 3)}  69.4 us
    all_to_all x1, blocking collectives, stats_to_all(): lax.all_to_all(jnp.broadcast_to(row[None], (n, *row.shape)), RA, 0, 0, ti...  19.1 us
    pallas_call x2, Pallas kernels, ffn(): pl.pallas_call(kernel, out_shape=[pltpu.VMEM((4 // cuts, nb // 16, tokens...  16 us
    unnamed x46, local copies, waits for them, and re-layouts  14 us
    ppermute x12, starting transfers between devices, shift(): return lax.ppermute(a, axis, [(i, (i + by) % n) for i in range(n)])  12.3 us
    ppermute x3, starting transfers between devices, flip(): return lax.ppermute(block, ALL, pairs['mid'][e]).astype(F32)  8.18 us
    ppermute x1, starting transfers between devices, body(): pair = jnp.stack([stream, lax.ppermute(stream, ALL, pairs['last'])])  6.29 us
  transfers between devices with their start and end apart: 42, of which 22 were waited for; matrix products, arithmetic and copies ran while one was open for 5% of the time, Pallas kernels for 3%

profile of v8, /device:TPU:32, one launch (start us, length us, event | category | flops | bytes accessed | tf_op | source)
XLA Modules:
  0.0 270.7 jit_solution(508465430803176593)
XLA Ops:
  2.5 1.6 collective-permute-start.7
  4.0 1.7 collective-permute-start.8
  5.8 6.3 %collective-permute-start = (bf16[384,128]{1,0:T(8,128)(2,1)S(1)}, bf16[384,128]{1,0:T(8,128)(2,1)S(1)}, u32[]{:S(2)}, u32[]{:S(2)}) collective-permute-start(bf16[384,128]{1,0:T(8,128)(2,1)S(1)} %copy-done.19), channel_id=1, source_target_pairs={{0,128},{16,144},{64,192},{80,208},{128,0},{144,16},{192,64},{208,... | collective-permute-start | bytes 294920 | tf_op jit(solution)/shard_map/ppermute | solution.py:282
  12.1 3.9 %collective-permute-done = bf16[384,128]{1,0:T(8,128)(2,1)S(1)} collective-permute-done((bf16[384,128]{1,0:T(8,128)(2,1)S(1)}, bf16[384,128]{1,0:T(8,128)(2,1)S(1)}, u32[]{:S(2)}, u32[]{:S(2)}) %collective-permute-start) | collective-permute-done | bytes 98336 | tf_op jit(solution)/shard_map/ppermute | solution.py:282
  16.1 4.3 %collective-permute-start.3 = (bf16[2,384,128]{2,1,0:T(8,128)(2,1)S(1)}, bf16[2,384,128]{2,1,0:T(8,128)(2,1)S(1)}, u32[]{:S(2)}, u32[]{:S(2)}) collective-permute-start(bf16[2,384,128]{2,1,0:T(8,128)(2,1)S(1)} %get-tuple-element.49), channel_id=1, source_target_pairs={{0,80},{16,64},{64,16},{80,0},{128,208},{144,192},{192,144},{208,1... | collective-permute-start | bytes 589832 | tf_op jit(solution)/shard_map/ppermute | solution.py:52
  20.3 1.4 collective-permute-start.1
  22.0 4.7 %collective-permute-done.3 = bf16[2,384,128]{2,1,0:T(8,128)(2,1)S(1)} collective-permute-done((bf16[2,384,128]{2,1,0:T(8,128)(2,1)S(1)}, bf16[2,384,128]{2,1,0:T(8,128)(2,1)S(1)}, u32[]{:S(2)}, u32[]{:S(2)}) %collective-permute-start.3) | collective-permute-done | bytes 196640 | tf_op jit(solution)/shard_map/ppermute | solution.py:52
  26.8 4.9 %collective-permute-done.1 = bf16[2,384,128]{2,1,0:T(8,128)(2,1)S(1)} collective-permute-done((bf16[2,384,128]{2,1,0:T(8,128)(2,1)S(1)}, bf16[2,384,128]{2,1,0:T(8,128)(2,1)S(1)}, u32[]{:S(2)}, u32[]{:S(2)}) %collective-permute-start.1) | collective-permute-done | bytes 196640 | tf_op jit(solution)/shard_map/ppermute | solution.py:52
  35.7 3.0 %collective-permute-start.10 = (bf16[512,512]{1,0:T(8,128)(2,1)S(1)}, bf16[512,512]{1,0:T(8,128)(2,1)S(1)}, u32[]{:S(2)}, u32[]{:S(2)}) collective-permute-start(bf16[512,512]{1,0:T(8,128)(2,1)S(1)} %slice.93), channel_id=1, source_target_pairs={{0,6},{2,0},{4,2},{6,4},{1,7},{3,1},{5,3},{7,5},{8,14},{10,8},{12,... | collective-permute-start | bytes 1572872 | tf_op jit(solution)/shard_map/ppermute | solution.py:85
  38.7 2.2 collective-permute-start.6
  40.9 2.9 %collective-permute-done.4.x1 = bf16[4,2,384,128]{3,2,1,0:T(8,128)(2,1)S(1)} collective-permute-done((bf16[4,2,384,128]{3,2,1,0:T(8,128)(2,1)S(1)}, bf16[4,2,384,128]{3,2,1,0:T(8,128)(2,1)S(1)}, u32[]{:S(2)}, u32[]{:S(2)}) %collective-permute-start.4) | collective-permute-done | bytes 786464 | tf_op jit(solution)/shard_map/ppermute | solution.py:52
  44.8 7.8 %collective-permute-done.5.x2 = bf16[4,2,384,128]{3,2,1,0:T(8,128)(2,1)S(1)} collective-permute-done((bf16[4,2,384,128]{3,2,1,0:T(8,128)(2,1)S(1)}, bf16[4,2,384,128]{3,2,1,0:T(8,128)(2,1)S(1)}, u32[]{:S(2)}, u32[]{:S(2)}) %collective-permute-start.5) | collective-permute-done | bytes 786464 | tf_op jit(solution)/shard_map/ppermute | solution.py:52
  58.4 2.5 collective-permute-start.29
  71.6 7.6 %shard_map.91 = (bf16[4,2,384,128]{3,2,1,0:T(8,128)(2,1)S(1)}, bf16[4,2,384,128]{3,2,1,0:T(8,128)(2,1)S(1)}, bf16[4,2,384,128]{3,2,1,0:T(8,128)(2,1)S(1)}, bf16[4,2,384,128]{3,2,1,0:T(8,128)(2,1)S(1)}) custom-call(s32[5]{0:T(128)S(1)} %stack.118.idx, bf16[4,2,384,128]{3,2,1,0:T(8,128)(2,1)S(1)} %copy-done.1, bf16[4,2,384,128]{3,2,1,0:T(8,128)(2,1)S(1)} %copy-done.5, ...), custom_call_target="tpu_custom_call" | custom-call | flops 3221225472 | bytes 14680064 | tf_op jit(solution)/shard_map/pallas_call | solution.py:250
  79.2 2.1 collective-permute-start.15
  82.1 2.0 collective-permute-done.28.m1
  84.1 24.5 %collective-permute-start.17 = (bf16[4,2,384,128]{3,2,1,0:T(8,128)(2,1)S(1)}, bf16[4,2,384,128]{3,2,1,0:T(8,128)(2,1)S(1)}, u32[]{:S(2)}, u32[]{:S(2)}) collective-permute-start(bf16[4,2,384,128]{3,2,1,0:T(8,128)(2,1)S(1)} %get-tuple-element.21), channel_id=1, source_target_pairs={{0,40},{8,32},{32,8},{40,0},{1,249},{25,225},{225,25},{249,1},{2,4... | collective-permute-start | bytes 2359304 | tf_op jit(solution)/shard_map/ppermute | solution.py:52
  108.6 2.0 pad_maximum_fusion
  110.6 8.8 %collective-permute-done.17 = bf16[4,2,384,128]{3,2,1,0:T(8,128)(2,1)S(1)} collective-permute-done((bf16[4,2,384,128]{3,2,1,0:T(8,128)(2,1)S(1)}, bf16[4,2,384,128]{3,2,1,0:T(8,128)(2,1)S(1)}, u32[]{:S(2)}, u32[]{:S(2)}) %collective-permute-start.17) | collective-permute-done | bytes 786464 | tf_op jit(solution)/shard_map/ppermute | solution.py:52
  121.5 5.5 %collective-permute-start.18 = (bf16[2,384,128]{2,1,0:T(8,128)(2,1)}, bf16[2,384,128]{2,1,0:T(8,128)(2,1)}, u32[]{:S(2)}, u32[]{:S(2)}) collective-permute-start(bf16[2,384,128]{2,1,0:T(8,128)(2,1)} %get-tuple-element.41), channel_id=1, source_target_pairs={{0,64},{16,80},{64,0},{80,16},{128,192},{144,208},{192,128},{208,1... | collective-permute-start | bytes 589832 | tf_op jit(solution)/shard_map/ppermute | solution.py:52
  127.0 3.0 %collective-permute-start.20 = (bf16[2,384,128]{2,1,0:T(8,128)(2,1)S(1)}, bf16[2,384,128]{2,1,0:T(8,128)(2,1)}, u32[]{:S(2)}, u32[]{:S(2)}) collective-permute-start(bf16[2,384,128]{2,1,0:T(8,128)(2,1)S(1)} %get-tuple-element.42), channel_id=1, source_target_pairs={{0,80},{16,64},{64,16},{80,0},{128,208},{144,192},{192,144},{208,1... | collective-permute-start | bytes 589832 | tf_op jit(solution)/shard_map/ppermute | solution.py:52
  131.8 4.8 %collective-permute-done.19 = bf16[2,384,128]{2,1,0:T(8,128)(2,1)} collective-permute-done((bf16[2,384,128]{2,1,0:T(8,128)(2,1)}, bf16[2,384,128]{2,1,0:T(8,128)(2,1)}, u32[]{:S(2)}, u32[]{:S(2)}) %collective-permute-start.19) | collective-permute-done | bytes 196640 | tf_op jit(solution)/shard_map/ppermute | solution.py:52
  136.6 1.7 collective-permute-done.20
  140.3 5.4 %collective-permute-start.21 = (bf16[2,392,128]{2,1,0:T(8,128)(2,1)}, bf16[2,392,128]{2,1,0:T(8,128)(2,1)}, u32[]{:S(2)}, u32[]{:S(2)}) collective-permute-start(bf16[2,392,128]{2,1,0:T(8,128)(2,1)} %pad_maximum_fusion.5), channel_id=1, source_target_pairs={{0,128},{16,144},{64,192},{80,208},{128,0},{144,16},{192,64},{208,... | collective-permute-start | bytes 602120 | tf_op jit(solution)/shard_map/ppermute | solution.py:298
  147.0 5.6 %collective-permute-done.21 = bf16[2,392,128]{2,1,0:T(8,128)(2,1)} collective-permute-done((bf16[2,392,128]{2,1,0:T(8,128)(2,1)}, bf16[2,392,128]{2,1,0:T(8,128)(2,1)}, u32[]{:S(2)}, u32[]{:S(2)}) %collective-permute-start.21) | collective-permute-done | bytes 200736 | tf_op jit(solution)/shard_map/ppermute | solution.py:298
  154.3 8.1 %collective-permute-start.22 = (bf16[2,392,128]{2,1,0:T(8,128)(2,1)S(1)}, bf16[2,392,128]{2,1,0:T(8,128)(2,1)S(1)}, u32[]{:S(2)}, u32[]{:S(2)}) collective-permute-start(bf16[2,392,128]{2,1,0:T(8,128)(2,1)S(1)} %get-tuple-element.47), channel_id=1, source_target_pairs={{0,64},{16,80},{64,0},{80,16},{128,192},{144,208},{192,128},{208,1... | collective-permute-start | bytes 602120 | tf_op jit(solution)/shard_map/ppermute | solution.py:52
  162.4 5.5 %collective-permute-start.23 = (bf16[2,392,128]{2,1,0:T(8,128)(2,1)S(1)}, bf16[2,392,128]{2,1,0:T(8,128)(2,1)S(1)}, u32[]{:S(2)}, u32[]{:S(2)}) collective-permute-start(bf16[2,392,128]{2,1,0:T(8,128)(2,1)S(1)} %get-tuple-element.47), channel_id=1, source_target_pairs={{0,16},{16,0},{64,80},{80,64},{128,144},{144,128},{192,208},{208,1... | collective-permute-start | bytes 602120 | tf_op jit(solution)/shard_map/ppermute | solution.py:52
  168.0 6.5 %collective-permute-done.23 = bf16[2,392,128]{2,1,0:T(8,128)(2,1)S(1)} collective-permute-done((bf16[2,392,128]{2,1,0:T(8,128)(2,1)S(1)}, bf16[2,392,128]{2,1,0:T(8,128)(2,1)S(1)}, u32[]{:S(2)}, u32[]{:S(2)}) %collective-permute-start.23) | collective-permute-done | bytes 200736 | tf_op jit(solution)/shard_map/ppermute | solution.py:52
  174.4 2.6 collective-permute-done.24
  178.0 2.7 collective-permute-start.27
  180.8 8.6 %collective-permute-done.25.x1 = bf16[4,2,392,128]{3,2,1,0:T(8,128)(2,1)S(1)} collective-permute-done((bf16[4,2,392,128]{3,2,1,0:T(8,128)(2,1)S(1)}, bf16[4,2,392,128]{3,2,1,0:T(8,128)(2,1)S(1)}, u32[]{:S(2)}, u32[]{:S(2)}) %collective-permute-start.25) | collective-permute-done | bytes 802848 | tf_op jit(solution)/shard_map/ppermute | solution.py:52
  189.4 8.7 %collective-permute-done.26.x2 = bf16[4,2,392,128]{3,2,1,0:T(8,128)(2,1)S(1)} collective-permute-done((bf16[4,2,392,128]{3,2,1,0:T(8,128)(2,1)S(1)}, bf16[4,2,392,128]{3,2,1,0:T(8,128)(2,1)S(1)}, u32[]{:S(2)}, u32[]{:S(2)}) %collective-permute-start.26) | collective-permute-done | bytes 802848 | tf_op jit(solution)/shard_map/ppermute | solution.py:52
  198.1 8.3 %shard_map.92 = (bf16[2,2,384,128]{3,2,1,0:T(8,128)(2,1)S(1)}, bf16[2,2,384,128]{3,2,1,0:T(8,128)(2,1)S(1)}, bf16[2,2,384,128]{3,2,1,0:T(8,128)(2,1)S(1)}, bf16[...) custom-call(s32[5]{0:T(128)S(1)} %stack.118.idx, ...), custom_call_target="tpu_custom_call" | custom-call | flops 3221225472 | bytes 14680064 | tf_op jit(solution)/shard_map/pallas_call | solution.py:250
  206.5 2.0 collective-permute-start.32
  208.5 1.6 collective-permute-start.34
  210.0 1.9 collective-permute-start.36
  212.0 2.4 collective-permute-done.32
  214.3 1.4 collective-permute-start.38
  215.7 4.8 %collective-permute-done.33 = bf16[2,2,384,128]{3,2,1,0:T(8,128)(2,1)S(1)} collective-permute-done((bf16[2,2,384,128]{3,2,1,0:T(8,128)(2,1)S(1)}, bf16[2,2,384,128]{3,2,1,0:T(8,128)(2,1)S(1)}, u32[]{:S(2)}, u32[]{:S(2)}) %collective-permute-start.33) | collective-permute-done | bytes 393248 | tf_op jit(solution)/shard_map/ppermute | solution.py:52
  220.7 2.0 collective-permute-start.35
  223.2 4.6 %collective-permute-done.37 = bf16[2,2,384,128]{3,2,1,0:T(8,128)(2,1)S(1)} collective-permute-done((bf16[2,2,384,128]{3,2,1,0:T(8,128)(2,1)S(1)}, bf16[2,2,384,128]{3,2,1,0:T(8,128)(2,1)S(1)}, u32[]{:S(2)}, u32[]{:S(2)}) %collective-permute-start.37) | collective-permute-done | bytes 393248 | tf_op jit(solution)/shard_map/ppermute | solution.py:52
  227.8 2.9 %collective-permute-done.38 = bf16[2,2,384,128]{3,2,1,0:T(8,128)(2,1)S(1)} collective-permute-done((bf16[2,2,384,128]{3,2,1,0:T(8,128)(2,1)S(1)}, bf16[2,2,384,128]{3,2,1,0:T(8,128)(2,1)S(1)}, u32[]{:S(2)}, u32[]{:S(2)}) %collective-permute-start.38) | collective-permute-done | bytes 393248 | tf_op jit(solution)/shard_map/ppermute | solution.py:52
  231.0 1.5 collective-permute-start.39
  232.5 4.7 %collective-permute-start.40 = (bf16[2,384,128]{2,1,0:T(8,128)(2,1)S(1)}, bf16[2,384,128]{2,1,0:T(8,128)(2,1)S(1)}, u32[]{:S(2)}, u32[]{:S(2)}) collective-permute-start(bf16[2,384,128]{2,1,0:T(8,128)(2,1)S(1)} %get-tuple-element.45), channel_id=1, source_target_pairs={{0,80},{16,64},{64,16},{80,0},{128,208},{144,192},{192,144},{208,1... | collective-permute-start | bytes 589832 | tf_op jit(solution)/shard_map/ppermute | solution.py:67
  238.3 3.2 %collective-permute-done.40 = bf16[2,384,128]{2,1,0:T(8,128)(2,1)S(1)} collective-permute-done((bf16[2,384,128]{2,1,0:T(8,128)(2,1)S(1)}, bf16[2,384,128]{2,1,0:T(8,128)(2,1)S(1)}, u32[]{:S(2)}, u32[]{:S(2)}) %collective-permute-start.40) | collective-permute-done | bytes 196640 | tf_op jit(solution)/shard_map/ppermute | solution.py:67
  241.7 5.2 %collective-permute-start.41 = (bf16[384,128]{1,0:T(8,128)(2,1)S(1)}, bf16[384,128]{1,0:T(8,128)(2,1)S(1)}, u32[]{:S(2)}, u32[]{:S(2)}) collective-permute-start(bf16[384,128]{1,0:T(8,128)(2,1)S(1)} %fusion.6), channel_id=1, source_target_pairs={{0,128},{16,144},{64,192},{80,208},{128,0},{144,16},{192,64},{208,... | collective-permute-start | bytes 294920 | tf_op jit(solution)/shard_map/ppermute | solution.py:311
  246.9 3.4 %collective-permute-done.41 = bf16[384,128]{1,0:T(8,128)(2,1)S(1)} collective-permute-done((bf16[384,128]{1,0:T(8,128)(2,1)S(1)}, bf16[384,128]{1,0:T(8,128)(2,1)S(1)}, u32[]{:S(2)}, u32[]{:S(2)}) %collective-permute-start.41) | collective-permute-done | bytes 98336 | tf_op jit(solution)/shard_map/ppermute | solution.py:311
  250.6 19.1 %all_to_all.5 = f32[32,1,768]{2,1,0:T(1,128)S(1)} all-to-all(f32[32,1,768]{2,1,0:T(1,128)S(1)} %broadcast_in_dim.11), channel_id=1, replica_groups=mesh['ra_0'=8,'ra_1'=4,'cb'=4,'dp'=2] {'ra_0','ra_1'}, dimensions={0} | all-to-all | bytes 196608 | tf_op jit(solution)/shard_map/all_to_all | solution.py:80
  (126 shorter events, 38.4 us)
Async XLA Ops:
  2.5 30.7 %collective-permute-start.7 = (bf16[1024,512]{1,0:T(8,128)(2,1)S(1)}, bf16[1024,512]{1,0:T(8,128)(2,1)}, u32[]{:S(2)}, u32[]{:S(2)}) collective-permute-start(bf16[1024,512]{1,0:T(8,128)(2,1)S(1)} %pad_maximum_fusion.1), channel_id=1, source_target_pairs={{0,2},{2,4},{4,6},{6,0},{1,3},{3,5},{5,7},{7,1},{8,10},{10,12},{12... | collective-permute-start | bytes 3145736 | tf_op jit(solution)/shard_map/ppermute | solution.py:85
  4.0 30.6 %collective-permute-start.8 = (bf16[1024,512]{1,0:T(8,128)(2,1)S(1)}, bf16[1024,512]{1,0:T(8,128)(2,1)}, u32[]{:S(2)}, u32[]{:S(2)}) collective-permute-start(bf16[1024,512]{1,0:T(8,128)(2,1)S(1)} %pad_maximum_fusion.1), channel_id=1, source_target_pairs={{0,6},{2,0},{4,2},{6,4},{1,7},{3,1},{5,3},{7,5},{8,14},{10,8},{12,... | collective-permute-start | bytes 3145736 | tf_op jit(solution)/shard_map/ppermute | solution.py:85
  5.8 10.2 %collective-permute-start = (bf16[384,128]{1,0:T(8,128)(2,1)S(1)}, bf16[384,128]{1,0:T(8,128)(2,1)S(1)}, u32[]{:S(2)}, u32[]{:S(2)}) collective-permute-start(bf16[384,128]{1,0:T(8,128)(2,1)S(1)} %copy-done.19), channel_id=1, source_target_pairs={{0,128},{16,144},{64,192},{80,208},{128,0},{144,16},{192,64},{208,... | collective-permute-start | bytes 294920 | tf_op jit(solution)/shard_map/ppermute | solution.py:282
  16.0 38.8 %copy-start.20 = (bf16[1024,512]{1,0:T(8,128)(2,1)S(1)}, bf16[1024,512]{1,0:T(8,128)(2,1)}, u32[]{:S(2)}) copy-start(bf16[1024,512]{1,0:T(8,128)(2,1)} %up.3) | copy-start | bytes 3145732
  16.1 10.7 %collective-permute-start.3 = (bf16[2,384,128]{2,1,0:T(8,128)(2,1)S(1)}, bf16[2,384,128]{2,1,0:T(8,128)(2,1)S(1)}, u32[]{:S(2)}, u32[]{:S(2)}) collective-permute-start(bf16[2,384,128]{2,1,0:T(8,128)(2,1)S(1)} %get-tuple-element.49), channel_id=1, source_target_pairs={{0,80},{16,64},{64,16},{80,0},{128,208},{144,192},{192,144},{208,1... | collective-permute-start | bytes 589832 | tf_op jit(solution)/shard_map/ppermute | solution.py:52
  20.3 11.3 %collective-permute-start.1 = (bf16[2,384,128]{2,1,0:T(8,128)(2,1)S(1)}, bf16[2,384,128]{2,1,0:T(8,128)(2,1)S(1)}, u32[]{:S(2)}, u32[]{:S(2)}) collective-permute-start(bf16[2,384,128]{2,1,0:T(8,128)(2,1)S(1)} %get-tuple-element.49), channel_id=1, source_target_pairs={{0,64},{16,80},{64,0},{80,16},{128,192},{144,208},{192,128},{208,1... | collective-permute-start | bytes 589832 | tf_op jit(solution)/shard_map/ppermute | solution.py:52
  21.7 10.0 %collective-permute-start.2 = (bf16[2,384,128]{2,1,0:T(8,128)(2,1)S(1)}, bf16[2,384,128]{2,1,0:T(8,128)(2,1)S(1)}, u32[]{:S(2)}, u32[]{:S(2)}) collective-permute-start(bf16[2,384,128]{2,1,0:T(8,128)(2,1)S(1)} %get-tuple-element.49), channel_id=1, source_target_pairs={{0,16},{16,0},{64,80},{80,64},{128,144},{144,128},{192,208},{208,1... | collective-permute-start | bytes 589832 | tf_op jit(solution)/shard_map/ppermute | solution.py:52
  31.8 24.1 %copy-start = (bf16[4,2,384,128]{3,2,1,0:T(8,128)(2,1)}, bf16[4,2,384,128]{3,2,1,0:T(8,128)(2,1)S(1)}, u32[]{:S(2)}) copy-start(bf16[4,2,384,128]{3,2,1,0:T(8,128)(2,1)S(1)} %pad_maximum_fusion.4.x0) | copy-start | bytes 2359300
  31.8 12.1 %collective-permute-start.4 = (bf16[4,2,384,128]{3,2,1,0:T(8,128)(2,1)S(1)}, bf16[4,2,384,128]{3,2,1,0:T(8,128)(2,1)S(1)}, u32[]{:S(2)}, u32[]{:S(2)}) collective-permute-start(bf16[4,2,384,128]{3,2,1,0:T(8,128)(2,1)S(1)} %pad_maximum_fusion.4.x0), channel_id=1, source_target_pairs={{0,32},{8,40},{32,0},{40,8},{1,225},{25,249},{225,1},{249,25},{2,3... | collective-permute-start | bytes 2359304 | tf_op jit(solution)/shard_map/ppermute | solution.py:52
  32.2 20.4 %collective-permute-start.5 = (bf16[4,2,384,128]{3,2,1,0:T(8,128)(2,1)S(1)}, bf16[4,2,384,128]{3,2,1,0:T(8,128)(2,1)S(1)}, u32[]{:S(2)}, u32[]{:S(2)}) collective-permute-start(bf16[4,2,384,128]{3,2,1,0:T(8,128)(2,1)S(1)} %pad_maximum_fusion.4.x0), channel_id=1, source_target_pairs={{0,8},{8,0},{32,40},{40,32},{1,25},{25,1},{225,249},{249,225},{2,1... | collective-permute-start | bytes 2359304 | tf_op jit(solution)/shard_map/ppermute | solution.py:52
  34.3 20.0 %collective-permute-start.9 = (bf16[512,512]{1,0:T(8,128)(2,1)S(1)}, bf16[512,512]{1,0:T(8,128)(2,1)S(1)}, u32[]{:S(2)}, u32[]{:S(2)}) collective-permute-start(bf16[512,512]{1,0:T(8,128)(2,1)S(1)} %slice.92), channel_id=1, source_target_pairs={{0,2},{2,4},{4,6},{6,0},{1,3},{3,5},{5,7},{7,1},{8,10},{10,12},{12... | collective-permute-start | bytes 1572872 | tf_op jit(solution)/shard_map/ppermute | solution.py:85
  35.7 18.7 %collective-permute-start.10 = (bf16[512,512]{1,0:T(8,128)(2,1)S(1)}, bf16[512,512]{1,0:T(8,128)(2,1)S(1)}, u32[]{:S(2)}, u32[]{:S(2)}) collective-permute-start(bf16[512,512]{1,0:T(8,128)(2,1)S(1)} %slice.93), channel_id=1, source_target_pairs={{0,6},{2,0},{4,2},{6,4},{1,7},{3,1},{5,3},{7,5},{8,14},{10,8},{12,... | collective-permute-start | bytes 1572872 | tf_op jit(solution)/shard_map/ppermute | solution.py:85
  38.7 17.2 %collective-permute-start.6 = (bf16[4,2,384,128]{3,2,1,0:T(8,128)(2,1)S(1)}, bf16[4,2,384,128]{3,2,1,0:T(8,128)(2,1)S(1)}, u32[]{:S(2)}, u32[]{:S(2)}) collective-permute-start(bf16[4,2,384,128]{3,2,1,0:T(8,128)(2,1)S(1)} %pad_maximum_fusion.4.x0), channel_id=1, source_target_pairs={{0,40},{8,32},{32,8},{40,0},{1,249},{25,225},{225,25},{249,1},{2,4... | collective-permute-start | bytes 2359304 | tf_op jit(solution)/shard_map/ppermute | solution.py:52
  44.8 18.2 %collective-permute-start.11 = (bf16[1024,512]{1,0:T(8,128)(2,1)}, bf16[1024,512]{1,0:T(8,128)(2,1)}, u32[]{:S(2)}, u32[]{:S(2)}) collective-permute-start(bf16[1024,512]{1,0:T(8,128)(2,1)} %collective-permute-done.7.m1), channel_id=1, source_target_pairs={{0,1},{1,0},{2,3},{3,2},{4,5},{5,4},{6,7},{7,6},{8,9},{9,8},{10,11... | collective-permute-start | bytes 3145736 | tf_op jit(solution)/shard_map/ppermute | solution.py:85
  53.5 9.4 %collective-permute-start.12 = (bf16[1024,512]{1,0:T(8,128)(2,1)}, bf16[1024,512]{1,0:T(8,128)(2,1)}, u32[]{:S(2)}, u32[]{:S(2)}) collective-permute-start(bf16[1024,512]{1,0:T(8,128)(2,1)} %collective-permute-done.8.m3), channel_id=1, source_target_pairs={{0,1},{1,0},{2,3},{3,2},{4,5},{5,4},{6,7},{7,6},{8,9},{9,8},{10,11... | collective-permute-start | bytes 3145736 | tf_op jit(solution)/shard_map/ppermute | solution.py:85
  54.3 3.3 %collective-permute-start.13 = (bf16[512,512]{1,0:T(8,128)(2,1)S(1)}, bf16[512,512]{1,0:T(8,128)(2,1)S(1)}, u32[]{:S(2)}, u32[]{:S(2)}) collective-permute-start(bf16[512,512]{1,0:T(8,128)(2,1)S(1)} %collective-permute-done.9.fu), channel_id=1, source_target_pairs={{0,1},{1,0},{2,3},{3,2},{4,5},{5,4},{6,7},{7,6},{8,9},{9,8},{10,11... | collective-permute-start | bytes 1572872 | tf_op jit(solution)/shard_map/ppermute | solution.py:85
  54.4 6.6 %collective-permute-start.14 = (bf16[512,512]{1,0:T(8,128)(2,1)S(1)}, bf16[512,512]{1,0:T(8,128)(2,1)S(1)}, u32[]{:S(2)}, u32[]{:S(2)}) collective-permute-start(bf16[512,512]{1,0:T(8,128)(2,1)S(1)} %collective-permute-done.10.fd), channel_id=1, source_target_pairs={{0,1},{1,0},{2,3},{3,2},{4,5},{5,4},{6,7},{7,6},{8,9},{9,8},{10,11... | collective-permute-start | bytes 1572872 | tf_op jit(solution)/shard_map/ppermute | solution.py:85
  56.9 27.2 %collective-permute-start.28 = (bf16[1024,512]{1,0:T(8,128)(2,1)}, bf16[1024,512]{1,0:T(8,128)(2,1)S(1)}, u32[]{:S(2)}, u32[]{:S(2)}) collective-permute-start(bf16[1024,512]{1,0:T(8,128)(2,1)} %pad_maximum_fusion.2), channel_id=1, source_target_pairs={{0,2},{2,4},{4,6},{6,0},{1,3},{3,5},{5,7},{7,1},{8,10},{10,12},{12... | collective-permute-start | bytes 3145736 | tf_op jit(solution)/shard_map/ppermute | solution.py:85
  58.4 50.2 %collective-permute-start.29 = (bf16[1024,512]{1,0:T(8,128)(2,1)}, bf16[1024,512]{1,0:T(8,128)(2,1)S(1)}, u32[]{:S(2)}, u32[]{:S(2)}) collective-permute-start(bf16[1024,512]{1,0:T(8,128)(2,1)} %pad_maximum_fusion.2), channel_id=1, source_target_pairs={{0,6},{2,0},{4,2},{6,4},{1,7},{3,1},{5,3},{7,5},{8,14},{10,8},{12,... | collective-permute-start | bytes 3145736 | tf_op jit(solution)/shard_map/ppermute | solution.py:85
  61.8 46.8 %collective-permute-start.30 = (bf16[1024,512]{1,0:T(8,128)(2,1)}, bf16[1024,512]{1,0:T(8,128)(2,1)S(1)}, u32[]{:S(2)}, u32[]{:S(2)}) collective-permute-start(bf16[1024,512]{1,0:T(8,128)(2,1)} %pad_maximum_fusion.2), channel_id=1, source_target_pairs={{0,4},{2,6},{4,0},{6,2},{1,5},{3,7},{5,1},{7,3},{8,12},{10,14},{12... | collective-permute-start | bytes 3145736 | tf_op jit(solution)/shard_map/ppermute | solution.py:85
  79.2 31.3 %collective-permute-start.15 = (bf16[4,2,384,128]{3,2,1,0:T(8,128)(2,1)S(1)}, bf16[4,2,384,128]{3,2,1,0:T(8,128)(2,1)S(1)}, u32[]{:S(2)}, u32[]{:S(2)}) collective-permute-start(bf16[4,2,384,128]{3,2,1,0:T(8,128)(2,1)S(1)} %get-tuple-element.19), channel_id=1, source_target_pairs={{0,32},{8,40},{32,0},{40,8},{1,225},{25,249},{225,1},{249,25},{2,3... | collective-permute-start | bytes 2359304 | tf_op jit(solution)/shard_map/ppermute | solution.py:52
  81.4 29.2 %collective-permute-start.16 = (bf16[4,2,384,128]{3,2,1,0:T(8,128)(2,1)S(1)}, bf16[4,2,384,128]{3,2,1,0:T(8,128)(2,1)S(1)}, u32[]{:S(2)}, u32[]{:S(2)}) collective-permute-start(bf16[4,2,384,128]{3,2,1,0:T(8,128)(2,1)S(1)} %get-tuple-element.20), channel_id=1, source_target_pairs={{0,8},{8,0},{32,40},{40,32},{1,25},{25,1},{225,249},{249,225},{2,1... | collective-permute-start | bytes 2359304 | tf_op jit(solution)/shard_map/ppermute | solution.py:52
  84.1 35.3 %collective-permute-start.17 = (bf16[4,2,384,128]{3,2,1,0:T(8,128)(2,1)S(1)}, bf16[4,2,384,128]{3,2,1,0:T(8,128)(2,1)S(1)}, u32[]{:S(2)}, u32[]{:S(2)}) collective-permute-start(bf16[4,2,384,128]{3,2,1,0:T(8,128)(2,1)S(1)} %get-tuple-element.21), channel_id=1, source_target_pairs={{0,40},{8,32},{32,8},{40,0},{1,249},{25,225},{225,25},{249,1},{2,4... | collective-permute-start | bytes 2359304 | tf_op jit(solution)/shard_map/ppermute | solution.py:52
  110.6 70.2 %collective-permute-start.31 = (bf16[3,1024,512]{2,1,0:T(8,128)(2,1)}, bf16[3,1024,512]{2,1,0:T(8,128)(2,1)}, u32[]{:S(2)}, u32[]{:S(2)}) collective-permute-start(bf16[3,1024,512]{2,1,0:T(8,128)(2,1)} %pad_maximum_fusion), channel_id=1, source_target_pairs={{0,1},{1,0},{2,3},{3,2},{4,5},{5,4},{6,7},{7,6},{8,9},{9,8},{10,11... | collective-permute-start | bytes 9437192 | tf_op jit(solution)/shard_map/ppermute | solution.py:85
  119.4 10.6 %copy-start.2 = (f32[128]{0:T(128)S(1)}, f32[128]{0:T(128)}, u32[]{:S(2)}) copy-start(f32[128]{0:T(128)} %param.15) | copy-start | bytes 1540
  119.4 10.6 %copy-start.3 = (f32[128]{0:T(128)S(1)}, f32[128]{0:T(128)}, u32[]{:S(2)}) copy-start(f32[128]{0:T(128)} %param.14) | copy-start | bytes 1540
  121.5 10.3 %collective-permute-start.18 = (bf16[2,384,128]{2,1,0:T(8,128)(2,1)}, bf16[2,384,128]{2,1,0:T(8,128)(2,1)}, u32[]{:S(2)}, u32[]{:S(2)}) collective-permute-start(bf16[2,384,128]{2,1,0:T(8,128)(2,1)} %get-tuple-element.41), channel_id=1, source_target_pairs={{0,64},{16,80},{64,0},{80,16},{128,192},{144,208},{192,128},{208,1... | collective-permute-start | bytes 589832 | tf_op jit(solution)/shard_map/ppermute | solution.py:52
  127.0 9.6 %collective-permute-start.19 = (bf16[2,384,128]{2,1,0:T(8,128)(2,1)}, bf16[2,384,128]{2,1,0:T(8,128)(2,1)}, u32[]{:S(2)}, u32[]{:S(2)}) collective-permute-start(bf16[2,384,128]{2,1,0:T(8,128)(2,1)} %get-tuple-element.43), channel_id=1, source_target_pairs={{0,16},{16,0},{64,80},{80,64},{128,144},{144,128},{192,208},{208,1... | collective-permute-start | bytes 589832 | tf_op jit(solution)/shard_map/ppermute | solution.py:52
  127.0 11.2 %collective-permute-start.20 = (bf16[2,384,128]{2,1,0:T(8,128)(2,1)S(1)}, bf16[2,384,128]{2,1,0:T(8,128)(2,1)}, u32[]{:S(2)}, u32[]{:S(2)}) collective-permute-start(bf16[2,384,128]{2,1,0:T(8,128)(2,1)S(1)} %get-tuple-element.42), channel_id=1, source_target_pairs={{0,80},{16,64},{64,16},{80,0},{128,208},{144,192},{192,144},{208,1... | collective-permute-start | bytes 589832 | tf_op jit(solution)/shard_map/ppermute | solution.py:52
  140.3 12.3 %collective-permute-start.21 = (bf16[2,392,128]{2,1,0:T(8,128)(2,1)}, bf16[2,392,128]{2,1,0:T(8,128)(2,1)}, u32[]{:S(2)}, u32[]{:S(2)}) collective-permute-start(bf16[2,392,128]{2,1,0:T(8,128)(2,1)} %pad_maximum_fusion.5), channel_id=1, source_target_pairs={{0,128},{16,144},{64,192},{80,208},{128,0},{144,16},{192,64},{208,... | collective-permute-start | bytes 602120 | tf_op jit(solution)/shard_map/ppermute | solution.py:298
  154.3 13.6 %collective-permute-start.22 = (bf16[2,392,128]{2,1,0:T(8,128)(2,1)S(1)}, bf16[2,392,128]{2,1,0:T(8,128)(2,1)S(1)}, u32[]{:S(2)}, u32[]{:S(2)}) collective-permute-start(bf16[2,392,128]{2,1,0:T(8,128)(2,1)S(1)} %get-tuple-element.47), channel_id=1, source_target_pairs={{0,64},{16,80},{64,0},{80,16},{128,192},{144,208},{192,128},{208,1... | collective-permute-start | bytes 602120 | tf_op jit(solution)/shard_map/ppermute | solution.py:52
  162.4 12.0 %collective-permute-start.23 = (bf16[2,392,128]{2,1,0:T(8,128)(2,1)S(1)}, bf16[2,392,128]{2,1,0:T(8,128)(2,1)S(1)}, u32[]{:S(2)}, u32[]{:S(2)}) collective-permute-start(bf16[2,392,128]{2,1,0:T(8,128)(2,1)S(1)} %get-tuple-element.47), channel_id=1, source_target_pairs={{0,16},{16,0},{64,80},{80,64},{128,144},{144,128},{192,208},{208,1... | collective-permute-start | bytes 602120 | tf_op jit(solution)/shard_map/ppermute | solution.py:52
  167.9 9.1 %collective-permute-start.24 = (bf16[2,392,128]{2,1,0:T(8,128)(2,1)S(1)}, bf16[2,392,128]{2,1,0:T(8,128)(2,1)S(1)}, u32[]{:S(2)}, u32[]{:S(2)}) collective-permute-start(bf16[2,392,128]{2,1,0:T(8,128)(2,1)S(1)} %get-tuple-element.47), channel_id=1, source_target_pairs={{0,80},{16,64},{64,16},{80,0},{128,208},{144,192},{192,144},{208,1... | collective-permute-start | bytes 602120 | tf_op jit(solution)/shard_map/ppermute | solution.py:52
  177.1 12.3 %collective-permute-start.25 = (bf16[4,2,392,128]{3,2,1,0:T(8,128)(2,1)S(1)}, bf16[4,2,392,128]{3,2,1,0:T(8,128)(2,1)S(1)}, u32[]{:S(2)}, u32[]{:S(2)}) collective-permute-start(bf16[4,2,392,128]{3,2,1,0:T(8,128)(2,1)S(1)} %pad_maximum_fusion.3.x0), channel_id=1, source_target_pairs={{0,32},{8,40},{32,0},{40,8},{1,225},{25,249},{225,1},{249,25},{2,3... | collective-permute-start | bytes 2408456 | tf_op jit(solution)/shard_map/ppermute | solution.py:52
  177.2 20.9 %collective-permute-start.26 = (bf16[4,2,392,128]{3,2,1,0:T(8,128)(2,1)S(1)}, bf16[4,2,392,128]{3,2,1,0:T(8,128)(2,1)S(1)}, u32[]{:S(2)}, u32[]{:S(2)}) collective-permute-start(bf16[4,2,392,128]{3,2,1,0:T(8,128)(2,1)S(1)} %pad_maximum_fusion.3.x0), channel_id=1, source_target_pairs={{0,8},{8,0},{32,40},{40,32},{1,25},{25,1},{225,249},{249,225},{2,1... | collective-permute-start | bytes 2408456 | tf_op jit(solution)/shard_map/ppermute | solution.py:52
  178.0 20.1 %collective-permute-start.27 = (bf16[4,2,392,128]{3,2,1,0:T(8,128)(2,1)S(1)}, bf16[4,2,392,128]{3,2,1,0:T(8,128)(2,1)S(1)}, u32[]{:S(2)}, u32[]{:S(2)}) collective-permute-start(bf16[4,2,392,128]{3,2,1,0:T(8,128)(2,1)S(1)} %pad_maximum_fusion.3.x0), channel_id=1, source_target_pairs={{0,40},{8,32},{32,8},{40,0},{1,249},{25,225},{225,25},{249,1},{2,4... | collective-permute-start | bytes 2408456 | tf_op jit(solution)/shard_map/ppermute | solution.py:52
  206.5 7.9 %collective-permute-start.32 = (bf16[2,2,384,128]{3,2,1,0:T(8,128)(2,1)S(1)}, bf16[2,2,384,128]{3,2,1,0:T(8,128)(2,1)S(1)}, u32[]{:S(2)}, u32[]{:S(2)}) collective-permute-start(bf16[2,2,384,128]{3,2,1,0:T(8,128)(2,1)S(1)} %get-tuple-element.24), channel_id=1, source_target_pairs={{0,32},{8,40},{32,0},{40,8},{1,225},{25,249},{225,1},{249,25},{2,3... | collective-permute-start | bytes 1179656 | tf_op jit(solution)/shard_map/ppermute | solution.py:52
  208.5 12.0 %collective-permute-start.33 = (bf16[2,2,384,128]{3,2,1,0:T(8,128)(2,1)S(1)}, bf16[2,2,384,128]{3,2,1,0:T(8,128)(2,1)S(1)}, u32[]{:S(2)}, u32[]{:S(2)}) collective-permute-start(bf16[2,2,384,128]{3,2,1,0:T(8,128)(2,1)S(1)} %get-tuple-element.25), channel_id=1, source_target_pairs={{0,8},{8,0},{32,40},{40,32},{1,25},{25,1},{225,249},{249,225},{2,1... | collective-permute-start | bytes 1179656 | tf_op jit(solution)/shard_map/ppermute | solution.py:52
  208.5 12.0 %collective-permute-start.34 = (bf16[2,2,384,128]{3,2,1,0:T(8,128)(2,1)S(1)}, bf16[2,2,384,128]{3,2,1,0:T(8,128)(2,1)S(1)}, u32[]{:S(2)}, u32[]{:S(2)}) collective-permute-start(bf16[2,2,384,128]{3,2,1,0:T(8,128)(2,1)S(1)} %get-tuple-element.26), channel_id=1, source_target_pairs={{0,40},{8,32},{32,8},{40,0},{1,249},{25,225},{225,25},{249,1},{2,4... | collective-permute-start | bytes 1179656 | tf_op jit(solution)/shard_map/ppermute | solution.py:52
  210.0 13.1 %collective-permute-start.36 = (bf16[2,2,384,128]{3,2,1,0:T(8,128)(2,1)S(1)}, bf16[2,2,384,128]{3,2,1,0:T(8,128)(2,1)S(1)}, u32[]{:S(2)}, u32[]{:S(2)}) collective-permute-start(bf16[2,2,384,128]{3,2,1,0:T(8,128)(2,1)S(1)} %get-tuple-element.28), channel_id=1, source_target_pairs={{0,32},{8,40},{32,0},{40,8},{1,225},{25,249},{225,1},{249,25},{2,3... | collective-permute-start | bytes 1179656 | tf_op jit(solution)/shard_map/ppermute | solution.py:52
  212.0 15.8 %collective-permute-start.37 = (bf16[2,2,384,128]{3,2,1,0:T(8,128)(2,1)S(1)}, bf16[2,2,384,128]{3,2,1,0:T(8,128)(2,1)S(1)}, u32[]{:S(2)}, u32[]{:S(2)}) collective-permute-start(bf16[2,2,384,128]{3,2,1,0:T(8,128)(2,1)S(1)} %get-tuple-element.29), channel_id=1, source_target_pairs={{0,8},{8,0},{32,40},{40,32},{1,25},{25,1},{225,249},{249,225},{2,1... | collective-permute-start | bytes 1179656 | tf_op jit(solution)/shard_map/ppermute | solution.py:52
  214.3 16.4 %collective-permute-start.38 = (bf16[2,2,384,128]{3,2,1,0:T(8,128)(2,1)S(1)}, bf16[2,2,384,128]{3,2,1,0:T(8,128)(2,1)S(1)}, u32[]{:S(2)}, u32[]{:S(2)}) collective-permute-start(bf16[2,2,384,128]{3,2,1,0:T(8,128)(2,1)S(1)} %get-tuple-element.30), channel_id=1, source_target_pairs={{0,40},{8,32},{32,8},{40,0},{1,249},{25,225},{225,25},{249,1},{2,4... | collective-permute-start | bytes 1179656 | tf_op jit(solution)/shard_map/ppermute | solution.py:52
  220.7 16.5 %collective-permute-start.35 = (bf16[2,384,128]{2,1,0:T(8,128)(2,1)S(1)}, bf16[2,384,128]{2,1,0:T(8,128)(2,1)S(1)}, u32[]{:S(2)}, u32[]{:S(2)}) collective-permute-start(bf16[2,384,128]{2,1,0:T(8,128)(2,1)S(1)} %slice_bitcast_fusion.3), channel_id=1, source_target_pairs={{0,64},{16,80},{64,0},{80,16},{128,192},{144,208},{192,128},{208,1... | collective-permute-start | bytes 589832 | tf_op jit(solution)/shard_map/ppermute | solution.py:67
  230.7 39.1 %copy-start.21 = (f32[128]{0:T(128)S(1)}, f32[128]{0:T(128)}, u32[]{:S(2)}) copy-start(f32[128]{0:T(128)} %param.17) | copy-start | bytes 1540
  230.7 39.1 %copy-start.22 = (f32[128]{0:T(128)S(1)}, f32[128]{0:T(128)}, u32[]{:S(2)}) copy-start(f32[128]{0:T(128)} %param.16) | copy-start | bytes 1540
  231.0 7.3 %collective-permute-start.39 = (bf16[2,384,128]{2,1,0:T(8,128)(2,1)S(1)}, bf16[2,384,128]{2,1,0:T(8,128)(2,1)S(1)}, u32[]{:S(2)}, u32[]{:S(2)}) collective-permute-start(bf16[2,384,128]{2,1,0:T(8,128)(2,1)S(1)} %get-tuple-element.44), channel_id=1, source_target_pairs={{0,16},{16,0},{64,80},{80,64},{128,144},{144,128},{192,208},{208,1... | collective-permute-start | bytes 589832 | tf_op jit(solution)/shard_map/ppermute | solution.py:67
  232.5 9.1 %collective-permute-start.40 = (bf16[2,384,128]{2,1,0:T(8,128)(2,1)S(1)}, bf16[2,384,128]{2,1,0:T(8,128)(2,1)S(1)}, u32[]{:S(2)}, u32[]{:S(2)}) collective-permute-start(bf16[2,384,128]{2,1,0:T(8,128)(2,1)S(1)} %get-tuple-element.45), channel_id=1, source_target_pairs={{0,80},{16,64},{64,16},{80,0},{128,208},{144,192},{192,144},{208,1... | collective-permute-start | bytes 589832 | tf_op jit(solution)/shard_map/ppermute | solution.py:67
  241.7 8.6 %collective-permute-start.41 = (bf16[384,128]{1,0:T(8,128)(2,1)S(1)}, bf16[384,128]{1,0:T(8,128)(2,1)S(1)}, u32[]{:S(2)}, u32[]{:S(2)}) collective-permute-start(bf16[384,128]{1,0:T(8,128)(2,1)S(1)} %fusion.6), channel_id=1, source_target_pairs={{0,128},{16,144},{64,192},{80,208},{128,0},{144,16},{192,64},{208,... | collective-permute-start | bytes 294920 | tf_op jit(solution)/shard_map/ppermute | solution.py:311
  (17 other events, 32.0 us)
